TPU v7x, 128 devices: a whole 4x4x4 slice. The times are simulated.
128 devices in a mesh: sp: 16 (over z, y), dp: 8 (over x, core).
Axes of the slice: x: 4, y: 4, z: 4, core: 2. Of those that a mesh axis runs over, the one named last changes fastest.
Arguments:
- inputs: bfloat16 [8, 3072, 2048], P('dp', 'sp'), may hold values from -6 to 6
- in_gain: float32 [2048], replicated, may hold values from 0.1 to 1.9
- w_query: bfloat16 [2048, 1024], P('dp', 'sp'), may hold values from -0.125 to 0.125
- w_key: bfloat16 [2048, 256], P('dp', 'sp'), may hold values from -0.375 to 0.375
- w_value: bfloat16 [2048, 256], P('dp', 'sp'), may hold values from -0.125 to 0.125
- key_bias: float32 [8, 3072, 16], P('dp', None, 'sp'), may hold values from -20 to 0
- out_gain: float32 [1024], replicated, may hold values from 0.1 to 1.9
- w_out: bfloat16 [1024, 2048], P('sp', 'dp'), may hold values from -0.1875 to 0.1875
Outputs:
- mixed: bfloat16 [8, 3072, 2048], P('dp', 'sp')
All inputs are finite; a program needn't handle non-finite values.
Results may differ from a plain program's by a relative error of at most 0.012.
The roundings to bfloat16 on the way count: a program that leaves them out, or rounds other values in their place, can miss the bound.
Values may be sent and summed in bfloat16 or wider, within the bound.
No kernel may reach another device: no remote copies, remote signals or barrier semaphores. Data moves between devices by JAX's collectives and lax.ppermute only.
A program may use at most 128 MiB of HBM per device.

v0:
```python
import functools
import math

import jax
import jax.numpy as jnp
from jax import lax
from jax.experimental import pallas as pl
from jax.experimental.pallas import tpu as pltpu
from jax.sharding import PartitionSpec as P

HEAD_DIM = 64
LOG2E = math.log2(math.e)
norm_eps = 1e-06
SIDE = 4
HOPS = (0, 1, 3, 2)


VMEM = pl.BlockSpec(memory_space=pltpu.VMEM)


def along_x(k):
    return [(i, (i + 2 * k) % (2 * SIDE)) for i in range(2 * SIDE)]


def other_core():
    return [(i, i ^ 1) for i in range(2 * SIDE)]


def along_zy(dz, dy):
    return [
        (s, ((s // SIDE + dz) % SIDE) * SIDE + (s % SIDE + dy) % SIDE) for s in range(SIDE * SIDE)
    ]


def near(*arrays):
    return [pltpu.with_memory_space_constraint(a, pltpu.VMEM) for a in arrays]


def place_of():
    dp, sp = lax.axis_index("dp"), lax.axis_index("sp")
    return lax.div(dp, 2), lax.rem(dp, 2), lax.div(sp, SIDE), lax.rem(sp, SIDE)


def project_kernel(normed_ref, own_a, own_b, far_a, far_b, out_ref, order_ref, sums_ref):
    bf = jnp.bfloat16
    x, c, z, y = place_of()
    rows = normed_ref.shape[0]
    for i in range(SIDE):
        for cc in range(2):
            chunk = 2 * lax.rem(x + SIDE - HOPS[i], SIDE) + lax.rem(c + cc, 2)
            order_ref[:, (2 * i + cc) * 256 : (2 * i + cc + 1) * 256] = normed_ref[
                :, pl.ds(pl.multiple_of(chunk * 256, 256), 256)
            ]
    for iz in range(SIDE):
        parts = []
        for i in range(SIDE):
            for ref_a, ref_b in ((own_a, own_b), (far_a, far_b)):
                if i < 2:
                    parts.append(jnp.concatenate([ref_a[iz, iy, i] for iy in range(SIDE)], axis=0))
                else:
                    parts.append(jnp.concatenate([ref_b[iy, iz, i - 2] for iy in range(SIDE)], axis=0))
        weights = jnp.concatenate(parts, axis=1)
        total = lax.dot_general(
            weights, order_ref[...], (((1,), (1,)), ((), ())), preferred_element_type=jnp.float32
        )
        for iy in range(SIDE):
            place = SIDE * lax.rem(z + SIDE - HOPS[iz], SIDE) + lax.rem(y + SIDE - HOPS[iy], SIDE)
            sums_ref[place] = total[96 * iy : 96 * (iy + 1), :]
    half = rows // 2
    for g in range(SIDE):
        key = jnp.concatenate([sums_ref[SIDE * g + j, 64:80, :] for j in range(SIDE)], axis=0)
        value = jnp.concatenate([sums_ref[SIDE * g + j, 80:96, :] for j in range(SIDE)], axis=0)
        turned = value.T.astype(bf)
        for j in range(SIDE):
            h = SIDE * g + j
            both = jnp.concatenate([sums_ref[h, :64, :], key], axis=0)
            out_ref[h, :rows, :] = both.T.astype(bf)
            out_ref[h, rows:, :] = jnp.concatenate([turned[:half], turned[half:]], axis=1)


def attend_kernel(got_ref, bias_ref, gain_ref, out_ref, qa_ref, kt_ref, v_ref, acc_ref, car_ref, *, src, rows, bq, bk):
    bf = jnp.bfloat16
    half = rows // 2
    length = src * rows
    lane = lax.broadcasted_iota(jnp.int32, (rows, 128), 1)
    ones = jnp.where(lane < 3, 1.0, 0.0).astype(bf)
    for b in range(src):
        both = got_ref[b, :rows, :]
        wide = both[:, :HEAD_DIM].astype(jnp.float32) * (LOG2E * HEAD_DIM ** -0.5)
        high = wide.astype(bf)
        low = (wide - high.astype(jnp.float32)).astype(bf)
        qa_ref[b * rows : (b + 1) * rows, :128] = jnp.concatenate([high, low], axis=1)
        qa_ref[b * rows : (b + 1) * rows, 128:] = ones
        vv = got_ref[b, rows:, :]
        v_ref[b * rows : b * rows + half, :] = vv[:, :HEAD_DIM]
        v_ref[b * rows + half : (b + 1) * rows, :] = vv[:, HEAD_DIM:]
    step = 2 * rows
    for b in range(src // 2):
        pair = jnp.concatenate([got_ref[2 * b, :rows, :], got_ref[2 * b + 1, :rows, :]], axis=0)
        kt = pair.astype(jnp.float32).T[HEAD_DIM:, :].astype(bf)
        kt_ref[:HEAD_DIM, b * step : (b + 1) * step] = kt
        kt_ref[HEAD_DIM : 2 * HEAD_DIM, b * step : (b + 1) * step] = kt
    b2 = bias_ref[...] * LOG2E
    b_high = b2.astype(bf).astype(jnp.float32)
    b_mid = (b2 - b_high).astype(bf).astype(jnp.float32)
    b_low = b2 - b_high - b_mid
    row = lax.broadcasted_iota(jnp.int32, (128, length), 0)
    tail = jnp.where(row == 0, b_high, jnp.where(row == 1, b_mid, jnp.where(row == 2, b_low, 0.0)))
    kt_ref[2 * HEAD_DIM :, :] = tail.astype(bf)

    tri = (
        lax.broadcasted_iota(jnp.int32, (bk, bk), 0) > lax.broadcasted_iota(jnp.int32, (bk, bk), 1)
    ).astype(bf)

    def tile(row0, nrows, acc0, col0, masked):
        x = jnp.dot(
            qa_ref[pl.ds(row0, nrows), :], kt_ref[:, pl.ds(col0, bk)], preferred_element_type=jnp.float32
        )
        soft = jnp.maximum(x, jnp.log2(1.0 + jnp.exp2(jnp.minimum(x, 126.0))))
        own = x - soft
        if masked:
            keep = lax.broadcasted_iota(jnp.int32, (nrows, bk), 1) < lax.broadcasted_iota(
                jnp.int32, (nrows, bk), 0
            )
            soft = jnp.where(keep, soft, 0.0)
        after = jnp.dot(soft.astype(bf), tri, preferred_element_type=jnp.float32)
        carry = car_ref[acc0 : acc0 + nrows, :]
        a = jnp.exp2(own - after - jnp.concatenate([carry] * (bk // 128), axis=1))
        if masked:
            a = jnp.where(keep, a, 0.0)
        acc_ref[acc0 : acc0 + nrows, :] += jnp.dot(
            a.astype(bf), v_ref[pl.ds(col0, bk), :], preferred_element_type=jnp.float32
        )
        car_ref[acc0 : acc0 + nrows, :] = carry + jnp.broadcast_to((after + soft)[:, :1], (nrows, 128))

    per = bq // bk
    quarter = rows // 2

    def q_tile(i, _):
        base = pl.multiple_of(i * bq, bq)
        acc_ref[...] = jnp.zeros_like(acc_ref)
        car_ref[...] = jnp.zeros_like(car_ref)
        for c in reversed(range(per)):
            for r in range(c, per):
                tile(base + r * bk, bk, r * bk, base + c * bk, r == c)

        def k_tile(j, _):
            col = pl.multiple_of((i - 1 - j) * bq, bq)
            for c in reversed(range(per)):
                tile(base, bq, 0, col + c * bk, False)
            return 0

        lax.fori_loop(0, i, k_tile, 0)
        att = acc_ref[...]
        scaled = att * lax.rsqrt(jnp.mean(att * att, axis=1, keepdims=True) + norm_eps) * gain_ref[...]
        head = scaled.astype(bf)
        count = bq // quarter
        for p in range(count // 2):
            out_ref[pl.ds(i * (count // 2) + p, 1)] = jnp.concatenate(
                [head[2 * p * quarter : (2 * p + 1) * quarter], head[(2 * p + 1) * quarter : (2 * p + 2) * quarter]],
                axis=1,
            )[None]
        return 0

    lax.fori_loop(0, length // bq, q_tile, 0)


def output_kernel(got_ref, own_ref, far_ref, out_ref, heads_ref):
    x, c, z, y = place_of()
    half = got_ref.shape[1]
    for iz in range(SIDE):
        for iy in range(SIDE):
            place = SIDE * lax.rem(z + SIDE - HOPS[iz], SIDE) + lax.rem(y + SIDE - HOPS[iy], SIDE)
            block = got_ref[place]
            at = (SIDE * iz + iy) * HEAD_DIM
            heads_ref[:half, at : at + HEAD_DIM] = block[:, :HEAD_DIM]
            heads_ref[half:, at : at + HEAD_DIM] = block[:, HEAD_DIM:]
    for i in range(SIDE):
        for cc, ref in ((0, own_ref), (1, far_ref)):
            parts = []
            for iz in range(SIDE):
                for iy in range(SIDE):
                    parts.append(ref[i, iz, iy])
            mixed = jnp.dot(
                heads_ref[...], jnp.concatenate(parts, axis=0), preferred_element_type=jnp.float32
            )
            chunk = 2 * lax.rem(x + SIDE - HOPS[i], SIDE) + lax.rem(c + cc, 2)
            out_ref[:, pl.ds(pl.multiple_of(chunk * 256, 256), 256)] = mixed.astype(jnp.bfloat16)


def body(inputs, in_gain, w_query, w_key, w_value, key_bias, out_gain, w_out):
    bf = jnp.bfloat16
    rows, width = inputs.shape[1], inputs.shape[2]
    sp_size = lax.axis_size("sp")
    sp = lax.axis_index("sp")

    wide = inputs[0].astype(jnp.float32)
    normed = (
        wide * lax.rsqrt(jnp.mean(wide * wide, axis=-1, keepdims=True) + norm_eps) * in_gain
    ).astype(bf)

    def spread(perm_of, a, axis):
        return [a] + [lax.ppermute(a, axis, perm_of(k)) for k in HOPS[1:]]

    piece = jnp.concatenate([w_query.T, w_key.T, w_value.T], axis=0)
    four = jnp.stack(spread(along_x, piece, "dp"))
    together = jnp.concatenate([four[:2].reshape(192, 256), w_out], axis=0)
    first_a = jnp.stack(spread(lambda k: along_zy(0, k), together, "sp"))
    first_b = jnp.stack(spread(lambda k: along_zy(k, 0), four[2:], "sp"))
    rest_y = first_a[:, 192:]
    first_a = first_a[:, :192].reshape(SIDE, 2, 96, 256)
    first_a, first_b, normed = lax.optimization_barrier((first_a, first_b, normed))
    own_a = spread(lambda k: along_zy(k, 0), first_a, "sp")
    own_b = spread(lambda k: along_zy(0, k), first_b, "sp")
    own_a, own_b = jnp.stack(own_a), jnp.stack(own_b)
    own_a, rest_y = lax.optimization_barrier((own_a, rest_y))
    far_a = lax.ppermute(own_a, "dp", other_core())
    far_b = lax.ppermute(own_b, "dp", other_core())
    packed = pl.pallas_call(
        project_kernel,
        out_shape=pltpu.VMEM((sp_size, rows + rows // 2, 128), bf),
        in_specs=[VMEM] * 5,
        out_specs=VMEM,
        scratch_shapes=[pltpu.VMEM((rows, width), bf), pltpu.VMEM((sp_size, 96, rows), jnp.float32)],
        compiler_params=pltpu.CompilerParams(vmem_limit_bytes=30 * 2**20),
        name="project",
    )(*near(normed, own_a, own_b, far_a, far_b))
    rest_z = spread(lambda k: along_zy(k, 0), rest_y, "sp")
    _, rest_z = lax.optimization_barrier((packed, rest_z))
    rest_x = spread(along_x, jnp.stack(rest_z), "dp")

    got = lax.all_to_all(packed, "sp", split_axis=0, concat_axis=0, tiled=True)
    gains = lax.dynamic_slice_in_dim(out_gain, sp * HEAD_DIM, HEAD_DIM, 0)[None]
    length = sp_size * rows
    bq, bk = 768, 256
    heads = pl.pallas_call(
        functools.partial(attend_kernel, src=sp_size, rows=rows, bq=bq, bk=bk),
        out_shape=pltpu.VMEM((sp_size, rows // 2, 128), bf),
        in_specs=[VMEM] * 3,
        out_specs=VMEM,
        scratch_shapes=[
            pltpu.VMEM((length, 256), bf),
            pltpu.VMEM((256, length), bf),
            pltpu.VMEM((length, HEAD_DIM), bf),
            pltpu.VMEM((bq, HEAD_DIM), jnp.float32),
            pltpu.VMEM((bq, 128), jnp.float32),
        ],
        compiler_params=pltpu.CompilerParams(vmem_limit_bytes=30 * 2**20),
        name="attend",
    )(*near(got, key_bias.reshape(1, length), gains))
    heads, rest_x = lax.optimization_barrier((heads, rest_x))
    own_out = jnp.stack(rest_x)
    far_out = lax.ppermute(own_out, "dp", other_core())
    returned = lax.all_to_all(heads, "sp", split_axis=0, concat_axis=0, tiled=True)
    mixed = pl.pallas_call(
        output_kernel,
        out_shape=jax.ShapeDtypeStruct((rows, width), bf),
        in_specs=[VMEM] * 3,
        out_specs=VMEM,
        scratch_shapes=[pltpu.VMEM((rows, sp_size * HEAD_DIM), bf)],
        compiler_params=pltpu.CompilerParams(vmem_limit_bytes=30 * 2**20),
        name="output",
    )(*near(returned, own_out, far_out))
    return mixed[None]


def solution(mesh):
    placed = (
        P("dp", "sp", None),
        P(),
        P("dp", "sp"),
        P("dp", "sp"),
        P("dp", "sp"),
        P("dp", None, "sp"),
        P(),
        P("sp", "dp"),
    )

    return jax.shard_map(body, mesh=mesh, in_specs=placed, out_specs=P("dp", "sp", None), check_vma=False)
```

profile of v0, /device:TPU:0, one launch (start us, length us, event | category | flops | bytes accessed | tf_op | source)
XLA Modules:
  0.0 130.4 jit_solution(13991816520030729671)
XLA Ops:
  0.0 0.9 fusion.3
  0.9 2.9 %collective-permute-start.4 = (bf16[96,256]{1,0:T(8,128)(2,1)S(1)}, bf16[96,256]{1,0:T(8,128)(2,1)S(1)}, u32[]{:S(2)}, u32[]{:S(2)}) collective-permute-start(bf16[96,256]{1,0:T(8,128)(2,1)S(1)} %get-tuple-element.38), channel_id=1, source_target_pairs={{0,6},{1,7},{2,0},{3,1},{4,2},{5,3},{6,4},{7,5},{8,14},{9,15},{10,... | collective-permute-start | bytes 147464 | tf_op jit(solution)/shard_map/ppermute | solution.py:203
  4.6 0.9 collective-permute-start
  5.5 1.4 %fusion = f32[192]{0:T(256)S(1)} fusion(bf16[1,192,2048]{2,1,0:T(8,128)(2,1)} %param.8), kind=kLoop, calls=%fused_computation.3 | loop fusion | flops 1179456 | bytes 787200 | tf_op jit(solution)/shard_map/reduce_sum | solution.py:199
  6.8 2.5 %collective-permute-done.5 = bf16[96,256]{1,0:T(8,128)(2,1)S(1)} collective-permute-done((bf16[96,256]{1,0:T(8,128)(2,1)S(1)}, bf16[96,256]{1,0:T(8,128)(2,1)S(1)}, u32[]{:S(2)}, u32[]{:S(2)}) %collective-permute-start.5) | collective-permute-done | bytes 49184 | tf_op jit(solution)/shard_map/ppermute | solution.py:203
  9.4 2.0 %collective-permute-start.6 = (bf16[2,96,256]{2,1,0:T(8,128)(2,1)S(1)}, bf16[2,96,256]{2,1,0:T(8,128)(2,1)S(1)}, u32[]{:S(2)}, u32[]{:S(2)}) collective-permute-start(bf16[2,96,256]{2,1,0:T(8,128)(2,1)S(1)} %get-tuple-element.36), channel_id=1, source_target_pairs={{0,32},{8,40},{16,48},{24,56},{32,64},{40,72},{48,80},{56,88},{64,... | collective-permute-start | bytes 294920 | tf_op jit(solution)/shard_map/ppermute | solution.py:203
  11.4 2.2 %collective-permute-start.7 = (bf16[2,96,256]{2,1,0:T(8,128)(2,1)S(1)}, bf16[2,96,256]{2,1,0:T(8,128)(2,1)S(1)}, u32[]{:S(2)}, u32[]{:S(2)}) collective-permute-start(bf16[2,96,256]{2,1,0:T(8,128)(2,1)S(1)} %get-tuple-element.36), channel_id=1, source_target_pairs={{0,96},{8,104},{16,112},{24,120},{32,0},{40,8},{48,16},{56,24},{64... | collective-permute-start | bytes 294920 | tf_op jit(solution)/shard_map/ppermute | solution.py:203
  13.6 1.8 %collective-permute-start.8 = (bf16[2,96,256]{2,1,0:T(8,128)(2,1)S(1)}, bf16[2,96,256]{2,1,0:T(8,128)(2,1)S(1)}, u32[]{:S(2)}, u32[]{:S(2)}) collective-permute-start(bf16[2,96,256]{2,1,0:T(8,128)(2,1)S(1)} %get-tuple-element.36), channel_id=1, source_target_pairs={{0,64},{8,72},{16,80},{24,88},{32,96},{40,104},{48,112},{56,120},{... | collective-permute-start | bytes 294920 | tf_op jit(solution)/shard_map/ppermute | solution.py:203
  16.2 1.6 %collective-permute-start.1 = (bf16[256,256]{1,0:T(8,128)(2,1)S(1)}, bf16[256,256]{1,0:T(8,128)(2,1)S(1)}, u32[]{:S(2)}, u32[]{:S(2)}) collective-permute-start(bf16[256,256]{1,0:T(8,128)(2,1)S(1)} %get-tuple-element.34), channel_id=1, source_target_pairs={{0,8},{8,16},{16,24},{24,0},{32,40},{40,48},{48,56},{56,32},{64,72... | collective-permute-start | bytes 393224 | tf_op jit(solution)/shard_map/ppermute | solution.py:203
  17.8 1.7 %collective-permute-start.2 = (bf16[256,256]{1,0:T(8,128)(2,1)S(1)}, bf16[256,256]{1,0:T(8,128)(2,1)S(1)}, u32[]{:S(2)}, u32[]{:S(2)}) collective-permute-start(bf16[256,256]{1,0:T(8,128)(2,1)S(1)} %get-tuple-element.34), channel_id=1, source_target_pairs={{0,24},{8,0},{16,8},{24,16},{32,56},{40,32},{48,40},{56,48},{64,88... | collective-permute-start | bytes 393224 | tf_op jit(solution)/shard_map/ppermute | solution.py:203
  19.5 2.0 %collective-permute-start.3 = (bf16[256,256]{1,0:T(8,128)(2,1)S(1)}, bf16[256,256]{1,0:T(8,128)(2,1)S(1)}, u32[]{:S(2)}, u32[]{:S(2)}) collective-permute-start(bf16[256,256]{1,0:T(8,128)(2,1)S(1)} %get-tuple-element.34), channel_id=1, source_target_pairs={{0,16},{8,24},{16,0},{24,8},{32,48},{40,56},{48,32},{56,40},{64,80... | collective-permute-start | bytes 393224 | tf_op jit(solution)/shard_map/ppermute | solution.py:203
  21.8 1.8 %collective-permute-done.1 = bf16[256,256]{1,0:T(8,128)(2,1)S(1)} collective-permute-done((bf16[256,256]{1,0:T(8,128)(2,1)S(1)}, bf16[256,256]{1,0:T(8,128)(2,1)S(1)}, u32[]{:S(2)}, u32[]{:S(2)}) %collective-permute-start.1) | collective-permute-done | bytes 131104 | tf_op jit(solution)/shard_map/ppermute | solution.py:203
  23.5 2.4 %collective-permute-done.3 = bf16[256,256]{1,0:T(8,128)(2,1)S(1)} collective-permute-done((bf16[256,256]{1,0:T(8,128)(2,1)S(1)}, bf16[256,256]{1,0:T(8,128)(2,1)S(1)}, u32[]{:S(2)}, u32[]{:S(2)}) %collective-permute-start.3) | collective-permute-done | bytes 131104 | tf_op jit(solution)/shard_map/ppermute | solution.py:203
  26.6 2.7 %collective-permute-start.13 = (bf16[4,2,96,256]{3,2,1,0:T(8,128)(2,1)S(1)}, bf16[4,2,96,256]{3,2,1,0:T(8,128)(2,1)S(1)}, u32[]{:S(2)}, u32[]{:S(2)}) collective-permute-start(bf16[4,2,96,256]{3,2,1,0:T(8,128)(2,1)S(1)} %pad_maximum_fusion.5), channel_id=1, source_target_pairs={{0,24},{8,0},{16,8},{24,16},{32,56},{40,32},{48,40},{56,48},{64,88... | collective-permute-start | bytes 1179656 | tf_op jit(solution)/shard_map/ppermute | solution.py:203
  29.4 1.8 %collective-permute-start.14 = (bf16[4,2,96,256]{3,2,1,0:T(8,128)(2,1)S(1)}, bf16[4,2,96,256]{3,2,1,0:T(8,128)(2,1)S(1)}, u32[]{:S(2)}, u32[]{:S(2)}) collective-permute-start(bf16[4,2,96,256]{3,2,1,0:T(8,128)(2,1)S(1)} %pad_maximum_fusion.5), channel_id=1, source_target_pairs={{0,16},{8,24},{16,0},{24,8},{32,48},{40,56},{48,32},{56,40},{64,80... | collective-permute-start | bytes 1179656 | tf_op jit(solution)/shard_map/ppermute | solution.py:203
  31.1 1.0 collective-permute-start.9
  32.2 2.2 %collective-permute-start.10 = (bf16[4,2,96,256]{3,2,1,0:T(8,128)(2,1)S(1)}, bf16[4,2,96,256]{3,2,1,0:T(8,128)(2,1)S(1)}, u32[]{:S(2)}, u32[]{:S(2)}) collective-permute-start(bf16[4,2,96,256]{3,2,1,0:T(8,128)(2,1)S(1)} %bitcast.47), channel_id=1, source_target_pairs={{0,96},{8,104},{16,112},{24,120},{32,0},{40,8},{48,16},{56,24},{64... | collective-permute-start | bytes 1179656 | tf_op jit(solution)/shard_map/ppermute | solution.py:203
  34.4 8.5 %collective-permute-done.12 = bf16[4,2,96,256]{3,2,1,0:T(8,128)(2,1)S(1)} collective-permute-done((bf16[4,2,96,256]{3,2,1,0:T(8,128)(2,1)S(1)}, bf16[4,2,96,256]{3,2,1,0:T(8,128)(2,1)S(1)}, u32[]{:S(2)}, u32[]{:S(2)}) %collective-permute-start.12) | collective-permute-done | bytes 393248 | tf_op jit(solution)/shard_map/ppermute | solution.py:203
  43.3 8.9 %collective-permute-done.11 = bf16[4,2,96,256]{3,2,1,0:T(8,128)(2,1)S(1)} collective-permute-done((bf16[4,2,96,256]{3,2,1,0:T(8,128)(2,1)S(1)}, bf16[4,2,96,256]{3,2,1,0:T(8,128)(2,1)S(1)}, u32[]{:S(2)}, u32[]{:S(2)}) %collective-permute-start.11) | collective-permute-done | bytes 393248 | tf_op jit(solution)/shard_map/ppermute | solution.py:203
  52.5 3.4 %collective-permute-done.15.far_a = bf16[4,4,2,96,256]{4,3,2,1,0:T(8,128)(2,1)S(1)} collective-permute-done((bf16[4,4,2,96,256]{4,3,2,1,0:T(8,128)(2,1)S(1)}, bf16[4,4,2,96,256]{4,3,2,1,0:T(8,128)(2,1)S(1)}, u32[]{:S(2)}, u32[]{:S(2)}) %collective-permute-start.15) | collective-permute-done | bytes 1572896 | tf_op jit(solution)/shard_map/ppermute | solution.py:217
  55.9 3.3 %project.1 = bf16[16,288,128]{2,1,0:T(8,128)(2,1)} custom-call(bf16[192,2048]{1,0:T(8,128)(2,1)S(1)} %fusion.2.normed_ref, bf16[4,4,2,96,256]{4,3,2,1,0:T(8,128)(2,1)S(1)} %pad_maximum_fusion.1.own_a, bf16[4,4,2,96,256]{4,3,2,1,0:T(8,128)(2,1)S(1)} %pad_maximum_fusion.2.own_b, bf16[4,4,2,96,256]{4,3,2,1,0:T(8,128)(2,1)S(1)} %collective-permute-done.15.far_a, ...), custom_call_target="tpu_custom_call" | custom-call | tf_op jit(solution)/shard_map/project/pallas_call | solution.py:219
  59.2 5.1 %all-to-all-start = ((bf16[16,288,128]{2,1,0:T(8,128)(2,1)}), bf16[16,288,128]{2,1,0:T(8,128)(2,1)S(1)}, u32[]{:S(2)}, u32[]{:S(2)}) async-start(bf16[16,288,128]{2,1,0:T(8,128)(2,1)} %project.1), calls=%async_computation | async-start | bytes 2359296 | tf_op jit(solution)/shard_map/all_to_all | solution.py:232
  64.3 1.9 %collective-permute-start.17 = (bf16[4,64,256]{2,1,0:T(8,128)(2,1)S(1)}, bf16[4,64,256]{2,1,0:T(8,128)(2,1)S(1)}, u32[]{:S(2)}, u32[]{:S(2)}) collective-permute-start(bf16[4,64,256]{2,1,0:T(8,128)(2,1)S(1)} %pad_maximum_fusion.6), channel_id=1, source_target_pairs={{0,32},{8,40},{16,48},{24,56},{32,64},{40,72},{48,80},{56,88},{64,... | collective-permute-start | bytes 393224 | tf_op jit(solution)/shard_map/ppermute | solution.py:203
  66.2 1.4 %collective-permute-start.18 = (bf16[4,64,256]{2,1,0:T(8,128)(2,1)S(1)}, bf16[4,64,256]{2,1,0:T(8,128)(2,1)S(1)}, u32[]{:S(2)}, u32[]{:S(2)}) collective-permute-start(bf16[4,64,256]{2,1,0:T(8,128)(2,1)S(1)} %pad_maximum_fusion.6), channel_id=1, source_target_pairs={{0,96},{8,104},{16,112},{24,120},{32,0},{40,8},{48,16},{56,24},{64... | collective-permute-start | bytes 393224 | tf_op jit(solution)/shard_map/ppermute | solution.py:203
  67.6 2.2 %collective-permute-start.19 = (bf16[4,64,256]{2,1,0:T(8,128)(2,1)S(1)}, bf16[4,64,256]{2,1,0:T(8,128)(2,1)S(1)}, u32[]{:S(2)}, u32[]{:S(2)}) collective-permute-start(bf16[4,64,256]{2,1,0:T(8,128)(2,1)S(1)} %pad_maximum_fusion.6), channel_id=1, source_target_pairs={{0,64},{8,72},{16,80},{24,88},{32,96},{40,104},{48,112},{56,120},{... | collective-permute-start | bytes 393224 | tf_op jit(solution)/shard_map/ppermute | solution.py:203
  69.8 13.4 %collective-permute-done.17 = bf16[4,64,256]{2,1,0:T(8,128)(2,1)S(1)} collective-permute-done((bf16[4,64,256]{2,1,0:T(8,128)(2,1)S(1)}, bf16[4,64,256]{2,1,0:T(8,128)(2,1)S(1)}, u32[]{:S(2)}, u32[]{:S(2)}) %collective-permute-start.17) | collective-permute-done | bytes 131104 | tf_op jit(solution)/shard_map/ppermute | solution.py:203
  83.4 3.2 %collective-permute-done.19 = bf16[4,64,256]{2,1,0:T(8,128)(2,1)S(1)} collective-permute-done((bf16[4,64,256]{2,1,0:T(8,128)(2,1)S(1)}, bf16[4,64,256]{2,1,0:T(8,128)(2,1)S(1)}, u32[]{:S(2)}, u32[]{:S(2)}) %collective-permute-start.19) | collective-permute-done | bytes 131104 | tf_op jit(solution)/shard_map/ppermute | solution.py:203
  86.8 3.2 %collective-permute-start.21 = (bf16[4,4,64,256]{3,2,1,0:T(8,128)(2,1)S(1)}, bf16[4,4,64,256]{3,2,1,0:T(8,128)(2,1)S(1)}, u32[]{:S(2)}, u32[]{:S(2)}) collective-permute-start(bf16[4,4,64,256]{3,2,1,0:T(8,128)(2,1)S(1)} %pad_maximum_fusion.4), channel_id=1, source_target_pairs={{0,6},{1,7},{2,0},{3,1},{4,2},{5,3},{6,4},{7,5},{8,14},{9,15},{10,... | collective-permute-start | bytes 1572872 | tf_op jit(solution)/shard_map/ppermute | solution.py:203
  90.1 17.2 %attend.1 = bf16[16,96,128]{2,1,0:T(8,128)(2,1)S(1)} custom-call(bf16[16,288,128]{2,1,0:T(8,128)(2,1)S(1)} %all-to-all-done.got_ref, f32[1,3072]{1,0:T(1,128)S(1)} %bitcast.44, f32[1,64]{1,0:T(1,128)S(1)} %dynamic-slice_bitcast_fusion.gain_ref), custom_call_target="tpu_custom_call" | custom-call | tf_op jit(solution)/shard_map/attend/pallas_call | solution.py:236
  107.3 4.7 %collective-permute-done.20 = bf16[4,4,64,256]{3,2,1,0:T(8,128)(2,1)S(1)} collective-permute-done((bf16[4,4,64,256]{3,2,1,0:T(8,128)(2,1)S(1)}, bf16[4,4,64,256]{3,2,1,0:T(8,128)(2,1)S(1)}, u32[]{:S(2)}, u32[]{:S(2)}) %collective-permute-start.20) | collective-permute-done | bytes 524320 | tf_op jit(solution)/shard_map/ppermute | solution.py:203
  112.4 15.9 %all_to_all.10.got_ref = bf16[16,96,128]{2,1,0:T(8,128)(2,1)S(1)} all-to-all(bf16[16,96,128]{2,1,0:T(8,128)(2,1)S(1)} %attend.1), channel_id=1, replica_groups=mesh['sp'=16,'dp'=8] {'sp'}, dimensions={0} | all-to-all | bytes 786432 | tf_op jit(solution)/shard_map/all_to_all | solution.py:254
  128.3 2.1 %output.1 = bf16[192,2048]{1,0:T(8,128)(2,1)} custom-call(bf16[16,96,128]{2,1,0:T(8,128)(2,1)S(1)} %all_to_all.10.got_ref, bf16[4,4,4,64,256]{4,3,2,1,0:T(8,128)(2,1)S(1)} %pad_maximum_fusion.own_ref, bf16[4,4,4,64,256]{4,3,2,1,0:T(8,128)(2,1)S(1)} %collective-permute-done.23.far_ref), custom_call_target="tpu_custom_call" | custom-call | tf_op jit(solution)/shard_map/output/pallas_call | solution.py:255
  (46 shorter events, 4.0 us)
Async XLA Ops:
  0.0 90.0 %copy-start = (f32[1024]{0:T(1024)S(1)}, f32[1024]{0:T(1024)}, u32[]{:S(2)}) copy-start(f32[1024]{0:T(1024)} %param.14) | copy-start | bytes 12292
  0.0 21.4 %copy-start.2 = (bf16[1,192,2048]{2,1,0:T(8,128)(2,1)S(1)}, bf16[1,192,2048]{2,1,0:T(8,128)(2,1)}, u32[]{:S(2)}) copy-start(bf16[1,192,2048]{2,1,0:T(8,128)(2,1)} %param.8) | copy-start | bytes 2359300
  0.0 21.4 %copy-start.3 = (f32[2048]{0:T(1024)S(1)}, f32[2048]{0:T(1024)}, u32[]{:S(2)}) copy-start(f32[2048]{0:T(1024)} %param.9) | copy-start | bytes 24580
  0.9 6.0 %collective-permute-start.4 = (bf16[96,256]{1,0:T(8,128)(2,1)S(1)}, bf16[96,256]{1,0:T(8,128)(2,1)S(1)}, u32[]{:S(2)}, u32[]{:S(2)}) collective-permute-start(bf16[96,256]{1,0:T(8,128)(2,1)S(1)} %get-tuple-element.38), channel_id=1, source_target_pairs={{0,6},{1,7},{2,0},{3,1},{4,2},{5,3},{6,4},{7,5},{8,14},{9,15},{10,... | collective-permute-start | bytes 147464 | tf_op jit(solution)/shard_map/ppermute | solution.py:203
  3.8 5.6 %collective-permute-start.5 = (bf16[96,256]{1,0:T(8,128)(2,1)S(1)}, bf16[96,256]{1,0:T(8,128)(2,1)S(1)}, u32[]{:S(2)}, u32[]{:S(2)}) collective-permute-start(bf16[96,256]{1,0:T(8,128)(2,1)S(1)} %get-tuple-element.38), channel_id=1, source_target_pairs={{0,4},{1,5},{2,6},{3,7},{4,0},{5,1},{6,2},{7,3},{8,12},{9,13},{10,... | collective-permute-start | bytes 147464 | tf_op jit(solution)/shard_map/ppermute | solution.py:203
  4.6 10.8 %collective-permute-start = (bf16[96,256]{1,0:T(8,128)(2,1)S(1)}, bf16[96,256]{1,0:T(8,128)(2,1)S(1)}, u32[]{:S(2)}, u32[]{:S(2)}) collective-permute-start(bf16[96,256]{1,0:T(8,128)(2,1)S(1)} %get-tuple-element.38), channel_id=1, source_target_pairs={{0,2},{1,3},{2,4},{3,5},{4,6},{5,7},{6,0},{7,1},{8,10},{9,11},{10,... | collective-permute-start | bytes 147464 | tf_op jit(solution)/shard_map/ppermute | solution.py:203
  9.4 10.1 %collective-permute-start.6 = (bf16[2,96,256]{2,1,0:T(8,128)(2,1)S(1)}, bf16[2,96,256]{2,1,0:T(8,128)(2,1)S(1)}, u32[]{:S(2)}, u32[]{:S(2)}) collective-permute-start(bf16[2,96,256]{2,1,0:T(8,128)(2,1)S(1)} %get-tuple-element.36), channel_id=1, source_target_pairs={{0,32},{8,40},{16,48},{24,56},{32,64},{40,72},{48,80},{56,88},{64,... | collective-permute-start | bytes 294920 | tf_op jit(solution)/shard_map/ppermute | solution.py:203
  11.4 10.3 %collective-permute-start.7 = (bf16[2,96,256]{2,1,0:T(8,128)(2,1)S(1)}, bf16[2,96,256]{2,1,0:T(8,128)(2,1)S(1)}, u32[]{:S(2)}, u32[]{:S(2)}) collective-permute-start(bf16[2,96,256]{2,1,0:T(8,128)(2,1)S(1)} %get-tuple-element.36), channel_id=1, source_target_pairs={{0,96},{8,104},{16,112},{24,120},{32,0},{40,8},{48,16},{56,24},{64... | collective-permute-start | bytes 294920 | tf_op jit(solution)/shard_map/ppermute | solution.py:203
  13.6 8.2 %collective-permute-start.8 = (bf16[2,96,256]{2,1,0:T(8,128)(2,1)S(1)}, bf16[2,96,256]{2,1,0:T(8,128)(2,1)S(1)}, u32[]{:S(2)}, u32[]{:S(2)}) collective-permute-start(bf16[2,96,256]{2,1,0:T(8,128)(2,1)S(1)} %get-tuple-element.36), channel_id=1, source_target_pairs={{0,64},{8,72},{16,80},{24,88},{32,96},{40,104},{48,112},{56,120},{... | collective-permute-start | bytes 294920 | tf_op jit(solution)/shard_map/ppermute | solution.py:203
  16.2 7.4 %collective-permute-start.1 = (bf16[256,256]{1,0:T(8,128)(2,1)S(1)}, bf16[256,256]{1,0:T(8,128)(2,1)S(1)}, u32[]{:S(2)}, u32[]{:S(2)}) collective-permute-start(bf16[256,256]{1,0:T(8,128)(2,1)S(1)} %get-tuple-element.34), channel_id=1, source_target_pairs={{0,8},{8,16},{16,24},{24,0},{32,40},{40,48},{48,56},{56,32},{64,72... | collective-permute-start | bytes 393224 | tf_op jit(solution)/shard_map/ppermute | solution.py:203
  17.8 5.7 %collective-permute-start.2 = (bf16[256,256]{1,0:T(8,128)(2,1)S(1)}, bf16[256,256]{1,0:T(8,128)(2,1)S(1)}, u32[]{:S(2)}, u32[]{:S(2)}) collective-permute-start(bf16[256,256]{1,0:T(8,128)(2,1)S(1)} %get-tuple-element.34), channel_id=1, source_target_pairs={{0,24},{8,0},{16,8},{24,16},{32,56},{40,32},{48,40},{56,48},{64,88... | collective-permute-start | bytes 393224 | tf_op jit(solution)/shard_map/ppermute | solution.py:203
  19.5 6.5 %collective-permute-start.3 = (bf16[256,256]{1,0:T(8,128)(2,1)S(1)}, bf16[256,256]{1,0:T(8,128)(2,1)S(1)}, u32[]{:S(2)}, u32[]{:S(2)}) collective-permute-start(bf16[256,256]{1,0:T(8,128)(2,1)S(1)} %get-tuple-element.34), channel_id=1, source_target_pairs={{0,16},{8,24},{16,0},{24,8},{32,48},{40,56},{48,32},{56,40},{64,80... | collective-permute-start | bytes 393224 | tf_op jit(solution)/shard_map/ppermute | solution.py:203
  26.0 16.8 %collective-permute-start.12 = (bf16[4,2,96,256]{3,2,1,0:T(8,128)(2,1)S(1)}, bf16[4,2,96,256]{3,2,1,0:T(8,128)(2,1)S(1)}, u32[]{:S(2)}, u32[]{:S(2)}) collective-permute-start(bf16[4,2,96,256]{3,2,1,0:T(8,128)(2,1)S(1)} %pad_maximum_fusion.5), channel_id=1, source_target_pairs={{0,8},{8,16},{16,24},{24,0},{32,40},{40,48},{48,56},{56,32},{64,72... | collective-permute-start | bytes 1179656 | tf_op jit(solution)/shard_map/ppermute | solution.py:203
  26.6 16.3 %collective-permute-start.13 = (bf16[4,2,96,256]{3,2,1,0:T(8,128)(2,1)S(1)}, bf16[4,2,96,256]{3,2,1,0:T(8,128)(2,1)S(1)}, u32[]{:S(2)}, u32[]{:S(2)}) collective-permute-start(bf16[4,2,96,256]{3,2,1,0:T(8,128)(2,1)S(1)} %pad_maximum_fusion.5), channel_id=1, source_target_pairs={{0,24},{8,0},{16,8},{24,16},{32,56},{40,32},{48,40},{56,48},{64,88... | collective-permute-start | bytes 1179656 | tf_op jit(solution)/shard_map/ppermute | solution.py:203
  29.4 13.6 %collective-permute-start.14 = (bf16[4,2,96,256]{3,2,1,0:T(8,128)(2,1)S(1)}, bf16[4,2,96,256]{3,2,1,0:T(8,128)(2,1)S(1)}, u32[]{:S(2)}, u32[]{:S(2)}) collective-permute-start(bf16[4,2,96,256]{3,2,1,0:T(8,128)(2,1)S(1)} %pad_maximum_fusion.5), channel_id=1, source_target_pairs={{0,16},{8,24},{16,0},{24,8},{32,48},{40,56},{48,32},{56,40},{64,80... | collective-permute-start | bytes 1179656 | tf_op jit(solution)/shard_map/ppermute | solution.py:203
  31.1 12.1 %collective-permute-start.9 = (bf16[4,2,96,256]{3,2,1,0:T(8,128)(2,1)S(1)}, bf16[4,2,96,256]{3,2,1,0:T(8,128)(2,1)S(1)}, u32[]{:S(2)}, u32[]{:S(2)}) collective-permute-start(bf16[4,2,96,256]{3,2,1,0:T(8,128)(2,1)S(1)} %bitcast.46), channel_id=1, source_target_pairs={{0,32},{8,40},{16,48},{24,56},{32,64},{40,72},{48,80},{56,88},{64,... | collective-permute-start | bytes 1179656 | tf_op jit(solution)/shard_map/ppermute | solution.py:203
  32.2 11.1 %collective-permute-start.10 = (bf16[4,2,96,256]{3,2,1,0:T(8,128)(2,1)S(1)}, bf16[4,2,96,256]{3,2,1,0:T(8,128)(2,1)S(1)}, u32[]{:S(2)}, u32[]{:S(2)}) collective-permute-start(bf16[4,2,96,256]{3,2,1,0:T(8,128)(2,1)S(1)} %bitcast.47), channel_id=1, source_target_pairs={{0,96},{8,104},{16,112},{24,120},{32,0},{40,8},{48,16},{56,24},{64... | collective-permute-start | bytes 1179656 | tf_op jit(solution)/shard_map/ppermute | solution.py:203
  42.9 9.3 %collective-permute-start.11 = (bf16[4,2,96,256]{3,2,1,0:T(8,128)(2,1)S(1)}, bf16[4,2,96,256]{3,2,1,0:T(8,128)(2,1)S(1)}, u32[]{:S(2)}, u32[]{:S(2)}) collective-permute-start(bf16[4,2,96,256]{3,2,1,0:T(8,128)(2,1)S(1)} %bitcast.48), channel_id=1, source_target_pairs={{0,64},{8,72},{16,80},{24,88},{32,96},{40,104},{48,112},{56,120},{... | collective-permute-start | bytes 1179656 | tf_op jit(solution)/shard_map/ppermute | solution.py:203
  43.1 9.3 %collective-permute-start.16 = (bf16[4,4,2,96,256]{4,3,2,1,0:T(8,128)(2,1)S(1)}, bf16[4,4,2,96,256]{4,3,2,1,0:T(8,128)(2,1)S(1)}, u32[]{:S(2)}, u32[]{:S(2)}) collective-permute-start(bf16[4,4,2,96,256]{4,3,2,1,0:T(8,128)(2,1)S(1)} %pad_maximum_fusion.2.own_b), channel_id=1, source_target_pairs={{0,1},{1,0},{2,3},{3,2},{4,5},{5,4},{6,7},{7,6},{8,9},{9,8},{10,11... | collective-permute-start | bytes 4718600 | tf_op jit(solution)/shard_map/ppermute | solution.py:218
  52.4 3.5 %collective-permute-start.15 = (bf16[4,4,2,96,256]{4,3,2,1,0:T(8,128)(2,1)S(1)}, bf16[4,4,2,96,256]{4,3,2,1,0:T(8,128)(2,1)S(1)}, u32[]{:S(2)}, u32[]{:S(2)}) collective-permute-start(bf16[4,4,2,96,256]{4,3,2,1,0:T(8,128)(2,1)S(1)} %pad_maximum_fusion.1.own_a), channel_id=1, source_target_pairs={{0,1},{1,0},{2,3},{3,2},{4,5},{5,4},{6,7},{7,6},{8,9},{9,8},{10,11... | collective-permute-start | bytes 4718600 | tf_op jit(solution)/shard_map/ppermute | solution.py:217
  59.2 30.9 %copy-start.1 = (f32[1,3072,1]{1,2,0:T(1,128)S(1)}, f32[1,3072,1]{1,2,0:T(1,128)}, u32[]{:S(2)}) copy-start(f32[1,3072,1]{1,2,0:T(1,128)} %param.13) | copy-start | bytes 36868
  59.2 30.9 %all-to-all-start = ((bf16[16,288,128]{2,1,0:T(8,128)(2,1)}), bf16[16,288,128]{2,1,0:T(8,128)(2,1)S(1)}, u32[]{:S(2)}, u32[]{:S(2)}) async-start(bf16[16,288,128]{2,1,0:T(8,128)(2,1)} %project.1), calls=%async_computation | async-start | bytes 2359296 | tf_op jit(solution)/shard_map/all_to_all | solution.py:232
  64.3 18.9 %collective-permute-start.17 = (bf16[4,64,256]{2,1,0:T(8,128)(2,1)S(1)}, bf16[4,64,256]{2,1,0:T(8,128)(2,1)S(1)}, u32[]{:S(2)}, u32[]{:S(2)}) collective-permute-start(bf16[4,64,256]{2,1,0:T(8,128)(2,1)S(1)} %pad_maximum_fusion.6), channel_id=1, source_target_pairs={{0,32},{8,40},{16,48},{24,56},{32,64},{40,72},{48,80},{56,88},{64,... | collective-permute-start | bytes 393224 | tf_op jit(solution)/shard_map/ppermute | solution.py:203
  66.2 17.2 %collective-permute-start.18 = (bf16[4,64,256]{2,1,0:T(8,128)(2,1)S(1)}, bf16[4,64,256]{2,1,0:T(8,128)(2,1)S(1)}, u32[]{:S(2)}, u32[]{:S(2)}) collective-permute-start(bf16[4,64,256]{2,1,0:T(8,128)(2,1)S(1)} %pad_maximum_fusion.6), channel_id=1, source_target_pairs={{0,96},{8,104},{16,112},{24,120},{32,0},{40,8},{48,16},{56,24},{64... | collective-permute-start | bytes 393224 | tf_op jit(solution)/shard_map/ppermute | solution.py:203
  67.6 19.0 %collective-permute-start.19 = (bf16[4,64,256]{2,1,0:T(8,128)(2,1)S(1)}, bf16[4,64,256]{2,1,0:T(8,128)(2,1)S(1)}, u32[]{:S(2)}, u32[]{:S(2)}) collective-permute-start(bf16[4,64,256]{2,1,0:T(8,128)(2,1)S(1)} %pad_maximum_fusion.6), channel_id=1, source_target_pairs={{0,64},{8,72},{16,80},{24,88},{32,96},{40,104},{48,112},{56,120},{... | collective-permute-start | bytes 393224 | tf_op jit(solution)/shard_map/ppermute | solution.py:203
  86.7 25.3 %collective-permute-start.20 = (bf16[4,4,64,256]{3,2,1,0:T(8,128)(2,1)S(1)}, bf16[4,4,64,256]{3,2,1,0:T(8,128)(2,1)S(1)}, u32[]{:S(2)}, u32[]{:S(2)}) collective-permute-start(bf16[4,4,64,256]{3,2,1,0:T(8,128)(2,1)S(1)} %pad_maximum_fusion.4), channel_id=1, source_target_pairs={{0,2},{1,3},{2,4},{3,5},{4,6},{5,7},{6,0},{7,1},{8,10},{9,11},{10,... | collective-permute-start | bytes 1572872 | tf_op jit(solution)/shard_map/ppermute | solution.py:203
  86.8 25.3 %collective-permute-start.21 = (bf16[4,4,64,256]{3,2,1,0:T(8,128)(2,1)S(1)}, bf16[4,4,64,256]{3,2,1,0:T(8,128)(2,1)S(1)}, u32[]{:S(2)}, u32[]{:S(2)}) collective-permute-start(bf16[4,4,64,256]{3,2,1,0:T(8,128)(2,1)S(1)} %pad_maximum_fusion.4), channel_id=1, source_target_pairs={{0,6},{1,7},{2,0},{3,1},{4,2},{5,3},{6,4},{7,5},{8,14},{9,15},{10,... | collective-permute-start | bytes 1572872 | tf_op jit(solution)/shard_map/ppermute | solution.py:203
  90.0 22.0 %collective-permute-start.22 = (bf16[4,4,64,256]{3,2,1,0:T(8,128)(2,1)S(1)}, bf16[4,4,64,256]{3,2,1,0:T(8,128)(2,1)S(1)}, u32[]{:S(2)}, u32[]{:S(2)}) collective-permute-start(bf16[4,4,64,256]{3,2,1,0:T(8,128)(2,1)S(1)} %pad_maximum_fusion.4), channel_id=1, source_target_pairs={{0,4},{1,5},{2,6},{3,7},{4,0},{5,1},{6,2},{7,3},{8,12},{9,13},{10,... | collective-permute-start | bytes 1572872 | tf_op jit(solution)/shard_map/ppermute | solution.py:203
  112.3 16.0 %collective-permute-start.23 = (bf16[4,4,4,64,256]{4,3,2,1,0:T(8,128)(2,1)S(1)}, bf16[4,4,4,64,256]{4,3,2,1,0:T(8,128)(2,1)S(1)}, u32[]{:S(2)}, u32[]{:S(2)}) collective-permute-start(bf16[4,4,4,64,256]{4,3,2,1,0:T(8,128)(2,1)S(1)} %pad_maximum_fusion.own_ref), channel_id=1, source_target_pairs={{0,1},{1,0},{2,3},{3,2},{4,5},{5,4},{6,7},{7,6},{8,9},{9,8},{10,11... | collective-permute-start | bytes 6291464 | tf_op jit(solution)/shard_map/ppermute | solution.py:253
where the time goes:
time: 131 us; the launch traced here: 130 us
  waiting for transfers between devices  49.1 us (37%)
  starting transfers between devices  38.3 us (29%)
  Pallas kernels  22.6 us (17%)
  blocking collectives  15.9 us (12%)
  other arithmetic  4.16 us (3%)
    ppermute x21, waiting for transfers between devices, spread(): return [a] + [lax.ppermute(a, axis, perm_of(k)) for k in HOPS[1:]]  45.7 us
    ppermute x21, starting transfers between devices, spread(): return [a] + [lax.ppermute(a, axis, perm_of(k)) for k in HOPS[1:]]  32.9 us
    pallas_call x1, Pallas kernels, body(): pl.pallas_call(functools.partial(attend_kernel, src=sp_size, rows=rows, b...  17.2 us
    all_to_all x1, blocking collectives, body(): lax.all_to_all(heads, 'sp', split_axis=0, concat_axis=0, tiled=True)  15.9 us
    all_to_all x1, starting transfers between devices, body(): got = lax.all_to_all(packed, 'sp', split_axis=0, concat_axis=0, tiled=True)  5.11 us
    ppermute x1, waiting for transfers between devices, body(): far_a = lax.ppermute(own_a, 'dp', other_core())  3.39 us
    pallas_call x1, Pallas kernels, body(): pl.pallas_call(project_kernel, out_shape=pltpu.VMEM((sp_size, rows + rows...  3.32 us
  transfers between devices with their start and end apart: 25, of which 10 were waited for; matrix products, arithmetic and copies ran while one was open for 2% of the time, Pallas kernels for 13%

commit v1 on v0

--- a/solution.py
+++ b/solution.py
@@ -78,7 +78,15 @@
             out_ref[h, rows:, :] = jnp.concatenate([turned[:half], turned[half:]], axis=1)
 
 
-def attend_kernel(got_ref, bias_ref, gain_ref, out_ref, qa_ref, kt_ref, v_ref, acc_ref, car_ref, *, src, rows, bq, bk):
+def masked(block, mask):
+    rows = mask.shape[0]
+    first = block[:rows] * mask
+    return first if block.shape[0] == rows else jnp.concatenate([first, block[rows:]], axis=0)
+
+
+def attend_kernel(
+    got_ref, bias_ref, gain_ref, out_ref, qa_ref, kt_ref, v_ref, acc_ref, car_ref, mask_ref, tri_ref, *, src, rows, bk
+):
     bf = jnp.bfloat16
     half = rows // 2
     length = src * rows
@@ -108,61 +116,31 @@
     tail = jnp.where(row == 0, b_high, jnp.where(row == 1, b_mid, jnp.where(row == 2, b_low, 0.0)))
     kt_ref[2 * HEAD_DIM :, :] = tail.astype(bf)
 
-    tri = (
-        lax.broadcasted_iota(jnp.int32, (bk, bk), 0) > lax.broadcasted_iota(jnp.int32, (bk, bk), 1)
-    ).astype(bf)
-
-    def tile(row0, nrows, acc0, col0, masked):
-        x = jnp.dot(
-            qa_ref[pl.ds(row0, nrows), :], kt_ref[:, pl.ds(col0, bk)], preferred_element_type=jnp.float32
-        )
+    below = lax.broadcasted_iota(jnp.int32, (bk, bk), 0) > lax.broadcasted_iota(jnp.int32, (bk, bk), 1)
+    mask_ref[...] = jnp.where(below, 1.0, 0.0)
+    tri_ref[...] = jnp.where(below, 1.0, 0.0).astype(bf)
+    acc_ref[...] = jnp.zeros_like(acc_ref)
+    car_ref[...] = jnp.zeros_like(car_ref)
+
+    for c in reversed(range(length // bk)):
+        at = c * bk
+        x = jnp.dot(qa_ref[at:, :], kt_ref[:, at : at + bk], preferred_element_type=jnp.float32)
         soft = jnp.maximum(x, jnp.log2(1.0 + jnp.exp2(jnp.minimum(x, 126.0))))
         own = x - soft
-        if masked:
-            keep = lax.broadcasted_iota(jnp.int32, (nrows, bk), 1) < lax.broadcasted_iota(
-                jnp.int32, (nrows, bk), 0
-            )
-            soft = jnp.where(keep, soft, 0.0)
-        after = jnp.dot(soft.astype(bf), tri, preferred_element_type=jnp.float32)
-        carry = car_ref[acc0 : acc0 + nrows, :]
-        a = jnp.exp2(own - after - jnp.concatenate([carry] * (bk // 128), axis=1))
-        if masked:
-            a = jnp.where(keep, a, 0.0)
-        acc_ref[acc0 : acc0 + nrows, :] += jnp.dot(
-            a.astype(bf), v_ref[pl.ds(col0, bk), :], preferred_element_type=jnp.float32
-        )
-        car_ref[acc0 : acc0 + nrows, :] = carry + jnp.broadcast_to((after + soft)[:, :1], (nrows, 128))
-
-    per = bq // bk
-    quarter = rows // 2
-
-    def q_tile(i, _):
-        base = pl.multiple_of(i * bq, bq)
-        acc_ref[...] = jnp.zeros_like(acc_ref)
-        car_ref[...] = jnp.zeros_like(car_ref)
-        for c in reversed(range(per)):
-            for r in range(c, per):
-                tile(base + r * bk, bk, r * bk, base + c * bk, r == c)
-
-        def k_tile(j, _):
-            col = pl.multiple_of((i - 1 - j) * bq, bq)
-            for c in reversed(range(per)):
-                tile(base, bq, 0, col + c * bk, False)
-            return 0
-
-        lax.fori_loop(0, i, k_tile, 0)
-        att = acc_ref[...]
+        soft = masked(soft, mask_ref[...])
+        after = jnp.dot(soft.astype(bf), tri_ref[...], preferred_element_type=jnp.float32)
+        a = masked(jnp.exp2(own - after), mask_ref[...])
+        carry = car_ref[at:, :]
+        here = jnp.dot(a.astype(bf), v_ref[at : at + bk, :], preferred_element_type=jnp.float32)
+        acc_ref[at:, :] += here * jnp.exp2(-carry)[:, :HEAD_DIM]
+        total = after[:, :128] + soft[:, :128]
+        car_ref[at:, :] = carry + jnp.broadcast_to(total[:, :1], carry.shape)
+
+    for b in range(src):
+        att = acc_ref[b * rows : (b + 1) * rows, :]
         scaled = att * lax.rsqrt(jnp.mean(att * att, axis=1, keepdims=True) + norm_eps) * gain_ref[...]
         head = scaled.astype(bf)
-        count = bq // quarter
-        for p in range(count // 2):
-            out_ref[pl.ds(i * (count // 2) + p, 1)] = jnp.concatenate(
-                [head[2 * p * quarter : (2 * p + 1) * quarter], head[(2 * p + 1) * quarter : (2 * p + 2) * quarter]],
-                axis=1,
-            )[None]
-        return 0
-
-    lax.fori_loop(0, length // bq, q_tile, 0)
+        out_ref[b] = jnp.concatenate([head[:half], head[half:]], axis=1)
 
 
 def output_kernel(got_ref, own_ref, far_ref, out_ref, heads_ref):
@@ -232,9 +210,9 @@
     got = lax.all_to_all(packed, "sp", split_axis=0, concat_axis=0, tiled=True)
     gains = lax.dynamic_slice_in_dim(out_gain, sp * HEAD_DIM, HEAD_DIM, 0)[None]
     length = sp_size * rows
-    bq, bk = 768, 256
+    bk = 256
     heads = pl.pallas_call(
-        functools.partial(attend_kernel, src=sp_size, rows=rows, bq=bq, bk=bk),
+        functools.partial(attend_kernel, src=sp_size, rows=rows, bk=bk),
         out_shape=pltpu.VMEM((sp_size, rows // 2, 128), bf),
         in_specs=[VMEM] * 3,
         out_specs=VMEM,
@@ -242,8 +220,10 @@
             pltpu.VMEM((length, 256), bf),
             pltpu.VMEM((256, length), bf),
             pltpu.VMEM((length, HEAD_DIM), bf),
-            pltpu.VMEM((bq, HEAD_DIM), jnp.float32),
-            pltpu.VMEM((bq, 128), jnp.float32),
+            pltpu.VMEM((length, HEAD_DIM), jnp.float32),
+            pltpu.VMEM((length, 128), jnp.float32),
+            pltpu.VMEM((bk, bk), jnp.float32),
+            pltpu.VMEM((bk, bk), bf),
         ],
         compiler_params=pltpu.CompilerParams(vmem_limit_bytes=30 * 2**20),
         name="attend",

time: 131 us -> 131 us (level)
  Pallas kernels: 22.6 us -> 17.7 us
  waiting for transfers between devices: 49.1 us -> 54 us
    ppermute x21, waiting for transfers between devices: 45.7 us -> 50.6 us  [spread(): return [a] + [lax.ppermute(a, axis, perm_of(k)) for k in HOPS[1:]]]
    pallas_call x1, Pallas kernels: 17.2 us -> 12.4 us  [body(): pl.pallas_call(functools.partial(attend_kernel, src=sp_size, rows=rows, b...]
  transfers between devices with their start and end apart: 25 -> 25, of which waited for: 10 -> 10; matrix products, arithmetic and copies ran while one was open for 2% -> 2% of each run, Pallas kernels for 13% -> 9%
where the time goes in v1:
time: 131 us; the launch traced here: 130 us
  waiting for transfers between devices  54 us (41%)
  starting transfers between devices  38.3 us (29%)
  Pallas kernels  17.7 us (14%)
  blocking collectives  15.9 us (12%)
  other arithmetic  4.16 us (3%)
    ppermute x21, waiting for transfers between devices, spread(): return [a] + [lax.ppermute(a, axis, perm_of(k)) for k in HOPS[1:]]  50.6 us
    ppermute x21, starting transfers between devices, spread(): return [a] + [lax.ppermute(a, axis, perm_of(k)) for k in HOPS[1:]]  32.9 us
    all_to_all x1, blocking collectives, body(): lax.all_to_all(heads, 'sp', split_axis=0, concat_axis=0, tiled=True)  15.9 us
    pallas_call x1, Pallas kernels, body(): pl.pallas_call(functools.partial(attend_kernel, src=sp_size, rows=rows, b...  12.4 us
    all_to_all x1, starting transfers between devices, body(): got = lax.all_to_all(packed, 'sp', split_axis=0, concat_axis=0, tiled=True)  5.11 us
    ppermute x1, waiting for transfers between devices, body(): far_a = lax.ppermute(own_a, 'dp', other_core())  3.39 us
    pallas_call x1, Pallas kernels, body(): pl.pallas_call(project_kernel, out_shape=pltpu.VMEM((sp_size, rows + rows...  3.32 us
  transfers between devices with their start and end apart: 25, of which 10 were waited for; matrix products, arithmetic and copies ran while one was open for 2% of the time, Pallas kernels for 9%

profile of v1, /device:TPU:0, one launch (start us, length us, event | category | flops | bytes accessed | tf_op | source)
XLA Modules:
  0.0 130.4 jit_solution(4758957385225601125)
XLA Ops:
  0.0 0.9 fusion.3
  0.9 2.9 %collective-permute-start.4 = (bf16[96,256]{1,0:T(8,128)(2,1)S(1)}, bf16[96,256]{1,0:T(8,128)(2,1)S(1)}, u32[]{:S(2)}, u32[]{:S(2)}) collective-permute-start(bf16[96,256]{1,0:T(8,128)(2,1)S(1)} %get-tuple-element.38), channel_id=1, source_target_pairs={{0,6},{1,7},{2,0},{3,1},{4,2},{5,3},{6,4},{7,5},{8,14},{9,15},{10,... | collective-permute-start | bytes 147464 | tf_op jit(solution)/shard_map/ppermute | solution.py:181
  4.6 0.9 collective-permute-start
  5.5 1.4 %fusion = f32[192]{0:T(256)S(1)} fusion(bf16[1,192,2048]{2,1,0:T(8,128)(2,1)} %param.8), kind=kLoop, calls=%fused_computation.3 | loop fusion | flops 1179456 | bytes 787200 | tf_op jit(solution)/shard_map/reduce_sum | solution.py:177
  6.8 2.5 %collective-permute-done.5 = bf16[96,256]{1,0:T(8,128)(2,1)S(1)} collective-permute-done((bf16[96,256]{1,0:T(8,128)(2,1)S(1)}, bf16[96,256]{1,0:T(8,128)(2,1)S(1)}, u32[]{:S(2)}, u32[]{:S(2)}) %collective-permute-start.5) | collective-permute-done | bytes 49184 | tf_op jit(solution)/shard_map/ppermute | solution.py:181
  9.4 2.0 %collective-permute-start.6 = (bf16[2,96,256]{2,1,0:T(8,128)(2,1)S(1)}, bf16[2,96,256]{2,1,0:T(8,128)(2,1)S(1)}, u32[]{:S(2)}, u32[]{:S(2)}) collective-permute-start(bf16[2,96,256]{2,1,0:T(8,128)(2,1)S(1)} %get-tuple-element.36), channel_id=1, source_target_pairs={{0,32},{8,40},{16,48},{24,56},{32,64},{40,72},{48,80},{56,88},{64,... | collective-permute-start | bytes 294920 | tf_op jit(solution)/shard_map/ppermute | solution.py:181
  11.4 2.2 %collective-permute-start.7 = (bf16[2,96,256]{2,1,0:T(8,128)(2,1)S(1)}, bf16[2,96,256]{2,1,0:T(8,128)(2,1)S(1)}, u32[]{:S(2)}, u32[]{:S(2)}) collective-permute-start(bf16[2,96,256]{2,1,0:T(8,128)(2,1)S(1)} %get-tuple-element.36), channel_id=1, source_target_pairs={{0,96},{8,104},{16,112},{24,120},{32,0},{40,8},{48,16},{56,24},{64... | collective-permute-start | bytes 294920 | tf_op jit(solution)/shard_map/ppermute | solution.py:181
  13.6 1.8 %collective-permute-start.8 = (bf16[2,96,256]{2,1,0:T(8,128)(2,1)S(1)}, bf16[2,96,256]{2,1,0:T(8,128)(2,1)S(1)}, u32[]{:S(2)}, u32[]{:S(2)}) collective-permute-start(bf16[2,96,256]{2,1,0:T(8,128)(2,1)S(1)} %get-tuple-element.36), channel_id=1, source_target_pairs={{0,64},{8,72},{16,80},{24,88},{32,96},{40,104},{48,112},{56,120},{... | collective-permute-start | bytes 294920 | tf_op jit(solution)/shard_map/ppermute | solution.py:181
  16.2 1.6 %collective-permute-start.1 = (bf16[256,256]{1,0:T(8,128)(2,1)S(1)}, bf16[256,256]{1,0:T(8,128)(2,1)S(1)}, u32[]{:S(2)}, u32[]{:S(2)}) collective-permute-start(bf16[256,256]{1,0:T(8,128)(2,1)S(1)} %get-tuple-element.34), channel_id=1, source_target_pairs={{0,8},{8,16},{16,24},{24,0},{32,40},{40,48},{48,56},{56,32},{64,72... | collective-permute-start | bytes 393224 | tf_op jit(solution)/shard_map/ppermute | solution.py:181
  17.8 1.7 %collective-permute-start.2 = (bf16[256,256]{1,0:T(8,128)(2,1)S(1)}, bf16[256,256]{1,0:T(8,128)(2,1)S(1)}, u32[]{:S(2)}, u32[]{:S(2)}) collective-permute-start(bf16[256,256]{1,0:T(8,128)(2,1)S(1)} %get-tuple-element.34), channel_id=1, source_target_pairs={{0,24},{8,0},{16,8},{24,16},{32,56},{40,32},{48,40},{56,48},{64,88... | collective-permute-start | bytes 393224 | tf_op jit(solution)/shard_map/ppermute | solution.py:181
  19.5 2.0 %collective-permute-start.3 = (bf16[256,256]{1,0:T(8,128)(2,1)S(1)}, bf16[256,256]{1,0:T(8,128)(2,1)S(1)}, u32[]{:S(2)}, u32[]{:S(2)}) collective-permute-start(bf16[256,256]{1,0:T(8,128)(2,1)S(1)} %get-tuple-element.34), channel_id=1, source_target_pairs={{0,16},{8,24},{16,0},{24,8},{32,48},{40,56},{48,32},{56,40},{64,80... | collective-permute-start | bytes 393224 | tf_op jit(solution)/shard_map/ppermute | solution.py:181
  21.8 1.8 %collective-permute-done.1 = bf16[256,256]{1,0:T(8,128)(2,1)S(1)} collective-permute-done((bf16[256,256]{1,0:T(8,128)(2,1)S(1)}, bf16[256,256]{1,0:T(8,128)(2,1)S(1)}, u32[]{:S(2)}, u32[]{:S(2)}) %collective-permute-start.1) | collective-permute-done | bytes 131104 | tf_op jit(solution)/shard_map/ppermute | solution.py:181
  23.5 2.4 %collective-permute-done.3 = bf16[256,256]{1,0:T(8,128)(2,1)S(1)} collective-permute-done((bf16[256,256]{1,0:T(8,128)(2,1)S(1)}, bf16[256,256]{1,0:T(8,128)(2,1)S(1)}, u32[]{:S(2)}, u32[]{:S(2)}) %collective-permute-start.3) | collective-permute-done | bytes 131104 | tf_op jit(solution)/shard_map/ppermute | solution.py:181
  26.6 2.7 %collective-permute-start.13 = (bf16[4,2,96,256]{3,2,1,0:T(8,128)(2,1)S(1)}, bf16[4,2,96,256]{3,2,1,0:T(8,128)(2,1)S(1)}, u32[]{:S(2)}, u32[]{:S(2)}) collective-permute-start(bf16[4,2,96,256]{3,2,1,0:T(8,128)(2,1)S(1)} %pad_maximum_fusion.5), channel_id=1, source_target_pairs={{0,24},{8,0},{16,8},{24,16},{32,56},{40,32},{48,40},{56,48},{64,88... | collective-permute-start | bytes 1179656 | tf_op jit(solution)/shard_map/ppermute | solution.py:181
  29.4 1.8 %collective-permute-start.14 = (bf16[4,2,96,256]{3,2,1,0:T(8,128)(2,1)S(1)}, bf16[4,2,96,256]{3,2,1,0:T(8,128)(2,1)S(1)}, u32[]{:S(2)}, u32[]{:S(2)}) collective-permute-start(bf16[4,2,96,256]{3,2,1,0:T(8,128)(2,1)S(1)} %pad_maximum_fusion.5), channel_id=1, source_target_pairs={{0,16},{8,24},{16,0},{24,8},{32,48},{40,56},{48,32},{56,40},{64,80... | collective-permute-start | bytes 1179656 | tf_op jit(solution)/shard_map/ppermute | solution.py:181
  31.1 1.0 collective-permute-start.9
  32.2 2.2 %collective-permute-start.10 = (bf16[4,2,96,256]{3,2,1,0:T(8,128)(2,1)S(1)}, bf16[4,2,96,256]{3,2,1,0:T(8,128)(2,1)S(1)}, u32[]{:S(2)}, u32[]{:S(2)}) collective-permute-start(bf16[4,2,96,256]{3,2,1,0:T(8,128)(2,1)S(1)} %bitcast.47), channel_id=1, source_target_pairs={{0,96},{8,104},{16,112},{24,120},{32,0},{40,8},{48,16},{56,24},{64... | collective-permute-start | bytes 1179656 | tf_op jit(solution)/shard_map/ppermute | solution.py:181
  34.4 8.5 %collective-permute-done.12 = bf16[4,2,96,256]{3,2,1,0:T(8,128)(2,1)S(1)} collective-permute-done((bf16[4,2,96,256]{3,2,1,0:T(8,128)(2,1)S(1)}, bf16[4,2,96,256]{3,2,1,0:T(8,128)(2,1)S(1)}, u32[]{:S(2)}, u32[]{:S(2)}) %collective-permute-start.12) | collective-permute-done | bytes 393248 | tf_op jit(solution)/shard_map/ppermute | solution.py:181
  43.3 8.9 %collective-permute-done.11 = bf16[4,2,96,256]{3,2,1,0:T(8,128)(2,1)S(1)} collective-permute-done((bf16[4,2,96,256]{3,2,1,0:T(8,128)(2,1)S(1)}, bf16[4,2,96,256]{3,2,1,0:T(8,128)(2,1)S(1)}, u32[]{:S(2)}, u32[]{:S(2)}) %collective-permute-start.11) | collective-permute-done | bytes 393248 | tf_op jit(solution)/shard_map/ppermute | solution.py:181
  52.5 3.4 %collective-permute-done.15.far_a = bf16[4,4,2,96,256]{4,3,2,1,0:T(8,128)(2,1)S(1)} collective-permute-done((bf16[4,4,2,96,256]{4,3,2,1,0:T(8,128)(2,1)S(1)}, bf16[4,4,2,96,256]{4,3,2,1,0:T(8,128)(2,1)S(1)}, u32[]{:S(2)}, u32[]{:S(2)}) %collective-permute-start.15) | collective-permute-done | bytes 1572896 | tf_op jit(solution)/shard_map/ppermute | solution.py:195
  55.9 3.3 %project.1 = bf16[16,288,128]{2,1,0:T(8,128)(2,1)} custom-call(bf16[192,2048]{1,0:T(8,128)(2,1)S(1)} %fusion.2.normed_ref, bf16[4,4,2,96,256]{4,3,2,1,0:T(8,128)(2,1)S(1)} %pad_maximum_fusion.1.own_a, bf16[4,4,2,96,256]{4,3,2,1,0:T(8,128)(2,1)S(1)} %pad_maximum_fusion.2.own_b, bf16[4,4,2,96,256]{4,3,2,1,0:T(8,128)(2,1)S(1)} %collective-permute-done.15.far_a, ...), custom_call_target="tpu_custom_call" | custom-call | tf_op jit(solution)/shard_map/project/pallas_call | solution.py:197
  59.2 5.1 %all-to-all-start = ((bf16[16,288,128]{2,1,0:T(8,128)(2,1)}), bf16[16,288,128]{2,1,0:T(8,128)(2,1)S(1)}, u32[]{:S(2)}, u32[]{:S(2)}) async-start(bf16[16,288,128]{2,1,0:T(8,128)(2,1)} %project.1), calls=%async_computation | async-start | bytes 2359296 | tf_op jit(solution)/shard_map/all_to_all | solution.py:210
  64.3 1.9 %collective-permute-start.17 = (bf16[4,64,256]{2,1,0:T(8,128)(2,1)S(1)}, bf16[4,64,256]{2,1,0:T(8,128)(2,1)S(1)}, u32[]{:S(2)}, u32[]{:S(2)}) collective-permute-start(bf16[4,64,256]{2,1,0:T(8,128)(2,1)S(1)} %pad_maximum_fusion.6), channel_id=1, source_target_pairs={{0,32},{8,40},{16,48},{24,56},{32,64},{40,72},{48,80},{56,88},{64,... | collective-permute-start | bytes 393224 | tf_op jit(solution)/shard_map/ppermute | solution.py:181
  66.2 1.4 %collective-permute-start.18 = (bf16[4,64,256]{2,1,0:T(8,128)(2,1)S(1)}, bf16[4,64,256]{2,1,0:T(8,128)(2,1)S(1)}, u32[]{:S(2)}, u32[]{:S(2)}) collective-permute-start(bf16[4,64,256]{2,1,0:T(8,128)(2,1)S(1)} %pad_maximum_fusion.6), channel_id=1, source_target_pairs={{0,96},{8,104},{16,112},{24,120},{32,0},{40,8},{48,16},{56,24},{64... | collective-permute-start | bytes 393224 | tf_op jit(solution)/shard_map/ppermute | solution.py:181
  67.6 2.2 %collective-permute-start.19 = (bf16[4,64,256]{2,1,0:T(8,128)(2,1)S(1)}, bf16[4,64,256]{2,1,0:T(8,128)(2,1)S(1)}, u32[]{:S(2)}, u32[]{:S(2)}) collective-permute-start(bf16[4,64,256]{2,1,0:T(8,128)(2,1)S(1)} %pad_maximum_fusion.6), channel_id=1, source_target_pairs={{0,64},{8,72},{16,80},{24,88},{32,96},{40,104},{48,112},{56,120},{... | collective-permute-start | bytes 393224 | tf_op jit(solution)/shard_map/ppermute | solution.py:181
  69.8 13.4 %collective-permute-done.17 = bf16[4,64,256]{2,1,0:T(8,128)(2,1)S(1)} collective-permute-done((bf16[4,64,256]{2,1,0:T(8,128)(2,1)S(1)}, bf16[4,64,256]{2,1,0:T(8,128)(2,1)S(1)}, u32[]{:S(2)}, u32[]{:S(2)}) %collective-permute-start.17) | collective-permute-done | bytes 131104 | tf_op jit(solution)/shard_map/ppermute | solution.py:181
  83.4 3.2 %collective-permute-done.19 = bf16[4,64,256]{2,1,0:T(8,128)(2,1)S(1)} collective-permute-done((bf16[4,64,256]{2,1,0:T(8,128)(2,1)S(1)}, bf16[4,64,256]{2,1,0:T(8,128)(2,1)S(1)}, u32[]{:S(2)}, u32[]{:S(2)}) %collective-permute-start.19) | collective-permute-done | bytes 131104 | tf_op jit(solution)/shard_map/ppermute | solution.py:181
  86.8 3.2 %collective-permute-start.21 = (bf16[4,4,64,256]{3,2,1,0:T(8,128)(2,1)S(1)}, bf16[4,4,64,256]{3,2,1,0:T(8,128)(2,1)S(1)}, u32[]{:S(2)}, u32[]{:S(2)}) collective-permute-start(bf16[4,4,64,256]{3,2,1,0:T(8,128)(2,1)S(1)} %pad_maximum_fusion.4), channel_id=1, source_target_pairs={{0,6},{1,7},{2,0},{3,1},{4,2},{5,3},{6,4},{7,5},{8,14},{9,15},{10,... | collective-permute-start | bytes 1572872 | tf_op jit(solution)/shard_map/ppermute | solution.py:181
  90.1 12.4 %attend.1 = bf16[16,96,128]{2,1,0:T(8,128)(2,1)S(1)} custom-call(bf16[16,288,128]{2,1,0:T(8,128)(2,1)S(1)} %all-to-all-done.got_ref, f32[1,3072]{1,0:T(1,128)S(1)} %bitcast.44, f32[1,64]{1,0:T(1,128)S(1)} %dynamic-slice_bitcast_fusion.gain_ref), custom_call_target="tpu_custom_call" | custom-call | tf_op jit(solution)/shard_map/attend/pallas_call | solution.py:214
  102.4 9.6 %collective-permute-done.20 = bf16[4,4,64,256]{3,2,1,0:T(8,128)(2,1)S(1)} collective-permute-done((bf16[4,4,64,256]{3,2,1,0:T(8,128)(2,1)S(1)}, bf16[4,4,64,256]{3,2,1,0:T(8,128)(2,1)S(1)}, u32[]{:S(2)}, u32[]{:S(2)}) %collective-permute-start.20) | collective-permute-done | bytes 524320 | tf_op jit(solution)/shard_map/ppermute | solution.py:181
  112.4 15.9 %all_to_all.10.got_ref = bf16[16,96,128]{2,1,0:T(8,128)(2,1)S(1)} all-to-all(bf16[16,96,128]{2,1,0:T(8,128)(2,1)S(1)} %attend.1), channel_id=1, replica_groups=mesh['sp'=16,'dp'=8] {'sp'}, dimensions={0} | all-to-all | bytes 786432 | tf_op jit(solution)/shard_map/all_to_all | solution.py:234
  128.3 2.1 %output.1 = bf16[192,2048]{1,0:T(8,128)(2,1)} custom-call(bf16[16,96,128]{2,1,0:T(8,128)(2,1)S(1)} %all_to_all.10.got_ref, bf16[4,4,4,64,256]{4,3,2,1,0:T(8,128)(2,1)S(1)} %pad_maximum_fusion.own_ref, bf16[4,4,4,64,256]{4,3,2,1,0:T(8,128)(2,1)S(1)} %collective-permute-done.23.far_ref), custom_call_target="tpu_custom_call" | custom-call | tf_op jit(solution)/shard_map/output/pallas_call | solution.py:235
  (46 shorter events, 4.0 us)
Async XLA Ops:
  0.0 90.0 %copy-start = (f32[1024]{0:T(1024)S(1)}, f32[1024]{0:T(1024)}, u32[]{:S(2)}) copy-start(f32[1024]{0:T(1024)} %param.14) | copy-start | bytes 12292
  0.0 21.4 %copy-start.2 = (bf16[1,192,2048]{2,1,0:T(8,128)(2,1)S(1)}, bf16[1,192,2048]{2,1,0:T(8,128)(2,1)}, u32[]{:S(2)}) copy-start(bf16[1,192,2048]{2,1,0:T(8,128)(2,1)} %param.8) | copy-start | bytes 2359300
  0.0 21.4 %copy-start.3 = (f32[2048]{0:T(1024)S(1)}, f32[2048]{0:T(1024)}, u32[]{:S(2)}) copy-start(f32[2048]{0:T(1024)} %param.9) | copy-start | bytes 24580
  0.9 6.0 %collective-permute-start.4 = (bf16[96,256]{1,0:T(8,128)(2,1)S(1)}, bf16[96,256]{1,0:T(8,128)(2,1)S(1)}, u32[]{:S(2)}, u32[]{:S(2)}) collective-permute-start(bf16[96,256]{1,0:T(8,128)(2,1)S(1)} %get-tuple-element.38), channel_id=1, source_target_pairs={{0,6},{1,7},{2,0},{3,1},{4,2},{5,3},{6,4},{7,5},{8,14},{9,15},{10,... | collective-permute-start | bytes 147464 | tf_op jit(solution)/shard_map/ppermute | solution.py:181
  3.8 5.6 %collective-permute-start.5 = (bf16[96,256]{1,0:T(8,128)(2,1)S(1)}, bf16[96,256]{1,0:T(8,128)(2,1)S(1)}, u32[]{:S(2)}, u32[]{:S(2)}) collective-permute-start(bf16[96,256]{1,0:T(8,128)(2,1)S(1)} %get-tuple-element.38), channel_id=1, source_target_pairs={{0,4},{1,5},{2,6},{3,7},{4,0},{5,1},{6,2},{7,3},{8,12},{9,13},{10,... | collective-permute-start | bytes 147464 | tf_op jit(solution)/shard_map/ppermute | solution.py:181
  4.6 10.8 %collective-permute-start = (bf16[96,256]{1,0:T(8,128)(2,1)S(1)}, bf16[96,256]{1,0:T(8,128)(2,1)S(1)}, u32[]{:S(2)}, u32[]{:S(2)}) collective-permute-start(bf16[96,256]{1,0:T(8,128)(2,1)S(1)} %get-tuple-element.38), channel_id=1, source_target_pairs={{0,2},{1,3},{2,4},{3,5},{4,6},{5,7},{6,0},{7,1},{8,10},{9,11},{10,... | collective-permute-start | bytes 147464 | tf_op jit(solution)/shard_map/ppermute | solution.py:181
  9.4 10.1 %collective-permute-start.6 = (bf16[2,96,256]{2,1,0:T(8,128)(2,1)S(1)}, bf16[2,96,256]{2,1,0:T(8,128)(2,1)S(1)}, u32[]{:S(2)}, u32[]{:S(2)}) collective-permute-start(bf16[2,96,256]{2,1,0:T(8,128)(2,1)S(1)} %get-tuple-element.36), channel_id=1, source_target_pairs={{0,32},{8,40},{16,48},{24,56},{32,64},{40,72},{48,80},{56,88},{64,... | collective-permute-start | bytes 294920 | tf_op jit(solution)/shard_map/ppermute | solution.py:181
  11.4 10.3 %collective-permute-start.7 = (bf16[2,96,256]{2,1,0:T(8,128)(2,1)S(1)}, bf16[2,96,256]{2,1,0:T(8,128)(2,1)S(1)}, u32[]{:S(2)}, u32[]{:S(2)}) collective-permute-start(bf16[2,96,256]{2,1,0:T(8,128)(2,1)S(1)} %get-tuple-element.36), channel_id=1, source_target_pairs={{0,96},{8,104},{16,112},{24,120},{32,0},{40,8},{48,16},{56,24},{64... | collective-permute-start | bytes 294920 | tf_op jit(solution)/shard_map/ppermute | solution.py:181
  13.6 8.2 %collective-permute-start.8 = (bf16[2,96,256]{2,1,0:T(8,128)(2,1)S(1)}, bf16[2,96,256]{2,1,0:T(8,128)(2,1)S(1)}, u32[]{:S(2)}, u32[]{:S(2)}) collective-permute-start(bf16[2,96,256]{2,1,0:T(8,128)(2,1)S(1)} %get-tuple-element.36), channel_id=1, source_target_pairs={{0,64},{8,72},{16,80},{24,88},{32,96},{40,104},{48,112},{56,120},{... | collective-permute-start | bytes 294920 | tf_op jit(solution)/shard_map/ppermute | solution.py:181
  16.2 7.4 %collective-permute-start.1 = (bf16[256,256]{1,0:T(8,128)(2,1)S(1)}, bf16[256,256]{1,0:T(8,128)(2,1)S(1)}, u32[]{:S(2)}, u32[]{:S(2)}) collective-permute-start(bf16[256,256]{1,0:T(8,128)(2,1)S(1)} %get-tuple-element.34), channel_id=1, source_target_pairs={{0,8},{8,16},{16,24},{24,0},{32,40},{40,48},{48,56},{56,32},{64,72... | collective-permute-start | bytes 393224 | tf_op jit(solution)/shard_map/ppermute | solution.py:181
  17.8 5.7 %collective-permute-start.2 = (bf16[256,256]{1,0:T(8,128)(2,1)S(1)}, bf16[256,256]{1,0:T(8,128)(2,1)S(1)}, u32[]{:S(2)}, u32[]{:S(2)}) collective-permute-start(bf16[256,256]{1,0:T(8,128)(2,1)S(1)} %get-tuple-element.34), channel_id=1, source_target_pairs={{0,24},{8,0},{16,8},{24,16},{32,56},{40,32},{48,40},{56,48},{64,88... | collective-permute-start | bytes 393224 | tf_op jit(solution)/shard_map/ppermute | solution.py:181
  19.5 6.5 %collective-permute-start.3 = (bf16[256,256]{1,0:T(8,128)(2,1)S(1)}, bf16[256,256]{1,0:T(8,128)(2,1)S(1)}, u32[]{:S(2)}, u32[]{:S(2)}) collective-permute-start(bf16[256,256]{1,0:T(8,128)(2,1)S(1)} %get-tuple-element.34), channel_id=1, source_target_pairs={{0,16},{8,24},{16,0},{24,8},{32,48},{40,56},{48,32},{56,40},{64,80... | collective-permute-start | bytes 393224 | tf_op jit(solution)/shard_map/ppermute | solution.py:181
  26.0 16.8 %collective-permute-start.12 = (bf16[4,2,96,256]{3,2,1,0:T(8,128)(2,1)S(1)}, bf16[4,2,96,256]{3,2,1,0:T(8,128)(2,1)S(1)}, u32[]{:S(2)}, u32[]{:S(2)}) collective-permute-start(bf16[4,2,96,256]{3,2,1,0:T(8,128)(2,1)S(1)} %pad_maximum_fusion.5), channel_id=1, source_target_pairs={{0,8},{8,16},{16,24},{24,0},{32,40},{40,48},{48,56},{56,32},{64,72... | collective-permute-start | bytes 1179656 | tf_op jit(solution)/shard_map/ppermute | solution.py:181
  26.6 16.3 %collective-permute-start.13 = (bf16[4,2,96,256]{3,2,1,0:T(8,128)(2,1)S(1)}, bf16[4,2,96,256]{3,2,1,0:T(8,128)(2,1)S(1)}, u32[]{:S(2)}, u32[]{:S(2)}) collective-permute-start(bf16[4,2,96,256]{3,2,1,0:T(8,128)(2,1)S(1)} %pad_maximum_fusion.5), channel_id=1, source_target_pairs={{0,24},{8,0},{16,8},{24,16},{32,56},{40,32},{48,40},{56,48},{64,88... | collective-permute-start | bytes 1179656 | tf_op jit(solution)/shard_map/ppermute | solution.py:181
  29.4 13.6 %collective-permute-start.14 = (bf16[4,2,96,256]{3,2,1,0:T(8,128)(2,1)S(1)}, bf16[4,2,96,256]{3,2,1,0:T(8,128)(2,1)S(1)}, u32[]{:S(2)}, u32[]{:S(2)}) collective-permute-start(bf16[4,2,96,256]{3,2,1,0:T(8,128)(2,1)S(1)} %pad_maximum_fusion.5), channel_id=1, source_target_pairs={{0,16},{8,24},{16,0},{24,8},{32,48},{40,56},{48,32},{56,40},{64,80... | collective-permute-start | bytes 1179656 | tf_op jit(solution)/shard_map/ppermute | solution.py:181
  31.1 12.1 %collective-permute-start.9 = (bf16[4,2,96,256]{3,2,1,0:T(8,128)(2,1)S(1)}, bf16[4,2,96,256]{3,2,1,0:T(8,128)(2,1)S(1)}, u32[]{:S(2)}, u32[]{:S(2)}) collective-permute-start(bf16[4,2,96,256]{3,2,1,0:T(8,128)(2,1)S(1)} %bitcast.46), channel_id=1, source_target_pairs={{0,32},{8,40},{16,48},{24,56},{32,64},{40,72},{48,80},{56,88},{64,... | collective-permute-start | bytes 1179656 | tf_op jit(solution)/shard_map/ppermute | solution.py:181
  32.2 11.1 %collective-permute-start.10 = (bf16[4,2,96,256]{3,2,1,0:T(8,128)(2,1)S(1)}, bf16[4,2,96,256]{3,2,1,0:T(8,128)(2,1)S(1)}, u32[]{:S(2)}, u32[]{:S(2)}) collective-permute-start(bf16[4,2,96,256]{3,2,1,0:T(8,128)(2,1)S(1)} %bitcast.47), channel_id=1, source_target_pairs={{0,96},{8,104},{16,112},{24,120},{32,0},{40,8},{48,16},{56,24},{64... | collective-permute-start | bytes 1179656 | tf_op jit(solution)/shard_map/ppermute | solution.py:181
  42.9 9.3 %collective-permute-start.11 = (bf16[4,2,96,256]{3,2,1,0:T(8,128)(2,1)S(1)}, bf16[4,2,96,256]{3,2,1,0:T(8,128)(2,1)S(1)}, u32[]{:S(2)}, u32[]{:S(2)}) collective-permute-start(bf16[4,2,96,256]{3,2,1,0:T(8,128)(2,1)S(1)} %bitcast.48), channel_id=1, source_target_pairs={{0,64},{8,72},{16,80},{24,88},{32,96},{40,104},{48,112},{56,120},{... | collective-permute-start | bytes 1179656 | tf_op jit(solution)/shard_map/ppermute | solution.py:181
  43.1 9.3 %collective-permute-start.16 = (bf16[4,4,2,96,256]{4,3,2,1,0:T(8,128)(2,1)S(1)}, bf16[4,4,2,96,256]{4,3,2,1,0:T(8,128)(2,1)S(1)}, u32[]{:S(2)}, u32[]{:S(2)}) collective-permute-start(bf16[4,4,2,96,256]{4,3,2,1,0:T(8,128)(2,1)S(1)} %pad_maximum_fusion.2.own_b), channel_id=1, source_target_pairs={{0,1},{1,0},{2,3},{3,2},{4,5},{5,4},{6,7},{7,6},{8,9},{9,8},{10,11... | collective-permute-start | bytes 4718600 | tf_op jit(solution)/shard_map/ppermute | solution.py:196
  52.4 3.5 %collective-permute-start.15 = (bf16[4,4,2,96,256]{4,3,2,1,0:T(8,128)(2,1)S(1)}, bf16[4,4,2,96,256]{4,3,2,1,0:T(8,128)(2,1)S(1)}, u32[]{:S(2)}, u32[]{:S(2)}) collective-permute-start(bf16[4,4,2,96,256]{4,3,2,1,0:T(8,128)(2,1)S(1)} %pad_maximum_fusion.1.own_a), channel_id=1, source_target_pairs={{0,1},{1,0},{2,3},{3,2},{4,5},{5,4},{6,7},{7,6},{8,9},{9,8},{10,11... | collective-permute-start | bytes 4718600 | tf_op jit(solution)/shard_map/ppermute | solution.py:195
  59.2 30.9 %copy-start.1 = (f32[1,3072,1]{1,2,0:T(1,128)S(1)}, f32[1,3072,1]{1,2,0:T(1,128)}, u32[]{:S(2)}) copy-start(f32[1,3072,1]{1,2,0:T(1,128)} %param.13) | copy-start | bytes 36868
  59.2 30.9 %all-to-all-start = ((bf16[16,288,128]{2,1,0:T(8,128)(2,1)}), bf16[16,288,128]{2,1,0:T(8,128)(2,1)S(1)}, u32[]{:S(2)}, u32[]{:S(2)}) async-start(bf16[16,288,128]{2,1,0:T(8,128)(2,1)} %project.1), calls=%async_computation | async-start | bytes 2359296 | tf_op jit(solution)/shard_map/all_to_all | solution.py:210
  64.3 18.9 %collective-permute-start.17 = (bf16[4,64,256]{2,1,0:T(8,128)(2,1)S(1)}, bf16[4,64,256]{2,1,0:T(8,128)(2,1)S(1)}, u32[]{:S(2)}, u32[]{:S(2)}) collective-permute-start(bf16[4,64,256]{2,1,0:T(8,128)(2,1)S(1)} %pad_maximum_fusion.6), channel_id=1, source_target_pairs={{0,32},{8,40},{16,48},{24,56},{32,64},{40,72},{48,80},{56,88},{64,... | collective-permute-start | bytes 393224 | tf_op jit(solution)/shard_map/ppermute | solution.py:181
  66.2 17.2 %collective-permute-start.18 = (bf16[4,64,256]{2,1,0:T(8,128)(2,1)S(1)}, bf16[4,64,256]{2,1,0:T(8,128)(2,1)S(1)}, u32[]{:S(2)}, u32[]{:S(2)}) collective-permute-start(bf16[4,64,256]{2,1,0:T(8,128)(2,1)S(1)} %pad_maximum_fusion.6), channel_id=1, source_target_pairs={{0,96},{8,104},{16,112},{24,120},{32,0},{40,8},{48,16},{56,24},{64... | collective-permute-start | bytes 393224 | tf_op jit(solution)/shard_map/ppermute | solution.py:181
  67.6 19.0 %collective-permute-start.19 = (bf16[4,64,256]{2,1,0:T(8,128)(2,1)S(1)}, bf16[4,64,256]{2,1,0:T(8,128)(2,1)S(1)}, u32[]{:S(2)}, u32[]{:S(2)}) collective-permute-start(bf16[4,64,256]{2,1,0:T(8,128)(2,1)S(1)} %pad_maximum_fusion.6), channel_id=1, source_target_pairs={{0,64},{8,72},{16,80},{24,88},{32,96},{40,104},{48,112},{56,120},{... | collective-permute-start | bytes 393224 | tf_op jit(solution)/shard_map/ppermute | solution.py:181
  86.7 25.3 %collective-permute-start.20 = (bf16[4,4,64,256]{3,2,1,0:T(8,128)(2,1)S(1)}, bf16[4,4,64,256]{3,2,1,0:T(8,128)(2,1)S(1)}, u32[]{:S(2)}, u32[]{:S(2)}) collective-permute-start(bf16[4,4,64,256]{3,2,1,0:T(8,128)(2,1)S(1)} %pad_maximum_fusion.4), channel_id=1, source_target_pairs={{0,2},{1,3},{2,4},{3,5},{4,6},{5,7},{6,0},{7,1},{8,10},{9,11},{10,... | collective-permute-start | bytes 1572872 | tf_op jit(solution)/shard_map/ppermute | solution.py:181
  86.8 25.3 %collective-permute-start.21 = (bf16[4,4,64,256]{3,2,1,0:T(8,128)(2,1)S(1)}, bf16[4,4,64,256]{3,2,1,0:T(8,128)(2,1)S(1)}, u32[]{:S(2)}, u32[]{:S(2)}) collective-permute-start(bf16[4,4,64,256]{3,2,1,0:T(8,128)(2,1)S(1)} %pad_maximum_fusion.4), channel_id=1, source_target_pairs={{0,6},{1,7},{2,0},{3,1},{4,2},{5,3},{6,4},{7,5},{8,14},{9,15},{10,... | collective-permute-start | bytes 1572872 | tf_op jit(solution)/shard_map/ppermute | solution.py:181
  90.0 22.0 %collective-permute-start.22 = (bf16[4,4,64,256]{3,2,1,0:T(8,128)(2,1)S(1)}, bf16[4,4,64,256]{3,2,1,0:T(8,128)(2,1)S(1)}, u32[]{:S(2)}, u32[]{:S(2)}) collective-permute-start(bf16[4,4,64,256]{3,2,1,0:T(8,128)(2,1)S(1)} %pad_maximum_fusion.4), channel_id=1, source_target_pairs={{0,4},{1,5},{2,6},{3,7},{4,0},{5,1},{6,2},{7,3},{8,12},{9,13},{10,... | collective-permute-start | bytes 1572872 | tf_op jit(solution)/shard_map/ppermute | solution.py:181
  112.3 16.0 %collective-permute-start.23 = (bf16[4,4,4,64,256]{4,3,2,1,0:T(8,128)(2,1)S(1)}, bf16[4,4,4,64,256]{4,3,2,1,0:T(8,128)(2,1)S(1)}, u32[]{:S(2)}, u32[]{:S(2)}) collective-permute-start(bf16[4,4,4,64,256]{4,3,2,1,0:T(8,128)(2,1)S(1)} %pad_maximum_fusion.own_ref), channel_id=1, source_target_pairs={{0,1},{1,0},{2,3},{3,2},{4,5},{5,4},{6,7},{7,6},{8,9},{9,8},{10,11... | collective-permute-start | bytes 6291464 | tf_op jit(solution)/shard_map/ppermute | solution.py:233

commit v2 on v1

--- a/solution.py
+++ b/solution.py
@@ -12,18 +12,17 @@
 LOG2E = math.log2(math.e)
 norm_eps = 1e-06
 SIDE = 4
-HOPS = (0, 1, 3, 2)
 
 
 VMEM = pl.BlockSpec(memory_space=pltpu.VMEM)
+
+
+def pairs(step, size):
+    return [(i, i ^ step) for i in range(size)]
 
 
 def along_x(k):
     return [(i, (i + 2 * k) % (2 * SIDE)) for i in range(2 * SIDE)]
-
-
-def other_core():
-    return [(i, i ^ 1) for i in range(2 * SIDE)]
 
 
 def along_zy(dz, dy):
@@ -32,6 +31,21 @@
     ]
 
 
+def doubled(a, axis, perms):
+    for perm in perms:
+        a = jnp.concatenate([a, lax.ppermute(a, axis, perm)], axis=0)
+    return a
+
+
+def both_ways(a, axis, perm_of):
+    back = lax.ppermute(a, axis, perm_of(1))
+    ahead = lax.ppermute(a, axis, perm_of(-1))
+    half = a.shape[0] // 2
+    low = lax.ppermute(back[:half], axis, perm_of(1))
+    high = lax.ppermute(ahead[half:], axis, perm_of(-1))
+    return jnp.stack([a, back, jnp.concatenate([low, high], axis=0), ahead])
+
+
 def near(*arrays):
     return [pltpu.with_memory_space_constraint(a, pltpu.VMEM) for a in arrays]
 
@@ -41,31 +55,35 @@
     return lax.div(dp, 2), lax.rem(dp, 2), lax.div(sp, SIDE), lax.rem(sp, SIDE)
 
 
-def project_kernel(normed_ref, own_a, own_b, far_a, far_b, out_ref, order_ref, sums_ref):
+def before(here, there):
+    return lax.rem(here + SIDE - there, SIDE)
+
+
+def project_kernel(normed_ref, own_a, own_b, far_a, far_b, out_ref, done_ref, order_ref, sums_ref):
     bf = jnp.bfloat16
     x, c, z, y = place_of()
     rows = normed_ref.shape[0]
     for i in range(SIDE):
         for cc in range(2):
-            chunk = 2 * lax.rem(x + SIDE - HOPS[i], SIDE) + lax.rem(c + cc, 2)
+            chunk = 2 * jnp.bitwise_xor(x, i) + jnp.bitwise_xor(c, cc)
             order_ref[:, (2 * i + cc) * 256 : (2 * i + cc + 1) * 256] = normed_ref[
                 :, pl.ds(pl.multiple_of(chunk * 256, 256), 256)
             ]
-    for iz in range(SIDE):
+    for zs in range(SIDE):
         parts = []
         for i in range(SIDE):
             for ref_a, ref_b in ((own_a, own_b), (far_a, far_b)):
                 if i < 2:
-                    parts.append(jnp.concatenate([ref_a[iz, iy, i] for iy in range(SIDE)], axis=0))
+                    several = [ref_a[before(z, zs), jnp.bitwise_xor(y, ys), i] for ys in range(SIDE)]
                 else:
-                    parts.append(jnp.concatenate([ref_b[iy, iz, i - 2] for iy in range(SIDE)], axis=0))
+                    several = [ref_b[before(y, ys), jnp.bitwise_xor(z, zs), i - 2] for ys in range(SIDE)]
+                parts.append(jnp.concatenate(several, axis=0))
         weights = jnp.concatenate(parts, axis=1)
         total = lax.dot_general(
             weights, order_ref[...], (((1,), (1,)), ((), ())), preferred_element_type=jnp.float32
         )
-        for iy in range(SIDE):
-            place = SIDE * lax.rem(z + SIDE - HOPS[iz], SIDE) + lax.rem(y + SIDE - HOPS[iy], SIDE)
-            sums_ref[place] = total[96 * iy : 96 * (iy + 1), :]
+        for ys in range(SIDE):
+            sums_ref[SIDE * zs + ys] = total[96 * ys : 96 * (ys + 1), :]
     half = rows // 2
     for g in range(SIDE):
         key = jnp.concatenate([sums_ref[SIDE * g + j, 64:80, :] for j in range(SIDE)], axis=0)
@@ -76,6 +94,7 @@
             both = jnp.concatenate([sums_ref[h, :64, :], key], axis=0)
             out_ref[h, :rows, :] = both.T.astype(bf)
             out_ref[h, rows:, :] = jnp.concatenate([turned[:half], turned[half:]], axis=1)
+    done_ref[...] = jnp.zeros_like(done_ref)
 
 
 def masked(block, mask):
@@ -146,23 +165,19 @@
 def output_kernel(got_ref, own_ref, far_ref, out_ref, heads_ref):
     x, c, z, y = place_of()
     half = got_ref.shape[1]
-    for iz in range(SIDE):
-        for iy in range(SIDE):
-            place = SIDE * lax.rem(z + SIDE - HOPS[iz], SIDE) + lax.rem(y + SIDE - HOPS[iy], SIDE)
-            block = got_ref[place]
-            at = (SIDE * iz + iy) * HEAD_DIM
-            heads_ref[:half, at : at + HEAD_DIM] = block[:, :HEAD_DIM]
-            heads_ref[half:, at : at + HEAD_DIM] = block[:, HEAD_DIM:]
+    for h in range(SIDE * SIDE):
+        block = got_ref[h]
+        heads_ref[:half, h * HEAD_DIM : (h + 1) * HEAD_DIM] = block[:, :HEAD_DIM]
+        heads_ref[half:, h * HEAD_DIM : (h + 1) * HEAD_DIM] = block[:, HEAD_DIM:]
     for i in range(SIDE):
         for cc, ref in ((0, own_ref), (1, far_ref)):
-            parts = []
-            for iz in range(SIDE):
-                for iy in range(SIDE):
-                    parts.append(ref[i, iz, iy])
+            parts = [
+                ref[i, before(z, zs), jnp.bitwise_xor(y, ys)] for zs in range(SIDE) for ys in range(SIDE)
+            ]
             mixed = jnp.dot(
                 heads_ref[...], jnp.concatenate(parts, axis=0), preferred_element_type=jnp.float32
             )
-            chunk = 2 * lax.rem(x + SIDE - HOPS[i], SIDE) + lax.rem(c + cc, 2)
+            chunk = 2 * before(x, i) + jnp.bitwise_xor(c, cc)
             out_ref[:, pl.ds(pl.multiple_of(chunk * 256, 256), 256)] = mixed.astype(jnp.bfloat16)
 
 
@@ -178,33 +193,35 @@
     ).astype(bf)
 
     def spread(perm_of, a, axis):
-        return [a] + [lax.ppermute(a, axis, perm_of(k)) for k in HOPS[1:]]
+        return [a] + [lax.ppermute(a, axis, perm_of(k)) for k in range(1, SIDE)]
 
     piece = jnp.concatenate([w_query.T, w_key.T, w_value.T], axis=0)
-    four = jnp.stack(spread(along_x, piece, "dp"))
-    together = jnp.concatenate([four[:2].reshape(192, 256), w_out], axis=0)
-    first_a = jnp.stack(spread(lambda k: along_zy(0, k), together, "sp"))
-    first_b = jnp.stack(spread(lambda k: along_zy(k, 0), four[2:], "sp"))
+    four = doubled(piece[None], "dp", (pairs(2, 8), pairs(4, 8)))
+    together = jnp.concatenate([four[:2].reshape(192, 256), w_out], axis=0)[None]
+    first_a = doubled(together, "sp", (pairs(1, 16), pairs(2, 16)))
+    first_b = doubled(four[2:][None], "sp", (pairs(4, 16), pairs(8, 16)))
     rest_y = first_a[:, 192:]
     first_a = first_a[:, :192].reshape(SIDE, 2, 96, 256)
     first_a, first_b, normed = lax.optimization_barrier((first_a, first_b, normed))
-    own_a = spread(lambda k: along_zy(k, 0), first_a, "sp")
-    own_b = spread(lambda k: along_zy(0, k), first_b, "sp")
-    own_a, own_b = jnp.stack(own_a), jnp.stack(own_b)
+    own_a = both_ways(first_a, "sp", lambda k: along_zy(k, 0))
+    own_b = both_ways(first_b, "sp", lambda k: along_zy(0, k))
     own_a, rest_y = lax.optimization_barrier((own_a, rest_y))
-    far_a = lax.ppermute(own_a, "dp", other_core())
-    far_b = lax.ppermute(own_b, "dp", other_core())
-    packed = pl.pallas_call(
+    far_a = lax.ppermute(own_a, "dp", pairs(1, 8))
+    far_b = lax.ppermute(own_b, "dp", pairs(1, 8))
+    packed, done = pl.pallas_call(
         project_kernel,
-        out_shape=pltpu.VMEM((sp_size, rows + rows // 2, 128), bf),
+        out_shape=(
+            pltpu.VMEM((sp_size, rows + rows // 2, 128), bf),
+            jax.ShapeDtypeStruct((8, 128), jnp.float32),
+        ),
         in_specs=[VMEM] * 5,
-        out_specs=VMEM,
+        out_specs=(VMEM, VMEM),
         scratch_shapes=[pltpu.VMEM((rows, width), bf), pltpu.VMEM((sp_size, 96, rows), jnp.float32)],
         compiler_params=pltpu.CompilerParams(vmem_limit_bytes=30 * 2**20),
         name="project",
     )(*near(normed, own_a, own_b, far_a, far_b))
     rest_z = spread(lambda k: along_zy(k, 0), rest_y, "sp")
-    _, rest_z = lax.optimization_barrier((packed, rest_z))
+    _, rest_z = lax.optimization_barrier((done, rest_z))
     rest_x = spread(along_x, jnp.stack(rest_z), "dp")
 
     got = lax.all_to_all(packed, "sp", split_axis=0, concat_axis=0, tiled=True)
@@ -230,7 +247,7 @@
     )(*near(got, key_bias.reshape(1, length), gains))
     heads, rest_x = lax.optimization_barrier((heads, rest_x))
     own_out = jnp.stack(rest_x)
-    far_out = lax.ppermute(own_out, "dp", other_core())
+    far_out = lax.ppermute(own_out, "dp", pairs(1, 8))
     returned = lax.all_to_all(heads, "sp", split_axis=0, concat_axis=0, tiled=True)
     mixed = pl.pallas_call(
         output_kernel,

time: 131 us -> 131 us (level)
  starting transfers between devices: 38.3 us -> 48.1 us
  waiting for transfers between devices: 54 us -> 44.4 us
    ppermute x24 -> x23, starting transfers between devices: 33.2 us -> 43.4 us  [the longest x6 15.7 us: doubled(): a = jnp.concatenate([a, lax.ppermute(a, axis, perm)], axis=0)]
    ppermute x24 -> x23, waiting for transfers between devices: 54 us -> 44.4 us  [the longest x6 24.6 us: spread(): return [a] + [lax.ppermute(a, axis, perm_of(k)) for k in range(1, SIDE)]]
    another operation x8 -> x4, other arithmetic: 2.19 us -> 0.47 us  [both_ways(): return jnp.stack([a, back, jnp.concatenate([low, high], axis=0), ahead])]
    broadcast_in_dim x0 -> x2, other arithmetic: none -> 1.64 us  [the longest x1 0.87 us: body(): four = doubled(piece[None], 'dp', (pairs(2, 8), pairs(4, 8)))]
  transfers between devices with their start and end apart: 25 -> 24, of which waited for: 10 -> 13; matrix products, arithmetic and copies ran while one was open for 2% -> 2% of each run, Pallas kernels for 9% -> 9%
where the time goes in v2:
time: 131 us
  starting transfers between devices  48.1 us (37%)
  waiting for transfers between devices  44.4 us (34%)
  Pallas kernels  17.5 us (13%)
  blocking collectives  15.9 us (12%)
  other arithmetic  4.22 us (3%)
    ppermute x6, waiting for transfers between devices, spread(): return [a] + [lax.ppermute(a, axis, perm_of(k)) for k in range(1, SIDE)]  24.6 us
    all_to_all x1, blocking collectives, body(): lax.all_to_all(heads, 'sp', split_axis=0, concat_axis=0, tiled=True)  15.9 us
    ppermute x6, starting transfers between devices, doubled(): a = jnp.concatenate([a, lax.ppermute(a, axis, perm)], axis=0)  15.7 us
    pallas_call x1, Pallas kernels, body(): pl.pallas_call(functools.partial(attend_kernel, src=sp_size, rows=rows, b...  12.3 us
    ppermute x6, starting transfers between devices, spread(): return [a] + [lax.ppermute(a, axis, perm_of(k)) for k in range(1, SIDE)]  11.6 us
    ppermute x2, starting transfers between devices, both_ways(): ahead = lax.ppermute(a, axis, perm_of(-1))  8.51 us
    ppermute x2, starting transfers between devices, both_ways(): high = lax.ppermute(ahead[half:], axis, perm_of(-1))  7.04 us
    ppermute x2, waiting for transfers between devices, both_ways(): low = lax.ppermute(back[:half], axis, perm_of(1))  6.51 us
  transfers between devices with their start and end apart: 24, of which 13 were waited for; matrix products, arithmetic and copies ran while one was open for 2% of the time, Pallas kernels for 9%

profile of v2, /device:TPU:0, one launch (start us, length us, event | category | flops | bytes accessed | tf_op | source)
XLA Modules:
  0.0 130.5 jit_solution(11687215270426736634)
XLA Ops:
  0.0 0.9 maximum_bitcast_fusion.3
  0.9 1.6 %collective-permute-start = (bf16[1,96,256]{2,1,0:T(8,128)(2,1)S(1)}, bf16[1,96,256]{2,1,0:T(8,128)(2,1)S(1)}, u32[]{:S(2)}, u32[]{:S(2)}) collective-permute-start(bf16[1,96,256]{2,1,0:T(8,128)(2,1)S(1)} %maximum_bitcast_fusion.3), channel_id=1, source_target_pairs={{0,2},{1,3},{2,0},{3,1},{4,6},{5,7},{6,4},{7,5},{8,10},{9,11},{10,... | collective-permute-start | bytes 147464 | tf_op jit(solution)/shard_map/ppermute | solution.py:36
  2.5 1.4 %fusion = f32[192]{0:T(256)S(1)} fusion(bf16[1,192,2048]{2,1,0:T(8,128)(2,1)} %param.8), kind=kLoop, calls=%fused_computation.3 | loop fusion | flops 1179456 | bytes 787200 | tf_op jit(solution)/shard_map/reduce_sum | solution.py:192
  3.9 1.1 collective-permute-done
  5.0 3.2 %collective-permute-start.3 = (bf16[2,96,256]{2,1,0:T(8,128)(2,1)S(1)}, bf16[2,96,256]{2,1,0:T(8,128)(2,1)S(1)}, u32[]{:S(2)}, u32[]{:S(2)}) collective-permute-start(bf16[2,96,256]{2,1,0:T(8,128)(2,1)S(1)} %pad_maximum_fusion.9), channel_id=1, source_target_pairs={{0,4},{1,5},{2,6},{3,7},{4,0},{5,1},{6,2},{7,3},{8,12},{9,13},{10,... | collective-permute-start | bytes 294920 | tf_op jit(solution)/shard_map/ppermute | solution.py:36
  9.0 1.7 %collective-permute-start.1 = (bf16[1,256,256]{2,1,0:T(8,128)(2,1)S(1)}, bf16[1,256,256]{2,1,0:T(8,128)(2,1)S(1)}, u32[]{:S(2)}, u32[]{:S(2)}) collective-permute-start(bf16[1,256,256]{2,1,0:T(8,128)(2,1)S(1)} %maximum_bitcast_fusion.2), channel_id=1, source_target_pairs={{0,8},{8,0},{16,24},{24,16},{32,40},{40,32},{48,56},{56,48},{64,72... | collective-permute-start | bytes 393224 | tf_op jit(solution)/shard_map/ppermute | solution.py:36
  11.2 2.0 %collective-permute-start.4 = (bf16[1,2,96,256]{3,2,1,0:T(8,128)(2,1)S(1)}, bf16[1,2,96,256]{3,2,1,0:T(8,128)(2,1)S(1)}, u32[]{:S(2)}, u32[]{:S(2)}) collective-permute-start(bf16[1,2,96,256]{3,2,1,0:T(8,128)(2,1)S(1)} %bitcast.50), channel_id=1, source_target_pairs={{0,32},{8,40},{16,48},{24,56},{32,0},{40,8},{48,16},{56,24},{64,96... | collective-permute-start | bytes 294920 | tf_op jit(solution)/shard_map/ppermute | solution.py:36
  14.0 3.3 %collective-permute-start.2 = (bf16[2,256,256]{2,1,0:T(8,128)(2,1)S(1)}, bf16[2,256,256]{2,1,0:T(8,128)(2,1)S(1)}, u32[]{:S(2)}, u32[]{:S(2)}) collective-permute-start(bf16[2,256,256]{2,1,0:T(8,128)(2,1)S(1)} %pad_maximum_fusion.6), channel_id=1, source_target_pairs={{0,16},{8,24},{16,0},{24,8},{32,48},{40,56},{48,32},{56,40},{64,80... | collective-permute-start | bytes 786440 | tf_op jit(solution)/shard_map/ppermute | solution.py:36
  17.4 4.0 %collective-permute-start.5 = (bf16[2,2,96,256]{3,2,1,0:T(8,128)(2,1)S(1)}, bf16[2,2,96,256]{3,2,1,0:T(8,128)(2,1)S(1)}, u32[]{:S(2)}, u32[]{:S(2)}) collective-permute-start(bf16[2,2,96,256]{3,2,1,0:T(8,128)(2,1)S(1)} %pad_maximum_fusion.7), channel_id=1, source_target_pairs={{0,64},{8,72},{16,80},{24,88},{32,96},{40,104},{48,112},{56,120},{... | collective-permute-start | bytes 589832 | tf_op jit(solution)/shard_map/ppermute | solution.py:36
  22.2 2.8 %collective-permute-done.5 = bf16[2,2,96,256]{3,2,1,0:T(8,128)(2,1)S(1)} collective-permute-done((bf16[2,2,96,256]{3,2,1,0:T(8,128)(2,1)S(1)}, bf16[2,2,96,256]{3,2,1,0:T(8,128)(2,1)S(1)}, u32[]{:S(2)}, u32[]{:S(2)}) %collective-permute-start.5) | collective-permute-done | bytes 196640 | tf_op jit(solution)/shard_map/ppermute | solution.py:36
  25.0 5.4 %collective-permute-start.8 = (bf16[4,2,96,256]{3,2,1,0:T(8,128)(2,1)S(1)}, bf16[4,2,96,256]{3,2,1,0:T(8,128)(2,1)S(1)}, u32[]{:S(2)}, u32[]{:S(2)}) collective-permute-start(bf16[4,2,96,256]{3,2,1,0:T(8,128)(2,1)S(1)} %bitcast.39), channel_id=1, source_target_pairs={{0,96},{8,104},{16,112},{24,120},{32,0},{40,8},{48,16},{56,24},{64... | collective-permute-start | bytes 1179656 | tf_op jit(solution)/shard_map/ppermute | solution.py:42
  30.4 3.1 %collective-permute-start.12 = (bf16[4,2,96,256]{3,2,1,0:T(8,128)(2,1)S(1)}, bf16[4,2,96,256]{3,2,1,0:T(8,128)(2,1)S(1)}, u32[]{:S(2)}, u32[]{:S(2)}) collective-permute-start(bf16[4,2,96,256]{3,2,1,0:T(8,128)(2,1)S(1)} %pad_maximum_fusion.5), channel_id=1, source_target_pairs={{0,24},{8,0},{16,8},{24,16},{32,56},{40,32},{48,40},{56,48},{64,88... | collective-permute-start | bytes 1179656 | tf_op jit(solution)/shard_map/ppermute | solution.py:42
  33.5 4.1 %collective-permute-done.8 = bf16[4,2,96,256]{3,2,1,0:T(8,128)(2,1)S(1)} collective-permute-done((bf16[4,2,96,256]{3,2,1,0:T(8,128)(2,1)S(1)}, bf16[4,2,96,256]{3,2,1,0:T(8,128)(2,1)S(1)}, u32[]{:S(2)}, u32[]{:S(2)}) %collective-permute-start.8) | collective-permute-done | bytes 393248 | tf_op jit(solution)/shard_map/ppermute | solution.py:42
  37.6 3.8 %collective-permute-start.9 = (bf16[2,2,96,256]{3,2,1,0:T(8,128)(2,1)S(1)}, bf16[2,2,96,256]{3,2,1,0:T(8,128)(2,1)S(1)}, u32[]{:S(2)}, u32[]{:S(2)}) collective-permute-start(bf16[2,2,96,256]{3,2,1,0:T(8,128)(2,1)S(1)} %slice.26), channel_id=1, source_target_pairs={{0,96},{8,104},{16,112},{24,120},{32,0},{40,8},{48,16},{56,24},{64... | collective-permute-start | bytes 589832 | tf_op jit(solution)/shard_map/ppermute | solution.py:45
  41.6 3.3 %collective-permute-start.13 = (bf16[2,2,96,256]{3,2,1,0:T(8,128)(2,1)S(1)}, bf16[2,2,96,256]{3,2,1,0:T(8,128)(2,1)S(1)}, u32[]{:S(2)}, u32[]{:S(2)}) collective-permute-start(bf16[2,2,96,256]{3,2,1,0:T(8,128)(2,1)S(1)} %slice.28), channel_id=1, source_target_pairs={{0,24},{8,0},{16,8},{24,16},{32,56},{40,32},{48,40},{56,48},{64,88... | collective-permute-start | bytes 589832 | tf_op jit(solution)/shard_map/ppermute | solution.py:45
  45.0 3.4 %collective-permute-done.7 = bf16[2,2,96,256]{3,2,1,0:T(8,128)(2,1)S(1)} collective-permute-done((bf16[2,2,96,256]{3,2,1,0:T(8,128)(2,1)S(1)}, bf16[2,2,96,256]{3,2,1,0:T(8,128)(2,1)S(1)}, u32[]{:S(2)}, u32[]{:S(2)}) %collective-permute-start.7) | collective-permute-done | bytes 196640 | tf_op jit(solution)/shard_map/ppermute | solution.py:44
  48.8 3.1 %collective-permute-done.11 = bf16[2,2,96,256]{3,2,1,0:T(8,128)(2,1)S(1)} collective-permute-done((bf16[2,2,96,256]{3,2,1,0:T(8,128)(2,1)S(1)}, bf16[2,2,96,256]{3,2,1,0:T(8,128)(2,1)S(1)}, u32[]{:S(2)}, u32[]{:S(2)}) %collective-permute-start.11) | collective-permute-done | bytes 196640 | tf_op jit(solution)/shard_map/ppermute | solution.py:44
  52.2 3.4 %collective-permute-done.15.far_b = bf16[4,4,2,96,256]{4,3,2,1,0:T(8,128)(2,1)S(1)} collective-permute-done((bf16[4,4,2,96,256]{4,3,2,1,0:T(8,128)(2,1)S(1)}, bf16[4,4,2,96,256]{4,3,2,1,0:T(8,128)(2,1)S(1)}, u32[]{:S(2)}, u32[]{:S(2)}) %collective-permute-start.15) | collective-permute-done | bytes 1572896 | tf_op jit(solution)/shard_map/ppermute | solution.py:210
  55.6 3.1 %project.1 = (bf16[16,288,128]{2,1,0:T(8,128)(2,1)}, f32[8,128]{1,0:T(8,128)}) custom-call(bf16[192,2048]{1,0:T(8,128)(2,1)S(1)} %fusion.2.normed_ref, bf16[4,4,2,96,256]{4,3,2,1,0:T(8,128)(2,1)S(1)} %pad_maximum_fusion.1.own_a, bf16[4,4,2,96,256]{4,3,2,1,0:T(8,128)(2,1)S(1)} %pad_maximum_fusion.2.own_b, ...), custom_call_target="tpu_custom_call" | custom-call | tf_op jit(solution)/shard_map/project/pallas_call | solution.py:211
  58.7 4.7 %all-to-all-start = ((bf16[16,288,128]{2,1,0:T(8,128)(2,1)}), bf16[16,288,128]{2,1,0:T(8,128)(2,1)S(1)}, u32[]{:S(2)}, u32[]{:S(2)}) async-start(bf16[16,288,128]{2,1,0:T(8,128)(2,1)} %get-tuple-element.24), calls=%async_computation | async-start | bytes 2359296 | tf_op jit(solution)/shard_map/all_to_all | solution.py:227
  63.5 1.9 %collective-permute-start.16 = (bf16[4,64,256]{2,1,0:T(8,128)(2,1)S(1)}, bf16[4,64,256]{2,1,0:T(8,128)(2,1)S(1)}, u32[]{:S(2)}, u32[]{:S(2)}) collective-permute-start(bf16[4,64,256]{2,1,0:T(8,128)(2,1)S(1)} %pad_maximum_fusion.8), channel_id=1, source_target_pairs={{0,32},{8,40},{16,48},{24,56},{32,64},{40,72},{48,80},{56,88},{64,... | collective-permute-start | bytes 393224 | tf_op jit(solution)/shard_map/ppermute | solution.py:196
  65.4 2.7 %collective-permute-start.17 = (bf16[4,64,256]{2,1,0:T(8,128)(2,1)S(1)}, bf16[4,64,256]{2,1,0:T(8,128)(2,1)S(1)}, u32[]{:S(2)}, u32[]{:S(2)}) collective-permute-start(bf16[4,64,256]{2,1,0:T(8,128)(2,1)S(1)} %pad_maximum_fusion.8), channel_id=1, source_target_pairs={{0,64},{8,72},{16,80},{24,88},{32,96},{40,104},{48,112},{56,120},{... | collective-permute-start | bytes 393224 | tf_op jit(solution)/shard_map/ppermute | solution.py:196
  68.1 1.5 %collective-permute-start.18 = (bf16[4,64,256]{2,1,0:T(8,128)(2,1)S(1)}, bf16[4,64,256]{2,1,0:T(8,128)(2,1)S(1)}, u32[]{:S(2)}, u32[]{:S(2)}) collective-permute-start(bf16[4,64,256]{2,1,0:T(8,128)(2,1)S(1)} %pad_maximum_fusion.8), channel_id=1, source_target_pairs={{0,96},{8,104},{16,112},{24,120},{32,0},{40,8},{48,16},{56,24},{64... | collective-permute-start | bytes 393224 | tf_op jit(solution)/shard_map/ppermute | solution.py:196
  69.6 14.0 %collective-permute-done.16 = bf16[4,64,256]{2,1,0:T(8,128)(2,1)S(1)} collective-permute-done((bf16[4,64,256]{2,1,0:T(8,128)(2,1)S(1)}, bf16[4,64,256]{2,1,0:T(8,128)(2,1)S(1)}, u32[]{:S(2)}, u32[]{:S(2)}) %collective-permute-start.16) | collective-permute-done | bytes 131104 | tf_op jit(solution)/shard_map/ppermute | solution.py:196
  83.5 2.3 %collective-permute-done.17 = bf16[4,64,256]{2,1,0:T(8,128)(2,1)S(1)} collective-permute-done((bf16[4,64,256]{2,1,0:T(8,128)(2,1)S(1)}, bf16[4,64,256]{2,1,0:T(8,128)(2,1)S(1)}, u32[]{:S(2)}, u32[]{:S(2)}) %collective-permute-start.17) | collective-permute-done | bytes 131104 | tf_op jit(solution)/shard_map/ppermute | solution.py:196
  85.9 1.6 %collective-permute-start.19 = (bf16[4,4,64,256]{3,2,1,0:T(8,128)(2,1)S(1)}, bf16[4,4,64,256]{3,2,1,0:T(8,128)(2,1)S(1)}, u32[]{:S(2)}, u32[]{:S(2)}) collective-permute-start(bf16[4,4,64,256]{3,2,1,0:T(8,128)(2,1)S(1)} %pad_maximum_fusion.4), channel_id=1, source_target_pairs={{0,2},{1,3},{2,4},{3,5},{4,6},{5,7},{6,0},{7,1},{8,10},{9,11},{10,... | collective-permute-start | bytes 1572872 | tf_op jit(solution)/shard_map/ppermute | solution.py:196
  87.4 2.7 %collective-permute-start.20 = (bf16[4,4,64,256]{3,2,1,0:T(8,128)(2,1)S(1)}, bf16[4,4,64,256]{3,2,1,0:T(8,128)(2,1)S(1)}, u32[]{:S(2)}, u32[]{:S(2)}) collective-permute-start(bf16[4,4,64,256]{3,2,1,0:T(8,128)(2,1)S(1)} %pad_maximum_fusion.4), channel_id=1, source_target_pairs={{0,4},{1,5},{2,6},{3,7},{4,0},{5,1},{6,2},{7,3},{8,12},{9,13},{10,... | collective-permute-start | bytes 1572872 | tf_op jit(solution)/shard_map/ppermute | solution.py:196
  90.2 1.3 collective-permute-start.21
  91.5 12.3 %attend.1 = bf16[16,96,128]{2,1,0:T(8,128)(2,1)S(1)} custom-call(bf16[16,288,128]{2,1,0:T(8,128)(2,1)S(1)} %all-to-all-done.got_ref, f32[1,3072]{1,0:T(1,128)S(1)} %bitcast.36, f32[1,64]{1,0:T(1,128)S(1)} %dynamic-slice_bitcast_fusion.gain_ref), custom_call_target="tpu_custom_call" | custom-call | tf_op jit(solution)/shard_map/attend/pallas_call | solution.py:231
  103.9 8.3 %collective-permute-done.20 = bf16[4,4,64,256]{3,2,1,0:T(8,128)(2,1)S(1)} collective-permute-done((bf16[4,4,64,256]{3,2,1,0:T(8,128)(2,1)S(1)}, bf16[4,4,64,256]{3,2,1,0:T(8,128)(2,1)S(1)}, u32[]{:S(2)}, u32[]{:S(2)}) %collective-permute-start.20) | collective-permute-done | bytes 524320 | tf_op jit(solution)/shard_map/ppermute | solution.py:196
  112.6 15.9 %all_to_all.10.got_ref = bf16[16,96,128]{2,1,0:T(8,128)(2,1)S(1)} all-to-all(bf16[16,96,128]{2,1,0:T(8,128)(2,1)S(1)} %attend.1), channel_id=1, replica_groups=mesh['sp'=16,'dp'=8] {'sp'}, dimensions={0} | all-to-all | bytes 786432 | tf_op jit(solution)/shard_map/all_to_all | solution.py:251
  128.5 2.0 %output.1 = bf16[192,2048]{1,0:T(8,128)(2,1)} custom-call(bf16[16,96,128]{2,1,0:T(8,128)(2,1)S(1)} %all_to_all.10.got_ref, bf16[4,4,4,64,256]{4,3,2,1,0:T(8,128)(2,1)S(1)} %pad_maximum_fusion.own_ref, bf16[4,4,4,64,256]{4,3,2,1,0:T(8,128)(2,1)S(1)} %collective-permute-done.22.far_ref), custom_call_target="tpu_custom_call" | custom-call | tf_op jit(solution)/shard_map/output/pallas_call | solution.py:252
  (51 shorter events, 4.6 us)
Async XLA Ops:
  0.0 91.5 %copy-start = (f32[1024]{0:T(1024)S(1)}, f32[1024]{0:T(1024)}, u32[]{:S(2)}) copy-start(f32[1024]{0:T(1024)} %param.14) | copy-start | bytes 12292
  0.0 21.3 %copy-start.2 = (bf16[1,192,2048]{2,1,0:T(8,128)(2,1)S(1)}, bf16[1,192,2048]{2,1,0:T(8,128)(2,1)}, u32[]{:S(2)}) copy-start(bf16[1,192,2048]{2,1,0:T(8,128)(2,1)} %param.8) | copy-start | bytes 2359300
  0.0 21.3 %copy-start.3 = (f32[2048]{0:T(1024)S(1)}, f32[2048]{0:T(1024)}, u32[]{:S(2)}) copy-start(f32[2048]{0:T(1024)} %param.9) | copy-start | bytes 24580
  0.9 4.1 %collective-permute-start = (bf16[1,96,256]{2,1,0:T(8,128)(2,1)S(1)}, bf16[1,96,256]{2,1,0:T(8,128)(2,1)S(1)}, u32[]{:S(2)}, u32[]{:S(2)}) collective-permute-start(bf16[1,96,256]{2,1,0:T(8,128)(2,1)S(1)} %maximum_bitcast_fusion.3), channel_id=1, source_target_pairs={{0,2},{1,3},{2,0},{3,1},{4,6},{5,7},{6,4},{7,5},{8,10},{9,11},{10,... | collective-permute-start | bytes 147464 | tf_op jit(solution)/shard_map/ppermute | solution.py:36
  5.0 6.2 %collective-permute-start.3 = (bf16[2,96,256]{2,1,0:T(8,128)(2,1)S(1)}, bf16[2,96,256]{2,1,0:T(8,128)(2,1)S(1)}, u32[]{:S(2)}, u32[]{:S(2)}) collective-permute-start(bf16[2,96,256]{2,1,0:T(8,128)(2,1)S(1)} %pad_maximum_fusion.9), channel_id=1, source_target_pairs={{0,4},{1,5},{2,6},{3,7},{4,0},{5,1},{6,2},{7,3},{8,12},{9,13},{10,... | collective-permute-start | bytes 294920 | tf_op jit(solution)/shard_map/ppermute | solution.py:36
  9.0 5.0 %collective-permute-start.1 = (bf16[1,256,256]{2,1,0:T(8,128)(2,1)S(1)}, bf16[1,256,256]{2,1,0:T(8,128)(2,1)S(1)}, u32[]{:S(2)}, u32[]{:S(2)}) collective-permute-start(bf16[1,256,256]{2,1,0:T(8,128)(2,1)S(1)} %maximum_bitcast_fusion.2), channel_id=1, source_target_pairs={{0,8},{8,0},{16,24},{24,16},{32,40},{40,32},{48,56},{56,48},{64,72... | collective-permute-start | bytes 393224 | tf_op jit(solution)/shard_map/ppermute | solution.py:36
  11.2 6.1 %collective-permute-start.4 = (bf16[1,2,96,256]{3,2,1,0:T(8,128)(2,1)S(1)}, bf16[1,2,96,256]{3,2,1,0:T(8,128)(2,1)S(1)}, u32[]{:S(2)}, u32[]{:S(2)}) collective-permute-start(bf16[1,2,96,256]{3,2,1,0:T(8,128)(2,1)S(1)} %bitcast.50), channel_id=1, source_target_pairs={{0,32},{8,40},{16,48},{24,56},{32,0},{40,8},{48,16},{56,24},{64,96... | collective-permute-start | bytes 294920 | tf_op jit(solution)/shard_map/ppermute | solution.py:36
  14.0 8.0 %collective-permute-start.2 = (bf16[2,256,256]{2,1,0:T(8,128)(2,1)S(1)}, bf16[2,256,256]{2,1,0:T(8,128)(2,1)S(1)}, u32[]{:S(2)}, u32[]{:S(2)}) collective-permute-start(bf16[2,256,256]{2,1,0:T(8,128)(2,1)S(1)} %pad_maximum_fusion.6), channel_id=1, source_target_pairs={{0,16},{8,24},{16,0},{24,8},{32,48},{40,56},{48,32},{56,40},{64,80... | collective-permute-start | bytes 786440 | tf_op jit(solution)/shard_map/ppermute | solution.py:36
  17.4 7.6 %collective-permute-start.5 = (bf16[2,2,96,256]{3,2,1,0:T(8,128)(2,1)S(1)}, bf16[2,2,96,256]{3,2,1,0:T(8,128)(2,1)S(1)}, u32[]{:S(2)}, u32[]{:S(2)}) collective-permute-start(bf16[2,2,96,256]{3,2,1,0:T(8,128)(2,1)S(1)} %pad_maximum_fusion.7), channel_id=1, source_target_pairs={{0,64},{8,72},{16,80},{24,88},{32,96},{40,104},{48,112},{56,120},{... | collective-permute-start | bytes 589832 | tf_op jit(solution)/shard_map/ppermute | solution.py:36
  25.0 12.6 %collective-permute-start.8 = (bf16[4,2,96,256]{3,2,1,0:T(8,128)(2,1)S(1)}, bf16[4,2,96,256]{3,2,1,0:T(8,128)(2,1)S(1)}, u32[]{:S(2)}, u32[]{:S(2)}) collective-permute-start(bf16[4,2,96,256]{3,2,1,0:T(8,128)(2,1)S(1)} %bitcast.39), channel_id=1, source_target_pairs={{0,96},{8,104},{16,112},{24,120},{32,0},{40,8},{48,16},{56,24},{64... | collective-permute-start | bytes 1179656 | tf_op jit(solution)/shard_map/ppermute | solution.py:42
  30.4 11.1 %collective-permute-start.6 = (bf16[4,2,96,256]{3,2,1,0:T(8,128)(2,1)S(1)}, bf16[4,2,96,256]{3,2,1,0:T(8,128)(2,1)S(1)}, u32[]{:S(2)}, u32[]{:S(2)}) collective-permute-start(bf16[4,2,96,256]{3,2,1,0:T(8,128)(2,1)S(1)} %bitcast.40), channel_id=1, source_target_pairs={{0,32},{8,40},{16,48},{24,56},{32,64},{40,72},{48,80},{56,88},{64,... | collective-permute-start | bytes 1179656 | tf_op jit(solution)/shard_map/ppermute | solution.py:41
  30.4 11.2 %collective-permute-start.12 = (bf16[4,2,96,256]{3,2,1,0:T(8,128)(2,1)S(1)}, bf16[4,2,96,256]{3,2,1,0:T(8,128)(2,1)S(1)}, u32[]{:S(2)}, u32[]{:S(2)}) collective-permute-start(bf16[4,2,96,256]{3,2,1,0:T(8,128)(2,1)S(1)} %pad_maximum_fusion.5), channel_id=1, source_target_pairs={{0,24},{8,0},{16,8},{24,16},{32,56},{40,32},{48,40},{56,48},{64,88... | collective-permute-start | bytes 1179656 | tf_op jit(solution)/shard_map/ppermute | solution.py:42
  33.5 11.4 %collective-permute-start.10 = (bf16[4,2,96,256]{3,2,1,0:T(8,128)(2,1)S(1)}, bf16[4,2,96,256]{3,2,1,0:T(8,128)(2,1)S(1)}, u32[]{:S(2)}, u32[]{:S(2)}) collective-permute-start(bf16[4,2,96,256]{3,2,1,0:T(8,128)(2,1)S(1)} %pad_maximum_fusion.5), channel_id=1, source_target_pairs={{0,8},{8,16},{16,24},{24,0},{32,40},{40,48},{48,56},{56,32},{64,72... | collective-permute-start | bytes 1179656 | tf_op jit(solution)/shard_map/ppermute | solution.py:41
  37.6 7.4 %collective-permute-start.9 = (bf16[2,2,96,256]{3,2,1,0:T(8,128)(2,1)S(1)}, bf16[2,2,96,256]{3,2,1,0:T(8,128)(2,1)S(1)}, u32[]{:S(2)}, u32[]{:S(2)}) collective-permute-start(bf16[2,2,96,256]{3,2,1,0:T(8,128)(2,1)S(1)} %slice.26), channel_id=1, source_target_pairs={{0,96},{8,104},{16,112},{24,120},{32,0},{40,8},{48,16},{56,24},{64... | collective-permute-start | bytes 589832 | tf_op jit(solution)/shard_map/ppermute | solution.py:45
  41.5 7.0 %collective-permute-start.7 = (bf16[2,2,96,256]{3,2,1,0:T(8,128)(2,1)S(1)}, bf16[2,2,96,256]{3,2,1,0:T(8,128)(2,1)S(1)}, u32[]{:S(2)}, u32[]{:S(2)}) collective-permute-start(bf16[2,2,96,256]{3,2,1,0:T(8,128)(2,1)S(1)} %slice.25), channel_id=1, source_target_pairs={{0,32},{8,40},{16,48},{24,56},{32,64},{40,72},{48,80},{56,88},{64,... | collective-permute-start | bytes 589832 | tf_op jit(solution)/shard_map/ppermute | solution.py:44
  41.6 7.2 %collective-permute-start.13 = (bf16[2,2,96,256]{3,2,1,0:T(8,128)(2,1)S(1)}, bf16[2,2,96,256]{3,2,1,0:T(8,128)(2,1)S(1)}, u32[]{:S(2)}, u32[]{:S(2)}) collective-permute-start(bf16[2,2,96,256]{3,2,1,0:T(8,128)(2,1)S(1)} %slice.28), channel_id=1, source_target_pairs={{0,24},{8,0},{16,8},{24,16},{32,56},{40,32},{48,40},{56,48},{64,88... | collective-permute-start | bytes 589832 | tf_op jit(solution)/shard_map/ppermute | solution.py:45
  44.9 6.9 %collective-permute-start.11 = (bf16[2,2,96,256]{3,2,1,0:T(8,128)(2,1)S(1)}, bf16[2,2,96,256]{3,2,1,0:T(8,128)(2,1)S(1)}, u32[]{:S(2)}, u32[]{:S(2)}) collective-permute-start(bf16[2,2,96,256]{3,2,1,0:T(8,128)(2,1)S(1)} %slice.27), channel_id=1, source_target_pairs={{0,8},{8,16},{16,24},{24,0},{32,40},{40,48},{48,56},{56,32},{64,72... | collective-permute-start | bytes 589832 | tf_op jit(solution)/shard_map/ppermute | solution.py:44
  48.7 3.5 %collective-permute-start.14 = (bf16[4,4,2,96,256]{4,3,2,1,0:T(8,128)(2,1)S(1)}, bf16[4,4,2,96,256]{4,3,2,1,0:T(8,128)(2,1)S(1)}, u32[]{:S(2)}, u32[]{:S(2)}) collective-permute-start(bf16[4,4,2,96,256]{4,3,2,1,0:T(8,128)(2,1)S(1)} %pad_maximum_fusion.1.own_a), channel_id=1, source_target_pairs={{0,1},{1,0},{2,3},{3,2},{4,5},{5,4},{6,7},{7,6},{8,9},{9,8},{10,11... | collective-permute-start | bytes 4718600 | tf_op jit(solution)/shard_map/ppermute | solution.py:209
  52.1 3.5 %collective-permute-start.15 = (bf16[4,4,2,96,256]{4,3,2,1,0:T(8,128)(2,1)S(1)}, bf16[4,4,2,96,256]{4,3,2,1,0:T(8,128)(2,1)S(1)}, u32[]{:S(2)}, u32[]{:S(2)}) collective-permute-start(bf16[4,4,2,96,256]{4,3,2,1,0:T(8,128)(2,1)S(1)} %pad_maximum_fusion.2.own_b), channel_id=1, source_target_pairs={{0,1},{1,0},{2,3},{3,2},{4,5},{5,4},{6,7},{7,6},{8,9},{9,8},{10,11... | collective-permute-start | bytes 4718600 | tf_op jit(solution)/shard_map/ppermute | solution.py:210
  58.7 32.8 %copy-start.1 = (f32[1,3072,1]{1,2,0:T(1,128)S(1)}, f32[1,3072,1]{1,2,0:T(1,128)}, u32[]{:S(2)}) copy-start(f32[1,3072,1]{1,2,0:T(1,128)} %param.13) | copy-start | bytes 36868
  58.7 32.8 %all-to-all-start = ((bf16[16,288,128]{2,1,0:T(8,128)(2,1)}), bf16[16,288,128]{2,1,0:T(8,128)(2,1)S(1)}, u32[]{:S(2)}, u32[]{:S(2)}) async-start(bf16[16,288,128]{2,1,0:T(8,128)(2,1)} %get-tuple-element.24), calls=%async_computation | async-start | bytes 2359296 | tf_op jit(solution)/shard_map/all_to_all | solution.py:227
  63.5 20.0 %collective-permute-start.16 = (bf16[4,64,256]{2,1,0:T(8,128)(2,1)S(1)}, bf16[4,64,256]{2,1,0:T(8,128)(2,1)S(1)}, u32[]{:S(2)}, u32[]{:S(2)}) collective-permute-start(bf16[4,64,256]{2,1,0:T(8,128)(2,1)S(1)} %pad_maximum_fusion.8), channel_id=1, source_target_pairs={{0,32},{8,40},{16,48},{24,56},{32,64},{40,72},{48,80},{56,88},{64,... | collective-permute-start | bytes 393224 | tf_op jit(solution)/shard_map/ppermute | solution.py:196
  65.4 20.4 %collective-permute-start.17 = (bf16[4,64,256]{2,1,0:T(8,128)(2,1)S(1)}, bf16[4,64,256]{2,1,0:T(8,128)(2,1)S(1)}, u32[]{:S(2)}, u32[]{:S(2)}) collective-permute-start(bf16[4,64,256]{2,1,0:T(8,128)(2,1)S(1)} %pad_maximum_fusion.8), channel_id=1, source_target_pairs={{0,64},{8,72},{16,80},{24,88},{32,96},{40,104},{48,112},{56,120},{... | collective-permute-start | bytes 393224 | tf_op jit(solution)/shard_map/ppermute | solution.py:196
  68.1 17.7 %collective-permute-start.18 = (bf16[4,64,256]{2,1,0:T(8,128)(2,1)S(1)}, bf16[4,64,256]{2,1,0:T(8,128)(2,1)S(1)}, u32[]{:S(2)}, u32[]{:S(2)}) collective-permute-start(bf16[4,64,256]{2,1,0:T(8,128)(2,1)S(1)} %pad_maximum_fusion.8), channel_id=1, source_target_pairs={{0,96},{8,104},{16,112},{24,120},{32,0},{40,8},{48,16},{56,24},{64... | collective-permute-start | bytes 393224 | tf_op jit(solution)/shard_map/ppermute | solution.py:196
  85.9 18.0 %collective-permute-start.19 = (bf16[4,4,64,256]{3,2,1,0:T(8,128)(2,1)S(1)}, bf16[4,4,64,256]{3,2,1,0:T(8,128)(2,1)S(1)}, u32[]{:S(2)}, u32[]{:S(2)}) collective-permute-start(bf16[4,4,64,256]{3,2,1,0:T(8,128)(2,1)S(1)} %pad_maximum_fusion.4), channel_id=1, source_target_pairs={{0,2},{1,3},{2,4},{3,5},{4,6},{5,7},{6,0},{7,1},{8,10},{9,11},{10,... | collective-permute-start | bytes 1572872 | tf_op jit(solution)/shard_map/ppermute | solution.py:196
  87.4 24.8 %collective-permute-start.20 = (bf16[4,4,64,256]{3,2,1,0:T(8,128)(2,1)S(1)}, bf16[4,4,64,256]{3,2,1,0:T(8,128)(2,1)S(1)}, u32[]{:S(2)}, u32[]{:S(2)}) collective-permute-start(bf16[4,4,64,256]{3,2,1,0:T(8,128)(2,1)S(1)} %pad_maximum_fusion.4), channel_id=1, source_target_pairs={{0,4},{1,5},{2,6},{3,7},{4,0},{5,1},{6,2},{7,3},{8,12},{9,13},{10,... | collective-permute-start | bytes 1572872 | tf_op jit(solution)/shard_map/ppermute | solution.py:196
  90.2 22.0 %collective-permute-start.21 = (bf16[4,4,64,256]{3,2,1,0:T(8,128)(2,1)S(1)}, bf16[4,4,64,256]{3,2,1,0:T(8,128)(2,1)S(1)}, u32[]{:S(2)}, u32[]{:S(2)}) collective-permute-start(bf16[4,4,64,256]{3,2,1,0:T(8,128)(2,1)S(1)} %pad_maximum_fusion.4), channel_id=1, source_target_pairs={{0,6},{1,7},{2,0},{3,1},{4,2},{5,3},{6,4},{7,5},{8,14},{9,15},{10,... | collective-permute-start | bytes 1572872 | tf_op jit(solution)/shard_map/ppermute | solution.py:196
  112.5 16.0 %collective-permute-start.22 = (bf16[4,4,4,64,256]{4,3,2,1,0:T(8,128)(2,1)S(1)}, bf16[4,4,4,64,256]{4,3,2,1,0:T(8,128)(2,1)S(1)}, u32[]{:S(2)}, u32[]{:S(2)}) collective-permute-start(bf16[4,4,4,64,256]{4,3,2,1,0:T(8,128)(2,1)S(1)} %pad_maximum_fusion.own_ref), channel_id=1, source_target_pairs={{0,1},{1,0},{2,3},{3,2},{4,5},{5,4},{6,7},{7,6},{8,9},{9,8},{10,11... | collective-permute-start | bytes 6291464 | tf_op jit(solution)/shard_map/ppermute | solution.py:250

commit v3 on v2

--- a/solution.py
+++ b/solution.py
@@ -35,15 +35,6 @@
     for perm in perms:
         a = jnp.concatenate([a, lax.ppermute(a, axis, perm)], axis=0)
     return a
-
-
-def both_ways(a, axis, perm_of):
-    back = lax.ppermute(a, axis, perm_of(1))
-    ahead = lax.ppermute(a, axis, perm_of(-1))
-    half = a.shape[0] // 2
-    low = lax.ppermute(back[:half], axis, perm_of(1))
-    high = lax.ppermute(ahead[half:], axis, perm_of(-1))
-    return jnp.stack([a, back, jnp.concatenate([low, high], axis=0), ahead])
 
 
 def near(*arrays):
@@ -203,8 +194,8 @@
     rest_y = first_a[:, 192:]
     first_a = first_a[:, :192].reshape(SIDE, 2, 96, 256)
     first_a, first_b, normed = lax.optimization_barrier((first_a, first_b, normed))
-    own_a = both_ways(first_a, "sp", lambda k: along_zy(k, 0))
-    own_b = both_ways(first_b, "sp", lambda k: along_zy(0, k))
+    own_a = jnp.stack(spread(lambda k: along_zy(k, 0), first_a, "sp"))
+    own_b = jnp.stack(spread(lambda k: along_zy(0, k), first_b, "sp"))
     own_a, rest_y = lax.optimization_barrier((own_a, rest_y))
     far_a = lax.ppermute(own_a, "dp", pairs(1, 8))
     far_b = lax.ppermute(own_b, "dp", pairs(1, 8))

time: 131 us -> 133 us (1.015)
  waiting for transfers between devices: 44.4 us -> 49.6 us
  starting transfers between devices: 48.1 us -> 45 us
    ppermute x6 -> x12, waiting for transfers between devices: 24.6 us -> 40.5 us  [spread(): return [a] + [lax.ppermute(a, axis, perm_of(k)) for k in range(1, SIDE)]]
    ppermute x8 -> x0, starting transfers between devices: 15.7 us -> none  [the longest x2 8.51 us: both_ways(): ahead = lax.ppermute(a, axis, perm_of(-1))]
    ppermute x6 -> x12, starting transfers between devices: 11.6 us -> 23.2 us  [spread(): return [a] + [lax.ppermute(a, axis, perm_of(k)) for k in range(1, SIDE)]]
    ppermute x8 -> x0, waiting for transfers between devices: 10.7 us -> none  [the longest x2 6.51 us: both_ways(): low = lax.ppermute(back[:half], axis, perm_of(1))]
  transfers between devices with their start and end apart: 24 -> 22, of which waited for: 13 -> 12; matrix products, arithmetic and copies ran while one was open for 2% -> 2% of each run, Pallas kernels for 9% -> 9%
where the time goes in v3:
time: 133 us; the launch traced here: 132 us
  waiting for transfers between devices  49.6 us (37%)
  starting transfers between devices  45 us (34%)
  Pallas kernels  17.5 us (13%)
  blocking collectives  15.9 us (12%)
  other arithmetic  4.14 us (3%)
    ppermute x12, waiting for transfers between devices, spread(): return [a] + [lax.ppermute(a, axis, perm_of(k)) for k in range(1, SIDE)]  40.5 us
    ppermute x12, starting transfers between devices, spread(): return [a] + [lax.ppermute(a, axis, perm_of(k)) for k in range(1, SIDE)]  23.2 us
    all_to_all x1, blocking collectives, body(): lax.all_to_all(heads, 'sp', split_axis=0, concat_axis=0, tiled=True)  15.9 us
    ppermute x6, starting transfers between devices, doubled(): a = jnp.concatenate([a, lax.ppermute(a, axis, perm)], axis=0)  15.7 us
    pallas_call x1, Pallas kernels, body(): pl.pallas_call(functools.partial(attend_kernel, src=sp_size, rows=rows, b...  12.3 us
    all_to_all x1, starting transfers between devices, body(): got = lax.all_to_all(packed, 'sp', split_axis=0, concat_axis=0, tiled=True)  5.88 us
    ppermute x6, waiting for transfers between devices, doubled(): a = jnp.concatenate([a, lax.ppermute(a, axis, perm)], axis=0)  5.76 us
    ppermute x1, waiting for transfers between devices, body(): far_b = lax.ppermute(own_b, 'dp', pairs(1, 8))  3.39 us
  transfers between devices with their start and end apart: 22, of which 12 were waited for; matrix products, arithmetic and copies ran while one was open for 2% of the time, Pallas kernels for 9%

profile of v3, /device:TPU:0, one launch (start us, length us, event | category | flops | bytes accessed | tf_op | source)
XLA Modules:
  0.0 132.5 jit_solution(7919472870386481437)
XLA Ops:
  0.0 0.9 maximum_bitcast_fusion.1
  0.9 1.6 %collective-permute-start = (bf16[1,96,256]{2,1,0:T(8,128)(2,1)S(1)}, bf16[1,96,256]{2,1,0:T(8,128)(2,1)S(1)}, u32[]{:S(2)}, u32[]{:S(2)}) collective-permute-start(bf16[1,96,256]{2,1,0:T(8,128)(2,1)S(1)} %maximum_bitcast_fusion.1), channel_id=1, source_target_pairs={{0,2},{1,3},{2,0},{3,1},{4,6},{5,7},{6,4},{7,5},{8,10},{9,11},{10,... | collective-permute-start | bytes 147464 | tf_op jit(solution)/shard_map/ppermute | solution.py:36
  2.5 1.4 %fusion = f32[192]{0:T(256)S(1)} fusion(bf16[1,192,2048]{2,1,0:T(8,128)(2,1)} %param.8), kind=kLoop, calls=%fused_computation.3 | loop fusion | flops 1179456 | bytes 787200 | tf_op jit(solution)/shard_map/reduce_sum | solution.py:183
  3.9 1.1 collective-permute-done
  5.0 3.2 %collective-permute-start.3 = (bf16[2,96,256]{2,1,0:T(8,128)(2,1)S(1)}, bf16[2,96,256]{2,1,0:T(8,128)(2,1)S(1)}, u32[]{:S(2)}, u32[]{:S(2)}) collective-permute-start(bf16[2,96,256]{2,1,0:T(8,128)(2,1)S(1)} %pad_maximum_fusion.9), channel_id=1, source_target_pairs={{0,4},{1,5},{2,6},{3,7},{4,0},{5,1},{6,2},{7,3},{8,12},{9,13},{10,... | collective-permute-start | bytes 294920 | tf_op jit(solution)/shard_map/ppermute | solution.py:36
  9.0 1.7 %collective-permute-start.1 = (bf16[1,256,256]{2,1,0:T(8,128)(2,1)S(1)}, bf16[1,256,256]{2,1,0:T(8,128)(2,1)S(1)}, u32[]{:S(2)}, u32[]{:S(2)}) collective-permute-start(bf16[1,256,256]{2,1,0:T(8,128)(2,1)S(1)} %maximum_bitcast_fusion), channel_id=1, source_target_pairs={{0,8},{8,0},{16,24},{24,16},{32,40},{40,32},{48,56},{56,48},{64,72... | collective-permute-start | bytes 393224 | tf_op jit(solution)/shard_map/ppermute | solution.py:36
  11.2 2.0 %collective-permute-start.4 = (bf16[1,2,96,256]{3,2,1,0:T(8,128)(2,1)S(1)}, bf16[1,2,96,256]{3,2,1,0:T(8,128)(2,1)S(1)}, u32[]{:S(2)}, u32[]{:S(2)}) collective-permute-start(bf16[1,2,96,256]{3,2,1,0:T(8,128)(2,1)S(1)} %bitcast.51), channel_id=1, source_target_pairs={{0,32},{8,40},{16,48},{24,56},{32,0},{40,8},{48,16},{56,24},{64,96... | collective-permute-start | bytes 294920 | tf_op jit(solution)/shard_map/ppermute | solution.py:36
  13.2 0.8 collective-permute-done.1
  14.0 3.3 %collective-permute-start.2 = (bf16[2,256,256]{2,1,0:T(8,128)(2,1)S(1)}, bf16[2,256,256]{2,1,0:T(8,128)(2,1)S(1)}, u32[]{:S(2)}, u32[]{:S(2)}) collective-permute-start(bf16[2,256,256]{2,1,0:T(8,128)(2,1)S(1)} %pad_maximum_fusion.6), channel_id=1, source_target_pairs={{0,16},{8,24},{16,0},{24,8},{32,48},{40,56},{48,32},{56,40},{64,80... | collective-permute-start | bytes 786440 | tf_op jit(solution)/shard_map/ppermute | solution.py:36
  17.4 4.0 %collective-permute-start.5 = (bf16[2,2,96,256]{3,2,1,0:T(8,128)(2,1)S(1)}, bf16[2,2,96,256]{3,2,1,0:T(8,128)(2,1)S(1)}, u32[]{:S(2)}, u32[]{:S(2)}) collective-permute-start(bf16[2,2,96,256]{3,2,1,0:T(8,128)(2,1)S(1)} %pad_maximum_fusion.7), channel_id=1, source_target_pairs={{0,64},{8,72},{16,80},{24,88},{32,96},{40,104},{48,112},{56,120},{... | collective-permute-start | bytes 589832 | tf_op jit(solution)/shard_map/ppermute | solution.py:36
  22.2 2.8 %collective-permute-done.5 = bf16[2,2,96,256]{3,2,1,0:T(8,128)(2,1)S(1)} collective-permute-done((bf16[2,2,96,256]{3,2,1,0:T(8,128)(2,1)S(1)}, bf16[2,2,96,256]{3,2,1,0:T(8,128)(2,1)S(1)}, u32[]{:S(2)}, u32[]{:S(2)}) %collective-permute-start.5) | collective-permute-done | bytes 196640 | tf_op jit(solution)/shard_map/ppermute | solution.py:36
  25.0 5.4 %collective-permute-start.8 = (bf16[4,2,96,256]{3,2,1,0:T(8,128)(2,1)S(1)}, bf16[4,2,96,256]{3,2,1,0:T(8,128)(2,1)S(1)}, u32[]{:S(2)}, u32[]{:S(2)}) collective-permute-start(bf16[4,2,96,256]{3,2,1,0:T(8,128)(2,1)S(1)} %bitcast.37), channel_id=1, source_target_pairs={{0,96},{8,104},{16,112},{24,120},{32,0},{40,8},{48,16},{56,24},{64... | collective-permute-start | bytes 1179656 | tf_op jit(solution)/shard_map/ppermute | solution.py:187
  30.4 0.9 collective-permute-start.6
  31.4 3.1 %collective-permute-start.11 = (bf16[4,2,96,256]{3,2,1,0:T(8,128)(2,1)S(1)}, bf16[4,2,96,256]{3,2,1,0:T(8,128)(2,1)S(1)}, u32[]{:S(2)}, u32[]{:S(2)}) collective-permute-start(bf16[4,2,96,256]{3,2,1,0:T(8,128)(2,1)S(1)} %pad_maximum_fusion.5), channel_id=1, source_target_pairs={{0,24},{8,0},{16,8},{24,16},{32,56},{40,32},{48,40},{56,48},{64,88... | collective-permute-start | bytes 1179656 | tf_op jit(solution)/shard_map/ppermute | solution.py:187
  35.2 8.5 %collective-permute-done.8 = bf16[4,2,96,256]{3,2,1,0:T(8,128)(2,1)S(1)} collective-permute-done((bf16[4,2,96,256]{3,2,1,0:T(8,128)(2,1)S(1)}, bf16[4,2,96,256]{3,2,1,0:T(8,128)(2,1)S(1)}, u32[]{:S(2)}, u32[]{:S(2)}) %collective-permute-start.8) | collective-permute-done | bytes 393248 | tf_op jit(solution)/shard_map/ppermute | solution.py:187
  43.6 1.5 %collective-permute-start.9 = (bf16[4,2,96,256]{3,2,1,0:T(8,128)(2,1)S(1)}, bf16[4,2,96,256]{3,2,1,0:T(8,128)(2,1)S(1)}, u32[]{:S(2)}, u32[]{:S(2)}) collective-permute-start(bf16[4,2,96,256]{3,2,1,0:T(8,128)(2,1)S(1)} %pad_maximum_fusion.5), channel_id=1, source_target_pairs={{0,8},{8,16},{16,24},{24,0},{32,40},{40,48},{48,56},{56,32},{64,72... | collective-permute-start | bytes 1179656 | tf_op jit(solution)/shard_map/ppermute | solution.py:187
  45.7 6.9 %collective-permute-done.9 = bf16[4,2,96,256]{3,2,1,0:T(8,128)(2,1)S(1)} collective-permute-done((bf16[4,2,96,256]{3,2,1,0:T(8,128)(2,1)S(1)}, bf16[4,2,96,256]{3,2,1,0:T(8,128)(2,1)S(1)}, u32[]{:S(2)}, u32[]{:S(2)}) %collective-permute-start.9) | collective-permute-done | bytes 393248 | tf_op jit(solution)/shard_map/ppermute | solution.py:187
  52.9 3.4 %collective-permute-done.13.far_b = bf16[4,4,2,96,256]{4,3,2,1,0:T(8,128)(2,1)S(1)} collective-permute-done((bf16[4,4,2,96,256]{4,3,2,1,0:T(8,128)(2,1)S(1)}, bf16[4,4,2,96,256]{4,3,2,1,0:T(8,128)(2,1)S(1)}, u32[]{:S(2)}, u32[]{:S(2)}) %collective-permute-start.13) | collective-permute-done | bytes 1572896 | tf_op jit(solution)/shard_map/ppermute | solution.py:201
  56.3 3.1 %project.1 = (bf16[16,288,128]{2,1,0:T(8,128)(2,1)}, f32[8,128]{1,0:T(8,128)}) custom-call(bf16[192,2048]{1,0:T(8,128)(2,1)S(1)} %fusion.2.normed_ref, bf16[4,4,2,96,256]{4,3,2,1,0:T(8,128)(2,1)S(1)} %pad_maximum_fusion.1.own_a, bf16[4,4,2,96,256]{4,3,2,1,0:T(8,128)(2,1)S(1)} %pad_maximum_fusion.2.own_b, ...), custom_call_target="tpu_custom_call" | custom-call | tf_op jit(solution)/shard_map/project/pallas_call | solution.py:202
  59.4 5.9 %all-to-all-start = ((bf16[16,288,128]{2,1,0:T(8,128)(2,1)}), bf16[16,288,128]{2,1,0:T(8,128)(2,1)S(1)}, u32[]{:S(2)}, u32[]{:S(2)}) async-start(bf16[16,288,128]{2,1,0:T(8,128)(2,1)} %get-tuple-element.24), calls=%async_computation | async-start | bytes 2359296 | tf_op jit(solution)/shard_map/all_to_all | solution.py:218
  65.3 1.9 %collective-permute-start.14 = (bf16[4,64,256]{2,1,0:T(8,128)(2,1)S(1)}, bf16[4,64,256]{2,1,0:T(8,128)(2,1)S(1)}, u32[]{:S(2)}, u32[]{:S(2)}) collective-permute-start(bf16[4,64,256]{2,1,0:T(8,128)(2,1)S(1)} %pad_maximum_fusion.8), channel_id=1, source_target_pairs={{0,32},{8,40},{16,48},{24,56},{32,64},{40,72},{48,80},{56,88},{64,... | collective-permute-start | bytes 393224 | tf_op jit(solution)/shard_map/ppermute | solution.py:187
  67.2 2.7 %collective-permute-start.15 = (bf16[4,64,256]{2,1,0:T(8,128)(2,1)S(1)}, bf16[4,64,256]{2,1,0:T(8,128)(2,1)S(1)}, u32[]{:S(2)}, u32[]{:S(2)}) collective-permute-start(bf16[4,64,256]{2,1,0:T(8,128)(2,1)S(1)} %pad_maximum_fusion.8), channel_id=1, source_target_pairs={{0,64},{8,72},{16,80},{24,88},{32,96},{40,104},{48,112},{56,120},{... | collective-permute-start | bytes 393224 | tf_op jit(solution)/shard_map/ppermute | solution.py:187
  69.9 1.5 %collective-permute-start.16 = (bf16[4,64,256]{2,1,0:T(8,128)(2,1)S(1)}, bf16[4,64,256]{2,1,0:T(8,128)(2,1)S(1)}, u32[]{:S(2)}, u32[]{:S(2)}) collective-permute-start(bf16[4,64,256]{2,1,0:T(8,128)(2,1)S(1)} %pad_maximum_fusion.8), channel_id=1, source_target_pairs={{0,96},{8,104},{16,112},{24,120},{32,0},{40,8},{48,16},{56,24},{64... | collective-permute-start | bytes 393224 | tf_op jit(solution)/shard_map/ppermute | solution.py:187
  71.4 12.8 %collective-permute-done.14 = bf16[4,64,256]{2,1,0:T(8,128)(2,1)S(1)} collective-permute-done((bf16[4,64,256]{2,1,0:T(8,128)(2,1)S(1)}, bf16[4,64,256]{2,1,0:T(8,128)(2,1)S(1)}, u32[]{:S(2)}, u32[]{:S(2)}) %collective-permute-start.14) | collective-permute-done | bytes 131104 | tf_op jit(solution)/shard_map/ppermute | solution.py:187
  84.2 3.4 %collective-permute-done.15 = bf16[4,64,256]{2,1,0:T(8,128)(2,1)S(1)} collective-permute-done((bf16[4,64,256]{2,1,0:T(8,128)(2,1)S(1)}, bf16[4,64,256]{2,1,0:T(8,128)(2,1)S(1)}, u32[]{:S(2)}, u32[]{:S(2)}) %collective-permute-start.15) | collective-permute-done | bytes 131104 | tf_op jit(solution)/shard_map/ppermute | solution.py:187
  87.7 1.7 %collective-permute-start.17 = (bf16[4,4,64,256]{3,2,1,0:T(8,128)(2,1)S(1)}, bf16[4,4,64,256]{3,2,1,0:T(8,128)(2,1)S(1)}, u32[]{:S(2)}, u32[]{:S(2)}) collective-permute-start(bf16[4,4,64,256]{3,2,1,0:T(8,128)(2,1)S(1)} %pad_maximum_fusion.4), channel_id=1, source_target_pairs={{0,2},{1,3},{2,4},{3,5},{4,6},{5,7},{6,0},{7,1},{8,10},{9,11},{10,... | collective-permute-start | bytes 1572872 | tf_op jit(solution)/shard_map/ppermute | solution.py:187
  89.4 2.7 %collective-permute-start.18 = (bf16[4,4,64,256]{3,2,1,0:T(8,128)(2,1)S(1)}, bf16[4,4,64,256]{3,2,1,0:T(8,128)(2,1)S(1)}, u32[]{:S(2)}, u32[]{:S(2)}) collective-permute-start(bf16[4,4,64,256]{3,2,1,0:T(8,128)(2,1)S(1)} %pad_maximum_fusion.4), channel_id=1, source_target_pairs={{0,4},{1,5},{2,6},{3,7},{4,0},{5,1},{6,2},{7,3},{8,12},{9,13},{10,... | collective-permute-start | bytes 1572872 | tf_op jit(solution)/shard_map/ppermute | solution.py:187
  92.1 1.0 collective-permute-start.19
  93.2 12.3 %attend.1 = bf16[16,96,128]{2,1,0:T(8,128)(2,1)S(1)} custom-call(bf16[16,288,128]{2,1,0:T(8,128)(2,1)S(1)} %all-to-all-done.got_ref, f32[1,3072]{1,0:T(1,128)S(1)} %bitcast.34, f32[1,64]{1,0:T(1,128)S(1)} %dynamic-slice_bitcast_fusion.gain_ref), custom_call_target="tpu_custom_call" | custom-call | tf_op jit(solution)/shard_map/attend/pallas_call | solution.py:222
  105.6 8.6 %collective-permute-done.18 = bf16[4,4,64,256]{3,2,1,0:T(8,128)(2,1)S(1)} collective-permute-done((bf16[4,4,64,256]{3,2,1,0:T(8,128)(2,1)S(1)}, bf16[4,4,64,256]{3,2,1,0:T(8,128)(2,1)S(1)}, u32[]{:S(2)}, u32[]{:S(2)}) %collective-permute-start.18) | collective-permute-done | bytes 524320 | tf_op jit(solution)/shard_map/ppermute | solution.py:187
  114.5 15.9 %all_to_all.10.got_ref = bf16[16,96,128]{2,1,0:T(8,128)(2,1)S(1)} all-to-all(bf16[16,96,128]{2,1,0:T(8,128)(2,1)S(1)} %attend.1), channel_id=1, replica_groups=mesh['sp'=16,'dp'=8] {'sp'}, dimensions={0} | all-to-all | bytes 786432 | tf_op jit(solution)/shard_map/all_to_all | solution.py:242
  130.4 2.0 %output.1 = bf16[192,2048]{1,0:T(8,128)(2,1)} custom-call(bf16[16,96,128]{2,1,0:T(8,128)(2,1)S(1)} %all_to_all.10.got_ref, bf16[4,4,4,64,256]{4,3,2,1,0:T(8,128)(2,1)S(1)} %pad_maximum_fusion.own_ref, bf16[4,4,4,64,256]{4,3,2,1,0:T(8,128)(2,1)S(1)} %collective-permute-done.20.far_ref), custom_call_target="tpu_custom_call" | custom-call | tf_op jit(solution)/shard_map/output/pallas_call | solution.py:243
  (41 shorter events, 4.3 us)
Async XLA Ops:
  0.0 93.1 %copy-start = (f32[1024]{0:T(1024)S(1)}, f32[1024]{0:T(1024)}, u32[]{:S(2)}) copy-start(f32[1024]{0:T(1024)} %param.14) | copy-start | bytes 12292
  0.0 21.3 %copy-start.2 = (bf16[1,192,2048]{2,1,0:T(8,128)(2,1)S(1)}, bf16[1,192,2048]{2,1,0:T(8,128)(2,1)}, u32[]{:S(2)}) copy-start(bf16[1,192,2048]{2,1,0:T(8,128)(2,1)} %param.8) | copy-start | bytes 2359300
  0.0 21.3 %copy-start.3 = (f32[2048]{0:T(1024)S(1)}, f32[2048]{0:T(1024)}, u32[]{:S(2)}) copy-start(f32[2048]{0:T(1024)} %param.9) | copy-start | bytes 24580
  0.9 4.1 %collective-permute-start = (bf16[1,96,256]{2,1,0:T(8,128)(2,1)S(1)}, bf16[1,96,256]{2,1,0:T(8,128)(2,1)S(1)}, u32[]{:S(2)}, u32[]{:S(2)}) collective-permute-start(bf16[1,96,256]{2,1,0:T(8,128)(2,1)S(1)} %maximum_bitcast_fusion.1), channel_id=1, source_target_pairs={{0,2},{1,3},{2,0},{3,1},{4,6},{5,7},{6,4},{7,5},{8,10},{9,11},{10,... | collective-permute-start | bytes 147464 | tf_op jit(solution)/shard_map/ppermute | solution.py:36
  5.0 6.2 %collective-permute-start.3 = (bf16[2,96,256]{2,1,0:T(8,128)(2,1)S(1)}, bf16[2,96,256]{2,1,0:T(8,128)(2,1)S(1)}, u32[]{:S(2)}, u32[]{:S(2)}) collective-permute-start(bf16[2,96,256]{2,1,0:T(8,128)(2,1)S(1)} %pad_maximum_fusion.9), channel_id=1, source_target_pairs={{0,4},{1,5},{2,6},{3,7},{4,0},{5,1},{6,2},{7,3},{8,12},{9,13},{10,... | collective-permute-start | bytes 294920 | tf_op jit(solution)/shard_map/ppermute | solution.py:36
  9.0 5.0 %collective-permute-start.1 = (bf16[1,256,256]{2,1,0:T(8,128)(2,1)S(1)}, bf16[1,256,256]{2,1,0:T(8,128)(2,1)S(1)}, u32[]{:S(2)}, u32[]{:S(2)}) collective-permute-start(bf16[1,256,256]{2,1,0:T(8,128)(2,1)S(1)} %maximum_bitcast_fusion), channel_id=1, source_target_pairs={{0,8},{8,0},{16,24},{24,16},{32,40},{40,32},{48,56},{56,48},{64,72... | collective-permute-start | bytes 393224 | tf_op jit(solution)/shard_map/ppermute | solution.py:36
  11.2 6.1 %collective-permute-start.4 = (bf16[1,2,96,256]{3,2,1,0:T(8,128)(2,1)S(1)}, bf16[1,2,96,256]{3,2,1,0:T(8,128)(2,1)S(1)}, u32[]{:S(2)}, u32[]{:S(2)}) collective-permute-start(bf16[1,2,96,256]{3,2,1,0:T(8,128)(2,1)S(1)} %bitcast.51), channel_id=1, source_target_pairs={{0,32},{8,40},{16,48},{24,56},{32,0},{40,8},{48,16},{56,24},{64,96... | collective-permute-start | bytes 294920 | tf_op jit(solution)/shard_map/ppermute | solution.py:36
  14.0 8.0 %collective-permute-start.2 = (bf16[2,256,256]{2,1,0:T(8,128)(2,1)S(1)}, bf16[2,256,256]{2,1,0:T(8,128)(2,1)S(1)}, u32[]{:S(2)}, u32[]{:S(2)}) collective-permute-start(bf16[2,256,256]{2,1,0:T(8,128)(2,1)S(1)} %pad_maximum_fusion.6), channel_id=1, source_target_pairs={{0,16},{8,24},{16,0},{24,8},{32,48},{40,56},{48,32},{56,40},{64,80... | collective-permute-start | bytes 786440 | tf_op jit(solution)/shard_map/ppermute | solution.py:36
  17.4 7.6 %collective-permute-start.5 = (bf16[2,2,96,256]{3,2,1,0:T(8,128)(2,1)S(1)}, bf16[2,2,96,256]{3,2,1,0:T(8,128)(2,1)S(1)}, u32[]{:S(2)}, u32[]{:S(2)}) collective-permute-start(bf16[2,2,96,256]{3,2,1,0:T(8,128)(2,1)S(1)} %pad_maximum_fusion.7), channel_id=1, source_target_pairs={{0,64},{8,72},{16,80},{24,88},{32,96},{40,104},{48,112},{56,120},{... | collective-permute-start | bytes 589832 | tf_op jit(solution)/shard_map/ppermute | solution.py:36
  25.0 18.6 %collective-permute-start.8 = (bf16[4,2,96,256]{3,2,1,0:T(8,128)(2,1)S(1)}, bf16[4,2,96,256]{3,2,1,0:T(8,128)(2,1)S(1)}, u32[]{:S(2)}, u32[]{:S(2)}) collective-permute-start(bf16[4,2,96,256]{3,2,1,0:T(8,128)(2,1)S(1)} %bitcast.37), channel_id=1, source_target_pairs={{0,96},{8,104},{16,112},{24,120},{32,0},{40,8},{48,16},{56,24},{64... | collective-permute-start | bytes 1179656 | tf_op jit(solution)/shard_map/ppermute | solution.py:187
  30.4 14.8 %collective-permute-start.7 = (bf16[4,2,96,256]{3,2,1,0:T(8,128)(2,1)S(1)}, bf16[4,2,96,256]{3,2,1,0:T(8,128)(2,1)S(1)}, u32[]{:S(2)}, u32[]{:S(2)}) collective-permute-start(bf16[4,2,96,256]{3,2,1,0:T(8,128)(2,1)S(1)} %bitcast.38), channel_id=1, source_target_pairs={{0,64},{8,72},{16,80},{24,88},{32,96},{40,104},{48,112},{56,120},{... | collective-permute-start | bytes 1179656 | tf_op jit(solution)/shard_map/ppermute | solution.py:187
  30.4 15.0 %collective-permute-start.6 = (bf16[4,2,96,256]{3,2,1,0:T(8,128)(2,1)S(1)}, bf16[4,2,96,256]{3,2,1,0:T(8,128)(2,1)S(1)}, u32[]{:S(2)}, u32[]{:S(2)}) collective-permute-start(bf16[4,2,96,256]{3,2,1,0:T(8,128)(2,1)S(1)} %bitcast.39), channel_id=1, source_target_pairs={{0,32},{8,40},{16,48},{24,56},{32,64},{40,72},{48,80},{56,88},{64,... | collective-permute-start | bytes 1179656 | tf_op jit(solution)/shard_map/ppermute | solution.py:187
  31.4 14.3 %collective-permute-start.11 = (bf16[4,2,96,256]{3,2,1,0:T(8,128)(2,1)S(1)}, bf16[4,2,96,256]{3,2,1,0:T(8,128)(2,1)S(1)}, u32[]{:S(2)}, u32[]{:S(2)}) collective-permute-start(bf16[4,2,96,256]{3,2,1,0:T(8,128)(2,1)S(1)} %pad_maximum_fusion.5), channel_id=1, source_target_pairs={{0,24},{8,0},{16,8},{24,16},{32,56},{40,32},{48,40},{56,48},{64,88... | collective-permute-start | bytes 1179656 | tf_op jit(solution)/shard_map/ppermute | solution.py:187
  34.5 11.2 %collective-permute-start.10 = (bf16[4,2,96,256]{3,2,1,0:T(8,128)(2,1)S(1)}, bf16[4,2,96,256]{3,2,1,0:T(8,128)(2,1)S(1)}, u32[]{:S(2)}, u32[]{:S(2)}) collective-permute-start(bf16[4,2,96,256]{3,2,1,0:T(8,128)(2,1)S(1)} %pad_maximum_fusion.5), channel_id=1, source_target_pairs={{0,16},{8,24},{16,0},{24,8},{32,48},{40,56},{48,32},{56,40},{64,80... | collective-permute-start | bytes 1179656 | tf_op jit(solution)/shard_map/ppermute | solution.py:187
  43.6 9.0 %collective-permute-start.9 = (bf16[4,2,96,256]{3,2,1,0:T(8,128)(2,1)S(1)}, bf16[4,2,96,256]{3,2,1,0:T(8,128)(2,1)S(1)}, u32[]{:S(2)}, u32[]{:S(2)}) collective-permute-start(bf16[4,2,96,256]{3,2,1,0:T(8,128)(2,1)S(1)} %pad_maximum_fusion.5), channel_id=1, source_target_pairs={{0,8},{8,16},{16,24},{24,0},{32,40},{40,48},{48,56},{56,32},{64,72... | collective-permute-start | bytes 1179656 | tf_op jit(solution)/shard_map/ppermute | solution.py:187
  45.6 7.3 %collective-permute-start.12 = (bf16[4,4,2,96,256]{4,3,2,1,0:T(8,128)(2,1)S(1)}, bf16[4,4,2,96,256]{4,3,2,1,0:T(8,128)(2,1)S(1)}, u32[]{:S(2)}, u32[]{:S(2)}) collective-permute-start(bf16[4,4,2,96,256]{4,3,2,1,0:T(8,128)(2,1)S(1)} %pad_maximum_fusion.1.own_a), channel_id=1, source_target_pairs={{0,1},{1,0},{2,3},{3,2},{4,5},{5,4},{6,7},{7,6},{8,9},{9,8},{10,11... | collective-permute-start | bytes 4718600 | tf_op jit(solution)/shard_map/ppermute | solution.py:200
  52.8 3.5 %collective-permute-start.13 = (bf16[4,4,2,96,256]{4,3,2,1,0:T(8,128)(2,1)S(1)}, bf16[4,4,2,96,256]{4,3,2,1,0:T(8,128)(2,1)S(1)}, u32[]{:S(2)}, u32[]{:S(2)}) collective-permute-start(bf16[4,4,2,96,256]{4,3,2,1,0:T(8,128)(2,1)S(1)} %pad_maximum_fusion.2.own_b), channel_id=1, source_target_pairs={{0,1},{1,0},{2,3},{3,2},{4,5},{5,4},{6,7},{7,6},{8,9},{9,8},{10,11... | collective-permute-start | bytes 4718600 | tf_op jit(solution)/shard_map/ppermute | solution.py:201
  59.4 33.8 %copy-start.1 = (f32[1,3072,1]{1,2,0:T(1,128)S(1)}, f32[1,3072,1]{1,2,0:T(1,128)}, u32[]{:S(2)}) copy-start(f32[1,3072,1]{1,2,0:T(1,128)} %param.13) | copy-start | bytes 36868
  59.4 33.8 %all-to-all-start = ((bf16[16,288,128]{2,1,0:T(8,128)(2,1)}), bf16[16,288,128]{2,1,0:T(8,128)(2,1)S(1)}, u32[]{:S(2)}, u32[]{:S(2)}) async-start(bf16[16,288,128]{2,1,0:T(8,128)(2,1)} %get-tuple-element.24), calls=%async_computation | async-start | bytes 2359296 | tf_op jit(solution)/shard_map/all_to_all | solution.py:218
  65.3 18.9 %collective-permute-start.14 = (bf16[4,64,256]{2,1,0:T(8,128)(2,1)S(1)}, bf16[4,64,256]{2,1,0:T(8,128)(2,1)S(1)}, u32[]{:S(2)}, u32[]{:S(2)}) collective-permute-start(bf16[4,64,256]{2,1,0:T(8,128)(2,1)S(1)} %pad_maximum_fusion.8), channel_id=1, source_target_pairs={{0,32},{8,40},{16,48},{24,56},{32,64},{40,72},{48,80},{56,88},{64,... | collective-permute-start | bytes 393224 | tf_op jit(solution)/shard_map/ppermute | solution.py:187
  67.2 20.4 %collective-permute-start.15 = (bf16[4,64,256]{2,1,0:T(8,128)(2,1)S(1)}, bf16[4,64,256]{2,1,0:T(8,128)(2,1)S(1)}, u32[]{:S(2)}, u32[]{:S(2)}) collective-permute-start(bf16[4,64,256]{2,1,0:T(8,128)(2,1)S(1)} %pad_maximum_fusion.8), channel_id=1, source_target_pairs={{0,64},{8,72},{16,80},{24,88},{32,96},{40,104},{48,112},{56,120},{... | collective-permute-start | bytes 393224 | tf_op jit(solution)/shard_map/ppermute | solution.py:187
  69.9 17.7 %collective-permute-start.16 = (bf16[4,64,256]{2,1,0:T(8,128)(2,1)S(1)}, bf16[4,64,256]{2,1,0:T(8,128)(2,1)S(1)}, u32[]{:S(2)}, u32[]{:S(2)}) collective-permute-start(bf16[4,64,256]{2,1,0:T(8,128)(2,1)S(1)} %pad_maximum_fusion.8), channel_id=1, source_target_pairs={{0,96},{8,104},{16,112},{24,120},{32,0},{40,8},{48,16},{56,24},{64... | collective-permute-start | bytes 393224 | tf_op jit(solution)/shard_map/ppermute | solution.py:187
  87.7 17.8 %collective-permute-start.17 = (bf16[4,4,64,256]{3,2,1,0:T(8,128)(2,1)S(1)}, bf16[4,4,64,256]{3,2,1,0:T(8,128)(2,1)S(1)}, u32[]{:S(2)}, u32[]{:S(2)}) collective-permute-start(bf16[4,4,64,256]{3,2,1,0:T(8,128)(2,1)S(1)} %pad_maximum_fusion.4), channel_id=1, source_target_pairs={{0,2},{1,3},{2,4},{3,5},{4,6},{5,7},{6,0},{7,1},{8,10},{9,11},{10,... | collective-permute-start | bytes 1572872 | tf_op jit(solution)/shard_map/ppermute | solution.py:187
  89.4 24.8 %collective-permute-start.18 = (bf16[4,4,64,256]{3,2,1,0:T(8,128)(2,1)S(1)}, bf16[4,4,64,256]{3,2,1,0:T(8,128)(2,1)S(1)}, u32[]{:S(2)}, u32[]{:S(2)}) collective-permute-start(bf16[4,4,64,256]{3,2,1,0:T(8,128)(2,1)S(1)} %pad_maximum_fusion.4), channel_id=1, source_target_pairs={{0,4},{1,5},{2,6},{3,7},{4,0},{5,1},{6,2},{7,3},{8,12},{9,13},{10,... | collective-permute-start | bytes 1572872 | tf_op jit(solution)/shard_map/ppermute | solution.py:187
  92.1 22.0 %collective-permute-start.19 = (bf16[4,4,64,256]{3,2,1,0:T(8,128)(2,1)S(1)}, bf16[4,4,64,256]{3,2,1,0:T(8,128)(2,1)S(1)}, u32[]{:S(2)}, u32[]{:S(2)}) collective-permute-start(bf16[4,4,64,256]{3,2,1,0:T(8,128)(2,1)S(1)} %pad_maximum_fusion.4), channel_id=1, source_target_pairs={{0,6},{1,7},{2,0},{3,1},{4,2},{5,3},{6,4},{7,5},{8,14},{9,15},{10,... | collective-permute-start | bytes 1572872 | tf_op jit(solution)/shard_map/ppermute | solution.py:187
  114.4 16.0 %collective-permute-start.20 = (bf16[4,4,4,64,256]{4,3,2,1,0:T(8,128)(2,1)S(1)}, bf16[4,4,4,64,256]{4,3,2,1,0:T(8,128)(2,1)S(1)}, u32[]{:S(2)}, u32[]{:S(2)}) collective-permute-start(bf16[4,4,4,64,256]{4,3,2,1,0:T(8,128)(2,1)S(1)} %pad_maximum_fusion.own_ref), channel_id=1, source_target_pairs={{0,1},{1,0},{2,3},{3,2},{4,5},{5,4},{6,7},{7,6},{8,9},{9,8},{10,11... | collective-permute-start | bytes 6291464 | tf_op jit(solution)/shard_map/ppermute | solution.py:241

commit v4 on v3

--- a/solution.py
+++ b/solution.py
@@ -29,12 +29,6 @@
     return [
         (s, ((s // SIDE + dz) % SIDE) * SIDE + (s % SIDE + dy) % SIDE) for s in range(SIDE * SIDE)
     ]
-
-
-def doubled(a, axis, perms):
-    for perm in perms:
-        a = jnp.concatenate([a, lax.ppermute(a, axis, perm)], axis=0)
-    return a
 
 
 def near(*arrays):
@@ -65,9 +59,9 @@
         for i in range(SIDE):
             for ref_a, ref_b in ((own_a, own_b), (far_a, far_b)):
                 if i < 2:
-                    several = [ref_a[before(z, zs), jnp.bitwise_xor(y, ys), i] for ys in range(SIDE)]
+                    several = [ref_a[before(z, zs), before(y, ys), i] for ys in range(SIDE)]
                 else:
-                    several = [ref_b[before(y, ys), jnp.bitwise_xor(z, zs), i - 2] for ys in range(SIDE)]
+                    several = [ref_b[before(y, ys), before(z, zs), i - 2] for ys in range(SIDE)]
                 parts.append(jnp.concatenate(several, axis=0))
         weights = jnp.concatenate(parts, axis=1)
         total = lax.dot_general(
@@ -163,7 +157,7 @@
     for i in range(SIDE):
         for cc, ref in ((0, own_ref), (1, far_ref)):
             parts = [
-                ref[i, before(z, zs), jnp.bitwise_xor(y, ys)] for zs in range(SIDE) for ys in range(SIDE)
+                ref[i, before(z, zs), before(y, ys)] for zs in range(SIDE) for ys in range(SIDE)
             ]
             mixed = jnp.dot(
                 heads_ref[...], jnp.concatenate(parts, axis=0), preferred_element_type=jnp.float32
@@ -187,16 +181,20 @@
         return [a] + [lax.ppermute(a, axis, perm_of(k)) for k in range(1, SIDE)]
 
     piece = jnp.concatenate([w_query.T, w_key.T, w_value.T], axis=0)
-    four = doubled(piece[None], "dp", (pairs(2, 8), pairs(4, 8)))
-    together = jnp.concatenate([four[:2].reshape(192, 256), w_out], axis=0)[None]
-    first_a = doubled(together, "sp", (pairs(1, 16), pairs(2, 16)))
-    first_b = doubled(four[2:][None], "sp", (pairs(4, 16), pairs(8, 16)))
+    two = jnp.stack([piece, lax.ppermute(piece, "dp", pairs(2, 8))])
+    four = lax.ppermute(two, "dp", pairs(4, 8))
+    together = jnp.concatenate([two.reshape(192, 256), w_out], axis=0)
+    first_a = spread(lambda k: along_zy(0, k), together, "sp")
+    first_a = jnp.stack(first_a)
+    first_b = jnp.stack(spread(lambda k: along_zy(k, 0), four, "sp"))
     rest_y = first_a[:, 192:]
     first_a = first_a[:, :192].reshape(SIDE, 2, 96, 256)
-    first_a, first_b, normed = lax.optimization_barrier((first_a, first_b, normed))
-    own_a = jnp.stack(spread(lambda k: along_zy(k, 0), first_a, "sp"))
-    own_b = jnp.stack(spread(lambda k: along_zy(0, k), first_b, "sp"))
-    own_a, rest_y = lax.optimization_barrier((own_a, rest_y))
+    first_a, first_b, rest_y = lax.optimization_barrier((first_a, first_b, rest_y))
+    own_b = spread(lambda k: along_zy(0, k), first_b, "sp")
+    own_a = spread(lambda k: along_zy(k, 0), first_a, "sp")
+    rest_z = spread(lambda k: along_zy(k, 0), rest_y, "sp")
+    own_b = jnp.stack(own_b)
+    own_a = jnp.stack(own_a)
     far_a = lax.ppermute(own_a, "dp", pairs(1, 8))
     far_b = lax.ppermute(own_b, "dp", pairs(1, 8))
     packed, done = pl.pallas_call(
@@ -211,7 +209,6 @@
         compiler_params=pltpu.CompilerParams(vmem_limit_bytes=30 * 2**20),
         name="project",
     )(*near(normed, own_a, own_b, far_a, far_b))
-    rest_z = spread(lambda k: along_zy(k, 0), rest_y, "sp")
     _, rest_z = lax.optimization_barrier((done, rest_z))
     rest_x = spread(along_x, jnp.stack(rest_z), "dp")
 
@@ -264,4 +261,6 @@
         P("sp", "dp"),
     )
 
-    return jax.shard_map(body, mesh=mesh, in_specs=placed, out_specs=P("dp", "sp", None), check_vma=False)
+    return jax.shard_map(
+        body, mesh=mesh, in_specs=placed, out_specs=P("dp", "sp", None), check_vma=False
+    )

time: 133 us -> 130 us (0.977)
  waiting for transfers between devices: 49.6 us -> 48.1 us
    ppermute x6 -> x2, starting transfers between devices: 15.7 us -> 4.65 us  [the longest x1 3.02 us: body(): four = lax.ppermute(two, 'dp', pairs(4, 8))]
    ppermute x12 -> x18, starting transfers between devices: 23.2 us -> 33.8 us  [spread(): return [a] + [lax.ppermute(a, axis, perm_of(k)) for k in range(1, SIDE)]]
    another operation x2 -> x7, other arithmetic: 0.39 us -> 2.11 us  [the longest x2 0.85 us: body(): first_a = jnp.stack(first_a)]
    broadcast_in_dim x2 -> x0, other arithmetic: 1.64 us -> none  [the longest x1 0.87 us: body(): four = doubled(piece[None], 'dp', (pairs(2, 8), pairs(4, 8)))]
    ppermute x1, waiting for transfers between devices: 3.39 us -> 2.04 us  [body(): far_b = lax.ppermute(own_b, 'dp', pairs(1, 8))]
    ppermute x6 -> x2, waiting for transfers between devices: 5.76 us -> 5.58 us  [the longest x1 3.1 us: body(): four = lax.ppermute(two, 'dp', pairs(4, 8))]
    ppermute x12 -> x18, waiting for transfers between devices: 40.5 us -> 40.4 us  [spread(): return [a] + [lax.ppermute(a, axis, perm_of(k)) for k in range(1, SIDE)]]
  transfers between devices with their start and end apart: 22 -> 24, of which waited for: 12 -> 13; matrix products, arithmetic and copies ran while one was open for 2% -> 1% of each run, Pallas kernels for 9% -> 10%
where the time goes in v4:
time: 130 us; the launch traced here: 129 us
  waiting for transfers between devices  48.1 us (37%)
  starting transfers between devices  43.8 us (34%)
  Pallas kernels  17.5 us (13%)
  blocking collectives  15.9 us (12%)
  other arithmetic  2.95 us (2%)
    ppermute x18, waiting for transfers between devices, spread(): return [a] + [lax.ppermute(a, axis, perm_of(k)) for k in range(1, SIDE)]  40.4 us
    ppermute x18, starting transfers between devices, spread(): return [a] + [lax.ppermute(a, axis, perm_of(k)) for k in range(1, SIDE)]  33.8 us
    all_to_all x1, blocking collectives, body(): lax.all_to_all(heads, 'sp', split_axis=0, concat_axis=0, tiled=True)  15.9 us
    pallas_call x1, Pallas kernels, body(): pl.pallas_call(functools.partial(attend_kernel, src=sp_size, rows=rows, b...  12.4 us
    all_to_all x1, starting transfers between devices, body(): got = lax.all_to_all(packed, 'sp', split_axis=0, concat_axis=0, tiled=True)  5.13 us
    ppermute x1, waiting for transfers between devices, body(): four = lax.ppermute(two, 'dp', pairs(4, 8))  3.1 us
    pallas_call x1, Pallas kernels, body(): pl.pallas_call(project_kernel, out_shape=(pltpu.VMEM((sp_size, rows + row...  3.09 us
    ppermute x1, starting transfers between devices, body(): four = lax.ppermute(two, 'dp', pairs(4, 8))  3.02 us
  transfers between devices with their start and end apart: 24, of which 13 were waited for; matrix products, arithmetic and copies ran while one was open for 1% of the time, Pallas kernels for 10%

profile of v4, /device:TPU:0, one launch (start us, length us, event | category | flops | bytes accessed | tf_op | source)
XLA Modules:
  0.0 129.3 jit_solution(14056403571517841566)
XLA Ops:
  0.8 1.6 %collective-permute-start = (bf16[96,256]{1,0:T(8,128)(2,1)S(1)}, bf16[96,256]{1,0:T(8,128)(2,1)S(1)}, u32[]{:S(2)}, u32[]{:S(2)}) collective-permute-start(bf16[96,256]{1,0:T(8,128)(2,1)S(1)} %get-tuple-element.34), channel_id=1, source_target_pairs={{0,2},{1,3},{2,0},{3,1},{4,6},{5,7},{6,4},{7,5},{8,10},{9,11},{10,... | collective-permute-start | bytes 147464 | tf_op jit(solution)/shard_map/ppermute | solution.py:184
  2.4 2.5 %collective-permute-done = bf16[96,256]{1,0:T(8,128)(2,1)S(1)} collective-permute-done((bf16[96,256]{1,0:T(8,128)(2,1)S(1)}, bf16[96,256]{1,0:T(8,128)(2,1)S(1)}, u32[]{:S(2)}, u32[]{:S(2)}) %collective-permute-start) | collective-permute-done | bytes 49184 | tf_op jit(solution)/shard_map/ppermute | solution.py:184
  5.7 3.2 %collective-permute-start.3 = (bf16[256,256]{1,0:T(8,128)(2,1)S(1)}, bf16[256,256]{1,0:T(8,128)(2,1)S(1)}, u32[]{:S(2)}, u32[]{:S(2)}) collective-permute-start(bf16[256,256]{1,0:T(8,128)(2,1)S(1)} %get-tuple-element.32), channel_id=1, source_target_pairs={{0,24},{8,0},{16,8},{24,16},{32,56},{40,32},{48,40},{56,48},{64,88... | collective-permute-start | bytes 393224 | tf_op jit(solution)/shard_map/ppermute | solution.py:181
  9.6 1.0 collective-permute-start.1
  10.5 3.0 %collective-permute-start.4 = (bf16[2,96,256]{2,1,0:T(8,128)(2,1)S(1)}, bf16[2,96,256]{2,1,0:T(8,128)(2,1)S(1)}, u32[]{:S(2)}, u32[]{:S(2)}) collective-permute-start(bf16[2,96,256]{2,1,0:T(8,128)(2,1)S(1)} %pad_maximum_fusion.8), channel_id=1, source_target_pairs={{0,4},{1,5},{2,6},{3,7},{4,0},{5,1},{6,2},{7,3},{8,12},{9,13},{10,... | collective-permute-start | bytes 294920 | tf_op jit(solution)/shard_map/ppermute | solution.py:185
  13.5 3.1 %collective-permute-done.4 = bf16[2,96,256]{2,1,0:T(8,128)(2,1)S(1)} collective-permute-done((bf16[2,96,256]{2,1,0:T(8,128)(2,1)S(1)}, bf16[2,96,256]{2,1,0:T(8,128)(2,1)S(1)}, u32[]{:S(2)}, u32[]{:S(2)}) %collective-permute-start.4) | collective-permute-done | bytes 98336 | tf_op jit(solution)/shard_map/ppermute | solution.py:185
  16.6 4.0 %collective-permute-start.7 = (bf16[2,96,256]{2,1,0:T(8,128)(2,1)S(1)}, bf16[2,96,256]{2,1,0:T(8,128)(2,1)S(1)}, u32[]{:S(2)}, u32[]{:S(2)}) collective-permute-start(bf16[2,96,256]{2,1,0:T(8,128)(2,1)S(1)} %collective-permute-done.4), channel_id=1, source_target_pairs={{0,96},{8,104},{16,112},{24,120},{32,0},{40,8},{48,16},{56,24},{64... | collective-permute-start | bytes 294920 | tf_op jit(solution)/shard_map/ppermute | solution.py:181
  20.7 1.3 collective-permute-start.5
  22.1 1.8 %collective-permute-done.7 = bf16[2,96,256]{2,1,0:T(8,128)(2,1)S(1)} collective-permute-done((bf16[2,96,256]{2,1,0:T(8,128)(2,1)S(1)}, bf16[2,96,256]{2,1,0:T(8,128)(2,1)S(1)}, u32[]{:S(2)}, u32[]{:S(2)}) %collective-permute-start.7) | collective-permute-done | bytes 98336 | tf_op jit(solution)/shard_map/ppermute | solution.py:181
  23.9 3.0 %collective-permute-done.6 = bf16[2,96,256]{2,1,0:T(8,128)(2,1)S(1)} collective-permute-done((bf16[2,96,256]{2,1,0:T(8,128)(2,1)S(1)}, bf16[2,96,256]{2,1,0:T(8,128)(2,1)S(1)}, u32[]{:S(2)}, u32[]{:S(2)}) %collective-permute-start.6) | collective-permute-done | bytes 98336 | tf_op jit(solution)/shard_map/ppermute | solution.py:181
  27.6 1.2 collective-permute-start.10
  28.8 5.0 %collective-permute-start.9 = (bf16[4,2,96,256]{3,2,1,0:T(8,128)(2,1)S(1)}, bf16[4,2,96,256]{3,2,1,0:T(8,128)(2,1)S(1)}, u32[]{:S(2)}, u32[]{:S(2)}) collective-permute-start(bf16[4,2,96,256]{3,2,1,0:T(8,128)(2,1)S(1)} %bitcast.45), channel_id=1, source_target_pairs={{0,64},{8,72},{16,80},{24,88},{32,96},{40,104},{48,112},{56,120},{... | collective-permute-start | bytes 1179656 | tf_op jit(solution)/shard_map/ppermute | solution.py:181
  33.9 1.3 %collective-permute-start.8 = (bf16[4,2,96,256]{3,2,1,0:T(8,128)(2,1)S(1)}, bf16[4,2,96,256]{3,2,1,0:T(8,128)(2,1)S(1)}, u32[]{:S(2)}, u32[]{:S(2)}) collective-permute-start(bf16[4,2,96,256]{3,2,1,0:T(8,128)(2,1)S(1)} %bitcast.46), channel_id=1, source_target_pairs={{0,32},{8,40},{16,48},{24,56},{32,64},{40,72},{48,80},{56,88},{64,... | collective-permute-start | bytes 1179656 | tf_op jit(solution)/shard_map/ppermute | solution.py:181
  35.2 1.7 %collective-permute-start.13 = (bf16[4,2,96,256]{3,2,1,0:T(8,128)(2,1)S(1)}, bf16[4,2,96,256]{3,2,1,0:T(8,128)(2,1)S(1)}, u32[]{:S(2)}, u32[]{:S(2)}) collective-permute-start(bf16[4,2,96,256]{3,2,1,0:T(8,128)(2,1)S(1)} %pad_maximum_fusion.5), channel_id=1, source_target_pairs={{0,24},{8,0},{16,8},{24,16},{32,56},{40,32},{48,40},{56,48},{64,88... | collective-permute-start | bytes 1179656 | tf_op jit(solution)/shard_map/ppermute | solution.py:181
  36.9 2.3 %collective-permute-start.12 = (bf16[4,2,96,256]{3,2,1,0:T(8,128)(2,1)S(1)}, bf16[4,2,96,256]{3,2,1,0:T(8,128)(2,1)S(1)}, u32[]{:S(2)}, u32[]{:S(2)}) collective-permute-start(bf16[4,2,96,256]{3,2,1,0:T(8,128)(2,1)S(1)} %pad_maximum_fusion.5), channel_id=1, source_target_pairs={{0,16},{8,24},{16,0},{24,8},{32,48},{40,56},{48,32},{56,40},{64,80... | collective-permute-start | bytes 1179656 | tf_op jit(solution)/shard_map/ppermute | solution.py:181
  40.6 4.1 %collective-permute-done.8 = bf16[4,2,96,256]{3,2,1,0:T(8,128)(2,1)S(1)} collective-permute-done((bf16[4,2,96,256]{3,2,1,0:T(8,128)(2,1)S(1)}, bf16[4,2,96,256]{3,2,1,0:T(8,128)(2,1)S(1)}, u32[]{:S(2)}, u32[]{:S(2)}) %collective-permute-start.8) | collective-permute-done | bytes 393248 | tf_op jit(solution)/shard_map/ppermute | solution.py:181
  45.1 1.2 collective-permute-done.12
  46.2 4.1 %collective-permute-done.11 = bf16[4,2,96,256]{3,2,1,0:T(8,128)(2,1)S(1)} collective-permute-done((bf16[4,2,96,256]{3,2,1,0:T(8,128)(2,1)S(1)}, bf16[4,2,96,256]{3,2,1,0:T(8,128)(2,1)S(1)}, u32[]{:S(2)}, u32[]{:S(2)}) %collective-permute-start.11) | collective-permute-done | bytes 393248 | tf_op jit(solution)/shard_map/ppermute | solution.py:181
  52.0 2.0 %collective-permute-done.15.far_b = bf16[4,4,2,96,256]{4,3,2,1,0:T(8,128)(2,1)S(1)} collective-permute-done((bf16[4,4,2,96,256]{4,3,2,1,0:T(8,128)(2,1)S(1)}, bf16[4,4,2,96,256]{4,3,2,1,0:T(8,128)(2,1)S(1)}, u32[]{:S(2)}, u32[]{:S(2)}) %collective-permute-start.15) | collective-permute-done | bytes 1572896 | tf_op jit(solution)/shard_map/ppermute | solution.py:199
  54.1 3.1 %project.1 = (bf16[16,288,128]{2,1,0:T(8,128)(2,1)}, f32[8,128]{1,0:T(8,128)}) custom-call(bf16[192,2048]{1,0:T(8,128)(2,1)S(1)} %fusion.2.normed_ref, bf16[4,4,2,96,256]{4,3,2,1,0:T(8,128)(2,1)S(1)} %pad_maximum_fusion.1.own_a, bf16[4,4,2,96,256]{4,3,2,1,0:T(8,128)(2,1)S(1)} %pad_maximum_fusion.2.own_b, ...), custom_call_target="tpu_custom_call" | custom-call | tf_op jit(solution)/shard_map/project/pallas_call | solution.py:200
  57.2 5.1 %all-to-all-start = ((bf16[16,288,128]{2,1,0:T(8,128)(2,1)}), bf16[16,288,128]{2,1,0:T(8,128)(2,1)S(1)}, u32[]{:S(2)}, u32[]{:S(2)}) async-start(bf16[16,288,128]{2,1,0:T(8,128)(2,1)} %get-tuple-element.20), calls=%async_computation | async-start | bytes 2359296 | tf_op jit(solution)/shard_map/all_to_all | solution.py:215
  62.3 1.9 %collective-permute-start.16 = (bf16[4,64,256]{2,1,0:T(8,128)(2,1)S(1)}, bf16[4,64,256]{2,1,0:T(8,128)(2,1)S(1)}, u32[]{:S(2)}, u32[]{:S(2)}) collective-permute-start(bf16[4,64,256]{2,1,0:T(8,128)(2,1)S(1)} %pad_maximum_fusion.6), channel_id=1, source_target_pairs={{0,32},{8,40},{16,48},{24,56},{32,64},{40,72},{48,80},{56,88},{64,... | collective-permute-start | bytes 393224 | tf_op jit(solution)/shard_map/ppermute | solution.py:181
  64.2 2.7 %collective-permute-start.17 = (bf16[4,64,256]{2,1,0:T(8,128)(2,1)S(1)}, bf16[4,64,256]{2,1,0:T(8,128)(2,1)S(1)}, u32[]{:S(2)}, u32[]{:S(2)}) collective-permute-start(bf16[4,64,256]{2,1,0:T(8,128)(2,1)S(1)} %pad_maximum_fusion.6), channel_id=1, source_target_pairs={{0,64},{8,72},{16,80},{24,88},{32,96},{40,104},{48,112},{56,120},{... | collective-permute-start | bytes 393224 | tf_op jit(solution)/shard_map/ppermute | solution.py:181
  66.9 1.5 %collective-permute-start.18 = (bf16[4,64,256]{2,1,0:T(8,128)(2,1)S(1)}, bf16[4,64,256]{2,1,0:T(8,128)(2,1)S(1)}, u32[]{:S(2)}, u32[]{:S(2)}) collective-permute-start(bf16[4,64,256]{2,1,0:T(8,128)(2,1)S(1)} %pad_maximum_fusion.6), channel_id=1, source_target_pairs={{0,96},{8,104},{16,112},{24,120},{32,0},{40,8},{48,16},{56,24},{64... | collective-permute-start | bytes 393224 | tf_op jit(solution)/shard_map/ppermute | solution.py:181
  68.4 12.8 %collective-permute-done.16 = bf16[4,64,256]{2,1,0:T(8,128)(2,1)S(1)} collective-permute-done((bf16[4,64,256]{2,1,0:T(8,128)(2,1)S(1)}, bf16[4,64,256]{2,1,0:T(8,128)(2,1)S(1)}, u32[]{:S(2)}, u32[]{:S(2)}) %collective-permute-start.16) | collective-permute-done | bytes 131104 | tf_op jit(solution)/shard_map/ppermute | solution.py:181
  81.2 3.4 %collective-permute-done.17 = bf16[4,64,256]{2,1,0:T(8,128)(2,1)S(1)} collective-permute-done((bf16[4,64,256]{2,1,0:T(8,128)(2,1)S(1)}, bf16[4,64,256]{2,1,0:T(8,128)(2,1)S(1)}, u32[]{:S(2)}, u32[]{:S(2)}) %collective-permute-start.17) | collective-permute-done | bytes 131104 | tf_op jit(solution)/shard_map/ppermute | solution.py:181
  84.7 1.0 collective-permute-start.19
  85.7 3.3 %collective-permute-start.20 = (bf16[4,4,64,256]{3,2,1,0:T(8,128)(2,1)S(1)}, bf16[4,4,64,256]{3,2,1,0:T(8,128)(2,1)S(1)}, u32[]{:S(2)}, u32[]{:S(2)}) collective-permute-start(bf16[4,4,64,256]{3,2,1,0:T(8,128)(2,1)S(1)} %pad_maximum_fusion.4), channel_id=1, source_target_pairs={{0,4},{1,5},{2,6},{3,7},{4,0},{5,1},{6,2},{7,3},{8,12},{9,13},{10,... | collective-permute-start | bytes 1572872 | tf_op jit(solution)/shard_map/ppermute | solution.py:181
  89.9 12.4 %attend.1 = bf16[16,96,128]{2,1,0:T(8,128)(2,1)S(1)} custom-call(bf16[16,288,128]{2,1,0:T(8,128)(2,1)S(1)} %all-to-all-done.got_ref, f32[1,3072]{1,0:T(1,128)S(1)} %bitcast.41, f32[1,64]{1,0:T(1,128)S(1)} %dynamic-slice_bitcast_fusion.gain_ref), custom_call_target="tpu_custom_call" | custom-call | tf_op jit(solution)/shard_map/attend/pallas_call | solution.py:219
  102.3 8.7 %collective-permute-done.20 = bf16[4,4,64,256]{3,2,1,0:T(8,128)(2,1)S(1)} collective-permute-done((bf16[4,4,64,256]{3,2,1,0:T(8,128)(2,1)S(1)}, bf16[4,4,64,256]{3,2,1,0:T(8,128)(2,1)S(1)}, u32[]{:S(2)}, u32[]{:S(2)}) %collective-permute-start.20) | collective-permute-done | bytes 524320 | tf_op jit(solution)/shard_map/ppermute | solution.py:181
  111.4 15.9 %all_to_all.10.got_ref = bf16[16,96,128]{2,1,0:T(8,128)(2,1)S(1)} all-to-all(bf16[16,96,128]{2,1,0:T(8,128)(2,1)S(1)} %attend.1), channel_id=1, replica_groups=mesh['sp'=16,'dp'=8] {'sp'}, dimensions={0} | all-to-all | bytes 786432 | tf_op jit(solution)/shard_map/all_to_all | solution.py:239
  127.3 2.0 %output.1 = bf16[192,2048]{1,0:T(8,128)(2,1)} custom-call(bf16[16,96,128]{2,1,0:T(8,128)(2,1)S(1)} %all_to_all.10.got_ref, bf16[4,4,4,64,256]{4,3,2,1,0:T(8,128)(2,1)S(1)} %pad_maximum_fusion.own_ref, bf16[4,4,4,64,256]{4,3,2,1,0:T(8,128)(2,1)S(1)} %collective-permute-done.22.far_ref), custom_call_target="tpu_custom_call" | custom-call | tf_op jit(solution)/shard_map/output/pallas_call | solution.py:240
  (43 shorter events, 7.8 us)
Async XLA Ops:
  0.0 89.8 %copy-start = (f32[1024]{0:T(1024)S(1)}, f32[1024]{0:T(1024)}, u32[]{:S(2)}) copy-start(f32[1024]{0:T(1024)} %param.14) | copy-start | bytes 12292
  0.8 4.1 %collective-permute-start = (bf16[96,256]{1,0:T(8,128)(2,1)S(1)}, bf16[96,256]{1,0:T(8,128)(2,1)S(1)}, u32[]{:S(2)}, u32[]{:S(2)}) collective-permute-start(bf16[96,256]{1,0:T(8,128)(2,1)S(1)} %get-tuple-element.34), channel_id=1, source_target_pairs={{0,2},{1,3},{2,0},{3,1},{4,6},{5,7},{6,4},{7,5},{8,10},{9,11},{10,... | collective-permute-start | bytes 147464 | tf_op jit(solution)/shard_map/ppermute | solution.py:184
  5.7 15.0 %collective-permute-start.3 = (bf16[256,256]{1,0:T(8,128)(2,1)S(1)}, bf16[256,256]{1,0:T(8,128)(2,1)S(1)}, u32[]{:S(2)}, u32[]{:S(2)}) collective-permute-start(bf16[256,256]{1,0:T(8,128)(2,1)S(1)} %get-tuple-element.32), channel_id=1, source_target_pairs={{0,24},{8,0},{16,8},{24,16},{32,56},{40,32},{48,40},{56,48},{64,88... | collective-permute-start | bytes 393224 | tf_op jit(solution)/shard_map/ppermute | solution.py:181
  8.9 13.0 %collective-permute-start.2 = (bf16[256,256]{1,0:T(8,128)(2,1)S(1)}, bf16[256,256]{1,0:T(8,128)(2,1)S(1)}, u32[]{:S(2)}, u32[]{:S(2)}) collective-permute-start(bf16[256,256]{1,0:T(8,128)(2,1)S(1)} %get-tuple-element.32), channel_id=1, source_target_pairs={{0,16},{8,24},{16,0},{24,8},{32,48},{40,56},{48,32},{56,40},{64,80... | collective-permute-start | bytes 393224 | tf_op jit(solution)/shard_map/ppermute | solution.py:181
  9.6 12.4 %collective-permute-start.1 = (bf16[256,256]{1,0:T(8,128)(2,1)S(1)}, bf16[256,256]{1,0:T(8,128)(2,1)S(1)}, u32[]{:S(2)}, u32[]{:S(2)}) collective-permute-start(bf16[256,256]{1,0:T(8,128)(2,1)S(1)} %get-tuple-element.32), channel_id=1, source_target_pairs={{0,8},{8,16},{16,24},{24,0},{32,40},{40,48},{48,56},{56,32},{64,72... | collective-permute-start | bytes 393224 | tf_op jit(solution)/shard_map/ppermute | solution.py:181
  10.5 6.1 %collective-permute-start.4 = (bf16[2,96,256]{2,1,0:T(8,128)(2,1)S(1)}, bf16[2,96,256]{2,1,0:T(8,128)(2,1)S(1)}, u32[]{:S(2)}, u32[]{:S(2)}) collective-permute-start(bf16[2,96,256]{2,1,0:T(8,128)(2,1)S(1)} %pad_maximum_fusion.8), channel_id=1, source_target_pairs={{0,4},{1,5},{2,6},{3,7},{4,0},{5,1},{6,2},{7,3},{8,12},{9,13},{10,... | collective-permute-start | bytes 294920 | tf_op jit(solution)/shard_map/ppermute | solution.py:185
  16.6 7.3 %collective-permute-start.7 = (bf16[2,96,256]{2,1,0:T(8,128)(2,1)S(1)}, bf16[2,96,256]{2,1,0:T(8,128)(2,1)S(1)}, u32[]{:S(2)}, u32[]{:S(2)}) collective-permute-start(bf16[2,96,256]{2,1,0:T(8,128)(2,1)S(1)} %collective-permute-done.4), channel_id=1, source_target_pairs={{0,96},{8,104},{16,112},{24,120},{32,0},{40,8},{48,16},{56,24},{64... | collective-permute-start | bytes 294920 | tf_op jit(solution)/shard_map/ppermute | solution.py:181
  20.7 6.2 %collective-permute-start.6 = (bf16[2,96,256]{2,1,0:T(8,128)(2,1)S(1)}, bf16[2,96,256]{2,1,0:T(8,128)(2,1)S(1)}, u32[]{:S(2)}, u32[]{:S(2)}) collective-permute-start(bf16[2,96,256]{2,1,0:T(8,128)(2,1)S(1)} %collective-permute-done.4), channel_id=1, source_target_pairs={{0,64},{8,72},{16,80},{24,88},{32,96},{40,104},{48,112},{56,120},{... | collective-permute-start | bytes 294920 | tf_op jit(solution)/shard_map/ppermute | solution.py:181
  20.7 6.9 %collective-permute-start.5 = (bf16[2,96,256]{2,1,0:T(8,128)(2,1)S(1)}, bf16[2,96,256]{2,1,0:T(8,128)(2,1)S(1)}, u32[]{:S(2)}, u32[]{:S(2)}) collective-permute-start(bf16[2,96,256]{2,1,0:T(8,128)(2,1)S(1)} %collective-permute-done.4), channel_id=1, source_target_pairs={{0,32},{8,40},{16,48},{24,56},{32,64},{40,72},{48,80},{56,88},{64,... | collective-permute-start | bytes 294920 | tf_op jit(solution)/shard_map/ppermute | solution.py:181
  27.6 11.5 %collective-permute-start.10 = (bf16[4,2,96,256]{3,2,1,0:T(8,128)(2,1)S(1)}, bf16[4,2,96,256]{3,2,1,0:T(8,128)(2,1)S(1)}, u32[]{:S(2)}, u32[]{:S(2)}) collective-permute-start(bf16[4,2,96,256]{3,2,1,0:T(8,128)(2,1)S(1)} %bitcast.44), channel_id=1, source_target_pairs={{0,96},{8,104},{16,112},{24,120},{32,0},{40,8},{48,16},{56,24},{64... | collective-permute-start | bytes 1179656 | tf_op jit(solution)/shard_map/ppermute | solution.py:181
  28.8 11.8 %collective-permute-start.9 = (bf16[4,2,96,256]{3,2,1,0:T(8,128)(2,1)S(1)}, bf16[4,2,96,256]{3,2,1,0:T(8,128)(2,1)S(1)}, u32[]{:S(2)}, u32[]{:S(2)}) collective-permute-start(bf16[4,2,96,256]{3,2,1,0:T(8,128)(2,1)S(1)} %bitcast.45), channel_id=1, source_target_pairs={{0,64},{8,72},{16,80},{24,88},{32,96},{40,104},{48,112},{56,120},{... | collective-permute-start | bytes 1179656 | tf_op jit(solution)/shard_map/ppermute | solution.py:181
  33.9 10.9 %collective-permute-start.8 = (bf16[4,2,96,256]{3,2,1,0:T(8,128)(2,1)S(1)}, bf16[4,2,96,256]{3,2,1,0:T(8,128)(2,1)S(1)}, u32[]{:S(2)}, u32[]{:S(2)}) collective-permute-start(bf16[4,2,96,256]{3,2,1,0:T(8,128)(2,1)S(1)} %bitcast.46), channel_id=1, source_target_pairs={{0,32},{8,40},{16,48},{24,56},{32,64},{40,72},{48,80},{56,88},{64,... | collective-permute-start | bytes 1179656 | tf_op jit(solution)/shard_map/ppermute | solution.py:181
  35.2 9.9 %collective-permute-start.13 = (bf16[4,2,96,256]{3,2,1,0:T(8,128)(2,1)S(1)}, bf16[4,2,96,256]{3,2,1,0:T(8,128)(2,1)S(1)}, u32[]{:S(2)}, u32[]{:S(2)}) collective-permute-start(bf16[4,2,96,256]{3,2,1,0:T(8,128)(2,1)S(1)} %pad_maximum_fusion.5), channel_id=1, source_target_pairs={{0,24},{8,0},{16,8},{24,16},{32,56},{40,32},{48,40},{56,48},{64,88... | collective-permute-start | bytes 1179656 | tf_op jit(solution)/shard_map/ppermute | solution.py:181
  36.9 9.4 %collective-permute-start.12 = (bf16[4,2,96,256]{3,2,1,0:T(8,128)(2,1)S(1)}, bf16[4,2,96,256]{3,2,1,0:T(8,128)(2,1)S(1)}, u32[]{:S(2)}, u32[]{:S(2)}) collective-permute-start(bf16[4,2,96,256]{3,2,1,0:T(8,128)(2,1)S(1)} %pad_maximum_fusion.5), channel_id=1, source_target_pairs={{0,16},{8,24},{16,0},{24,8},{32,48},{40,56},{48,32},{56,40},{64,80... | collective-permute-start | bytes 1179656 | tf_op jit(solution)/shard_map/ppermute | solution.py:181
  39.2 11.2 %collective-permute-start.11 = (bf16[4,2,96,256]{3,2,1,0:T(8,128)(2,1)S(1)}, bf16[4,2,96,256]{3,2,1,0:T(8,128)(2,1)S(1)}, u32[]{:S(2)}, u32[]{:S(2)}) collective-permute-start(bf16[4,2,96,256]{3,2,1,0:T(8,128)(2,1)S(1)} %pad_maximum_fusion.5), channel_id=1, source_target_pairs={{0,8},{8,16},{16,24},{24,0},{32,40},{40,48},{48,56},{56,32},{64,72... | collective-permute-start | bytes 1179656 | tf_op jit(solution)/shard_map/ppermute | solution.py:181
  45.0 7.0 %collective-permute-start.14 = (bf16[4,4,2,96,256]{4,3,2,1,0:T(8,128)(2,1)S(1)}, bf16[4,4,2,96,256]{4,3,2,1,0:T(8,128)(2,1)S(1)}, u32[]{:S(2)}, u32[]{:S(2)}) collective-permute-start(bf16[4,4,2,96,256]{4,3,2,1,0:T(8,128)(2,1)S(1)} %pad_maximum_fusion.1.own_a), channel_id=1, source_target_pairs={{0,1},{1,0},{2,3},{3,2},{4,5},{5,4},{6,7},{7,6},{8,9},{9,8},{10,11... | collective-permute-start | bytes 4718600 | tf_op jit(solution)/shard_map/ppermute | solution.py:198
  50.4 1.1 copy-start.2
  50.4 1.4 %copy-start.3 = (f32[2048]{0:T(1024)S(1)}, f32[2048]{0:T(1024)}, u32[]{:S(2)}) copy-start(f32[2048]{0:T(1024)} %param.9) | copy-start | bytes 24580
  50.6 3.5 %collective-permute-start.15 = (bf16[4,4,2,96,256]{4,3,2,1,0:T(8,128)(2,1)S(1)}, bf16[4,4,2,96,256]{4,3,2,1,0:T(8,128)(2,1)S(1)}, u32[]{:S(2)}, u32[]{:S(2)}) collective-permute-start(bf16[4,4,2,96,256]{4,3,2,1,0:T(8,128)(2,1)S(1)} %pad_maximum_fusion.2.own_b), channel_id=1, source_target_pairs={{0,1},{1,0},{2,3},{3,2},{4,5},{5,4},{6,7},{7,6},{8,9},{9,8},{10,11... | collective-permute-start | bytes 4718600 | tf_op jit(solution)/shard_map/ppermute | solution.py:199
  57.1 32.8 %copy-start.1 = (f32[1,3072,1]{1,2,0:T(1,128)S(1)}, f32[1,3072,1]{1,2,0:T(1,128)}, u32[]{:S(2)}) copy-start(f32[1,3072,1]{1,2,0:T(1,128)} %param.13) | copy-start | bytes 36868
  57.2 32.8 %all-to-all-start = ((bf16[16,288,128]{2,1,0:T(8,128)(2,1)}), bf16[16,288,128]{2,1,0:T(8,128)(2,1)S(1)}, u32[]{:S(2)}, u32[]{:S(2)}) async-start(bf16[16,288,128]{2,1,0:T(8,128)(2,1)} %get-tuple-element.20), calls=%async_computation | async-start | bytes 2359296 | tf_op jit(solution)/shard_map/all_to_all | solution.py:215
  62.3 18.9 %collective-permute-start.16 = (bf16[4,64,256]{2,1,0:T(8,128)(2,1)S(1)}, bf16[4,64,256]{2,1,0:T(8,128)(2,1)S(1)}, u32[]{:S(2)}, u32[]{:S(2)}) collective-permute-start(bf16[4,64,256]{2,1,0:T(8,128)(2,1)S(1)} %pad_maximum_fusion.6), channel_id=1, source_target_pairs={{0,32},{8,40},{16,48},{24,56},{32,64},{40,72},{48,80},{56,88},{64,... | collective-permute-start | bytes 393224 | tf_op jit(solution)/shard_map/ppermute | solution.py:181
  64.2 20.4 %collective-permute-start.17 = (bf16[4,64,256]{2,1,0:T(8,128)(2,1)S(1)}, bf16[4,64,256]{2,1,0:T(8,128)(2,1)S(1)}, u32[]{:S(2)}, u32[]{:S(2)}) collective-permute-start(bf16[4,64,256]{2,1,0:T(8,128)(2,1)S(1)} %pad_maximum_fusion.6), channel_id=1, source_target_pairs={{0,64},{8,72},{16,80},{24,88},{32,96},{40,104},{48,112},{56,120},{... | collective-permute-start | bytes 393224 | tf_op jit(solution)/shard_map/ppermute | solution.py:181
  66.9 17.7 %collective-permute-start.18 = (bf16[4,64,256]{2,1,0:T(8,128)(2,1)S(1)}, bf16[4,64,256]{2,1,0:T(8,128)(2,1)S(1)}, u32[]{:S(2)}, u32[]{:S(2)}) collective-permute-start(bf16[4,64,256]{2,1,0:T(8,128)(2,1)S(1)} %pad_maximum_fusion.6), channel_id=1, source_target_pairs={{0,96},{8,104},{16,112},{24,120},{32,0},{40,8},{48,16},{56,24},{64... | collective-permute-start | bytes 393224 | tf_op jit(solution)/shard_map/ppermute | solution.py:181
  84.7 17.6 %collective-permute-start.19 = (bf16[4,4,64,256]{3,2,1,0:T(8,128)(2,1)S(1)}, bf16[4,4,64,256]{3,2,1,0:T(8,128)(2,1)S(1)}, u32[]{:S(2)}, u32[]{:S(2)}) collective-permute-start(bf16[4,4,64,256]{3,2,1,0:T(8,128)(2,1)S(1)} %pad_maximum_fusion.4), channel_id=1, source_target_pairs={{0,2},{1,3},{2,4},{3,5},{4,6},{5,7},{6,0},{7,1},{8,10},{9,11},{10,... | collective-permute-start | bytes 1572872 | tf_op jit(solution)/shard_map/ppermute | solution.py:181
  85.7 25.4 %collective-permute-start.20 = (bf16[4,4,64,256]{3,2,1,0:T(8,128)(2,1)S(1)}, bf16[4,4,64,256]{3,2,1,0:T(8,128)(2,1)S(1)}, u32[]{:S(2)}, u32[]{:S(2)}) collective-permute-start(bf16[4,4,64,256]{3,2,1,0:T(8,128)(2,1)S(1)} %pad_maximum_fusion.4), channel_id=1, source_target_pairs={{0,4},{1,5},{2,6},{3,7},{4,0},{5,1},{6,2},{7,3},{8,12},{9,13},{10,... | collective-permute-start | bytes 1572872 | tf_op jit(solution)/shard_map/ppermute | solution.py:181
  89.0 22.0 %collective-permute-start.21 = (bf16[4,4,64,256]{3,2,1,0:T(8,128)(2,1)S(1)}, bf16[4,4,64,256]{3,2,1,0:T(8,128)(2,1)S(1)}, u32[]{:S(2)}, u32[]{:S(2)}) collective-permute-start(bf16[4,4,64,256]{3,2,1,0:T(8,128)(2,1)S(1)} %pad_maximum_fusion.4), channel_id=1, source_target_pairs={{0,6},{1,7},{2,0},{3,1},{4,2},{5,3},{6,4},{7,5},{8,14},{9,15},{10,... | collective-permute-start | bytes 1572872 | tf_op jit(solution)/shard_map/ppermute | solution.py:181
  111.3 16.0 %collective-permute-start.22 = (bf16[4,4,4,64,256]{4,3,2,1,0:T(8,128)(2,1)S(1)}, bf16[4,4,4,64,256]{4,3,2,1,0:T(8,128)(2,1)S(1)}, u32[]{:S(2)}, u32[]{:S(2)}) collective-permute-start(bf16[4,4,4,64,256]{4,3,2,1,0:T(8,128)(2,1)S(1)} %pad_maximum_fusion.own_ref), channel_id=1, source_target_pairs={{0,1},{1,0},{2,3},{3,2},{4,5},{5,4},{6,7},{7,6},{8,9},{9,8},{10,11... | collective-permute-start | bytes 6291464 | tf_op jit(solution)/shard_map/ppermute | solution.py:238

commit v5 on v4

--- a/solution.py
+++ b/solution.py
@@ -12,6 +12,7 @@
 LOG2E = math.log2(math.e)
 norm_eps = 1e-06
 SIDE = 4
+ARRIVAL = (0, 1, 3, 2)
 
 
 VMEM = pl.BlockSpec(memory_space=pltpu.VMEM)
@@ -44,7 +45,11 @@
     return lax.rem(here + SIDE - there, SIDE)
 
 
-def project_kernel(normed_ref, own_a, own_b, far_a, far_b, out_ref, done_ref, order_ref, sums_ref):
+def project_kernel(normed_ref, *refs):
+    own_a, own_b, far_a, far_b = (
+        {k: refs[at + 2 * i] for i, k in enumerate(ARRIVAL)} for at in (0, 1, 2 * SIDE, 2 * SIDE + 1)
+    )
+    out_ref, done_ref, order_ref, sums_ref = refs[4 * SIDE :]
     bf = jnp.bfloat16
     x, c, z, y = place_of()
     rows = normed_ref.shape[0]
@@ -54,21 +59,21 @@
             order_ref[:, (2 * i + cc) * 256 : (2 * i + cc + 1) * 256] = normed_ref[
                 :, pl.ds(pl.multiple_of(chunk * 256, 256), 256)
             ]
-    for zs in range(SIDE):
+    for kz in range(SIDE):
         parts = []
         for i in range(SIDE):
-            for ref_a, ref_b in ((own_a, own_b), (far_a, far_b)):
+            for refs_a, refs_b in ((own_a, own_b), (far_a, far_b)):
                 if i < 2:
-                    several = [ref_a[before(z, zs), before(y, ys), i] for ys in range(SIDE)]
+                    several = [refs_a[kz][ky, i] for ky in range(SIDE)]
                 else:
-                    several = [ref_b[before(y, ys), before(z, zs), i - 2] for ys in range(SIDE)]
+                    several = [refs_b[ky][kz, i - 2] for ky in range(SIDE)]
                 parts.append(jnp.concatenate(several, axis=0))
         weights = jnp.concatenate(parts, axis=1)
         total = lax.dot_general(
             weights, order_ref[...], (((1,), (1,)), ((), ())), preferred_element_type=jnp.float32
         )
-        for ys in range(SIDE):
-            sums_ref[SIDE * zs + ys] = total[96 * ys : 96 * (ys + 1), :]
+        for ky in range(SIDE):
+            sums_ref[SIDE * before(z, kz) + before(y, ky)] = total[96 * ky : 96 * (ky + 1), :]
     half = rows // 2
     for g in range(SIDE):
         key = jnp.concatenate([sums_ref[SIDE * g + j, 64:80, :] for j in range(SIDE)], axis=0)
@@ -190,25 +195,25 @@
     rest_y = first_a[:, 192:]
     first_a = first_a[:, :192].reshape(SIDE, 2, 96, 256)
     first_a, first_b, rest_y = lax.optimization_barrier((first_a, first_b, rest_y))
-    own_b = spread(lambda k: along_zy(0, k), first_b, "sp")
-    own_a = spread(lambda k: along_zy(k, 0), first_a, "sp")
+    own_a, own_b = {0: first_a}, {0: first_b}
+    for k in ARRIVAL[1:]:
+        own_a[k] = lax.ppermute(first_a, "sp", along_zy(k, 0))
+        own_b[k] = lax.ppermute(first_b, "sp", along_zy(0, k))
     rest_z = spread(lambda k: along_zy(k, 0), rest_y, "sp")
-    own_b = jnp.stack(own_b)
-    own_a = jnp.stack(own_a)
-    far_a = lax.ppermute(own_a, "dp", pairs(1, 8))
-    far_b = lax.ppermute(own_b, "dp", pairs(1, 8))
+    own = [group[k] for k in ARRIVAL for group in (own_a, own_b)]
+    far = [lax.ppermute(block, "dp", pairs(1, 8)) for block in own]
     packed, done = pl.pallas_call(
         project_kernel,
         out_shape=(
             pltpu.VMEM((sp_size, rows + rows // 2, 128), bf),
             jax.ShapeDtypeStruct((8, 128), jnp.float32),
         ),
-        in_specs=[VMEM] * 5,
+        in_specs=[VMEM] * (1 + 4 * SIDE),
         out_specs=(VMEM, VMEM),
         scratch_shapes=[pltpu.VMEM((rows, width), bf), pltpu.VMEM((sp_size, 96, rows), jnp.float32)],
         compiler_params=pltpu.CompilerParams(vmem_limit_bytes=30 * 2**20),
         name="project",
-    )(*near(normed, own_a, own_b, far_a, far_b))
+    )(*near(normed, *own, *far))
     _, rest_z = lax.optimization_barrier((done, rest_z))
     rest_x = spread(along_x, jnp.stack(rest_z), "dp")
 

time: 130 us -> 132 us (1.015)
  waiting for transfers between devices: 48.1 us -> 50.4 us
    ppermute x2 -> x14, waiting for transfers between devices: 2.04 us -> 14.5 us  [the longest x3 7.63 us: body(): own_a[k] = lax.ppermute(first_a, 'sp', along_zy(k, 0))]
    ppermute x18 -> x12, starting transfers between devices: 33.8 us -> 21.9 us  [spread(): return [a] + [lax.ppermute(a, axis, perm_of(k)) for k in range(1, SIDE)]]
    ppermute x2 -> x14, starting transfers between devices: 0.17 us -> 10.5 us  [the longest x3 4.89 us: body(): own_b[k] = lax.ppermute(first_b, 'sp', along_zy(0, k))]
    ppermute x18 -> x12, waiting for transfers between devices: 40.4 us -> 30.2 us  [spread(): return [a] + [lax.ppermute(a, axis, perm_of(k)) for k in range(1, SIDE)]]
    all_to_all x1, starting transfers between devices: 5.13 us -> 7.53 us  [body(): got = lax.all_to_all(packed, 'sp', split_axis=0, concat_axis=0, tiled=True)]
  transfers between devices with their start and end apart: 24 -> 30, of which waited for: 13 -> 15; matrix products, arithmetic and copies ran while one was open for 1% -> 1% of each run, Pallas kernels for 10% -> 9%
where the time goes in v5:
time: 132 us
  waiting for transfers between devices  50.4 us (38%)
  starting transfers between devices  44.7 us (34%)
  Pallas kernels  17.7 us (13%)
  blocking collectives  15.9 us (12%)
  other arithmetic  2.62 us (2%)
    ppermute x12, waiting for transfers between devices, spread(): return [a] + [lax.ppermute(a, axis, perm_of(k)) for k in range(1, SIDE)]  30.2 us
    ppermute x12, starting transfers between devices, spread(): return [a] + [lax.ppermute(a, axis, perm_of(k)) for k in range(1, SIDE)]  21.9 us
    all_to_all x1, blocking collectives, body(): lax.all_to_all(heads, 'sp', split_axis=0, concat_axis=0, tiled=True)  15.9 us
    pallas_call x1, Pallas kernels, body(): pl.pallas_call(functools.partial(attend_kernel, src=sp_size, rows=rows, b...  12.3 us
    ppermute x3, waiting for transfers between devices, body(): own_a[k] = lax.ppermute(first_a, 'sp', along_zy(k, 0))  7.63 us
    all_to_all x1, starting transfers between devices, body(): got = lax.all_to_all(packed, 'sp', split_axis=0, concat_axis=0, tiled=True)  7.53 us
    ppermute x3, starting transfers between devices, body(): own_b[k] = lax.ppermute(first_b, 'sp', along_zy(0, k))  4.89 us
    ppermute x3, waiting for transfers between devices, body(): own_b[k] = lax.ppermute(first_b, 'sp', along_zy(0, k))  4.77 us
  transfers between devices with their start and end apart: 30, of which 15 were waited for; matrix products, arithmetic and copies ran while one was open for 1% of the time, Pallas kernels for 9%

profile of v5, /device:TPU:0, one launch (start us, length us, event | category | flops | bytes accessed | tf_op | source)
XLA Modules:
  0.0 131.5 jit_solution(693512065608945989)
XLA Ops:
  0.0 0.9 fusion.3
  0.9 1.6 %collective-permute-start = (bf16[96,256]{1,0:T(8,128)(2,1)S(1)}, bf16[96,256]{1,0:T(8,128)(2,1)S(1)}, u32[]{:S(2)}, u32[]{:S(2)}) collective-permute-start(bf16[96,256]{1,0:T(8,128)(2,1)S(1)} %get-tuple-element.34), channel_id=1, source_target_pairs={{0,2},{1,3},{2,0},{3,1},{4,6},{5,7},{6,4},{7,5},{8,10},{9,11},{10,... | collective-permute-start | bytes 147464 | tf_op jit(solution)/shard_map/ppermute | solution.py:189
  2.5 2.5 %collective-permute-done = bf16[96,256]{1,0:T(8,128)(2,1)S(1)} collective-permute-done((bf16[96,256]{1,0:T(8,128)(2,1)S(1)}, bf16[96,256]{1,0:T(8,128)(2,1)S(1)}, u32[]{:S(2)}, u32[]{:S(2)}) %collective-permute-start) | collective-permute-done | bytes 49184 | tf_op jit(solution)/shard_map/ppermute | solution.py:189
  5.8 3.2 %collective-permute-start.3 = (bf16[256,256]{1,0:T(8,128)(2,1)S(1)}, bf16[256,256]{1,0:T(8,128)(2,1)S(1)}, u32[]{:S(2)}, u32[]{:S(2)}) collective-permute-start(bf16[256,256]{1,0:T(8,128)(2,1)S(1)} %get-tuple-element.32), channel_id=1, source_target_pairs={{0,24},{8,0},{16,8},{24,16},{32,56},{40,32},{48,40},{56,48},{64,88... | collective-permute-start | bytes 393224 | tf_op jit(solution)/shard_map/ppermute | solution.py:186
  9.6 1.0 collective-permute-start.1
  10.6 3.0 %collective-permute-start.4 = (bf16[2,96,256]{2,1,0:T(8,128)(2,1)S(1)}, bf16[2,96,256]{2,1,0:T(8,128)(2,1)S(1)}, u32[]{:S(2)}, u32[]{:S(2)}) collective-permute-start(bf16[2,96,256]{2,1,0:T(8,128)(2,1)S(1)} %pad_maximum_fusion.6), channel_id=1, source_target_pairs={{0,4},{1,5},{2,6},{3,7},{4,0},{5,1},{6,2},{7,3},{8,12},{9,13},{10,... | collective-permute-start | bytes 294920 | tf_op jit(solution)/shard_map/ppermute | solution.py:190
  13.6 3.1 %collective-permute-done.4 = bf16[2,96,256]{2,1,0:T(8,128)(2,1)S(1)} collective-permute-done((bf16[2,96,256]{2,1,0:T(8,128)(2,1)S(1)}, bf16[2,96,256]{2,1,0:T(8,128)(2,1)S(1)}, u32[]{:S(2)}, u32[]{:S(2)}) %collective-permute-start.4) | collective-permute-done | bytes 98336 | tf_op jit(solution)/shard_map/ppermute | solution.py:190
  16.7 4.0 %collective-permute-start.7 = (bf16[2,96,256]{2,1,0:T(8,128)(2,1)S(1)}, bf16[2,96,256]{2,1,0:T(8,128)(2,1)S(1)}, u32[]{:S(2)}, u32[]{:S(2)}) collective-permute-start(bf16[2,96,256]{2,1,0:T(8,128)(2,1)S(1)} %collective-permute-done.4), channel_id=1, source_target_pairs={{0,96},{8,104},{16,112},{24,120},{32,0},{40,8},{48,16},{56,24},{64... | collective-permute-start | bytes 294920 | tf_op jit(solution)/shard_map/ppermute | solution.py:186
  20.8 1.3 collective-permute-start.5
  22.2 1.8 %collective-permute-done.7 = bf16[2,96,256]{2,1,0:T(8,128)(2,1)S(1)} collective-permute-done((bf16[2,96,256]{2,1,0:T(8,128)(2,1)S(1)}, bf16[2,96,256]{2,1,0:T(8,128)(2,1)S(1)}, u32[]{:S(2)}, u32[]{:S(2)}) %collective-permute-start.7) | collective-permute-done | bytes 98336 | tf_op jit(solution)/shard_map/ppermute | solution.py:186
  24.0 3.8 %collective-permute-done.6 = bf16[2,96,256]{2,1,0:T(8,128)(2,1)S(1)} collective-permute-done((bf16[2,96,256]{2,1,0:T(8,128)(2,1)S(1)}, bf16[2,96,256]{2,1,0:T(8,128)(2,1)S(1)}, u32[]{:S(2)}, u32[]{:S(2)}) %collective-permute-start.6) | collective-permute-done | bytes 98336 | tf_op jit(solution)/shard_map/ppermute | solution.py:186
  28.1 2.0 %collective-permute-start.9 = (bf16[4,2,96,256]{3,2,1,0:T(8,128)(2,1)S(1)}, bf16[4,2,96,256]{3,2,1,0:T(8,128)(2,1)S(1)}, u32[]{:S(2)}, u32[]{:S(2)}) collective-permute-start(bf16[4,2,96,256]{3,2,1,0:T(8,128)(2,1)S(1)} %pad_maximum_fusion.3.refs_1_), channel_id=1, source_target_pairs={{0,8},{8,16},{16,24},{24,0},{32,40},{40,48},{48,56},{56,32},{64,72... | collective-permute-start | bytes 1179656 | tf_op jit(solution)/shard_map/ppermute | solution.py:201
  30.1 3.2 %collective-permute-start.10 = (bf16[4,2,96,256]{3,2,1,0:T(8,128)(2,1)S(1)}, bf16[4,2,96,256]{3,2,1,0:T(8,128)(2,1)S(1)}, u32[]{:S(2)}, u32[]{:S(2)}) collective-permute-start(bf16[4,2,96,256]{3,2,1,0:T(8,128)(2,1)S(1)} %bitcast.34), channel_id=1, source_target_pairs={{0,96},{8,104},{16,112},{24,120},{32,0},{40,8},{48,16},{56,24},{64... | collective-permute-start | bytes 1179656 | tf_op jit(solution)/shard_map/ppermute | solution.py:200
  33.2 1.3 %collective-permute-start.11 = (bf16[4,2,96,256]{3,2,1,0:T(8,128)(2,1)S(1)}, bf16[4,2,96,256]{3,2,1,0:T(8,128)(2,1)S(1)}, u32[]{:S(2)}, u32[]{:S(2)}) collective-permute-start(bf16[4,2,96,256]{3,2,1,0:T(8,128)(2,1)S(1)} %pad_maximum_fusion.3.refs_1_), channel_id=1, source_target_pairs={{0,24},{8,0},{16,8},{24,16},{32,56},{40,32},{48,40},{56,48},{64,88... | collective-permute-start | bytes 1179656 | tf_op jit(solution)/shard_map/ppermute | solution.py:201
  35.3 5.6 %collective-permute-done.8.refs_2_ = bf16[4,2,96,256]{3,2,1,0:T(8,128)(2,1)S(1)} collective-permute-done((bf16[4,2,96,256]{3,2,1,0:T(8,128)(2,1)S(1)}, bf16[4,2,96,256]{3,2,1,0:T(8,128)(2,1)S(1)}, u32[]{:S(2)}, u32[]{:S(2)}) %collective-permute-start.8) | collective-permute-done | bytes 393248 | tf_op jit(solution)/shard_map/ppermute | solution.py:200
  40.9 1.6 %collective-permute-start.13 = (bf16[4,2,96,256]{3,2,1,0:T(8,128)(2,1)S(1)}, bf16[4,2,96,256]{3,2,1,0:T(8,128)(2,1)S(1)}, u32[]{:S(2)}, u32[]{:S(2)}) collective-permute-start(bf16[4,2,96,256]{3,2,1,0:T(8,128)(2,1)S(1)} %pad_maximum_fusion.3.refs_1_), channel_id=1, source_target_pairs={{0,16},{8,24},{16,0},{24,8},{32,48},{40,56},{48,32},{56,40},{64,80... | collective-permute-start | bytes 1179656 | tf_op jit(solution)/shard_map/ppermute | solution.py:201
  42.5 2.1 %collective-permute-done.10.refs_4_ = bf16[4,2,96,256]{3,2,1,0:T(8,128)(2,1)S(1)} collective-permute-done((bf16[4,2,96,256]{3,2,1,0:T(8,128)(2,1)S(1)}, bf16[4,2,96,256]{3,2,1,0:T(8,128)(2,1)S(1)}, u32[]{:S(2)}, u32[]{:S(2)}) %collective-permute-start.10) | collective-permute-done | bytes 393248 | tf_op jit(solution)/shard_map/ppermute | solution.py:200
  45.4 4.8 %collective-permute-done.13.refs_7_ = bf16[4,2,96,256]{3,2,1,0:T(8,128)(2,1)S(1)} collective-permute-done((bf16[4,2,96,256]{3,2,1,0:T(8,128)(2,1)S(1)}, bf16[4,2,96,256]{3,2,1,0:T(8,128)(2,1)S(1)}, u32[]{:S(2)}, u32[]{:S(2)}) %collective-permute-start.13) | collective-permute-done | bytes 393248 | tf_op jit(solution)/shard_map/ppermute | solution.py:201
  53.6 3.3 %project.1 = (bf16[16,288,128]{2,1,0:T(8,128)(2,1)}, f32[8,128]{1,0:T(8,128)}) custom-call(bf16[192,2048]{1,0:T(8,128)(2,1)S(1)} %fusion.2.normed_ref, bf16[4,2,96,256]{3,2,1,0:T(8,128)(2,1)S(1)} %bitcast.37, bf16[4,2,96,256]{3,2,1,0:T(8,128)(2,1)S(1)} %pad_maximum_fusion.3.refs_1_, bf16[4,2,96,256]{3,2,1,0:T(8,128)(2,1)S(1)} %collective-permute-done.8.refs_2_, ...), custom_call_target="tpu_custom_call" | custom-call | tf_op jit(solution)/shard_map/project/pallas_call | solution.py:205
  56.9 7.5 %all-to-all-start = ((bf16[16,288,128]{2,1,0:T(8,128)(2,1)}), bf16[16,288,128]{2,1,0:T(8,128)(2,1)S(1)}, u32[]{:S(2)}, u32[]{:S(2)}) async-start(bf16[16,288,128]{2,1,0:T(8,128)(2,1)} %get-tuple-element.20), calls=%async_computation | async-start | bytes 2359296 | tf_op jit(solution)/shard_map/all_to_all | solution.py:220
  64.5 1.9 %collective-permute-start.22 = (bf16[4,64,256]{2,1,0:T(8,128)(2,1)S(1)}, bf16[4,64,256]{2,1,0:T(8,128)(2,1)S(1)}, u32[]{:S(2)}, u32[]{:S(2)}) collective-permute-start(bf16[4,64,256]{2,1,0:T(8,128)(2,1)S(1)} %pad_maximum_fusion.4), channel_id=1, source_target_pairs={{0,32},{8,40},{16,48},{24,56},{32,64},{40,72},{48,80},{56,88},{64,... | collective-permute-start | bytes 393224 | tf_op jit(solution)/shard_map/ppermute | solution.py:186
  66.4 2.7 %collective-permute-start.23 = (bf16[4,64,256]{2,1,0:T(8,128)(2,1)S(1)}, bf16[4,64,256]{2,1,0:T(8,128)(2,1)S(1)}, u32[]{:S(2)}, u32[]{:S(2)}) collective-permute-start(bf16[4,64,256]{2,1,0:T(8,128)(2,1)S(1)} %pad_maximum_fusion.4), channel_id=1, source_target_pairs={{0,64},{8,72},{16,80},{24,88},{32,96},{40,104},{48,112},{56,120},{... | collective-permute-start | bytes 393224 | tf_op jit(solution)/shard_map/ppermute | solution.py:186
  69.1 1.5 %collective-permute-start.24 = (bf16[4,64,256]{2,1,0:T(8,128)(2,1)S(1)}, bf16[4,64,256]{2,1,0:T(8,128)(2,1)S(1)}, u32[]{:S(2)}, u32[]{:S(2)}) collective-permute-start(bf16[4,64,256]{2,1,0:T(8,128)(2,1)S(1)} %pad_maximum_fusion.4), channel_id=1, source_target_pairs={{0,96},{8,104},{16,112},{24,120},{32,0},{40,8},{48,16},{56,24},{64... | collective-permute-start | bytes 393224 | tf_op jit(solution)/shard_map/ppermute | solution.py:186
  70.6 14.0 %collective-permute-done.22 = bf16[4,64,256]{2,1,0:T(8,128)(2,1)S(1)} collective-permute-done((bf16[4,64,256]{2,1,0:T(8,128)(2,1)S(1)}, bf16[4,64,256]{2,1,0:T(8,128)(2,1)S(1)}, u32[]{:S(2)}, u32[]{:S(2)}) %collective-permute-start.22) | collective-permute-done | bytes 131104 | tf_op jit(solution)/shard_map/ppermute | solution.py:186
  84.5 2.3 %collective-permute-done.23 = bf16[4,64,256]{2,1,0:T(8,128)(2,1)S(1)} collective-permute-done((bf16[4,64,256]{2,1,0:T(8,128)(2,1)S(1)}, bf16[4,64,256]{2,1,0:T(8,128)(2,1)S(1)}, u32[]{:S(2)}, u32[]{:S(2)}) %collective-permute-start.23) | collective-permute-done | bytes 131104 | tf_op jit(solution)/shard_map/ppermute | solution.py:186
  86.9 1.6 %collective-permute-start.25 = (bf16[4,4,64,256]{3,2,1,0:T(8,128)(2,1)S(1)}, bf16[4,4,64,256]{3,2,1,0:T(8,128)(2,1)S(1)}, u32[]{:S(2)}, u32[]{:S(2)}) collective-permute-start(bf16[4,4,64,256]{3,2,1,0:T(8,128)(2,1)S(1)} %pad_maximum_fusion.2), channel_id=1, source_target_pairs={{0,2},{1,3},{2,4},{3,5},{4,6},{5,7},{6,0},{7,1},{8,10},{9,11},{10,... | collective-permute-start | bytes 1572872 | tf_op jit(solution)/shard_map/ppermute | solution.py:186
  88.4 2.7 %collective-permute-start.26 = (bf16[4,4,64,256]{3,2,1,0:T(8,128)(2,1)S(1)}, bf16[4,4,64,256]{3,2,1,0:T(8,128)(2,1)S(1)}, u32[]{:S(2)}, u32[]{:S(2)}) collective-permute-start(bf16[4,4,64,256]{3,2,1,0:T(8,128)(2,1)S(1)} %pad_maximum_fusion.2), channel_id=1, source_target_pairs={{0,4},{1,5},{2,6},{3,7},{4,0},{5,1},{6,2},{7,3},{8,12},{9,13},{10,... | collective-permute-start | bytes 1572872 | tf_op jit(solution)/shard_map/ppermute | solution.py:186
  91.2 1.4 %collective-permute-start.27 = (bf16[4,4,64,256]{3,2,1,0:T(8,128)(2,1)S(1)}, bf16[4,4,64,256]{3,2,1,0:T(8,128)(2,1)S(1)}, u32[]{:S(2)}, u32[]{:S(2)}) collective-permute-start(bf16[4,4,64,256]{3,2,1,0:T(8,128)(2,1)S(1)} %pad_maximum_fusion.2), channel_id=1, source_target_pairs={{0,6},{1,7},{2,0},{3,1},{4,2},{5,3},{6,4},{7,5},{8,14},{9,15},{10,... | collective-permute-start | bytes 1572872 | tf_op jit(solution)/shard_map/ppermute | solution.py:186
  92.7 12.3 %attend.1 = bf16[16,96,128]{2,1,0:T(8,128)(2,1)S(1)} custom-call(bf16[16,288,128]{2,1,0:T(8,128)(2,1)S(1)} %all-to-all-done.got_ref, f32[1,3072]{1,0:T(1,128)S(1)} %bitcast.38, f32[1,64]{1,0:T(1,128)S(1)} %dynamic-slice_bitcast_fusion.gain_ref), custom_call_target="tpu_custom_call" | custom-call | tf_op jit(solution)/shard_map/attend/pallas_call | solution.py:224
  105.0 8.2 %collective-permute-done.26 = bf16[4,4,64,256]{3,2,1,0:T(8,128)(2,1)S(1)} collective-permute-done((bf16[4,4,64,256]{3,2,1,0:T(8,128)(2,1)S(1)}, bf16[4,4,64,256]{3,2,1,0:T(8,128)(2,1)S(1)}, u32[]{:S(2)}, u32[]{:S(2)}) %collective-permute-start.26) | collective-permute-done | bytes 524320 | tf_op jit(solution)/shard_map/ppermute | solution.py:186
  113.6 15.9 %all_to_all.10.got_ref = bf16[16,96,128]{2,1,0:T(8,128)(2,1)S(1)} all-to-all(bf16[16,96,128]{2,1,0:T(8,128)(2,1)S(1)} %attend.1), channel_id=1, replica_groups=mesh['sp'=16,'dp'=8] {'sp'}, dimensions={0} | all-to-all | bytes 786432 | tf_op jit(solution)/shard_map/all_to_all | solution.py:244
  129.5 2.0 %output.1 = bf16[192,2048]{1,0:T(8,128)(2,1)} custom-call(bf16[16,96,128]{2,1,0:T(8,128)(2,1)S(1)} %all_to_all.10.got_ref, bf16[4,4,4,64,256]{4,3,2,1,0:T(8,128)(2,1)S(1)} %pad_maximum_fusion.own_ref, bf16[4,4,4,64,256]{4,3,2,1,0:T(8,128)(2,1)S(1)} %collective-permute-done.28.far_ref), custom_call_target="tpu_custom_call" | custom-call | tf_op jit(solution)/shard_map/output/pallas_call | solution.py:245
  (53 shorter events, 7.4 us)
Async XLA Ops:
  0.0 92.6 %copy-start = (f32[1024]{0:T(1024)S(1)}, f32[1024]{0:T(1024)}, u32[]{:S(2)}) copy-start(f32[1024]{0:T(1024)} %param.14) | copy-start | bytes 12292
  0.9 4.1 %collective-permute-start = (bf16[96,256]{1,0:T(8,128)(2,1)S(1)}, bf16[96,256]{1,0:T(8,128)(2,1)S(1)}, u32[]{:S(2)}, u32[]{:S(2)}) collective-permute-start(bf16[96,256]{1,0:T(8,128)(2,1)S(1)} %get-tuple-element.34), channel_id=1, source_target_pairs={{0,2},{1,3},{2,0},{3,1},{4,6},{5,7},{6,4},{7,5},{8,10},{9,11},{10,... | collective-permute-start | bytes 147464 | tf_op jit(solution)/shard_map/ppermute | solution.py:189
  5.8 45.4 %copy-start.3 = (f32[2048]{0:T(1024)S(1)}, f32[2048]{0:T(1024)}, u32[]{:S(2)}) copy-start(f32[2048]{0:T(1024)} %param.9) | copy-start | bytes 24580
  5.8 15.0 %collective-permute-start.3 = (bf16[256,256]{1,0:T(8,128)(2,1)S(1)}, bf16[256,256]{1,0:T(8,128)(2,1)S(1)}, u32[]{:S(2)}, u32[]{:S(2)}) collective-permute-start(bf16[256,256]{1,0:T(8,128)(2,1)S(1)} %get-tuple-element.32), channel_id=1, source_target_pairs={{0,24},{8,0},{16,8},{24,16},{32,56},{40,32},{48,40},{56,48},{64,88... | collective-permute-start | bytes 393224 | tf_op jit(solution)/shard_map/ppermute | solution.py:186
  9.0 13.0 %collective-permute-start.2 = (bf16[256,256]{1,0:T(8,128)(2,1)S(1)}, bf16[256,256]{1,0:T(8,128)(2,1)S(1)}, u32[]{:S(2)}, u32[]{:S(2)}) collective-permute-start(bf16[256,256]{1,0:T(8,128)(2,1)S(1)} %get-tuple-element.32), channel_id=1, source_target_pairs={{0,16},{8,24},{16,0},{24,8},{32,48},{40,56},{48,32},{56,40},{64,80... | collective-permute-start | bytes 393224 | tf_op jit(solution)/shard_map/ppermute | solution.py:186
  9.6 12.4 %collective-permute-start.1 = (bf16[256,256]{1,0:T(8,128)(2,1)S(1)}, bf16[256,256]{1,0:T(8,128)(2,1)S(1)}, u32[]{:S(2)}, u32[]{:S(2)}) collective-permute-start(bf16[256,256]{1,0:T(8,128)(2,1)S(1)} %get-tuple-element.32), channel_id=1, source_target_pairs={{0,8},{8,16},{16,24},{24,0},{32,40},{40,48},{48,56},{56,32},{64,72... | collective-permute-start | bytes 393224 | tf_op jit(solution)/shard_map/ppermute | solution.py:186
  10.6 6.1 %collective-permute-start.4 = (bf16[2,96,256]{2,1,0:T(8,128)(2,1)S(1)}, bf16[2,96,256]{2,1,0:T(8,128)(2,1)S(1)}, u32[]{:S(2)}, u32[]{:S(2)}) collective-permute-start(bf16[2,96,256]{2,1,0:T(8,128)(2,1)S(1)} %pad_maximum_fusion.6), channel_id=1, source_target_pairs={{0,4},{1,5},{2,6},{3,7},{4,0},{5,1},{6,2},{7,3},{8,12},{9,13},{10,... | collective-permute-start | bytes 294920 | tf_op jit(solution)/shard_map/ppermute | solution.py:190
  16.7 7.3 %collective-permute-start.7 = (bf16[2,96,256]{2,1,0:T(8,128)(2,1)S(1)}, bf16[2,96,256]{2,1,0:T(8,128)(2,1)S(1)}, u32[]{:S(2)}, u32[]{:S(2)}) collective-permute-start(bf16[2,96,256]{2,1,0:T(8,128)(2,1)S(1)} %collective-permute-done.4), channel_id=1, source_target_pairs={{0,96},{8,104},{16,112},{24,120},{32,0},{40,8},{48,16},{56,24},{64... | collective-permute-start | bytes 294920 | tf_op jit(solution)/shard_map/ppermute | solution.py:186
  20.8 7.0 %collective-permute-start.6 = (bf16[2,96,256]{2,1,0:T(8,128)(2,1)S(1)}, bf16[2,96,256]{2,1,0:T(8,128)(2,1)S(1)}, u32[]{:S(2)}, u32[]{:S(2)}) collective-permute-start(bf16[2,96,256]{2,1,0:T(8,128)(2,1)S(1)} %collective-permute-done.4), channel_id=1, source_target_pairs={{0,64},{8,72},{16,80},{24,88},{32,96},{40,104},{48,112},{56,120},{... | collective-permute-start | bytes 294920 | tf_op jit(solution)/shard_map/ppermute | solution.py:186
  20.8 7.2 %collective-permute-start.5 = (bf16[2,96,256]{2,1,0:T(8,128)(2,1)S(1)}, bf16[2,96,256]{2,1,0:T(8,128)(2,1)S(1)}, u32[]{:S(2)}, u32[]{:S(2)}) collective-permute-start(bf16[2,96,256]{2,1,0:T(8,128)(2,1)S(1)} %collective-permute-done.4), channel_id=1, source_target_pairs={{0,32},{8,40},{16,48},{24,56},{32,64},{40,72},{48,80},{56,88},{64,... | collective-permute-start | bytes 294920 | tf_op jit(solution)/shard_map/ppermute | solution.py:186
  28.0 12.9 %collective-permute-start.8 = (bf16[4,2,96,256]{3,2,1,0:T(8,128)(2,1)S(1)}, bf16[4,2,96,256]{3,2,1,0:T(8,128)(2,1)S(1)}, u32[]{:S(2)}, u32[]{:S(2)}) collective-permute-start(bf16[4,2,96,256]{3,2,1,0:T(8,128)(2,1)S(1)} %bitcast.33), channel_id=1, source_target_pairs={{0,32},{8,40},{16,48},{24,56},{32,64},{40,72},{48,80},{56,88},{64,... | collective-permute-start | bytes 1179656 | tf_op jit(solution)/shard_map/ppermute | solution.py:200
  28.1 14.4 %collective-permute-start.9 = (bf16[4,2,96,256]{3,2,1,0:T(8,128)(2,1)S(1)}, bf16[4,2,96,256]{3,2,1,0:T(8,128)(2,1)S(1)}, u32[]{:S(2)}, u32[]{:S(2)}) collective-permute-start(bf16[4,2,96,256]{3,2,1,0:T(8,128)(2,1)S(1)} %pad_maximum_fusion.3.refs_1_), channel_id=1, source_target_pairs={{0,8},{8,16},{16,24},{24,0},{32,40},{40,48},{48,56},{56,32},{64,72... | collective-permute-start | bytes 1179656 | tf_op jit(solution)/shard_map/ppermute | solution.py:201
  30.1 14.5 %collective-permute-start.10 = (bf16[4,2,96,256]{3,2,1,0:T(8,128)(2,1)S(1)}, bf16[4,2,96,256]{3,2,1,0:T(8,128)(2,1)S(1)}, u32[]{:S(2)}, u32[]{:S(2)}) collective-permute-start(bf16[4,2,96,256]{3,2,1,0:T(8,128)(2,1)S(1)} %bitcast.34), channel_id=1, source_target_pairs={{0,96},{8,104},{16,112},{24,120},{32,0},{40,8},{48,16},{56,24},{64... | collective-permute-start | bytes 1179656 | tf_op jit(solution)/shard_map/ppermute | solution.py:200
  33.2 11.4 %collective-permute-start.11 = (bf16[4,2,96,256]{3,2,1,0:T(8,128)(2,1)S(1)}, bf16[4,2,96,256]{3,2,1,0:T(8,128)(2,1)S(1)}, u32[]{:S(2)}, u32[]{:S(2)}) collective-permute-start(bf16[4,2,96,256]{3,2,1,0:T(8,128)(2,1)S(1)} %pad_maximum_fusion.3.refs_1_), channel_id=1, source_target_pairs={{0,24},{8,0},{16,8},{24,16},{32,56},{40,32},{48,40},{56,48},{64,88... | collective-permute-start | bytes 1179656 | tf_op jit(solution)/shard_map/ppermute | solution.py:201
  34.6 10.8 %collective-permute-start.12 = (bf16[4,2,96,256]{3,2,1,0:T(8,128)(2,1)S(1)}, bf16[4,2,96,256]{3,2,1,0:T(8,128)(2,1)S(1)}, u32[]{:S(2)}, u32[]{:S(2)}) collective-permute-start(bf16[4,2,96,256]{3,2,1,0:T(8,128)(2,1)S(1)} %bitcast.35), channel_id=1, source_target_pairs={{0,64},{8,72},{16,80},{24,88},{32,96},{40,104},{48,112},{56,120},{... | collective-permute-start | bytes 1179656 | tf_op jit(solution)/shard_map/ppermute | solution.py:200
  40.9 9.3 %collective-permute-start.13 = (bf16[4,2,96,256]{3,2,1,0:T(8,128)(2,1)S(1)}, bf16[4,2,96,256]{3,2,1,0:T(8,128)(2,1)S(1)}, u32[]{:S(2)}, u32[]{:S(2)}) collective-permute-start(bf16[4,2,96,256]{3,2,1,0:T(8,128)(2,1)S(1)} %pad_maximum_fusion.3.refs_1_), channel_id=1, source_target_pairs={{0,16},{8,24},{16,0},{24,8},{32,48},{40,56},{48,32},{56,40},{64,80... | collective-permute-start | bytes 1179656 | tf_op jit(solution)/shard_map/ppermute | solution.py:201
  42.5 7.7 %collective-permute-start.14 = (bf16[4,2,96,256]{3,2,1,0:T(8,128)(2,1)S(1)}, bf16[4,2,96,256]{3,2,1,0:T(8,128)(2,1)S(1)}, u32[]{:S(2)}, u32[]{:S(2)}) collective-permute-start(bf16[4,2,96,256]{3,2,1,0:T(8,128)(2,1)S(1)} %bitcast.36), channel_id=1, source_target_pairs={{0,1},{1,0},{2,3},{3,2},{4,5},{5,4},{6,7},{7,6},{8,9},{9,8},{10,11... | collective-permute-start | bytes 1179656 | tf_op jit(solution)/shard_map/ppermute | solution.py:204
  44.6 6.1 %collective-permute-start.15 = (bf16[4,2,96,256]{3,2,1,0:T(8,128)(2,1)S(1)}, bf16[4,2,96,256]{3,2,1,0:T(8,128)(2,1)S(1)}, u32[]{:S(2)}, u32[]{:S(2)}) collective-permute-start(bf16[4,2,96,256]{3,2,1,0:T(8,128)(2,1)S(1)} %pad_maximum_fusion.3.refs_1_), channel_id=1, source_target_pairs={{0,1},{1,0},{2,3},{3,2},{4,5},{5,4},{6,7},{7,6},{8,9},{9,8},{10,11... | collective-permute-start | bytes 1179656 | tf_op jit(solution)/shard_map/ppermute | solution.py:204
  44.6 6.2 %collective-permute-start.16 = (bf16[4,2,96,256]{3,2,1,0:T(8,128)(2,1)S(1)}, bf16[4,2,96,256]{3,2,1,0:T(8,128)(2,1)S(1)}, u32[]{:S(2)}, u32[]{:S(2)}) collective-permute-start(bf16[4,2,96,256]{3,2,1,0:T(8,128)(2,1)S(1)} %collective-permute-done.8.refs_2_), channel_id=1, source_target_pairs={{0,1},{1,0},{2,3},{3,2},{4,5},{5,4},{6,7},{7,6},{8,9},{9,8},{10,11... | collective-permute-start | bytes 1179656 | tf_op jit(solution)/shard_map/ppermute | solution.py:204
  45.3 6.2 %collective-permute-start.17 = (bf16[4,2,96,256]{3,2,1,0:T(8,128)(2,1)S(1)}, bf16[4,2,96,256]{3,2,1,0:T(8,128)(2,1)S(1)}, u32[]{:S(2)}, u32[]{:S(2)}) collective-permute-start(bf16[4,2,96,256]{3,2,1,0:T(8,128)(2,1)S(1)} %collective-permute-done.9.refs_3_), channel_id=1, source_target_pairs={{0,1},{1,0},{2,3},{3,2},{4,5},{5,4},{6,7},{7,6},{8,9},{9,8},{10,11... | collective-permute-start | bytes 1179656 | tf_op jit(solution)/shard_map/ppermute | solution.py:204
  50.2 1.7 %collective-permute-start.18 = (bf16[4,2,96,256]{3,2,1,0:T(8,128)(2,1)S(1)}, bf16[4,2,96,256]{3,2,1,0:T(8,128)(2,1)S(1)}, u32[]{:S(2)}, u32[]{:S(2)}) collective-permute-start(bf16[4,2,96,256]{3,2,1,0:T(8,128)(2,1)S(1)} %collective-permute-done.10.refs_4_), channel_id=1, source_target_pairs={{0,1},{1,0},{2,3},{3,2},{4,5},{5,4},{6,7},{7,6},{8,9},{9,8},{10,11... | collective-permute-start | bytes 1179656 | tf_op jit(solution)/shard_map/ppermute | solution.py:204
  50.2 2.3 %collective-permute-start.19 = (bf16[4,2,96,256]{3,2,1,0:T(8,128)(2,1)S(1)}, bf16[4,2,96,256]{3,2,1,0:T(8,128)(2,1)S(1)}, u32[]{:S(2)}, u32[]{:S(2)}) collective-permute-start(bf16[4,2,96,256]{3,2,1,0:T(8,128)(2,1)S(1)} %collective-permute-done.11.refs_5_), channel_id=1, source_target_pairs={{0,1},{1,0},{2,3},{3,2},{4,5},{5,4},{6,7},{7,6},{8,9},{9,8},{10,11... | collective-permute-start | bytes 1179656 | tf_op jit(solution)/shard_map/ppermute | solution.py:204
  50.7 2.3 %collective-permute-start.20 = (bf16[4,2,96,256]{3,2,1,0:T(8,128)(2,1)S(1)}, bf16[4,2,96,256]{3,2,1,0:T(8,128)(2,1)S(1)}, u32[]{:S(2)}, u32[]{:S(2)}) collective-permute-start(bf16[4,2,96,256]{3,2,1,0:T(8,128)(2,1)S(1)} %collective-permute-done.12.refs_6_), channel_id=1, source_target_pairs={{0,1},{1,0},{2,3},{3,2},{4,5},{5,4},{6,7},{7,6},{8,9},{9,8},{10,11... | collective-permute-start | bytes 1179656 | tf_op jit(solution)/shard_map/ppermute | solution.py:204
  50.8 2.8 %collective-permute-start.21 = (bf16[4,2,96,256]{3,2,1,0:T(8,128)(2,1)S(1)}, bf16[4,2,96,256]{3,2,1,0:T(8,128)(2,1)S(1)}, u32[]{:S(2)}, u32[]{:S(2)}) collective-permute-start(bf16[4,2,96,256]{3,2,1,0:T(8,128)(2,1)S(1)} %collective-permute-done.13.refs_7_), channel_id=1, source_target_pairs={{0,1},{1,0},{2,3},{3,2},{4,5},{5,4},{6,7},{7,6},{8,9},{9,8},{10,11... | collective-permute-start | bytes 1179656 | tf_op jit(solution)/shard_map/ppermute | solution.py:204
  56.9 35.7 %all-to-all-start = ((bf16[16,288,128]{2,1,0:T(8,128)(2,1)}), bf16[16,288,128]{2,1,0:T(8,128)(2,1)S(1)}, u32[]{:S(2)}, u32[]{:S(2)}) async-start(bf16[16,288,128]{2,1,0:T(8,128)(2,1)} %get-tuple-element.20), calls=%async_computation | async-start | bytes 2359296 | tf_op jit(solution)/shard_map/all_to_all | solution.py:220
  64.5 20.0 %collective-permute-start.22 = (bf16[4,64,256]{2,1,0:T(8,128)(2,1)S(1)}, bf16[4,64,256]{2,1,0:T(8,128)(2,1)S(1)}, u32[]{:S(2)}, u32[]{:S(2)}) collective-permute-start(bf16[4,64,256]{2,1,0:T(8,128)(2,1)S(1)} %pad_maximum_fusion.4), channel_id=1, source_target_pairs={{0,32},{8,40},{16,48},{24,56},{32,64},{40,72},{48,80},{56,88},{64,... | collective-permute-start | bytes 393224 | tf_op jit(solution)/shard_map/ppermute | solution.py:186
  66.4 20.4 %collective-permute-start.23 = (bf16[4,64,256]{2,1,0:T(8,128)(2,1)S(1)}, bf16[4,64,256]{2,1,0:T(8,128)(2,1)S(1)}, u32[]{:S(2)}, u32[]{:S(2)}) collective-permute-start(bf16[4,64,256]{2,1,0:T(8,128)(2,1)S(1)} %pad_maximum_fusion.4), channel_id=1, source_target_pairs={{0,64},{8,72},{16,80},{24,88},{32,96},{40,104},{48,112},{56,120},{... | collective-permute-start | bytes 393224 | tf_op jit(solution)/shard_map/ppermute | solution.py:186
  69.1 17.7 %collective-permute-start.24 = (bf16[4,64,256]{2,1,0:T(8,128)(2,1)S(1)}, bf16[4,64,256]{2,1,0:T(8,128)(2,1)S(1)}, u32[]{:S(2)}, u32[]{:S(2)}) collective-permute-start(bf16[4,64,256]{2,1,0:T(8,128)(2,1)S(1)} %pad_maximum_fusion.4), channel_id=1, source_target_pairs={{0,96},{8,104},{16,112},{24,120},{32,0},{40,8},{48,16},{56,24},{64... | collective-permute-start | bytes 393224 | tf_op jit(solution)/shard_map/ppermute | solution.py:186
  86.9 18.2 %collective-permute-start.25 = (bf16[4,4,64,256]{3,2,1,0:T(8,128)(2,1)S(1)}, bf16[4,4,64,256]{3,2,1,0:T(8,128)(2,1)S(1)}, u32[]{:S(2)}, u32[]{:S(2)}) collective-permute-start(bf16[4,4,64,256]{3,2,1,0:T(8,128)(2,1)S(1)} %pad_maximum_fusion.2), channel_id=1, source_target_pairs={{0,2},{1,3},{2,4},{3,5},{4,6},{5,7},{6,0},{7,1},{8,10},{9,11},{10,... | collective-permute-start | bytes 1572872 | tf_op jit(solution)/shard_map/ppermute | solution.py:186
  88.4 24.8 %collective-permute-start.26 = (bf16[4,4,64,256]{3,2,1,0:T(8,128)(2,1)S(1)}, bf16[4,4,64,256]{3,2,1,0:T(8,128)(2,1)S(1)}, u32[]{:S(2)}, u32[]{:S(2)}) collective-permute-start(bf16[4,4,64,256]{3,2,1,0:T(8,128)(2,1)S(1)} %pad_maximum_fusion.2), channel_id=1, source_target_pairs={{0,4},{1,5},{2,6},{3,7},{4,0},{5,1},{6,2},{7,3},{8,12},{9,13},{10,... | collective-permute-start | bytes 1572872 | tf_op jit(solution)/shard_map/ppermute | solution.py:186
  91.2 22.0 %collective-permute-start.27 = (bf16[4,4,64,256]{3,2,1,0:T(8,128)(2,1)S(1)}, bf16[4,4,64,256]{3,2,1,0:T(8,128)(2,1)S(1)}, u32[]{:S(2)}, u32[]{:S(2)}) collective-permute-start(bf16[4,4,64,256]{3,2,1,0:T(8,128)(2,1)S(1)} %pad_maximum_fusion.2), channel_id=1, source_target_pairs={{0,6},{1,7},{2,0},{3,1},{4,2},{5,3},{6,4},{7,5},{8,14},{9,15},{10,... | collective-permute-start | bytes 1572872 | tf_op jit(solution)/shard_map/ppermute | solution.py:186
  113.5 16.0 %collective-permute-start.28 = (bf16[4,4,4,64,256]{4,3,2,1,0:T(8,128)(2,1)S(1)}, bf16[4,4,4,64,256]{4,3,2,1,0:T(8,128)(2,1)S(1)}, u32[]{:S(2)}, u32[]{:S(2)}) collective-permute-start(bf16[4,4,4,64,256]{4,3,2,1,0:T(8,128)(2,1)S(1)} %pad_maximum_fusion.own_ref), channel_id=1, source_target_pairs={{0,1},{1,0},{2,3},{3,2},{4,5},{5,4},{6,7},{7,6},{8,9},{9,8},{10,11... | collective-permute-start | bytes 6291464 | tf_op jit(solution)/shard_map/ppermute | solution.py:243
  (2 other events, 80.8 us)

commit v6 on v5

--- a/solution.py
+++ b/solution.py
@@ -12,7 +12,6 @@
 LOG2E = math.log2(math.e)
 norm_eps = 1e-06
 SIDE = 4
-ARRIVAL = (0, 1, 3, 2)
 
 
 VMEM = pl.BlockSpec(memory_space=pltpu.VMEM)
@@ -46,9 +45,7 @@
 
 
 def project_kernel(normed_ref, *refs):
-    own_a, own_b, far_a, far_b = (
-        {k: refs[at + 2 * i] for i, k in enumerate(ARRIVAL)} for at in (0, 1, 2 * SIDE, 2 * SIDE + 1)
-    )
+    own_a, own_b, far_a, far_b = (refs[SIDE * i : SIDE * (i + 1)] for i in range(4))
     out_ref, done_ref, order_ref, sums_ref = refs[4 * SIDE :]
     bf = jnp.bfloat16
     x, c, z, y = place_of()
@@ -63,10 +60,14 @@
         parts = []
         for i in range(SIDE):
             for refs_a, refs_b in ((own_a, own_b), (far_a, far_b)):
-                if i < 2:
-                    several = [refs_a[kz][ky, i] for ky in range(SIDE)]
-                else:
-                    several = [refs_b[ky][kz, i - 2] for ky in range(SIDE)]
+                several = []
+                for ky in range(SIDE):
+                    if i == 0:
+                        several.append(refs_a[kz][ky, :96])
+                    elif i == 1:
+                        several += [refs_a[kz][ky, 96:], refs_b[ky][kz, :32]]
+                    else:
+                        several.append(refs_b[ky][kz, 96 * i - 160 : 96 * i - 64])
                 parts.append(jnp.concatenate(several, axis=0))
         weights = jnp.concatenate(parts, axis=1)
         total = lax.dot_general(
@@ -188,20 +189,19 @@
     piece = jnp.concatenate([w_query.T, w_key.T, w_value.T], axis=0)
     two = jnp.stack([piece, lax.ppermute(piece, "dp", pairs(2, 8))])
     four = lax.ppermute(two, "dp", pairs(4, 8))
-    together = jnp.concatenate([two.reshape(192, 256), w_out], axis=0)
+    together = jnp.concatenate([two[0], two[1, :64], w_out], axis=0)
+    together_b = jnp.concatenate([two[1, 64:], four.reshape(192, 256)], axis=0)
     first_a = spread(lambda k: along_zy(0, k), together, "sp")
     first_a = jnp.stack(first_a)
-    first_b = jnp.stack(spread(lambda k: along_zy(k, 0), four, "sp"))
-    rest_y = first_a[:, 192:]
-    first_a = first_a[:, :192].reshape(SIDE, 2, 96, 256)
+    first_b = jnp.stack(spread(lambda k: along_zy(k, 0), together_b, "sp"))
+    rest_y = first_a[:, 160:]
+    first_a = first_a[:, :160]
     first_a, first_b, rest_y = lax.optimization_barrier((first_a, first_b, rest_y))
-    own_a, own_b = {0: first_a}, {0: first_b}
-    for k in ARRIVAL[1:]:
-        own_a[k] = lax.ppermute(first_a, "sp", along_zy(k, 0))
-        own_b[k] = lax.ppermute(first_b, "sp", along_zy(0, k))
+    own_b = spread(lambda k: along_zy(0, k), first_b, "sp")
+    own_a = spread(lambda k: along_zy(k, 0), first_a, "sp")
     rest_z = spread(lambda k: along_zy(k, 0), rest_y, "sp")
-    own = [group[k] for k in ARRIVAL for group in (own_a, own_b)]
-    far = [lax.ppermute(block, "dp", pairs(1, 8)) for block in own]
+    far_a = [lax.ppermute(block, "dp", pairs(1, 8)) for block in own_a]
+    far_b = [lax.ppermute(block, "dp", pairs(1, 8)) for block in own_b]
     packed, done = pl.pallas_call(
         project_kernel,
         out_shape=(
@@ -213,7 +213,7 @@
         scratch_shapes=[pltpu.VMEM((rows, width), bf), pltpu.VMEM((sp_size, 96, rows), jnp.float32)],
         compiler_params=pltpu.CompilerParams(vmem_limit_bytes=30 * 2**20),
         name="project",
-    )(*near(normed, *own, *far))
+    )(*near(normed, *own_a, *own_b, *far_a, *far_b))
     _, rest_z = lax.optimization_barrier((done, rest_z))
     rest_x = spread(along_x, jnp.stack(rest_z), "dp")
 

time: 132 us -> 137 us (1.038)
  waiting for transfers between devices: 50.4 us -> 53.9 us
  local copies, waits for them, and re-layouts: 0.12 us -> 3.03 us
    ppermute x12 -> x18, waiting for transfers between devices: 30.2 us -> 48.1 us  [spread(): return [a] + [lax.ppermute(a, axis, perm_of(k)) for k in range(1, SIDE)]]
    ppermute x14 -> x8, waiting for transfers between devices: 14.5 us -> 2.31 us  [the longest x4 1.97 us: body(): far_b = [lax.ppermute(block, 'dp', pairs(1, 8)) for block in own_b]]
    ppermute x12 -> x18, starting transfers between devices: 21.9 us -> 33.3 us  [spread(): return [a] + [lax.ppermute(a, axis, perm_of(k)) for k in range(1, SIDE)]]
    ppermute x14 -> x8, starting transfers between devices: 10.5 us -> 1.4 us  [the longest x4 0.89 us: body(): far_b = [lax.ppermute(block, 'dp', pairs(1, 8)) for block in own_b]]
    all_to_all x1, starting transfers between devices: 7.53 us -> 4.53 us  [body(): got = lax.all_to_all(packed, 'sp', split_axis=0, concat_axis=0, tiled=True)]
    ppermute x1, waiting for transfers between devices: 2.49 us -> 0.33 us  [body(): two = jnp.stack([piece, lax.ppermute(piece, 'dp', pairs(2, 8))])]
    unnamed x8 -> x12, local copies, waits for them, and re-layouts: 0.02 us -> 2.17 us
  transfers between devices with their start and end apart: 30 -> 30, of which waited for: 15 -> 17; matrix products, arithmetic and copies ran while one was open for 1% -> 2% of each run, Pallas kernels for 9% -> 9%
where the time goes in v6:
time: 137 us
  waiting for transfers between devices  53.9 us (39%)
  starting transfers between devices  44 us (32%)
  Pallas kernels  17.7 us (13%)
  blocking collectives  15.9 us (12%)
  local copies, waits for them, and re-layouts  3.03 us (2%)
  other arithmetic  1.86 us (1%)
    ppermute x18, waiting for transfers between devices, spread(): return [a] + [lax.ppermute(a, axis, perm_of(k)) for k in range(1, SIDE)]  48.1 us
    ppermute x18, starting transfers between devices, spread(): return [a] + [lax.ppermute(a, axis, perm_of(k)) for k in range(1, SIDE)]  33.3 us
    all_to_all x1, blocking collectives, body(): lax.all_to_all(heads, 'sp', split_axis=0, concat_axis=0, tiled=True)  15.9 us
    pallas_call x1, Pallas kernels, body(): pl.pallas_call(functools.partial(attend_kernel, src=sp_size, rows=rows, b...  12.4 us
    all_to_all x1, starting transfers between devices, body(): got = lax.all_to_all(packed, 'sp', split_axis=0, concat_axis=0, tiled=True)  4.53 us
    pallas_call x1, Pallas kernels, body(): pl.pallas_call(project_kernel, out_shape=(pltpu.VMEM((sp_size, rows + row...  3.32 us
    ppermute x1, starting transfers between devices, body(): four = lax.ppermute(two, 'dp', pairs(4, 8))  3.1 us
    ppermute x1, waiting for transfers between devices, body(): four = lax.ppermute(two, 'dp', pairs(4, 8))  3.09 us
  transfers between devices with their start and end apart: 30, of which 17 were waited for; matrix products, arithmetic and copies ran while one was open for 2% of the time, Pallas kernels for 9%

profile of v6, /device:TPU:0, one launch (start us, length us, event | category | flops | bytes accessed | tf_op | source)
XLA Modules:
  0.0 136.5 jit_solution(4849878602617053742)
XLA Ops:
  0.9 1.6 %collective-permute-start = (bf16[96,256]{1,0:T(8,128)(2,1)S(1)}, bf16[96,256]{1,0:T(8,128)(2,1)S(1)}, u32[]{:S(2)}, u32[]{:S(2)}) collective-permute-start(bf16[96,256]{1,0:T(8,128)(2,1)S(1)} %get-tuple-element.34), channel_id=1, source_target_pairs={{0,2},{1,3},{2,0},{3,1},{4,6},{5,7},{6,4},{7,5},{8,10},{9,11},{10,... | collective-permute-start | bytes 147464 | tf_op jit(solution)/shard_map/ppermute | solution.py:190
  5.8 3.1 %collective-permute-start.3 = (bf16[224,256]{1,0:T(8,128)(2,1)S(1)}, bf16[224,256]{1,0:T(8,128)(2,1)S(1)}, u32[]{:S(2)}, u32[]{:S(2)}) collective-permute-start(bf16[224,256]{1,0:T(8,128)(2,1)S(1)} %constant_dynamic-update-slice_fusion), channel_id=1, source_target_pairs={{0,24},{8,0},{16,8},{24,16},{32,56},{40,32},{48,40},{56,48},{64,88... | collective-permute-start | bytes 344072 | tf_op jit(solution)/shard_map/ppermute | solution.py:187
  9.5 1.0 collective-permute-start.1
  10.5 3.1 %collective-permute-start.4 = (bf16[2,96,256]{2,1,0:T(8,128)(2,1)S(1)}, bf16[2,96,256]{2,1,0:T(8,128)(2,1)S(1)}, u32[]{:S(2)}, u32[]{:S(2)}) collective-permute-start(bf16[2,96,256]{2,1,0:T(8,128)(2,1)S(1)} %pad_maximum_fusion.6), channel_id=1, source_target_pairs={{0,4},{1,5},{2,6},{3,7},{4,0},{5,1},{6,2},{7,3},{8,12},{9,13},{10,... | collective-permute-start | bytes 294920 | tf_op jit(solution)/shard_map/ppermute | solution.py:191
  13.6 3.1 %collective-permute-done.4 = bf16[2,96,256]{2,1,0:T(8,128)(2,1)S(1)} collective-permute-done((bf16[2,96,256]{2,1,0:T(8,128)(2,1)S(1)}, bf16[2,96,256]{2,1,0:T(8,128)(2,1)S(1)}, u32[]{:S(2)}, u32[]{:S(2)}) %collective-permute-start.4) | collective-permute-done | bytes 98336 | tf_op jit(solution)/shard_map/ppermute | solution.py:191
  16.7 4.1 %collective-permute-start.7 = (bf16[224,256]{1,0:T(8,128)(2,1)S(1)}, bf16[224,256]{1,0:T(8,128)(2,1)S(1)}, u32[]{:S(2)}, u32[]{:S(2)}) collective-permute-start(bf16[224,256]{1,0:T(8,128)(2,1)S(1)} %get-tuple-element.32), channel_id=1, source_target_pairs={{0,96},{8,104},{16,112},{24,120},{32,0},{40,8},{48,16},{56,24},{64... | collective-permute-start | bytes 344072 | tf_op jit(solution)/shard_map/ppermute | solution.py:187
  20.8 1.3 collective-permute-start.5
  22.2 2.2 %collective-permute-done.7 = bf16[224,256]{1,0:T(8,128)(2,1)S(1)} collective-permute-done((bf16[224,256]{1,0:T(8,128)(2,1)S(1)}, bf16[224,256]{1,0:T(8,128)(2,1)S(1)}, u32[]{:S(2)}, u32[]{:S(2)}) %collective-permute-start.7) | collective-permute-done | bytes 114720 | tf_op jit(solution)/shard_map/ppermute | solution.py:187
  24.4 2.8 %collective-permute-done.6 = bf16[224,256]{1,0:T(8,128)(2,1)S(1)} collective-permute-done((bf16[224,256]{1,0:T(8,128)(2,1)S(1)}, bf16[224,256]{1,0:T(8,128)(2,1)S(1)}, u32[]{:S(2)}, u32[]{:S(2)}) %collective-permute-start.6) | collective-permute-done | bytes 114720 | tf_op jit(solution)/shard_map/ppermute | solution.py:187
  28.3 3.6 %collective-permute-start.9 = (bf16[4,160,256]{2,1,0:T(8,128)(2,1)S(1)}, bf16[4,160,256]{2,1,0:T(8,128)(2,1)S(1)}, u32[]{:S(2)}, u32[]{:S(2)}) collective-permute-start(bf16[4,160,256]{2,1,0:T(8,128)(2,1)S(1)} %slice.17.refs_0_), channel_id=1, source_target_pairs={{0,64},{8,72},{16,80},{24,88},{32,96},{40,104},{48,112},{56,120},{... | collective-permute-start | bytes 983048 | tf_op jit(solution)/shard_map/ppermute | solution.py:187
  31.8 1.3 collective-permute-start.10
  33.2 1.9 %collective-permute-start.11 = (bf16[4,224,256]{2,1,0:T(8,128)(2,1)S(1)}, bf16[4,224,256]{2,1,0:T(8,128)(2,1)S(1)}, u32[]{:S(2)}, u32[]{:S(2)}) collective-permute-start(bf16[4,224,256]{2,1,0:T(8,128)(2,1)S(1)} %pad_maximum_fusion.3.refs_4_), channel_id=1, source_target_pairs={{0,8},{8,16},{16,24},{24,0},{32,40},{40,48},{48,56},{56,32},{64,72... | collective-permute-start | bytes 1376264 | tf_op jit(solution)/shard_map/ppermute | solution.py:187
  35.0 3.9 %collective-permute-done.8.refs_1_ = bf16[4,160,256]{2,1,0:T(8,128)(2,1)S(1)} collective-permute-done((bf16[4,160,256]{2,1,0:T(8,128)(2,1)S(1)}, bf16[4,160,256]{2,1,0:T(8,128)(2,1)S(1)}, u32[]{:S(2)}, u32[]{:S(2)}) %collective-permute-start.8) | collective-permute-done | bytes 327712 | tf_op jit(solution)/shard_map/ppermute | solution.py:187
  38.9 1.9 %collective-permute-start.12 = (bf16[4,224,256]{2,1,0:T(8,128)(2,1)S(1)}, bf16[4,224,256]{2,1,0:T(8,128)(2,1)S(1)}, u32[]{:S(2)}, u32[]{:S(2)}) collective-permute-start(bf16[4,224,256]{2,1,0:T(8,128)(2,1)S(1)} %pad_maximum_fusion.3.refs_4_), channel_id=1, source_target_pairs={{0,16},{8,24},{16,0},{24,8},{32,48},{40,56},{48,32},{56,40},{64,80... | collective-permute-start | bytes 1376264 | tf_op jit(solution)/shard_map/ppermute | solution.py:187
  40.9 1.6 %collective-permute-done.9.refs_2_ = bf16[4,160,256]{2,1,0:T(8,128)(2,1)S(1)} collective-permute-done((bf16[4,160,256]{2,1,0:T(8,128)(2,1)S(1)}, bf16[4,160,256]{2,1,0:T(8,128)(2,1)S(1)}, u32[]{:S(2)}, u32[]{:S(2)}) %collective-permute-start.9) | collective-permute-done | bytes 327712 | tf_op jit(solution)/shard_map/ppermute | solution.py:187
  42.4 2.2 %collective-permute-start.13 = (bf16[4,224,256]{2,1,0:T(8,128)(2,1)S(1)}, bf16[4,224,256]{2,1,0:T(8,128)(2,1)S(1)}, u32[]{:S(2)}, u32[]{:S(2)}) collective-permute-start(bf16[4,224,256]{2,1,0:T(8,128)(2,1)S(1)} %pad_maximum_fusion.3.refs_4_), channel_id=1, source_target_pairs={{0,24},{8,0},{16,8},{24,16},{32,56},{40,32},{48,40},{56,48},{64,88... | collective-permute-start | bytes 1376264 | tf_op jit(solution)/shard_map/ppermute | solution.py:187
  45.4 1.9 %collective-permute-done.11.refs_5_ = bf16[4,224,256]{2,1,0:T(8,128)(2,1)S(1)} collective-permute-done((bf16[4,224,256]{2,1,0:T(8,128)(2,1)S(1)}, bf16[4,224,256]{2,1,0:T(8,128)(2,1)S(1)}, u32[]{:S(2)}, u32[]{:S(2)}) %collective-permute-start.11) | collective-permute-done | bytes 458784 | tf_op jit(solution)/shard_map/ppermute | solution.py:187
  47.3 10.3 %collective-permute-done.12.refs_6_ = bf16[4,224,256]{2,1,0:T(8,128)(2,1)S(1)} collective-permute-done((bf16[4,224,256]{2,1,0:T(8,128)(2,1)S(1)}, bf16[4,224,256]{2,1,0:T(8,128)(2,1)S(1)}, u32[]{:S(2)}, u32[]{:S(2)}) %collective-permute-start.12) | collective-permute-done | bytes 458784 | tf_op jit(solution)/shard_map/ppermute | solution.py:187
  61.2 3.3 %project.1 = (bf16[16,288,128]{2,1,0:T(8,128)(2,1)}, f32[8,128]{1,0:T(8,128)}) custom-call(bf16[192,2048]{1,0:T(8,128)(2,1)S(1)} %fusion.2.normed_ref, bf16[4,160,256]{2,1,0:T(8,128)(2,1)S(1)} %slice.17.refs_0_, bf16[4,160,256]{2,1,0:T(8,128)(2,1)S(1)} %collective-permute-done.8.refs_1_, bf16[4,160,256]{2,1,0:T(8,128)(2,1)S(1)} %collective-permute-done.9.refs_2_, ...), custom_call_target="tpu_custom_call" | custom-call | tf_op jit(solution)/shard_map/project/pallas_call | solution.py:205
  64.5 4.5 %all-to-all-start = ((bf16[16,288,128]{2,1,0:T(8,128)(2,1)}), bf16[16,288,128]{2,1,0:T(8,128)(2,1)S(1)}, u32[]{:S(2)}, u32[]{:S(2)}) async-start(bf16[16,288,128]{2,1,0:T(8,128)(2,1)} %get-tuple-element.20), calls=%async_computation | async-start | bytes 2359296 | tf_op jit(solution)/shard_map/all_to_all | solution.py:220
  69.1 1.9 %collective-permute-start.22 = (bf16[4,64,256]{2,1,0:T(8,128)(2,1)S(1)}, bf16[4,64,256]{2,1,0:T(8,128)(2,1)S(1)}, u32[]{:S(2)}, u32[]{:S(2)}) collective-permute-start(bf16[4,64,256]{2,1,0:T(8,128)(2,1)S(1)} %pad_maximum_fusion.4), channel_id=1, source_target_pairs={{0,32},{8,40},{16,48},{24,56},{32,64},{40,72},{48,80},{56,88},{64,... | collective-permute-start | bytes 393224 | tf_op jit(solution)/shard_map/ppermute | solution.py:187
  71.0 2.7 %collective-permute-start.23 = (bf16[4,64,256]{2,1,0:T(8,128)(2,1)S(1)}, bf16[4,64,256]{2,1,0:T(8,128)(2,1)S(1)}, u32[]{:S(2)}, u32[]{:S(2)}) collective-permute-start(bf16[4,64,256]{2,1,0:T(8,128)(2,1)S(1)} %pad_maximum_fusion.4), channel_id=1, source_target_pairs={{0,64},{8,72},{16,80},{24,88},{32,96},{40,104},{48,112},{56,120},{... | collective-permute-start | bytes 393224 | tf_op jit(solution)/shard_map/ppermute | solution.py:187
  73.7 1.5 %collective-permute-start.24 = (bf16[4,64,256]{2,1,0:T(8,128)(2,1)S(1)}, bf16[4,64,256]{2,1,0:T(8,128)(2,1)S(1)}, u32[]{:S(2)}, u32[]{:S(2)}) collective-permute-start(bf16[4,64,256]{2,1,0:T(8,128)(2,1)S(1)} %pad_maximum_fusion.4), channel_id=1, source_target_pairs={{0,96},{8,104},{16,112},{24,120},{32,0},{40,8},{48,16},{56,24},{64... | collective-permute-start | bytes 393224 | tf_op jit(solution)/shard_map/ppermute | solution.py:187
  75.1 12.8 %collective-permute-done.22 = bf16[4,64,256]{2,1,0:T(8,128)(2,1)S(1)} collective-permute-done((bf16[4,64,256]{2,1,0:T(8,128)(2,1)S(1)}, bf16[4,64,256]{2,1,0:T(8,128)(2,1)S(1)}, u32[]{:S(2)}, u32[]{:S(2)}) %collective-permute-start.22) | collective-permute-done | bytes 131104 | tf_op jit(solution)/shard_map/ppermute | solution.py:187
  88.0 3.4 %collective-permute-done.23 = bf16[4,64,256]{2,1,0:T(8,128)(2,1)S(1)} collective-permute-done((bf16[4,64,256]{2,1,0:T(8,128)(2,1)S(1)}, bf16[4,64,256]{2,1,0:T(8,128)(2,1)S(1)}, u32[]{:S(2)}, u32[]{:S(2)}) %collective-permute-start.23) | collective-permute-done | bytes 131104 | tf_op jit(solution)/shard_map/ppermute | solution.py:187
  91.5 2.0 %collective-permute-start.25 = (bf16[4,4,64,256]{3,2,1,0:T(8,128)(2,1)S(1)}, bf16[4,4,64,256]{3,2,1,0:T(8,128)(2,1)S(1)}, u32[]{:S(2)}, u32[]{:S(2)}) collective-permute-start(bf16[4,4,64,256]{3,2,1,0:T(8,128)(2,1)S(1)} %pad_maximum_fusion.1), channel_id=1, source_target_pairs={{0,2},{1,3},{2,4},{3,5},{4,6},{5,7},{6,0},{7,1},{8,10},{9,11},{10,... | collective-permute-start | bytes 1572872 | tf_op jit(solution)/shard_map/ppermute | solution.py:187
  93.5 2.7 %collective-permute-start.26 = (bf16[4,4,64,256]{3,2,1,0:T(8,128)(2,1)S(1)}, bf16[4,4,64,256]{3,2,1,0:T(8,128)(2,1)S(1)}, u32[]{:S(2)}, u32[]{:S(2)}) collective-permute-start(bf16[4,4,64,256]{3,2,1,0:T(8,128)(2,1)S(1)} %pad_maximum_fusion.1), channel_id=1, source_target_pairs={{0,4},{1,5},{2,6},{3,7},{4,0},{5,1},{6,2},{7,3},{8,12},{9,13},{10,... | collective-permute-start | bytes 1572872 | tf_op jit(solution)/shard_map/ppermute | solution.py:187
  96.2 1.4 %collective-permute-start.27 = (bf16[4,4,64,256]{3,2,1,0:T(8,128)(2,1)S(1)}, bf16[4,4,64,256]{3,2,1,0:T(8,128)(2,1)S(1)}, u32[]{:S(2)}, u32[]{:S(2)}) collective-permute-start(bf16[4,4,64,256]{3,2,1,0:T(8,128)(2,1)S(1)} %pad_maximum_fusion.1), channel_id=1, source_target_pairs={{0,6},{1,7},{2,0},{3,1},{4,2},{5,3},{6,4},{7,5},{8,14},{9,15},{10,... | collective-permute-start | bytes 1572872 | tf_op jit(solution)/shard_map/ppermute | solution.py:187
  97.7 12.4 %attend.1 = bf16[16,96,128]{2,1,0:T(8,128)(2,1)S(1)} custom-call(bf16[16,288,128]{2,1,0:T(8,128)(2,1)S(1)} %all-to-all-done.got_ref, f32[1,3072]{1,0:T(1,128)S(1)} %bitcast.41, f32[1,64]{1,0:T(1,128)S(1)} %dynamic-slice_bitcast_fusion.gain_ref), custom_call_target="tpu_custom_call" | custom-call | tf_op jit(solution)/shard_map/attend/pallas_call | solution.py:224
  110.1 8.2 %collective-permute-done.26 = bf16[4,4,64,256]{3,2,1,0:T(8,128)(2,1)S(1)} collective-permute-done((bf16[4,4,64,256]{3,2,1,0:T(8,128)(2,1)S(1)}, bf16[4,4,64,256]{3,2,1,0:T(8,128)(2,1)S(1)}, u32[]{:S(2)}, u32[]{:S(2)}) %collective-permute-start.26) | collective-permute-done | bytes 524320 | tf_op jit(solution)/shard_map/ppermute | solution.py:187
  118.6 15.9 %all_to_all.10.got_ref = bf16[16,96,128]{2,1,0:T(8,128)(2,1)S(1)} all-to-all(bf16[16,96,128]{2,1,0:T(8,128)(2,1)S(1)} %attend.1), channel_id=1, replica_groups=mesh['sp'=16,'dp'=8] {'sp'}, dimensions={0} | all-to-all | bytes 786432 | tf_op jit(solution)/shard_map/all_to_all | solution.py:244
  134.5 2.0 %output.1 = bf16[192,2048]{1,0:T(8,128)(2,1)} custom-call(bf16[16,96,128]{2,1,0:T(8,128)(2,1)S(1)} %all_to_all.10.got_ref, bf16[4,4,4,64,256]{4,3,2,1,0:T(8,128)(2,1)S(1)} %pad_maximum_fusion.own_ref, bf16[4,4,4,64,256]{4,3,2,1,0:T(8,128)(2,1)S(1)} %collective-permute-done.28.far_ref), custom_call_target="tpu_custom_call" | custom-call | tf_op jit(solution)/shard_map/output/pallas_call | solution.py:245
  (59 shorter events, 10.8 us)
Async XLA Ops:
  0.0 97.6 %copy-start = (f32[1024]{0:T(1024)S(1)}, f32[1024]{0:T(1024)}, u32[]{:S(2)}) copy-start(f32[1024]{0:T(1024)} %param.14) | copy-start | bytes 12292
  0.0 45.2 %copy-start.2 = (bf16[1,192,2048]{2,1,0:T(8,128)(2,1)S(1)}, bf16[1,192,2048]{2,1,0:T(8,128)(2,1)}, u32[]{:S(2)}) copy-start(bf16[1,192,2048]{2,1,0:T(8,128)(2,1)} %param.8) | copy-start | bytes 2359300
  0.9 4.1 %collective-permute-start = (bf16[96,256]{1,0:T(8,128)(2,1)S(1)}, bf16[96,256]{1,0:T(8,128)(2,1)S(1)}, u32[]{:S(2)}, u32[]{:S(2)}) collective-permute-start(bf16[96,256]{1,0:T(8,128)(2,1)S(1)} %get-tuple-element.34), channel_id=1, source_target_pairs={{0,2},{1,3},{2,0},{3,1},{4,6},{5,7},{6,4},{7,5},{8,10},{9,11},{10,... | collective-permute-start | bytes 147464 | tf_op jit(solution)/shard_map/ppermute | solution.py:190
  5.8 15.1 %collective-permute-start.3 = (bf16[224,256]{1,0:T(8,128)(2,1)S(1)}, bf16[224,256]{1,0:T(8,128)(2,1)S(1)}, u32[]{:S(2)}, u32[]{:S(2)}) collective-permute-start(bf16[224,256]{1,0:T(8,128)(2,1)S(1)} %constant_dynamic-update-slice_fusion), channel_id=1, source_target_pairs={{0,24},{8,0},{16,8},{24,16},{32,56},{40,32},{48,40},{56,48},{64,88... | collective-permute-start | bytes 344072 | tf_op jit(solution)/shard_map/ppermute | solution.py:187
  8.9 13.2 %collective-permute-start.2 = (bf16[224,256]{1,0:T(8,128)(2,1)S(1)}, bf16[224,256]{1,0:T(8,128)(2,1)S(1)}, u32[]{:S(2)}, u32[]{:S(2)}) collective-permute-start(bf16[224,256]{1,0:T(8,128)(2,1)S(1)} %constant_dynamic-update-slice_fusion), channel_id=1, source_target_pairs={{0,16},{8,24},{16,0},{24,8},{32,48},{40,56},{48,32},{56,40},{64,80... | collective-permute-start | bytes 344072 | tf_op jit(solution)/shard_map/ppermute | solution.py:187
  9.5 12.6 %collective-permute-start.1 = (bf16[224,256]{1,0:T(8,128)(2,1)S(1)}, bf16[224,256]{1,0:T(8,128)(2,1)S(1)}, u32[]{:S(2)}, u32[]{:S(2)}) collective-permute-start(bf16[224,256]{1,0:T(8,128)(2,1)S(1)} %constant_dynamic-update-slice_fusion), channel_id=1, source_target_pairs={{0,8},{8,16},{16,24},{24,0},{32,40},{40,48},{48,56},{56,32},{64,72... | collective-permute-start | bytes 344072 | tf_op jit(solution)/shard_map/ppermute | solution.py:187
  10.5 6.2 %collective-permute-start.4 = (bf16[2,96,256]{2,1,0:T(8,128)(2,1)S(1)}, bf16[2,96,256]{2,1,0:T(8,128)(2,1)S(1)}, u32[]{:S(2)}, u32[]{:S(2)}) collective-permute-start(bf16[2,96,256]{2,1,0:T(8,128)(2,1)S(1)} %pad_maximum_fusion.6), channel_id=1, source_target_pairs={{0,4},{1,5},{2,6},{3,7},{4,0},{5,1},{6,2},{7,3},{8,12},{9,13},{10,... | collective-permute-start | bytes 294920 | tf_op jit(solution)/shard_map/ppermute | solution.py:191
  16.7 7.7 %collective-permute-start.7 = (bf16[224,256]{1,0:T(8,128)(2,1)S(1)}, bf16[224,256]{1,0:T(8,128)(2,1)S(1)}, u32[]{:S(2)}, u32[]{:S(2)}) collective-permute-start(bf16[224,256]{1,0:T(8,128)(2,1)S(1)} %get-tuple-element.32), channel_id=1, source_target_pairs={{0,96},{8,104},{16,112},{24,120},{32,0},{40,8},{48,16},{56,24},{64... | collective-permute-start | bytes 344072 | tf_op jit(solution)/shard_map/ppermute | solution.py:187
  20.8 6.4 %collective-permute-start.6 = (bf16[224,256]{1,0:T(8,128)(2,1)S(1)}, bf16[224,256]{1,0:T(8,128)(2,1)S(1)}, u32[]{:S(2)}, u32[]{:S(2)}) collective-permute-start(bf16[224,256]{1,0:T(8,128)(2,1)S(1)} %get-tuple-element.32), channel_id=1, source_target_pairs={{0,64},{8,72},{16,80},{24,88},{32,96},{40,104},{48,112},{56,120},{... | collective-permute-start | bytes 344072 | tf_op jit(solution)/shard_map/ppermute | solution.py:187
  20.8 7.3 %collective-permute-start.5 = (bf16[224,256]{1,0:T(8,128)(2,1)S(1)}, bf16[224,256]{1,0:T(8,128)(2,1)S(1)}, u32[]{:S(2)}, u32[]{:S(2)}) collective-permute-start(bf16[224,256]{1,0:T(8,128)(2,1)S(1)} %get-tuple-element.32), channel_id=1, source_target_pairs={{0,32},{8,40},{16,48},{24,56},{32,64},{40,72},{48,80},{56,88},{64,... | collective-permute-start | bytes 344072 | tf_op jit(solution)/shard_map/ppermute | solution.py:187
  28.2 10.7 %collective-permute-start.8 = (bf16[4,160,256]{2,1,0:T(8,128)(2,1)S(1)}, bf16[4,160,256]{2,1,0:T(8,128)(2,1)S(1)}, u32[]{:S(2)}, u32[]{:S(2)}) collective-permute-start(bf16[4,160,256]{2,1,0:T(8,128)(2,1)S(1)} %slice.17.refs_0_), channel_id=1, source_target_pairs={{0,32},{8,40},{16,48},{24,56},{32,64},{40,72},{48,80},{56,88},{64,... | collective-permute-start | bytes 983048 | tf_op jit(solution)/shard_map/ppermute | solution.py:187
  28.3 14.2 %collective-permute-start.9 = (bf16[4,160,256]{2,1,0:T(8,128)(2,1)S(1)}, bf16[4,160,256]{2,1,0:T(8,128)(2,1)S(1)}, u32[]{:S(2)}, u32[]{:S(2)}) collective-permute-start(bf16[4,160,256]{2,1,0:T(8,128)(2,1)S(1)} %slice.17.refs_0_), channel_id=1, source_target_pairs={{0,64},{8,72},{16,80},{24,88},{32,96},{40,104},{48,112},{56,120},{... | collective-permute-start | bytes 983048 | tf_op jit(solution)/shard_map/ppermute | solution.py:187
  31.8 12.8 %collective-permute-start.10 = (bf16[4,160,256]{2,1,0:T(8,128)(2,1)S(1)}, bf16[4,160,256]{2,1,0:T(8,128)(2,1)S(1)}, u32[]{:S(2)}, u32[]{:S(2)}) collective-permute-start(bf16[4,160,256]{2,1,0:T(8,128)(2,1)S(1)} %slice.17.refs_0_), channel_id=1, source_target_pairs={{0,96},{8,104},{16,112},{24,120},{32,0},{40,8},{48,16},{56,24},{64... | collective-permute-start | bytes 983048 | tf_op jit(solution)/shard_map/ppermute | solution.py:187
  33.2 11.5 %collective-permute-start.14 = (bf16[4,160,256]{2,1,0:T(8,128)(2,1)S(1)}, bf16[4,160,256]{2,1,0:T(8,128)(2,1)S(1)}, u32[]{:S(2)}, u32[]{:S(2)}) collective-permute-start(bf16[4,160,256]{2,1,0:T(8,128)(2,1)S(1)} %slice.17.refs_0_), channel_id=1, source_target_pairs={{0,1},{1,0},{2,3},{3,2},{4,5},{5,4},{6,7},{7,6},{8,9},{9,8},{10,11... | collective-permute-start | bytes 983048 | tf_op jit(solution)/shard_map/ppermute | solution.py:203
  33.2 14.1 %collective-permute-start.11 = (bf16[4,224,256]{2,1,0:T(8,128)(2,1)S(1)}, bf16[4,224,256]{2,1,0:T(8,128)(2,1)S(1)}, u32[]{:S(2)}, u32[]{:S(2)}) collective-permute-start(bf16[4,224,256]{2,1,0:T(8,128)(2,1)S(1)} %pad_maximum_fusion.3.refs_4_), channel_id=1, source_target_pairs={{0,8},{8,16},{16,24},{24,0},{32,40},{40,48},{48,56},{56,32},{64,72... | collective-permute-start | bytes 1376264 | tf_op jit(solution)/shard_map/ppermute | solution.py:187
  38.9 18.7 %collective-permute-start.12 = (bf16[4,224,256]{2,1,0:T(8,128)(2,1)S(1)}, bf16[4,224,256]{2,1,0:T(8,128)(2,1)S(1)}, u32[]{:S(2)}, u32[]{:S(2)}) collective-permute-start(bf16[4,224,256]{2,1,0:T(8,128)(2,1)S(1)} %pad_maximum_fusion.3.refs_4_), channel_id=1, source_target_pairs={{0,16},{8,24},{16,0},{24,8},{32,48},{40,56},{48,32},{56,40},{64,80... | collective-permute-start | bytes 1376264 | tf_op jit(solution)/shard_map/ppermute | solution.py:187
  42.4 15.3 %collective-permute-start.13 = (bf16[4,224,256]{2,1,0:T(8,128)(2,1)S(1)}, bf16[4,224,256]{2,1,0:T(8,128)(2,1)S(1)}, u32[]{:S(2)}, u32[]{:S(2)}) collective-permute-start(bf16[4,224,256]{2,1,0:T(8,128)(2,1)S(1)} %pad_maximum_fusion.3.refs_4_), channel_id=1, source_target_pairs={{0,24},{8,0},{16,8},{24,16},{32,56},{40,32},{48,40},{56,48},{64,88... | collective-permute-start | bytes 1376264 | tf_op jit(solution)/shard_map/ppermute | solution.py:187
  44.7 13.5 %collective-permute-start.18 = (bf16[4,224,256]{2,1,0:T(8,128)(2,1)S(1)}, bf16[4,224,256]{2,1,0:T(8,128)(2,1)S(1)}, u32[]{:S(2)}, u32[]{:S(2)}) collective-permute-start(bf16[4,224,256]{2,1,0:T(8,128)(2,1)S(1)} %pad_maximum_fusion.3.refs_4_), channel_id=1, source_target_pairs={{0,1},{1,0},{2,3},{3,2},{4,5},{5,4},{6,7},{7,6},{8,9},{9,8},{10,11... | collective-permute-start | bytes 1376264 | tf_op jit(solution)/shard_map/ppermute | solution.py:204
  44.7 13.6 %collective-permute-start.15 = (bf16[4,160,256]{2,1,0:T(8,128)(2,1)S(1)}, bf16[4,160,256]{2,1,0:T(8,128)(2,1)S(1)}, u32[]{:S(2)}, u32[]{:S(2)}) collective-permute-start(bf16[4,160,256]{2,1,0:T(8,128)(2,1)S(1)} %collective-permute-done.8.refs_1_), channel_id=1, source_target_pairs={{0,1},{1,0},{2,3},{3,2},{4,5},{5,4},{6,7},{7,6},{8,9},{9,8},{10,11... | collective-permute-start | bytes 983048 | tf_op jit(solution)/shard_map/ppermute | solution.py:203
  47.3 11.6 %collective-permute-start.16 = (bf16[4,160,256]{2,1,0:T(8,128)(2,1)S(1)}, bf16[4,160,256]{2,1,0:T(8,128)(2,1)S(1)}, u32[]{:S(2)}, u32[]{:S(2)}) collective-permute-start(bf16[4,160,256]{2,1,0:T(8,128)(2,1)S(1)} %collective-permute-done.9.refs_2_), channel_id=1, source_target_pairs={{0,1},{1,0},{2,3},{3,2},{4,5},{5,4},{6,7},{7,6},{8,9},{9,8},{10,11... | collective-permute-start | bytes 983048 | tf_op jit(solution)/shard_map/ppermute | solution.py:203
  57.6 1.6 %collective-permute-start.17 = (bf16[4,160,256]{2,1,0:T(8,128)(2,1)S(1)}, bf16[4,160,256]{2,1,0:T(8,128)(2,1)S(1)}, u32[]{:S(2)}, u32[]{:S(2)}) collective-permute-start(bf16[4,160,256]{2,1,0:T(8,128)(2,1)S(1)} %collective-permute-done.10.refs_3_), channel_id=1, source_target_pairs={{0,1},{1,0},{2,3},{3,2},{4,5},{5,4},{6,7},{7,6},{8,9},{9,8},{10,11... | collective-permute-start | bytes 983048 | tf_op jit(solution)/shard_map/ppermute | solution.py:203
  57.8 2.1 %collective-permute-start.19 = (bf16[4,224,256]{2,1,0:T(8,128)(2,1)S(1)}, bf16[4,224,256]{2,1,0:T(8,128)(2,1)S(1)}, u32[]{:S(2)}, u32[]{:S(2)}) collective-permute-start(bf16[4,224,256]{2,1,0:T(8,128)(2,1)S(1)} %collective-permute-done.11.refs_5_), channel_id=1, source_target_pairs={{0,1},{1,0},{2,3},{3,2},{4,5},{5,4},{6,7},{7,6},{8,9},{9,8},{10,11... | collective-permute-start | bytes 1376264 | tf_op jit(solution)/shard_map/ppermute | solution.py:204
  58.1 2.4 %collective-permute-start.20 = (bf16[4,224,256]{2,1,0:T(8,128)(2,1)S(1)}, bf16[4,224,256]{2,1,0:T(8,128)(2,1)S(1)}, u32[]{:S(2)}, u32[]{:S(2)}) collective-permute-start(bf16[4,224,256]{2,1,0:T(8,128)(2,1)S(1)} %collective-permute-done.12.refs_6_), channel_id=1, source_target_pairs={{0,1},{1,0},{2,3},{3,2},{4,5},{5,4},{6,7},{7,6},{8,9},{9,8},{10,11... | collective-permute-start | bytes 1376264 | tf_op jit(solution)/shard_map/ppermute | solution.py:204
  58.3 2.9 %collective-permute-start.21 = (bf16[4,224,256]{2,1,0:T(8,128)(2,1)S(1)}, bf16[4,224,256]{2,1,0:T(8,128)(2,1)S(1)}, u32[]{:S(2)}, u32[]{:S(2)}) collective-permute-start(bf16[4,224,256]{2,1,0:T(8,128)(2,1)S(1)} %collective-permute-done.13.refs_7_), channel_id=1, source_target_pairs={{0,1},{1,0},{2,3},{3,2},{4,5},{5,4},{6,7},{7,6},{8,9},{9,8},{10,11... | collective-permute-start | bytes 1376264 | tf_op jit(solution)/shard_map/ppermute | solution.py:204
  64.5 33.2 %all-to-all-start = ((bf16[16,288,128]{2,1,0:T(8,128)(2,1)}), bf16[16,288,128]{2,1,0:T(8,128)(2,1)S(1)}, u32[]{:S(2)}, u32[]{:S(2)}) async-start(bf16[16,288,128]{2,1,0:T(8,128)(2,1)} %get-tuple-element.20), calls=%async_computation | async-start | bytes 2359296 | tf_op jit(solution)/shard_map/all_to_all | solution.py:220
  69.1 18.9 %collective-permute-start.22 = (bf16[4,64,256]{2,1,0:T(8,128)(2,1)S(1)}, bf16[4,64,256]{2,1,0:T(8,128)(2,1)S(1)}, u32[]{:S(2)}, u32[]{:S(2)}) collective-permute-start(bf16[4,64,256]{2,1,0:T(8,128)(2,1)S(1)} %pad_maximum_fusion.4), channel_id=1, source_target_pairs={{0,32},{8,40},{16,48},{24,56},{32,64},{40,72},{48,80},{56,88},{64,... | collective-permute-start | bytes 393224 | tf_op jit(solution)/shard_map/ppermute | solution.py:187
  71.0 20.4 %collective-permute-start.23 = (bf16[4,64,256]{2,1,0:T(8,128)(2,1)S(1)}, bf16[4,64,256]{2,1,0:T(8,128)(2,1)S(1)}, u32[]{:S(2)}, u32[]{:S(2)}) collective-permute-start(bf16[4,64,256]{2,1,0:T(8,128)(2,1)S(1)} %pad_maximum_fusion.4), channel_id=1, source_target_pairs={{0,64},{8,72},{16,80},{24,88},{32,96},{40,104},{48,112},{56,120},{... | collective-permute-start | bytes 393224 | tf_op jit(solution)/shard_map/ppermute | solution.py:187
  73.7 17.7 %collective-permute-start.24 = (bf16[4,64,256]{2,1,0:T(8,128)(2,1)S(1)}, bf16[4,64,256]{2,1,0:T(8,128)(2,1)S(1)}, u32[]{:S(2)}, u32[]{:S(2)}) collective-permute-start(bf16[4,64,256]{2,1,0:T(8,128)(2,1)S(1)} %pad_maximum_fusion.4), channel_id=1, source_target_pairs={{0,96},{8,104},{16,112},{24,120},{32,0},{40,8},{48,16},{56,24},{64... | collective-permute-start | bytes 393224 | tf_op jit(solution)/shard_map/ppermute | solution.py:187
  91.5 18.6 %collective-permute-start.25 = (bf16[4,4,64,256]{3,2,1,0:T(8,128)(2,1)S(1)}, bf16[4,4,64,256]{3,2,1,0:T(8,128)(2,1)S(1)}, u32[]{:S(2)}, u32[]{:S(2)}) collective-permute-start(bf16[4,4,64,256]{3,2,1,0:T(8,128)(2,1)S(1)} %pad_maximum_fusion.1), channel_id=1, source_target_pairs={{0,2},{1,3},{2,4},{3,5},{4,6},{5,7},{6,0},{7,1},{8,10},{9,11},{10,... | collective-permute-start | bytes 1572872 | tf_op jit(solution)/shard_map/ppermute | solution.py:187
  93.5 24.8 %collective-permute-start.26 = (bf16[4,4,64,256]{3,2,1,0:T(8,128)(2,1)S(1)}, bf16[4,4,64,256]{3,2,1,0:T(8,128)(2,1)S(1)}, u32[]{:S(2)}, u32[]{:S(2)}) collective-permute-start(bf16[4,4,64,256]{3,2,1,0:T(8,128)(2,1)S(1)} %pad_maximum_fusion.1), channel_id=1, source_target_pairs={{0,4},{1,5},{2,6},{3,7},{4,0},{5,1},{6,2},{7,3},{8,12},{9,13},{10,... | collective-permute-start | bytes 1572872 | tf_op jit(solution)/shard_map/ppermute | solution.py:187
  96.2 22.0 %collective-permute-start.27 = (bf16[4,4,64,256]{3,2,1,0:T(8,128)(2,1)S(1)}, bf16[4,4,64,256]{3,2,1,0:T(8,128)(2,1)S(1)}, u32[]{:S(2)}, u32[]{:S(2)}) collective-permute-start(bf16[4,4,64,256]{3,2,1,0:T(8,128)(2,1)S(1)} %pad_maximum_fusion.1), channel_id=1, source_target_pairs={{0,6},{1,7},{2,0},{3,1},{4,2},{5,3},{6,4},{7,5},{8,14},{9,15},{10,... | collective-permute-start | bytes 1572872 | tf_op jit(solution)/shard_map/ppermute | solution.py:187
  118.5 16.0 %collective-permute-start.28 = (bf16[4,4,4,64,256]{4,3,2,1,0:T(8,128)(2,1)S(1)}, bf16[4,4,4,64,256]{4,3,2,1,0:T(8,128)(2,1)S(1)}, u32[]{:S(2)}, u32[]{:S(2)}) collective-permute-start(bf16[4,4,4,64,256]{4,3,2,1,0:T(8,128)(2,1)S(1)} %pad_maximum_fusion.own_ref), channel_id=1, source_target_pairs={{0,1},{1,0},{2,3},{3,2},{4,5},{5,4},{6,7},{7,6},{8,9},{9,8},{10,11... | collective-permute-start | bytes 6291464 | tf_op jit(solution)/shard_map/ppermute | solution.py:243
  (2 other events, 75.1 us)

commit v7 on v5

--- a/solution.py
+++ b/solution.py
@@ -12,7 +12,6 @@
 LOG2E = math.log2(math.e)
 norm_eps = 1e-06
 SIDE = 4
-ARRIVAL = (0, 1, 3, 2)
 
 
 VMEM = pl.BlockSpec(memory_space=pltpu.VMEM)
@@ -46,9 +45,7 @@
 
 
 def project_kernel(normed_ref, *refs):
-    own_a, own_b, far_a, far_b = (
-        {k: refs[at + 2 * i] for i, k in enumerate(ARRIVAL)} for at in (0, 1, 2 * SIDE, 2 * SIDE + 1)
-    )
+    own_a, own_b, far_a, far_b = (refs[SIDE * i : SIDE * (i + 1)] for i in range(4))
     out_ref, done_ref, order_ref, sums_ref = refs[4 * SIDE :]
     bf = jnp.bfloat16
     x, c, z, y = place_of()
@@ -101,30 +98,33 @@
     length = src * rows
     lane = lax.broadcasted_iota(jnp.int32, (rows, 128), 1)
     ones = jnp.where(lane < 3, 1.0, 0.0).astype(bf)
-    for b in range(src):
-        both = got_ref[b, :rows, :]
-        wide = both[:, :HEAD_DIM].astype(jnp.float32) * (LOG2E * HEAD_DIM ** -0.5)
-        high = wide.astype(bf)
-        low = (wide - high.astype(jnp.float32)).astype(bf)
-        qa_ref[b * rows : (b + 1) * rows, :128] = jnp.concatenate([high, low], axis=1)
-        qa_ref[b * rows : (b + 1) * rows, 128:] = ones
-        vv = got_ref[b, rows:, :]
-        v_ref[b * rows : b * rows + half, :] = vv[:, :HEAD_DIM]
-        v_ref[b * rows + half : (b + 1) * rows, :] = vv[:, HEAD_DIM:]
     step = 2 * rows
-    for b in range(src // 2):
-        pair = jnp.concatenate([got_ref[2 * b, :rows, :], got_ref[2 * b + 1, :rows, :]], axis=0)
+    row = lax.broadcasted_iota(jnp.int32, (128, step), 0)
+
+    def prepare(p):
+        for b in (2 * p, 2 * p + 1):
+            both = got_ref[b, :rows, :]
+            wide = both[:, :HEAD_DIM].astype(jnp.float32) * (LOG2E * HEAD_DIM ** -0.5)
+            high = wide.astype(bf)
+            low = (wide - high.astype(jnp.float32)).astype(bf)
+            qa_ref[b * rows : (b + 1) * rows, :128] = jnp.concatenate([high, low], axis=1)
+            qa_ref[b * rows : (b + 1) * rows, 128:] = ones
+            vv = got_ref[b, rows:, :]
+            v_ref[b * rows : b * rows + half, :] = vv[:, :HEAD_DIM]
+            v_ref[b * rows + half : (b + 1) * rows, :] = vv[:, HEAD_DIM:]
+        pair = jnp.concatenate([got_ref[2 * p, :rows, :], got_ref[2 * p + 1, :rows, :]], axis=0)
         kt = pair.astype(jnp.float32).T[HEAD_DIM:, :].astype(bf)
-        kt_ref[:HEAD_DIM, b * step : (b + 1) * step] = kt
-        kt_ref[HEAD_DIM : 2 * HEAD_DIM, b * step : (b + 1) * step] = kt
-    b2 = bias_ref[...] * LOG2E
-    b_high = b2.astype(bf).astype(jnp.float32)
-    b_mid = (b2 - b_high).astype(bf).astype(jnp.float32)
-    b_low = b2 - b_high - b_mid
-    row = lax.broadcasted_iota(jnp.int32, (128, length), 0)
-    tail = jnp.where(row == 0, b_high, jnp.where(row == 1, b_mid, jnp.where(row == 2, b_low, 0.0)))
-    kt_ref[2 * HEAD_DIM :, :] = tail.astype(bf)
-
+        at = slice(p * step, (p + 1) * step)
+        kt_ref[:HEAD_DIM, at] = kt
+        kt_ref[HEAD_DIM : 2 * HEAD_DIM, at] = kt
+        b2 = bias_ref[:, at] * LOG2E
+        b_high = b2.astype(bf).astype(jnp.float32)
+        b_mid = (b2 - b_high).astype(bf).astype(jnp.float32)
+        b_low = b2 - b_high - b_mid
+        tail = jnp.where(row == 0, b_high, jnp.where(row == 1, b_mid, jnp.where(row == 2, b_low, 0.0)))
+        kt_ref[2 * HEAD_DIM :, at] = tail.astype(bf)
+
+    ready = src // 2
     below = lax.broadcasted_iota(jnp.int32, (bk, bk), 0) > lax.broadcasted_iota(jnp.int32, (bk, bk), 1)
     mask_ref[...] = jnp.where(below, 1.0, 0.0)
     tri_ref[...] = jnp.where(below, 1.0, 0.0).astype(bf)
@@ -133,6 +133,9 @@
 
     for c in reversed(range(length // bk)):
         at = c * bk
+        while ready * step > at:
+            ready -= 1
+            prepare(ready)
         x = jnp.dot(qa_ref[at:, :], kt_ref[:, at : at + bk], preferred_element_type=jnp.float32)
         soft = jnp.maximum(x, jnp.log2(1.0 + jnp.exp2(jnp.minimum(x, 126.0))))
         own = x - soft
@@ -195,13 +198,11 @@
     rest_y = first_a[:, 192:]
     first_a = first_a[:, :192].reshape(SIDE, 2, 96, 256)
     first_a, first_b, rest_y = lax.optimization_barrier((first_a, first_b, rest_y))
-    own_a, own_b = {0: first_a}, {0: first_b}
-    for k in ARRIVAL[1:]:
-        own_a[k] = lax.ppermute(first_a, "sp", along_zy(k, 0))
-        own_b[k] = lax.ppermute(first_b, "sp", along_zy(0, k))
+    own_b = spread(lambda k: along_zy(0, k), first_b, "sp")
+    own_a = spread(lambda k: along_zy(k, 0), first_a, "sp")
     rest_z = spread(lambda k: along_zy(k, 0), rest_y, "sp")
-    own = [group[k] for k in ARRIVAL for group in (own_a, own_b)]
-    far = [lax.ppermute(block, "dp", pairs(1, 8)) for block in own]
+    far_a = [lax.ppermute(block, "dp", pairs(1, 8)) for block in own_a]
+    far_b = [lax.ppermute(block, "dp", pairs(1, 8)) for block in own_b]
     packed, done = pl.pallas_call(
         project_kernel,
         out_shape=(
@@ -213,7 +214,7 @@
         scratch_shapes=[pltpu.VMEM((rows, width), bf), pltpu.VMEM((sp_size, 96, rows), jnp.float32)],
         compiler_params=pltpu.CompilerParams(vmem_limit_bytes=30 * 2**20),
         name="project",
-    )(*near(normed, *own, *far))
+    )(*near(normed, *own_a, *own_b, *far_a, *far_b))
     _, rest_z = lax.optimization_barrier((done, rest_z))
     rest_x = spread(along_x, jnp.stack(rest_z), "dp")
 

time: 132 us -> 132 us (level)
  waiting for transfers between devices: 50.4 us -> 46.2 us
  starting transfers between devices: 44.7 us -> 48 us
    ppermute x14 -> x8, waiting for transfers between devices: 14.5 us -> 2.12 us  [the longest x4 1.69 us: body(): far_b = [lax.ppermute(block, 'dp', pairs(1, 8)) for block in own_b]]
    ppermute x12 -> x18, starting transfers between devices: 21.9 us -> 32.5 us  [spread(): return [a] + [lax.ppermute(a, axis, perm_of(k)) for k in range(1, SIDE)]]
    ppermute x14 -> x8, starting transfers between devices: 10.5 us -> 1.62 us  [the longest x4 1.53 us: body(): far_b = [lax.ppermute(block, 'dp', pairs(1, 8)) for block in own_b]]
    ppermute x12 -> x18, waiting for transfers between devices: 30.2 us -> 38.5 us  [spread(): return [a] + [lax.ppermute(a, axis, perm_of(k)) for k in range(1, SIDE)]]
    all_to_all x1, starting transfers between devices: 7.53 us -> 9.09 us  [body(): got = lax.all_to_all(packed, 'sp', split_axis=0, concat_axis=0, tiled=True)]
  transfers between devices with their start and end apart: 30 -> 30, of which waited for: 15 -> 16; matrix products, arithmetic and copies ran while one was open for 1% -> 1% of each run, Pallas kernels for 9% -> 10%
where the time goes in v7:
time: 132 us; the launch traced here: 131 us
  starting transfers between devices  48 us (36%)
  waiting for transfers between devices  46.2 us (35%)
  Pallas kernels  18.3 us (14%)
  blocking collectives  15.9 us (12%)
  other arithmetic  2.62 us (2%)
    ppermute x18, waiting for transfers between devices, spread(): return [a] + [lax.ppermute(a, axis, perm_of(k)) for k in range(1, SIDE)]  38.5 us
    ppermute x18, starting transfers between devices, spread(): return [a] + [lax.ppermute(a, axis, perm_of(k)) for k in range(1, SIDE)]  32.5 us
    all_to_all x1, blocking collectives, body(): lax.all_to_all(heads, 'sp', split_axis=0, concat_axis=0, tiled=True)  15.9 us
    pallas_call x1, Pallas kernels, body(): pl.pallas_call(functools.partial(attend_kernel, src=sp_size, rows=rows, b...  12.9 us
    all_to_all x1, starting transfers between devices, body(): got = lax.all_to_all(packed, 'sp', split_axis=0, concat_axis=0, tiled=True)  9.09 us
    pallas_call x1, Pallas kernels, body(): pl.pallas_call(project_kernel, out_shape=(pltpu.VMEM((sp_size, rows + row...  3.32 us
    ppermute x1, waiting for transfers between devices, body(): four = lax.ppermute(two, 'dp', pairs(4, 8))  3.1 us
    ppermute x1, starting transfers between devices, body(): four = lax.ppermute(two, 'dp', pairs(4, 8))  3.02 us
  transfers between devices with their start and end apart: 30, of which 16 were waited for; matrix products, arithmetic and copies ran while one was open for 1% of the time, Pallas kernels for 10%

profile of v7, /device:TPU:0, one launch (start us, length us, event | category | flops | bytes accessed | tf_op | source)
XLA Modules:
  0.0 131.2 jit_solution(14147088905243910958)
XLA Ops:
  0.0 0.9 fusion.3
  0.9 1.6 %collective-permute-start = (bf16[96,256]{1,0:T(8,128)(2,1)S(1)}, bf16[96,256]{1,0:T(8,128)(2,1)S(1)}, u32[]{:S(2)}, u32[]{:S(2)}) collective-permute-start(bf16[96,256]{1,0:T(8,128)(2,1)S(1)} %get-tuple-element.34), channel_id=1, source_target_pairs={{0,2},{1,3},{2,0},{3,1},{4,6},{5,7},{6,4},{7,5},{8,10},{9,11},{10,... | collective-permute-start | bytes 147464 | tf_op jit(solution)/shard_map/ppermute | solution.py:192
  2.5 2.5 %collective-permute-done = bf16[96,256]{1,0:T(8,128)(2,1)S(1)} collective-permute-done((bf16[96,256]{1,0:T(8,128)(2,1)S(1)}, bf16[96,256]{1,0:T(8,128)(2,1)S(1)}, u32[]{:S(2)}, u32[]{:S(2)}) %collective-permute-start) | collective-permute-done | bytes 49184 | tf_op jit(solution)/shard_map/ppermute | solution.py:192
  5.8 3.2 %collective-permute-start.3 = (bf16[256,256]{1,0:T(8,128)(2,1)S(1)}, bf16[256,256]{1,0:T(8,128)(2,1)S(1)}, u32[]{:S(2)}, u32[]{:S(2)}) collective-permute-start(bf16[256,256]{1,0:T(8,128)(2,1)S(1)} %get-tuple-element.32), channel_id=1, source_target_pairs={{0,24},{8,0},{16,8},{24,16},{32,56},{40,32},{48,40},{56,48},{64,88... | collective-permute-start | bytes 393224 | tf_op jit(solution)/shard_map/ppermute | solution.py:189
  9.6 1.0 collective-permute-start.1
  10.6 3.0 %collective-permute-start.4 = (bf16[2,96,256]{2,1,0:T(8,128)(2,1)S(1)}, bf16[2,96,256]{2,1,0:T(8,128)(2,1)S(1)}, u32[]{:S(2)}, u32[]{:S(2)}) collective-permute-start(bf16[2,96,256]{2,1,0:T(8,128)(2,1)S(1)} %pad_maximum_fusion.6), channel_id=1, source_target_pairs={{0,4},{1,5},{2,6},{3,7},{4,0},{5,1},{6,2},{7,3},{8,12},{9,13},{10,... | collective-permute-start | bytes 294920 | tf_op jit(solution)/shard_map/ppermute | solution.py:193
  13.6 3.1 %collective-permute-done.4 = bf16[2,96,256]{2,1,0:T(8,128)(2,1)S(1)} collective-permute-done((bf16[2,96,256]{2,1,0:T(8,128)(2,1)S(1)}, bf16[2,96,256]{2,1,0:T(8,128)(2,1)S(1)}, u32[]{:S(2)}, u32[]{:S(2)}) %collective-permute-start.4) | collective-permute-done | bytes 98336 | tf_op jit(solution)/shard_map/ppermute | solution.py:193
  16.7 4.0 %collective-permute-start.7 = (bf16[2,96,256]{2,1,0:T(8,128)(2,1)S(1)}, bf16[2,96,256]{2,1,0:T(8,128)(2,1)S(1)}, u32[]{:S(2)}, u32[]{:S(2)}) collective-permute-start(bf16[2,96,256]{2,1,0:T(8,128)(2,1)S(1)} %collective-permute-done.4), channel_id=1, source_target_pairs={{0,96},{8,104},{16,112},{24,120},{32,0},{40,8},{48,16},{56,24},{64... | collective-permute-start | bytes 294920 | tf_op jit(solution)/shard_map/ppermute | solution.py:189
  20.8 1.3 collective-permute-start.5
  22.2 1.8 %collective-permute-done.7 = bf16[2,96,256]{2,1,0:T(8,128)(2,1)S(1)} collective-permute-done((bf16[2,96,256]{2,1,0:T(8,128)(2,1)S(1)}, bf16[2,96,256]{2,1,0:T(8,128)(2,1)S(1)}, u32[]{:S(2)}, u32[]{:S(2)}) %collective-permute-start.7) | collective-permute-done | bytes 98336 | tf_op jit(solution)/shard_map/ppermute | solution.py:189
  24.0 3.8 %collective-permute-done.6 = bf16[2,96,256]{2,1,0:T(8,128)(2,1)S(1)} collective-permute-done((bf16[2,96,256]{2,1,0:T(8,128)(2,1)S(1)}, bf16[2,96,256]{2,1,0:T(8,128)(2,1)S(1)}, u32[]{:S(2)}, u32[]{:S(2)}) %collective-permute-start.6) | collective-permute-done | bytes 98336 | tf_op jit(solution)/shard_map/ppermute | solution.py:189
  28.1 3.9 %collective-permute-start.9 = (bf16[4,2,96,256]{3,2,1,0:T(8,128)(2,1)S(1)}, bf16[4,2,96,256]{3,2,1,0:T(8,128)(2,1)S(1)}, u32[]{:S(2)}, u32[]{:S(2)}) collective-permute-start(bf16[4,2,96,256]{3,2,1,0:T(8,128)(2,1)S(1)} %bitcast.34), channel_id=1, source_target_pairs={{0,64},{8,72},{16,80},{24,88},{32,96},{40,104},{48,112},{56,120},{... | collective-permute-start | bytes 1179656 | tf_op jit(solution)/shard_map/ppermute | solution.py:189
  32.7 1.9 %collective-permute-start.11 = (bf16[4,2,96,256]{3,2,1,0:T(8,128)(2,1)S(1)}, bf16[4,2,96,256]{3,2,1,0:T(8,128)(2,1)S(1)}, u32[]{:S(2)}, u32[]{:S(2)}) collective-permute-start(bf16[4,2,96,256]{3,2,1,0:T(8,128)(2,1)S(1)} %pad_maximum_fusion.3.refs_4_), channel_id=1, source_target_pairs={{0,8},{8,16},{16,24},{24,0},{32,40},{40,48},{48,56},{56,32},{64,72... | collective-permute-start | bytes 1179656 | tf_op jit(solution)/shard_map/ppermute | solution.py:189
  34.6 1.8 %collective-permute-start.12 = (bf16[4,2,96,256]{3,2,1,0:T(8,128)(2,1)S(1)}, bf16[4,2,96,256]{3,2,1,0:T(8,128)(2,1)S(1)}, u32[]{:S(2)}, u32[]{:S(2)}) collective-permute-start(bf16[4,2,96,256]{3,2,1,0:T(8,128)(2,1)S(1)} %pad_maximum_fusion.3.refs_4_), channel_id=1, source_target_pairs={{0,16},{8,24},{16,0},{24,8},{32,48},{40,56},{48,32},{56,40},{64,80... | collective-permute-start | bytes 1179656 | tf_op jit(solution)/shard_map/ppermute | solution.py:189
  36.4 4.1 %collective-permute-done.8.refs_1_ = bf16[4,2,96,256]{3,2,1,0:T(8,128)(2,1)S(1)} collective-permute-done((bf16[4,2,96,256]{3,2,1,0:T(8,128)(2,1)S(1)}, bf16[4,2,96,256]{3,2,1,0:T(8,128)(2,1)S(1)}, u32[]{:S(2)}, u32[]{:S(2)}) %collective-permute-start.8) | collective-permute-done | bytes 393248 | tf_op jit(solution)/shard_map/ppermute | solution.py:189
  40.6 2.3 %collective-permute-start.13 = (bf16[4,2,96,256]{3,2,1,0:T(8,128)(2,1)S(1)}, bf16[4,2,96,256]{3,2,1,0:T(8,128)(2,1)S(1)}, u32[]{:S(2)}, u32[]{:S(2)}) collective-permute-start(bf16[4,2,96,256]{3,2,1,0:T(8,128)(2,1)S(1)} %pad_maximum_fusion.3.refs_4_), channel_id=1, source_target_pairs={{0,24},{8,0},{16,8},{24,16},{32,56},{40,32},{48,40},{56,48},{64,88... | collective-permute-start | bytes 1179656 | tf_op jit(solution)/shard_map/ppermute | solution.py:189
  42.8 1.9 %collective-permute-done.9.refs_2_ = bf16[4,2,96,256]{3,2,1,0:T(8,128)(2,1)S(1)} collective-permute-done((bf16[4,2,96,256]{3,2,1,0:T(8,128)(2,1)S(1)}, bf16[4,2,96,256]{3,2,1,0:T(8,128)(2,1)S(1)}, u32[]{:S(2)}, u32[]{:S(2)}) %collective-permute-start.9) | collective-permute-done | bytes 393248 | tf_op jit(solution)/shard_map/ppermute | solution.py:189
  45.6 1.9 %collective-permute-done.12.refs_6_ = bf16[4,2,96,256]{3,2,1,0:T(8,128)(2,1)S(1)} collective-permute-done((bf16[4,2,96,256]{3,2,1,0:T(8,128)(2,1)S(1)}, bf16[4,2,96,256]{3,2,1,0:T(8,128)(2,1)S(1)}, u32[]{:S(2)}, u32[]{:S(2)}) %collective-permute-start.12) | collective-permute-done | bytes 393248 | tf_op jit(solution)/shard_map/ppermute | solution.py:189
  51.8 3.3 %project.1 = (bf16[16,288,128]{2,1,0:T(8,128)(2,1)}, f32[8,128]{1,0:T(8,128)}) custom-call(bf16[192,2048]{1,0:T(8,128)(2,1)S(1)} %fusion.2.normed_ref, bf16[4,2,96,256]{3,2,1,0:T(8,128)(2,1)S(1)} %bitcast.37, bf16[4,2,96,256]{3,2,1,0:T(8,128)(2,1)S(1)} %collective-permute-done.8.refs_1_, bf16[4,2,96,256]{3,2,1,0:T(8,128)(2,1)S(1)} %collective-permute-done.9.refs_2_, ...), custom_call_target="tpu_custom_call" | custom-call | tf_op jit(solution)/shard_map/project/pallas_call | solution.py:206
  55.1 9.1 %all-to-all-start = ((bf16[16,288,128]{2,1,0:T(8,128)(2,1)}), bf16[16,288,128]{2,1,0:T(8,128)(2,1)S(1)}, u32[]{:S(2)}, u32[]{:S(2)}) async-start(bf16[16,288,128]{2,1,0:T(8,128)(2,1)} %get-tuple-element.20), calls=%async_computation | async-start | bytes 2359296 | tf_op jit(solution)/shard_map/all_to_all | solution.py:221
  64.2 1.9 %collective-permute-start.22 = (bf16[4,64,256]{2,1,0:T(8,128)(2,1)S(1)}, bf16[4,64,256]{2,1,0:T(8,128)(2,1)S(1)}, u32[]{:S(2)}, u32[]{:S(2)}) collective-permute-start(bf16[4,64,256]{2,1,0:T(8,128)(2,1)S(1)} %pad_maximum_fusion.4), channel_id=1, source_target_pairs={{0,32},{8,40},{16,48},{24,56},{32,64},{40,72},{48,80},{56,88},{64,... | collective-permute-start | bytes 393224 | tf_op jit(solution)/shard_map/ppermute | solution.py:189
  66.1 2.7 %collective-permute-start.23 = (bf16[4,64,256]{2,1,0:T(8,128)(2,1)S(1)}, bf16[4,64,256]{2,1,0:T(8,128)(2,1)S(1)}, u32[]{:S(2)}, u32[]{:S(2)}) collective-permute-start(bf16[4,64,256]{2,1,0:T(8,128)(2,1)S(1)} %pad_maximum_fusion.4), channel_id=1, source_target_pairs={{0,64},{8,72},{16,80},{24,88},{32,96},{40,104},{48,112},{56,120},{... | collective-permute-start | bytes 393224 | tf_op jit(solution)/shard_map/ppermute | solution.py:189
  68.8 1.5 %collective-permute-start.24 = (bf16[4,64,256]{2,1,0:T(8,128)(2,1)S(1)}, bf16[4,64,256]{2,1,0:T(8,128)(2,1)S(1)}, u32[]{:S(2)}, u32[]{:S(2)}) collective-permute-start(bf16[4,64,256]{2,1,0:T(8,128)(2,1)S(1)} %pad_maximum_fusion.4), channel_id=1, source_target_pairs={{0,96},{8,104},{16,112},{24,120},{32,0},{40,8},{48,16},{56,24},{64... | collective-permute-start | bytes 393224 | tf_op jit(solution)/shard_map/ppermute | solution.py:189
  70.2 12.8 %collective-permute-done.22 = bf16[4,64,256]{2,1,0:T(8,128)(2,1)S(1)} collective-permute-done((bf16[4,64,256]{2,1,0:T(8,128)(2,1)S(1)}, bf16[4,64,256]{2,1,0:T(8,128)(2,1)S(1)}, u32[]{:S(2)}, u32[]{:S(2)}) %collective-permute-start.22) | collective-permute-done | bytes 131104 | tf_op jit(solution)/shard_map/ppermute | solution.py:189
  83.1 3.4 %collective-permute-done.23 = bf16[4,64,256]{2,1,0:T(8,128)(2,1)S(1)} collective-permute-done((bf16[4,64,256]{2,1,0:T(8,128)(2,1)S(1)}, bf16[4,64,256]{2,1,0:T(8,128)(2,1)S(1)}, u32[]{:S(2)}, u32[]{:S(2)}) %collective-permute-start.23) | collective-permute-done | bytes 131104 | tf_op jit(solution)/shard_map/ppermute | solution.py:189
  86.6 1.6 %collective-permute-start.25 = (bf16[4,4,64,256]{3,2,1,0:T(8,128)(2,1)S(1)}, bf16[4,4,64,256]{3,2,1,0:T(8,128)(2,1)S(1)}, u32[]{:S(2)}, u32[]{:S(2)}) collective-permute-start(bf16[4,4,64,256]{3,2,1,0:T(8,128)(2,1)S(1)} %pad_maximum_fusion.2), channel_id=1, source_target_pairs={{0,2},{1,3},{2,4},{3,5},{4,6},{5,7},{6,0},{7,1},{8,10},{9,11},{10,... | collective-permute-start | bytes 1572872 | tf_op jit(solution)/shard_map/ppermute | solution.py:189
  88.1 2.7 %collective-permute-start.26 = (bf16[4,4,64,256]{3,2,1,0:T(8,128)(2,1)S(1)}, bf16[4,4,64,256]{3,2,1,0:T(8,128)(2,1)S(1)}, u32[]{:S(2)}, u32[]{:S(2)}) collective-permute-start(bf16[4,4,64,256]{3,2,1,0:T(8,128)(2,1)S(1)} %pad_maximum_fusion.2), channel_id=1, source_target_pairs={{0,4},{1,5},{2,6},{3,7},{4,0},{5,1},{6,2},{7,3},{8,12},{9,13},{10,... | collective-permute-start | bytes 1572872 | tf_op jit(solution)/shard_map/ppermute | solution.py:189
  90.9 1.4 %collective-permute-start.27 = (bf16[4,4,64,256]{3,2,1,0:T(8,128)(2,1)S(1)}, bf16[4,4,64,256]{3,2,1,0:T(8,128)(2,1)S(1)}, u32[]{:S(2)}, u32[]{:S(2)}) collective-permute-start(bf16[4,4,64,256]{3,2,1,0:T(8,128)(2,1)S(1)} %pad_maximum_fusion.2), channel_id=1, source_target_pairs={{0,6},{1,7},{2,0},{3,1},{4,2},{5,3},{6,4},{7,5},{8,14},{9,15},{10,... | collective-permute-start | bytes 1572872 | tf_op jit(solution)/shard_map/ppermute | solution.py:189
  92.4 12.9 %attend.1 = bf16[16,96,128]{2,1,0:T(8,128)(2,1)S(1)} custom-call(bf16[16,288,128]{2,1,0:T(8,128)(2,1)S(1)} %all-to-all-done.got_ref, f32[1,3072]{1,0:T(1,128)S(1)} %bitcast.38, f32[1,64]{1,0:T(1,128)S(1)} %dynamic-slice_bitcast_fusion.gain_ref), custom_call_target="tpu_custom_call" | custom-call | tf_op jit(solution)/shard_map/attend/pallas_call | solution.py:225
  105.3 7.6 %collective-permute-done.26 = bf16[4,4,64,256]{3,2,1,0:T(8,128)(2,1)S(1)} collective-permute-done((bf16[4,4,64,256]{3,2,1,0:T(8,128)(2,1)S(1)}, bf16[4,4,64,256]{3,2,1,0:T(8,128)(2,1)S(1)}, u32[]{:S(2)}, u32[]{:S(2)}) %collective-permute-start.26) | collective-permute-done | bytes 524320 | tf_op jit(solution)/shard_map/ppermute | solution.py:189
  113.3 15.9 %all_to_all.10.got_ref = bf16[16,96,128]{2,1,0:T(8,128)(2,1)S(1)} all-to-all(bf16[16,96,128]{2,1,0:T(8,128)(2,1)S(1)} %attend.1), channel_id=1, replica_groups=mesh['sp'=16,'dp'=8] {'sp'}, dimensions={0} | all-to-all | bytes 786432 | tf_op jit(solution)/shard_map/all_to_all | solution.py:245
  129.2 2.0 %output.1 = bf16[192,2048]{1,0:T(8,128)(2,1)} custom-call(bf16[16,96,128]{2,1,0:T(8,128)(2,1)S(1)} %all_to_all.10.got_ref, bf16[4,4,4,64,256]{4,3,2,1,0:T(8,128)(2,1)S(1)} %pad_maximum_fusion.own_ref, bf16[4,4,4,64,256]{4,3,2,1,0:T(8,128)(2,1)S(1)} %collective-permute-done.28.far_ref), custom_call_target="tpu_custom_call" | custom-call | tf_op jit(solution)/shard_map/output/pallas_call | solution.py:246
  (53 shorter events, 8.1 us)
Async XLA Ops:
  0.0 92.3 %copy-start = (f32[1024]{0:T(1024)S(1)}, f32[1024]{0:T(1024)}, u32[]{:S(2)}) copy-start(f32[1024]{0:T(1024)} %param.14) | copy-start | bytes 12292
  0.0 45.4 %copy-start.2 = (bf16[1,192,2048]{2,1,0:T(8,128)(2,1)S(1)}, bf16[1,192,2048]{2,1,0:T(8,128)(2,1)}, u32[]{:S(2)}) copy-start(bf16[1,192,2048]{2,1,0:T(8,128)(2,1)} %param.8) | copy-start | bytes 2359300
  0.9 4.1 %collective-permute-start = (bf16[96,256]{1,0:T(8,128)(2,1)S(1)}, bf16[96,256]{1,0:T(8,128)(2,1)S(1)}, u32[]{:S(2)}, u32[]{:S(2)}) collective-permute-start(bf16[96,256]{1,0:T(8,128)(2,1)S(1)} %get-tuple-element.34), channel_id=1, source_target_pairs={{0,2},{1,3},{2,0},{3,1},{4,6},{5,7},{6,4},{7,5},{8,10},{9,11},{10,... | collective-permute-start | bytes 147464 | tf_op jit(solution)/shard_map/ppermute | solution.py:192
  5.8 15.0 %collective-permute-start.3 = (bf16[256,256]{1,0:T(8,128)(2,1)S(1)}, bf16[256,256]{1,0:T(8,128)(2,1)S(1)}, u32[]{:S(2)}, u32[]{:S(2)}) collective-permute-start(bf16[256,256]{1,0:T(8,128)(2,1)S(1)} %get-tuple-element.32), channel_id=1, source_target_pairs={{0,24},{8,0},{16,8},{24,16},{32,56},{40,32},{48,40},{56,48},{64,88... | collective-permute-start | bytes 393224 | tf_op jit(solution)/shard_map/ppermute | solution.py:189
  9.0 13.0 %collective-permute-start.2 = (bf16[256,256]{1,0:T(8,128)(2,1)S(1)}, bf16[256,256]{1,0:T(8,128)(2,1)S(1)}, u32[]{:S(2)}, u32[]{:S(2)}) collective-permute-start(bf16[256,256]{1,0:T(8,128)(2,1)S(1)} %get-tuple-element.32), channel_id=1, source_target_pairs={{0,16},{8,24},{16,0},{24,8},{32,48},{40,56},{48,32},{56,40},{64,80... | collective-permute-start | bytes 393224 | tf_op jit(solution)/shard_map/ppermute | solution.py:189
  9.6 12.4 %collective-permute-start.1 = (bf16[256,256]{1,0:T(8,128)(2,1)S(1)}, bf16[256,256]{1,0:T(8,128)(2,1)S(1)}, u32[]{:S(2)}, u32[]{:S(2)}) collective-permute-start(bf16[256,256]{1,0:T(8,128)(2,1)S(1)} %get-tuple-element.32), channel_id=1, source_target_pairs={{0,8},{8,16},{16,24},{24,0},{32,40},{40,48},{48,56},{56,32},{64,72... | collective-permute-start | bytes 393224 | tf_op jit(solution)/shard_map/ppermute | solution.py:189
  10.6 6.1 %collective-permute-start.4 = (bf16[2,96,256]{2,1,0:T(8,128)(2,1)S(1)}, bf16[2,96,256]{2,1,0:T(8,128)(2,1)S(1)}, u32[]{:S(2)}, u32[]{:S(2)}) collective-permute-start(bf16[2,96,256]{2,1,0:T(8,128)(2,1)S(1)} %pad_maximum_fusion.6), channel_id=1, source_target_pairs={{0,4},{1,5},{2,6},{3,7},{4,0},{5,1},{6,2},{7,3},{8,12},{9,13},{10,... | collective-permute-start | bytes 294920 | tf_op jit(solution)/shard_map/ppermute | solution.py:193
  16.7 7.3 %collective-permute-start.7 = (bf16[2,96,256]{2,1,0:T(8,128)(2,1)S(1)}, bf16[2,96,256]{2,1,0:T(8,128)(2,1)S(1)}, u32[]{:S(2)}, u32[]{:S(2)}) collective-permute-start(bf16[2,96,256]{2,1,0:T(8,128)(2,1)S(1)} %collective-permute-done.4), channel_id=1, source_target_pairs={{0,96},{8,104},{16,112},{24,120},{32,0},{40,8},{48,16},{56,24},{64... | collective-permute-start | bytes 294920 | tf_op jit(solution)/shard_map/ppermute | solution.py:189
  20.8 7.0 %collective-permute-start.6 = (bf16[2,96,256]{2,1,0:T(8,128)(2,1)S(1)}, bf16[2,96,256]{2,1,0:T(8,128)(2,1)S(1)}, u32[]{:S(2)}, u32[]{:S(2)}) collective-permute-start(bf16[2,96,256]{2,1,0:T(8,128)(2,1)S(1)} %collective-permute-done.4), channel_id=1, source_target_pairs={{0,64},{8,72},{16,80},{24,88},{32,96},{40,104},{48,112},{56,120},{... | collective-permute-start | bytes 294920 | tf_op jit(solution)/shard_map/ppermute | solution.py:189
  20.8 7.2 %collective-permute-start.5 = (bf16[2,96,256]{2,1,0:T(8,128)(2,1)S(1)}, bf16[2,96,256]{2,1,0:T(8,128)(2,1)S(1)}, u32[]{:S(2)}, u32[]{:S(2)}) collective-permute-start(bf16[2,96,256]{2,1,0:T(8,128)(2,1)S(1)} %collective-permute-done.4), channel_id=1, source_target_pairs={{0,32},{8,40},{16,48},{24,56},{32,64},{40,72},{48,80},{56,88},{64,... | collective-permute-start | bytes 294920 | tf_op jit(solution)/shard_map/ppermute | solution.py:189
  28.0 12.5 %collective-permute-start.8 = (bf16[4,2,96,256]{3,2,1,0:T(8,128)(2,1)S(1)}, bf16[4,2,96,256]{3,2,1,0:T(8,128)(2,1)S(1)}, u32[]{:S(2)}, u32[]{:S(2)}) collective-permute-start(bf16[4,2,96,256]{3,2,1,0:T(8,128)(2,1)S(1)} %bitcast.33), channel_id=1, source_target_pairs={{0,32},{8,40},{16,48},{24,56},{32,64},{40,72},{48,80},{56,88},{64,... | collective-permute-start | bytes 1179656 | tf_op jit(solution)/shard_map/ppermute | solution.py:189
  28.1 16.7 %collective-permute-start.9 = (bf16[4,2,96,256]{3,2,1,0:T(8,128)(2,1)S(1)}, bf16[4,2,96,256]{3,2,1,0:T(8,128)(2,1)S(1)}, u32[]{:S(2)}, u32[]{:S(2)}) collective-permute-start(bf16[4,2,96,256]{3,2,1,0:T(8,128)(2,1)S(1)} %bitcast.34), channel_id=1, source_target_pairs={{0,64},{8,72},{16,80},{24,88},{32,96},{40,104},{48,112},{56,120},{... | collective-permute-start | bytes 1179656 | tf_op jit(solution)/shard_map/ppermute | solution.py:189
  32.0 12.7 %collective-permute-start.10 = (bf16[4,2,96,256]{3,2,1,0:T(8,128)(2,1)S(1)}, bf16[4,2,96,256]{3,2,1,0:T(8,128)(2,1)S(1)}, u32[]{:S(2)}, u32[]{:S(2)}) collective-permute-start(bf16[4,2,96,256]{3,2,1,0:T(8,128)(2,1)S(1)} %bitcast.35), channel_id=1, source_target_pairs={{0,96},{8,104},{16,112},{24,120},{32,0},{40,8},{48,16},{56,24},{64... | collective-permute-start | bytes 1179656 | tf_op jit(solution)/shard_map/ppermute | solution.py:189
  32.7 12.6 %collective-permute-start.11 = (bf16[4,2,96,256]{3,2,1,0:T(8,128)(2,1)S(1)}, bf16[4,2,96,256]{3,2,1,0:T(8,128)(2,1)S(1)}, u32[]{:S(2)}, u32[]{:S(2)}) collective-permute-start(bf16[4,2,96,256]{3,2,1,0:T(8,128)(2,1)S(1)} %pad_maximum_fusion.3.refs_4_), channel_id=1, source_target_pairs={{0,8},{8,16},{16,24},{24,0},{32,40},{40,48},{48,56},{56,32},{64,72... | collective-permute-start | bytes 1179656 | tf_op jit(solution)/shard_map/ppermute | solution.py:189
  34.6 12.9 %collective-permute-start.12 = (bf16[4,2,96,256]{3,2,1,0:T(8,128)(2,1)S(1)}, bf16[4,2,96,256]{3,2,1,0:T(8,128)(2,1)S(1)}, u32[]{:S(2)}, u32[]{:S(2)}) collective-permute-start(bf16[4,2,96,256]{3,2,1,0:T(8,128)(2,1)S(1)} %pad_maximum_fusion.3.refs_4_), channel_id=1, source_target_pairs={{0,16},{8,24},{16,0},{24,8},{32,48},{40,56},{48,32},{56,40},{64,80... | collective-permute-start | bytes 1179656 | tf_op jit(solution)/shard_map/ppermute | solution.py:189
  40.6 7.8 %collective-permute-start.13 = (bf16[4,2,96,256]{3,2,1,0:T(8,128)(2,1)S(1)}, bf16[4,2,96,256]{3,2,1,0:T(8,128)(2,1)S(1)}, u32[]{:S(2)}, u32[]{:S(2)}) collective-permute-start(bf16[4,2,96,256]{3,2,1,0:T(8,128)(2,1)S(1)} %pad_maximum_fusion.3.refs_4_), channel_id=1, source_target_pairs={{0,24},{8,0},{16,8},{24,16},{32,56},{40,32},{48,40},{56,48},{64,88... | collective-permute-start | bytes 1179656 | tf_op jit(solution)/shard_map/ppermute | solution.py:189
  44.8 3.6 %collective-permute-start.14 = (bf16[4,2,96,256]{3,2,1,0:T(8,128)(2,1)S(1)}, bf16[4,2,96,256]{3,2,1,0:T(8,128)(2,1)S(1)}, u32[]{:S(2)}, u32[]{:S(2)}) collective-permute-start(bf16[4,2,96,256]{3,2,1,0:T(8,128)(2,1)S(1)} %bitcast.36), channel_id=1, source_target_pairs={{0,1},{1,0},{2,3},{3,2},{4,5},{5,4},{6,7},{7,6},{8,9},{9,8},{10,11... | collective-permute-start | bytes 1179656 | tf_op jit(solution)/shard_map/ppermute | solution.py:204
  44.8 4.1 %collective-permute-start.18 = (bf16[4,2,96,256]{3,2,1,0:T(8,128)(2,1)S(1)}, bf16[4,2,96,256]{3,2,1,0:T(8,128)(2,1)S(1)}, u32[]{:S(2)}, u32[]{:S(2)}) collective-permute-start(bf16[4,2,96,256]{3,2,1,0:T(8,128)(2,1)S(1)} %pad_maximum_fusion.3.refs_4_), channel_id=1, source_target_pairs={{0,1},{1,0},{2,3},{3,2},{4,5},{5,4},{6,7},{7,6},{8,9},{9,8},{10,11... | collective-permute-start | bytes 1179656 | tf_op jit(solution)/shard_map/ppermute | solution.py:205
  45.3 3.7 %collective-permute-start.15 = (bf16[4,2,96,256]{3,2,1,0:T(8,128)(2,1)S(1)}, bf16[4,2,96,256]{3,2,1,0:T(8,128)(2,1)S(1)}, u32[]{:S(2)}, u32[]{:S(2)}) collective-permute-start(bf16[4,2,96,256]{3,2,1,0:T(8,128)(2,1)S(1)} %collective-permute-done.8.refs_1_), channel_id=1, source_target_pairs={{0,1},{1,0},{2,3},{3,2},{4,5},{5,4},{6,7},{7,6},{8,9},{9,8},{10,11... | collective-permute-start | bytes 1179656 | tf_op jit(solution)/shard_map/ppermute | solution.py:204
  47.6 2.1 %collective-permute-start.16 = (bf16[4,2,96,256]{3,2,1,0:T(8,128)(2,1)S(1)}, bf16[4,2,96,256]{3,2,1,0:T(8,128)(2,1)S(1)}, u32[]{:S(2)}, u32[]{:S(2)}) collective-permute-start(bf16[4,2,96,256]{3,2,1,0:T(8,128)(2,1)S(1)} %collective-permute-done.9.refs_2_), channel_id=1, source_target_pairs={{0,1},{1,0},{2,3},{3,2},{4,5},{5,4},{6,7},{7,6},{8,9},{9,8},{10,11... | collective-permute-start | bytes 1179656 | tf_op jit(solution)/shard_map/ppermute | solution.py:204
  48.4 1.7 %collective-permute-start.17 = (bf16[4,2,96,256]{3,2,1,0:T(8,128)(2,1)S(1)}, bf16[4,2,96,256]{3,2,1,0:T(8,128)(2,1)S(1)}, u32[]{:S(2)}, u32[]{:S(2)}) collective-permute-start(bf16[4,2,96,256]{3,2,1,0:T(8,128)(2,1)S(1)} %collective-permute-done.10.refs_3_), channel_id=1, source_target_pairs={{0,1},{1,0},{2,3},{3,2},{4,5},{5,4},{6,7},{7,6},{8,9},{9,8},{10,11... | collective-permute-start | bytes 1179656 | tf_op jit(solution)/shard_map/ppermute | solution.py:204
  48.4 2.3 %collective-permute-start.19 = (bf16[4,2,96,256]{3,2,1,0:T(8,128)(2,1)S(1)}, bf16[4,2,96,256]{3,2,1,0:T(8,128)(2,1)S(1)}, u32[]{:S(2)}, u32[]{:S(2)}) collective-permute-start(bf16[4,2,96,256]{3,2,1,0:T(8,128)(2,1)S(1)} %collective-permute-done.11.refs_5_), channel_id=1, source_target_pairs={{0,1},{1,0},{2,3},{3,2},{4,5},{5,4},{6,7},{7,6},{8,9},{9,8},{10,11... | collective-permute-start | bytes 1179656 | tf_op jit(solution)/shard_map/ppermute | solution.py:205
  48.9 2.3 %collective-permute-start.20 = (bf16[4,2,96,256]{3,2,1,0:T(8,128)(2,1)S(1)}, bf16[4,2,96,256]{3,2,1,0:T(8,128)(2,1)S(1)}, u32[]{:S(2)}, u32[]{:S(2)}) collective-permute-start(bf16[4,2,96,256]{3,2,1,0:T(8,128)(2,1)S(1)} %collective-permute-done.12.refs_6_), channel_id=1, source_target_pairs={{0,1},{1,0},{2,3},{3,2},{4,5},{5,4},{6,7},{7,6},{8,9},{9,8},{10,11... | collective-permute-start | bytes 1179656 | tf_op jit(solution)/shard_map/ppermute | solution.py:205
  49.0 2.8 %collective-permute-start.21 = (bf16[4,2,96,256]{3,2,1,0:T(8,128)(2,1)S(1)}, bf16[4,2,96,256]{3,2,1,0:T(8,128)(2,1)S(1)}, u32[]{:S(2)}, u32[]{:S(2)}) collective-permute-start(bf16[4,2,96,256]{3,2,1,0:T(8,128)(2,1)S(1)} %collective-permute-done.13.refs_7_), channel_id=1, source_target_pairs={{0,1},{1,0},{2,3},{3,2},{4,5},{5,4},{6,7},{7,6},{8,9},{9,8},{10,11... | collective-permute-start | bytes 1179656 | tf_op jit(solution)/shard_map/ppermute | solution.py:205
  55.1 37.3 %all-to-all-start = ((bf16[16,288,128]{2,1,0:T(8,128)(2,1)}), bf16[16,288,128]{2,1,0:T(8,128)(2,1)S(1)}, u32[]{:S(2)}, u32[]{:S(2)}) async-start(bf16[16,288,128]{2,1,0:T(8,128)(2,1)} %get-tuple-element.20), calls=%async_computation | async-start | bytes 2359296 | tf_op jit(solution)/shard_map/all_to_all | solution.py:221
  64.2 18.9 %collective-permute-start.22 = (bf16[4,64,256]{2,1,0:T(8,128)(2,1)S(1)}, bf16[4,64,256]{2,1,0:T(8,128)(2,1)S(1)}, u32[]{:S(2)}, u32[]{:S(2)}) collective-permute-start(bf16[4,64,256]{2,1,0:T(8,128)(2,1)S(1)} %pad_maximum_fusion.4), channel_id=1, source_target_pairs={{0,32},{8,40},{16,48},{24,56},{32,64},{40,72},{48,80},{56,88},{64,... | collective-permute-start | bytes 393224 | tf_op jit(solution)/shard_map/ppermute | solution.py:189
  66.1 20.4 %collective-permute-start.23 = (bf16[4,64,256]{2,1,0:T(8,128)(2,1)S(1)}, bf16[4,64,256]{2,1,0:T(8,128)(2,1)S(1)}, u32[]{:S(2)}, u32[]{:S(2)}) collective-permute-start(bf16[4,64,256]{2,1,0:T(8,128)(2,1)S(1)} %pad_maximum_fusion.4), channel_id=1, source_target_pairs={{0,64},{8,72},{16,80},{24,88},{32,96},{40,104},{48,112},{56,120},{... | collective-permute-start | bytes 393224 | tf_op jit(solution)/shard_map/ppermute | solution.py:189
  68.8 17.7 %collective-permute-start.24 = (bf16[4,64,256]{2,1,0:T(8,128)(2,1)S(1)}, bf16[4,64,256]{2,1,0:T(8,128)(2,1)S(1)}, u32[]{:S(2)}, u32[]{:S(2)}) collective-permute-start(bf16[4,64,256]{2,1,0:T(8,128)(2,1)S(1)} %pad_maximum_fusion.4), channel_id=1, source_target_pairs={{0,96},{8,104},{16,112},{24,120},{32,0},{40,8},{48,16},{56,24},{64... | collective-permute-start | bytes 393224 | tf_op jit(solution)/shard_map/ppermute | solution.py:189
  86.6 18.7 %collective-permute-start.25 = (bf16[4,4,64,256]{3,2,1,0:T(8,128)(2,1)S(1)}, bf16[4,4,64,256]{3,2,1,0:T(8,128)(2,1)S(1)}, u32[]{:S(2)}, u32[]{:S(2)}) collective-permute-start(bf16[4,4,64,256]{3,2,1,0:T(8,128)(2,1)S(1)} %pad_maximum_fusion.2), channel_id=1, source_target_pairs={{0,2},{1,3},{2,4},{3,5},{4,6},{5,7},{6,0},{7,1},{8,10},{9,11},{10,... | collective-permute-start | bytes 1572872 | tf_op jit(solution)/shard_map/ppermute | solution.py:189
  88.1 24.8 %collective-permute-start.26 = (bf16[4,4,64,256]{3,2,1,0:T(8,128)(2,1)S(1)}, bf16[4,4,64,256]{3,2,1,0:T(8,128)(2,1)S(1)}, u32[]{:S(2)}, u32[]{:S(2)}) collective-permute-start(bf16[4,4,64,256]{3,2,1,0:T(8,128)(2,1)S(1)} %pad_maximum_fusion.2), channel_id=1, source_target_pairs={{0,4},{1,5},{2,6},{3,7},{4,0},{5,1},{6,2},{7,3},{8,12},{9,13},{10,... | collective-permute-start | bytes 1572872 | tf_op jit(solution)/shard_map/ppermute | solution.py:189
  90.9 22.0 %collective-permute-start.27 = (bf16[4,4,64,256]{3,2,1,0:T(8,128)(2,1)S(1)}, bf16[4,4,64,256]{3,2,1,0:T(8,128)(2,1)S(1)}, u32[]{:S(2)}, u32[]{:S(2)}) collective-permute-start(bf16[4,4,64,256]{3,2,1,0:T(8,128)(2,1)S(1)} %pad_maximum_fusion.2), channel_id=1, source_target_pairs={{0,6},{1,7},{2,0},{3,1},{4,2},{5,3},{6,4},{7,5},{8,14},{9,15},{10,... | collective-permute-start | bytes 1572872 | tf_op jit(solution)/shard_map/ppermute | solution.py:189
  113.2 16.0 %collective-permute-start.28 = (bf16[4,4,4,64,256]{4,3,2,1,0:T(8,128)(2,1)S(1)}, bf16[4,4,4,64,256]{4,3,2,1,0:T(8,128)(2,1)S(1)}, u32[]{:S(2)}, u32[]{:S(2)}) collective-permute-start(bf16[4,4,4,64,256]{4,3,2,1,0:T(8,128)(2,1)S(1)} %pad_maximum_fusion.own_ref), channel_id=1, source_target_pairs={{0,1},{1,0},{2,3},{3,2},{4,5},{5,4},{6,7},{7,6},{8,9},{9,8},{10,11... | collective-permute-start | bytes 6291464 | tf_op jit(solution)/shard_map/ppermute | solution.py:244
  (2 other events, 80.9 us)

commit v8 on v5

--- a/solution.py
+++ b/solution.py
@@ -12,7 +12,6 @@
 LOG2E = math.log2(math.e)
 norm_eps = 1e-06
 SIDE = 4
-ARRIVAL = (0, 1, 3, 2)
 
 
 VMEM = pl.BlockSpec(memory_space=pltpu.VMEM)
@@ -46,9 +45,7 @@
 
 
 def project_kernel(normed_ref, *refs):
-    own_a, own_b, far_a, far_b = (
-        {k: refs[at + 2 * i] for i, k in enumerate(ARRIVAL)} for at in (0, 1, 2 * SIDE, 2 * SIDE + 1)
-    )
+    own_a, own_b, far_a, far_b = (refs[SIDE * i : SIDE * (i + 1)] for i in range(4))
     out_ref, done_ref, order_ref, sums_ref = refs[4 * SIDE :]
     bf = jnp.bfloat16
     x, c, z, y = place_of()
@@ -195,13 +192,11 @@
     rest_y = first_a[:, 192:]
     first_a = first_a[:, :192].reshape(SIDE, 2, 96, 256)
     first_a, first_b, rest_y = lax.optimization_barrier((first_a, first_b, rest_y))
-    own_a, own_b = {0: first_a}, {0: first_b}
-    for k in ARRIVAL[1:]:
-        own_a[k] = lax.ppermute(first_a, "sp", along_zy(k, 0))
-        own_b[k] = lax.ppermute(first_b, "sp", along_zy(0, k))
+    own_b = spread(lambda k: along_zy(0, k), first_b, "sp")
+    own_a = spread(lambda k: along_zy(k, 0), first_a, "sp")
     rest_z = spread(lambda k: along_zy(k, 0), rest_y, "sp")
-    own = [group[k] for k in ARRIVAL for group in (own_a, own_b)]
-    far = [lax.ppermute(block, "dp", pairs(1, 8)) for block in own]
+    far_a = [lax.ppermute(block, "dp", pairs(1, 8)) for block in own_a]
+    far_b = [lax.ppermute(block, "dp", pairs(1, 8)) for block in own_b]
     packed, done = pl.pallas_call(
         project_kernel,
         out_shape=(
@@ -213,7 +208,7 @@
         scratch_shapes=[pltpu.VMEM((rows, width), bf), pltpu.VMEM((sp_size, 96, rows), jnp.float32)],
         compiler_params=pltpu.CompilerParams(vmem_limit_bytes=30 * 2**20),
         name="project",
-    )(*near(normed, *own, *far))
+    )(*near(normed, *own_a, *own_b, *far_a, *far_b))
     _, rest_z = lax.optimization_barrier((done, rest_z))
     rest_x = spread(along_x, jnp.stack(rest_z), "dp")
 

time: 132 us -> 132 us (level)
  waiting for transfers between devices: 50.4 us -> 46.8 us
  starting transfers between devices: 44.7 us -> 48 us
    ppermute x14 -> x8, waiting for transfers between devices: 14.5 us -> 2.12 us  [the longest x4 1.69 us: body(): far_b = [lax.ppermute(block, 'dp', pairs(1, 8)) for block in own_b]]
    ppermute x12 -> x18, starting transfers between devices: 21.9 us -> 32.5 us  [spread(): return [a] + [lax.ppermute(a, axis, perm_of(k)) for k in range(1, SIDE)]]
    ppermute x14 -> x8, starting transfers between devices: 10.5 us -> 1.62 us  [the longest x4 1.53 us: body(): far_b = [lax.ppermute(block, 'dp', pairs(1, 8)) for block in own_b]]
    ppermute x12 -> x18, waiting for transfers between devices: 30.2 us -> 39 us  [spread(): return [a] + [lax.ppermute(a, axis, perm_of(k)) for k in range(1, SIDE)]]
    all_to_all x1, starting transfers between devices: 7.53 us -> 9.09 us  [body(): got = lax.all_to_all(packed, 'sp', split_axis=0, concat_axis=0, tiled=True)]
  transfers between devices with their start and end apart: 30 -> 30, of which waited for: 15 -> 16; matrix products, arithmetic and copies ran while one was open for 1% -> 1% of each run, Pallas kernels for 9% -> 9%
where the time goes in v8:
time: 132 us; the launch traced here: 131 us
  starting transfers between devices  48 us (36%)
  waiting for transfers between devices  46.8 us (35%)
  Pallas kernels  17.7 us (13%)
  blocking collectives  15.9 us (12%)
  other arithmetic  2.62 us (2%)
    ppermute x18, waiting for transfers between devices, spread(): return [a] + [lax.ppermute(a, axis, perm_of(k)) for k in range(1, SIDE)]  39 us
    ppermute x18, starting transfers between devices, spread(): return [a] + [lax.ppermute(a, axis, perm_of(k)) for k in range(1, SIDE)]  32.5 us
    all_to_all x1, blocking collectives, body(): lax.all_to_all(heads, 'sp', split_axis=0, concat_axis=0, tiled=True)  15.9 us
    pallas_call x1, Pallas kernels, body(): pl.pallas_call(functools.partial(attend_kernel, src=sp_size, rows=rows, b...  12.3 us
    all_to_all x1, starting transfers between devices, body(): got = lax.all_to_all(packed, 'sp', split_axis=0, concat_axis=0, tiled=True)  9.09 us
    pallas_call x1, Pallas kernels, body(): pl.pallas_call(project_kernel, out_shape=(pltpu.VMEM((sp_size, rows + row...  3.32 us
    ppermute x1, waiting for transfers between devices, body(): four = lax.ppermute(two, 'dp', pairs(4, 8))  3.1 us
    ppermute x1, starting transfers between devices, body(): four = lax.ppermute(two, 'dp', pairs(4, 8))  3.02 us
  transfers between devices with their start and end apart: 30, of which 16 were waited for; matrix products, arithmetic and copies ran while one was open for 1% of the time, Pallas kernels for 9%

profile of v8, /device:TPU:0, one launch (start us, length us, event | category | flops | bytes accessed | tf_op | source)
XLA Modules:
  0.0 131.2 jit_solution(12904231981674931877)
XLA Ops:
  0.0 0.9 fusion.3
  0.9 1.6 %collective-permute-start = (bf16[96,256]{1,0:T(8,128)(2,1)S(1)}, bf16[96,256]{1,0:T(8,128)(2,1)S(1)}, u32[]{:S(2)}, u32[]{:S(2)}) collective-permute-start(bf16[96,256]{1,0:T(8,128)(2,1)S(1)} %get-tuple-element.34), channel_id=1, source_target_pairs={{0,2},{1,3},{2,0},{3,1},{4,6},{5,7},{6,4},{7,5},{8,10},{9,11},{10,... | collective-permute-start | bytes 147464 | tf_op jit(solution)/shard_map/ppermute | solution.py:186
  2.5 2.5 %collective-permute-done = bf16[96,256]{1,0:T(8,128)(2,1)S(1)} collective-permute-done((bf16[96,256]{1,0:T(8,128)(2,1)S(1)}, bf16[96,256]{1,0:T(8,128)(2,1)S(1)}, u32[]{:S(2)}, u32[]{:S(2)}) %collective-permute-start) | collective-permute-done | bytes 49184 | tf_op jit(solution)/shard_map/ppermute | solution.py:186
  5.8 3.2 %collective-permute-start.3 = (bf16[256,256]{1,0:T(8,128)(2,1)S(1)}, bf16[256,256]{1,0:T(8,128)(2,1)S(1)}, u32[]{:S(2)}, u32[]{:S(2)}) collective-permute-start(bf16[256,256]{1,0:T(8,128)(2,1)S(1)} %get-tuple-element.32), channel_id=1, source_target_pairs={{0,24},{8,0},{16,8},{24,16},{32,56},{40,32},{48,40},{56,48},{64,88... | collective-permute-start | bytes 393224 | tf_op jit(solution)/shard_map/ppermute | solution.py:183
  9.6 1.0 collective-permute-start.1
  10.6 3.0 %collective-permute-start.4 = (bf16[2,96,256]{2,1,0:T(8,128)(2,1)S(1)}, bf16[2,96,256]{2,1,0:T(8,128)(2,1)S(1)}, u32[]{:S(2)}, u32[]{:S(2)}) collective-permute-start(bf16[2,96,256]{2,1,0:T(8,128)(2,1)S(1)} %pad_maximum_fusion.6), channel_id=1, source_target_pairs={{0,4},{1,5},{2,6},{3,7},{4,0},{5,1},{6,2},{7,3},{8,12},{9,13},{10,... | collective-permute-start | bytes 294920 | tf_op jit(solution)/shard_map/ppermute | solution.py:187
  13.6 3.1 %collective-permute-done.4 = bf16[2,96,256]{2,1,0:T(8,128)(2,1)S(1)} collective-permute-done((bf16[2,96,256]{2,1,0:T(8,128)(2,1)S(1)}, bf16[2,96,256]{2,1,0:T(8,128)(2,1)S(1)}, u32[]{:S(2)}, u32[]{:S(2)}) %collective-permute-start.4) | collective-permute-done | bytes 98336 | tf_op jit(solution)/shard_map/ppermute | solution.py:187
  16.7 4.0 %collective-permute-start.7 = (bf16[2,96,256]{2,1,0:T(8,128)(2,1)S(1)}, bf16[2,96,256]{2,1,0:T(8,128)(2,1)S(1)}, u32[]{:S(2)}, u32[]{:S(2)}) collective-permute-start(bf16[2,96,256]{2,1,0:T(8,128)(2,1)S(1)} %collective-permute-done.4), channel_id=1, source_target_pairs={{0,96},{8,104},{16,112},{24,120},{32,0},{40,8},{48,16},{56,24},{64... | collective-permute-start | bytes 294920 | tf_op jit(solution)/shard_map/ppermute | solution.py:183
  20.8 1.3 collective-permute-start.5
  22.2 1.8 %collective-permute-done.7 = bf16[2,96,256]{2,1,0:T(8,128)(2,1)S(1)} collective-permute-done((bf16[2,96,256]{2,1,0:T(8,128)(2,1)S(1)}, bf16[2,96,256]{2,1,0:T(8,128)(2,1)S(1)}, u32[]{:S(2)}, u32[]{:S(2)}) %collective-permute-start.7) | collective-permute-done | bytes 98336 | tf_op jit(solution)/shard_map/ppermute | solution.py:183
  24.0 3.8 %collective-permute-done.6 = bf16[2,96,256]{2,1,0:T(8,128)(2,1)S(1)} collective-permute-done((bf16[2,96,256]{2,1,0:T(8,128)(2,1)S(1)}, bf16[2,96,256]{2,1,0:T(8,128)(2,1)S(1)}, u32[]{:S(2)}, u32[]{:S(2)}) %collective-permute-start.6) | collective-permute-done | bytes 98336 | tf_op jit(solution)/shard_map/ppermute | solution.py:183
  28.1 3.9 %collective-permute-start.9 = (bf16[4,2,96,256]{3,2,1,0:T(8,128)(2,1)S(1)}, bf16[4,2,96,256]{3,2,1,0:T(8,128)(2,1)S(1)}, u32[]{:S(2)}, u32[]{:S(2)}) collective-permute-start(bf16[4,2,96,256]{3,2,1,0:T(8,128)(2,1)S(1)} %bitcast.34), channel_id=1, source_target_pairs={{0,64},{8,72},{16,80},{24,88},{32,96},{40,104},{48,112},{56,120},{... | collective-permute-start | bytes 1179656 | tf_op jit(solution)/shard_map/ppermute | solution.py:183
  32.7 1.9 %collective-permute-start.11 = (bf16[4,2,96,256]{3,2,1,0:T(8,128)(2,1)S(1)}, bf16[4,2,96,256]{3,2,1,0:T(8,128)(2,1)S(1)}, u32[]{:S(2)}, u32[]{:S(2)}) collective-permute-start(bf16[4,2,96,256]{3,2,1,0:T(8,128)(2,1)S(1)} %pad_maximum_fusion.3.refs_4_), channel_id=1, source_target_pairs={{0,8},{8,16},{16,24},{24,0},{32,40},{40,48},{48,56},{56,32},{64,72... | collective-permute-start | bytes 1179656 | tf_op jit(solution)/shard_map/ppermute | solution.py:183
  34.6 1.8 %collective-permute-start.12 = (bf16[4,2,96,256]{3,2,1,0:T(8,128)(2,1)S(1)}, bf16[4,2,96,256]{3,2,1,0:T(8,128)(2,1)S(1)}, u32[]{:S(2)}, u32[]{:S(2)}) collective-permute-start(bf16[4,2,96,256]{3,2,1,0:T(8,128)(2,1)S(1)} %pad_maximum_fusion.3.refs_4_), channel_id=1, source_target_pairs={{0,16},{8,24},{16,0},{24,8},{32,48},{40,56},{48,32},{56,40},{64,80... | collective-permute-start | bytes 1179656 | tf_op jit(solution)/shard_map/ppermute | solution.py:183
  36.4 4.1 %collective-permute-done.8.refs_1_ = bf16[4,2,96,256]{3,2,1,0:T(8,128)(2,1)S(1)} collective-permute-done((bf16[4,2,96,256]{3,2,1,0:T(8,128)(2,1)S(1)}, bf16[4,2,96,256]{3,2,1,0:T(8,128)(2,1)S(1)}, u32[]{:S(2)}, u32[]{:S(2)}) %collective-permute-start.8) | collective-permute-done | bytes 393248 | tf_op jit(solution)/shard_map/ppermute | solution.py:183
  40.6 2.3 %collective-permute-start.13 = (bf16[4,2,96,256]{3,2,1,0:T(8,128)(2,1)S(1)}, bf16[4,2,96,256]{3,2,1,0:T(8,128)(2,1)S(1)}, u32[]{:S(2)}, u32[]{:S(2)}) collective-permute-start(bf16[4,2,96,256]{3,2,1,0:T(8,128)(2,1)S(1)} %pad_maximum_fusion.3.refs_4_), channel_id=1, source_target_pairs={{0,24},{8,0},{16,8},{24,16},{32,56},{40,32},{48,40},{56,48},{64,88... | collective-permute-start | bytes 1179656 | tf_op jit(solution)/shard_map/ppermute | solution.py:183
  42.8 1.9 %collective-permute-done.9.refs_2_ = bf16[4,2,96,256]{3,2,1,0:T(8,128)(2,1)S(1)} collective-permute-done((bf16[4,2,96,256]{3,2,1,0:T(8,128)(2,1)S(1)}, bf16[4,2,96,256]{3,2,1,0:T(8,128)(2,1)S(1)}, u32[]{:S(2)}, u32[]{:S(2)}) %collective-permute-start.9) | collective-permute-done | bytes 393248 | tf_op jit(solution)/shard_map/ppermute | solution.py:183
  45.6 1.9 %collective-permute-done.12.refs_6_ = bf16[4,2,96,256]{3,2,1,0:T(8,128)(2,1)S(1)} collective-permute-done((bf16[4,2,96,256]{3,2,1,0:T(8,128)(2,1)S(1)}, bf16[4,2,96,256]{3,2,1,0:T(8,128)(2,1)S(1)}, u32[]{:S(2)}, u32[]{:S(2)}) %collective-permute-start.12) | collective-permute-done | bytes 393248 | tf_op jit(solution)/shard_map/ppermute | solution.py:183
  51.8 3.3 %project.1 = (bf16[16,288,128]{2,1,0:T(8,128)(2,1)}, f32[8,128]{1,0:T(8,128)}) custom-call(bf16[192,2048]{1,0:T(8,128)(2,1)S(1)} %fusion.2.normed_ref, bf16[4,2,96,256]{3,2,1,0:T(8,128)(2,1)S(1)} %bitcast.37, bf16[4,2,96,256]{3,2,1,0:T(8,128)(2,1)S(1)} %collective-permute-done.8.refs_1_, bf16[4,2,96,256]{3,2,1,0:T(8,128)(2,1)S(1)} %collective-permute-done.9.refs_2_, ...), custom_call_target="tpu_custom_call" | custom-call | tf_op jit(solution)/shard_map/project/pallas_call | solution.py:200
  55.1 9.1 %all-to-all-start = ((bf16[16,288,128]{2,1,0:T(8,128)(2,1)}), bf16[16,288,128]{2,1,0:T(8,128)(2,1)S(1)}, u32[]{:S(2)}, u32[]{:S(2)}) async-start(bf16[16,288,128]{2,1,0:T(8,128)(2,1)} %get-tuple-element.20), calls=%async_computation | async-start | bytes 2359296 | tf_op jit(solution)/shard_map/all_to_all | solution.py:215
  64.2 1.9 %collective-permute-start.22 = (bf16[4,64,256]{2,1,0:T(8,128)(2,1)S(1)}, bf16[4,64,256]{2,1,0:T(8,128)(2,1)S(1)}, u32[]{:S(2)}, u32[]{:S(2)}) collective-permute-start(bf16[4,64,256]{2,1,0:T(8,128)(2,1)S(1)} %pad_maximum_fusion.4), channel_id=1, source_target_pairs={{0,32},{8,40},{16,48},{24,56},{32,64},{40,72},{48,80},{56,88},{64,... | collective-permute-start | bytes 393224 | tf_op jit(solution)/shard_map/ppermute | solution.py:183
  66.1 2.7 %collective-permute-start.23 = (bf16[4,64,256]{2,1,0:T(8,128)(2,1)S(1)}, bf16[4,64,256]{2,1,0:T(8,128)(2,1)S(1)}, u32[]{:S(2)}, u32[]{:S(2)}) collective-permute-start(bf16[4,64,256]{2,1,0:T(8,128)(2,1)S(1)} %pad_maximum_fusion.4), channel_id=1, source_target_pairs={{0,64},{8,72},{16,80},{24,88},{32,96},{40,104},{48,112},{56,120},{... | collective-permute-start | bytes 393224 | tf_op jit(solution)/shard_map/ppermute | solution.py:183
  68.8 1.5 %collective-permute-start.24 = (bf16[4,64,256]{2,1,0:T(8,128)(2,1)S(1)}, bf16[4,64,256]{2,1,0:T(8,128)(2,1)S(1)}, u32[]{:S(2)}, u32[]{:S(2)}) collective-permute-start(bf16[4,64,256]{2,1,0:T(8,128)(2,1)S(1)} %pad_maximum_fusion.4), channel_id=1, source_target_pairs={{0,96},{8,104},{16,112},{24,120},{32,0},{40,8},{48,16},{56,24},{64... | collective-permute-start | bytes 393224 | tf_op jit(solution)/shard_map/ppermute | solution.py:183
  70.2 12.8 %collective-permute-done.22 = bf16[4,64,256]{2,1,0:T(8,128)(2,1)S(1)} collective-permute-done((bf16[4,64,256]{2,1,0:T(8,128)(2,1)S(1)}, bf16[4,64,256]{2,1,0:T(8,128)(2,1)S(1)}, u32[]{:S(2)}, u32[]{:S(2)}) %collective-permute-start.22) | collective-permute-done | bytes 131104 | tf_op jit(solution)/shard_map/ppermute | solution.py:183
  83.1 3.4 %collective-permute-done.23 = bf16[4,64,256]{2,1,0:T(8,128)(2,1)S(1)} collective-permute-done((bf16[4,64,256]{2,1,0:T(8,128)(2,1)S(1)}, bf16[4,64,256]{2,1,0:T(8,128)(2,1)S(1)}, u32[]{:S(2)}, u32[]{:S(2)}) %collective-permute-start.23) | collective-permute-done | bytes 131104 | tf_op jit(solution)/shard_map/ppermute | solution.py:183
  86.6 1.6 %collective-permute-start.25 = (bf16[4,4,64,256]{3,2,1,0:T(8,128)(2,1)S(1)}, bf16[4,4,64,256]{3,2,1,0:T(8,128)(2,1)S(1)}, u32[]{:S(2)}, u32[]{:S(2)}) collective-permute-start(bf16[4,4,64,256]{3,2,1,0:T(8,128)(2,1)S(1)} %pad_maximum_fusion.2), channel_id=1, source_target_pairs={{0,2},{1,3},{2,4},{3,5},{4,6},{5,7},{6,0},{7,1},{8,10},{9,11},{10,... | collective-permute-start | bytes 1572872 | tf_op jit(solution)/shard_map/ppermute | solution.py:183
  88.1 2.7 %collective-permute-start.26 = (bf16[4,4,64,256]{3,2,1,0:T(8,128)(2,1)S(1)}, bf16[4,4,64,256]{3,2,1,0:T(8,128)(2,1)S(1)}, u32[]{:S(2)}, u32[]{:S(2)}) collective-permute-start(bf16[4,4,64,256]{3,2,1,0:T(8,128)(2,1)S(1)} %pad_maximum_fusion.2), channel_id=1, source_target_pairs={{0,4},{1,5},{2,6},{3,7},{4,0},{5,1},{6,2},{7,3},{8,12},{9,13},{10,... | collective-permute-start | bytes 1572872 | tf_op jit(solution)/shard_map/ppermute | solution.py:183
  90.9 1.4 %collective-permute-start.27 = (bf16[4,4,64,256]{3,2,1,0:T(8,128)(2,1)S(1)}, bf16[4,4,64,256]{3,2,1,0:T(8,128)(2,1)S(1)}, u32[]{:S(2)}, u32[]{:S(2)}) collective-permute-start(bf16[4,4,64,256]{3,2,1,0:T(8,128)(2,1)S(1)} %pad_maximum_fusion.2), channel_id=1, source_target_pairs={{0,6},{1,7},{2,0},{3,1},{4,2},{5,3},{6,4},{7,5},{8,14},{9,15},{10,... | collective-permute-start | bytes 1572872 | tf_op jit(solution)/shard_map/ppermute | solution.py:183
  92.4 12.3 %attend.1 = bf16[16,96,128]{2,1,0:T(8,128)(2,1)S(1)} custom-call(bf16[16,288,128]{2,1,0:T(8,128)(2,1)S(1)} %all-to-all-done.got_ref, f32[1,3072]{1,0:T(1,128)S(1)} %bitcast.38, f32[1,64]{1,0:T(1,128)S(1)} %dynamic-slice_bitcast_fusion.gain_ref), custom_call_target="tpu_custom_call" | custom-call | tf_op jit(solution)/shard_map/attend/pallas_call | solution.py:219
  104.8 8.2 %collective-permute-done.26 = bf16[4,4,64,256]{3,2,1,0:T(8,128)(2,1)S(1)} collective-permute-done((bf16[4,4,64,256]{3,2,1,0:T(8,128)(2,1)S(1)}, bf16[4,4,64,256]{3,2,1,0:T(8,128)(2,1)S(1)}, u32[]{:S(2)}, u32[]{:S(2)}) %collective-permute-start.26) | collective-permute-done | bytes 524320 | tf_op jit(solution)/shard_map/ppermute | solution.py:183
  113.3 15.9 %all_to_all.10.got_ref = bf16[16,96,128]{2,1,0:T(8,128)(2,1)S(1)} all-to-all(bf16[16,96,128]{2,1,0:T(8,128)(2,1)S(1)} %attend.1), channel_id=1, replica_groups=mesh['sp'=16,'dp'=8] {'sp'}, dimensions={0} | all-to-all | bytes 786432 | tf_op jit(solution)/shard_map/all_to_all | solution.py:239
  129.2 2.0 %output.1 = bf16[192,2048]{1,0:T(8,128)(2,1)} custom-call(bf16[16,96,128]{2,1,0:T(8,128)(2,1)S(1)} %all_to_all.10.got_ref, bf16[4,4,4,64,256]{4,3,2,1,0:T(8,128)(2,1)S(1)} %pad_maximum_fusion.own_ref, bf16[4,4,4,64,256]{4,3,2,1,0:T(8,128)(2,1)S(1)} %collective-permute-done.28.far_ref), custom_call_target="tpu_custom_call" | custom-call | tf_op jit(solution)/shard_map/output/pallas_call | solution.py:240
  (53 shorter events, 8.1 us)
Async XLA Ops:
  0.0 92.3 %copy-start = (f32[1024]{0:T(1024)S(1)}, f32[1024]{0:T(1024)}, u32[]{:S(2)}) copy-start(f32[1024]{0:T(1024)} %param.14) | copy-start | bytes 12292
  0.0 45.4 %copy-start.2 = (bf16[1,192,2048]{2,1,0:T(8,128)(2,1)S(1)}, bf16[1,192,2048]{2,1,0:T(8,128)(2,1)}, u32[]{:S(2)}) copy-start(bf16[1,192,2048]{2,1,0:T(8,128)(2,1)} %param.8) | copy-start | bytes 2359300
  0.9 4.1 %collective-permute-start = (bf16[96,256]{1,0:T(8,128)(2,1)S(1)}, bf16[96,256]{1,0:T(8,128)(2,1)S(1)}, u32[]{:S(2)}, u32[]{:S(2)}) collective-permute-start(bf16[96,256]{1,0:T(8,128)(2,1)S(1)} %get-tuple-element.34), channel_id=1, source_target_pairs={{0,2},{1,3},{2,0},{3,1},{4,6},{5,7},{6,4},{7,5},{8,10},{9,11},{10,... | collective-permute-start | bytes 147464 | tf_op jit(solution)/shard_map/ppermute | solution.py:186
  5.8 15.0 %collective-permute-start.3 = (bf16[256,256]{1,0:T(8,128)(2,1)S(1)}, bf16[256,256]{1,0:T(8,128)(2,1)S(1)}, u32[]{:S(2)}, u32[]{:S(2)}) collective-permute-start(bf16[256,256]{1,0:T(8,128)(2,1)S(1)} %get-tuple-element.32), channel_id=1, source_target_pairs={{0,24},{8,0},{16,8},{24,16},{32,56},{40,32},{48,40},{56,48},{64,88... | collective-permute-start | bytes 393224 | tf_op jit(solution)/shard_map/ppermute | solution.py:183
  9.0 13.0 %collective-permute-start.2 = (bf16[256,256]{1,0:T(8,128)(2,1)S(1)}, bf16[256,256]{1,0:T(8,128)(2,1)S(1)}, u32[]{:S(2)}, u32[]{:S(2)}) collective-permute-start(bf16[256,256]{1,0:T(8,128)(2,1)S(1)} %get-tuple-element.32), channel_id=1, source_target_pairs={{0,16},{8,24},{16,0},{24,8},{32,48},{40,56},{48,32},{56,40},{64,80... | collective-permute-start | bytes 393224 | tf_op jit(solution)/shard_map/ppermute | solution.py:183
  9.6 12.4 %collective-permute-start.1 = (bf16[256,256]{1,0:T(8,128)(2,1)S(1)}, bf16[256,256]{1,0:T(8,128)(2,1)S(1)}, u32[]{:S(2)}, u32[]{:S(2)}) collective-permute-start(bf16[256,256]{1,0:T(8,128)(2,1)S(1)} %get-tuple-element.32), channel_id=1, source_target_pairs={{0,8},{8,16},{16,24},{24,0},{32,40},{40,48},{48,56},{56,32},{64,72... | collective-permute-start | bytes 393224 | tf_op jit(solution)/shard_map/ppermute | solution.py:183
  10.6 6.1 %collective-permute-start.4 = (bf16[2,96,256]{2,1,0:T(8,128)(2,1)S(1)}, bf16[2,96,256]{2,1,0:T(8,128)(2,1)S(1)}, u32[]{:S(2)}, u32[]{:S(2)}) collective-permute-start(bf16[2,96,256]{2,1,0:T(8,128)(2,1)S(1)} %pad_maximum_fusion.6), channel_id=1, source_target_pairs={{0,4},{1,5},{2,6},{3,7},{4,0},{5,1},{6,2},{7,3},{8,12},{9,13},{10,... | collective-permute-start | bytes 294920 | tf_op jit(solution)/shard_map/ppermute | solution.py:187
  16.7 7.3 %collective-permute-start.7 = (bf16[2,96,256]{2,1,0:T(8,128)(2,1)S(1)}, bf16[2,96,256]{2,1,0:T(8,128)(2,1)S(1)}, u32[]{:S(2)}, u32[]{:S(2)}) collective-permute-start(bf16[2,96,256]{2,1,0:T(8,128)(2,1)S(1)} %collective-permute-done.4), channel_id=1, source_target_pairs={{0,96},{8,104},{16,112},{24,120},{32,0},{40,8},{48,16},{56,24},{64... | collective-permute-start | bytes 294920 | tf_op jit(solution)/shard_map/ppermute | solution.py:183
  20.8 7.0 %collective-permute-start.6 = (bf16[2,96,256]{2,1,0:T(8,128)(2,1)S(1)}, bf16[2,96,256]{2,1,0:T(8,128)(2,1)S(1)}, u32[]{:S(2)}, u32[]{:S(2)}) collective-permute-start(bf16[2,96,256]{2,1,0:T(8,128)(2,1)S(1)} %collective-permute-done.4), channel_id=1, source_target_pairs={{0,64},{8,72},{16,80},{24,88},{32,96},{40,104},{48,112},{56,120},{... | collective-permute-start | bytes 294920 | tf_op jit(solution)/shard_map/ppermute | solution.py:183
  20.8 7.2 %collective-permute-start.5 = (bf16[2,96,256]{2,1,0:T(8,128)(2,1)S(1)}, bf16[2,96,256]{2,1,0:T(8,128)(2,1)S(1)}, u32[]{:S(2)}, u32[]{:S(2)}) collective-permute-start(bf16[2,96,256]{2,1,0:T(8,128)(2,1)S(1)} %collective-permute-done.4), channel_id=1, source_target_pairs={{0,32},{8,40},{16,48},{24,56},{32,64},{40,72},{48,80},{56,88},{64,... | collective-permute-start | bytes 294920 | tf_op jit(solution)/shard_map/ppermute | solution.py:183
  28.0 12.5 %collective-permute-start.8 = (bf16[4,2,96,256]{3,2,1,0:T(8,128)(2,1)S(1)}, bf16[4,2,96,256]{3,2,1,0:T(8,128)(2,1)S(1)}, u32[]{:S(2)}, u32[]{:S(2)}) collective-permute-start(bf16[4,2,96,256]{3,2,1,0:T(8,128)(2,1)S(1)} %bitcast.33), channel_id=1, source_target_pairs={{0,32},{8,40},{16,48},{24,56},{32,64},{40,72},{48,80},{56,88},{64,... | collective-permute-start | bytes 1179656 | tf_op jit(solution)/shard_map/ppermute | solution.py:183
  28.1 16.7 %collective-permute-start.9 = (bf16[4,2,96,256]{3,2,1,0:T(8,128)(2,1)S(1)}, bf16[4,2,96,256]{3,2,1,0:T(8,128)(2,1)S(1)}, u32[]{:S(2)}, u32[]{:S(2)}) collective-permute-start(bf16[4,2,96,256]{3,2,1,0:T(8,128)(2,1)S(1)} %bitcast.34), channel_id=1, source_target_pairs={{0,64},{8,72},{16,80},{24,88},{32,96},{40,104},{48,112},{56,120},{... | collective-permute-start | bytes 1179656 | tf_op jit(solution)/shard_map/ppermute | solution.py:183
  32.0 12.7 %collective-permute-start.10 = (bf16[4,2,96,256]{3,2,1,0:T(8,128)(2,1)S(1)}, bf16[4,2,96,256]{3,2,1,0:T(8,128)(2,1)S(1)}, u32[]{:S(2)}, u32[]{:S(2)}) collective-permute-start(bf16[4,2,96,256]{3,2,1,0:T(8,128)(2,1)S(1)} %bitcast.35), channel_id=1, source_target_pairs={{0,96},{8,104},{16,112},{24,120},{32,0},{40,8},{48,16},{56,24},{64... | collective-permute-start | bytes 1179656 | tf_op jit(solution)/shard_map/ppermute | solution.py:183
  32.7 12.6 %collective-permute-start.11 = (bf16[4,2,96,256]{3,2,1,0:T(8,128)(2,1)S(1)}, bf16[4,2,96,256]{3,2,1,0:T(8,128)(2,1)S(1)}, u32[]{:S(2)}, u32[]{:S(2)}) collective-permute-start(bf16[4,2,96,256]{3,2,1,0:T(8,128)(2,1)S(1)} %pad_maximum_fusion.3.refs_4_), channel_id=1, source_target_pairs={{0,8},{8,16},{16,24},{24,0},{32,40},{40,48},{48,56},{56,32},{64,72... | collective-permute-start | bytes 1179656 | tf_op jit(solution)/shard_map/ppermute | solution.py:183
  34.6 12.9 %collective-permute-start.12 = (bf16[4,2,96,256]{3,2,1,0:T(8,128)(2,1)S(1)}, bf16[4,2,96,256]{3,2,1,0:T(8,128)(2,1)S(1)}, u32[]{:S(2)}, u32[]{:S(2)}) collective-permute-start(bf16[4,2,96,256]{3,2,1,0:T(8,128)(2,1)S(1)} %pad_maximum_fusion.3.refs_4_), channel_id=1, source_target_pairs={{0,16},{8,24},{16,0},{24,8},{32,48},{40,56},{48,32},{56,40},{64,80... | collective-permute-start | bytes 1179656 | tf_op jit(solution)/shard_map/ppermute | solution.py:183
  40.6 7.8 %collective-permute-start.13 = (bf16[4,2,96,256]{3,2,1,0:T(8,128)(2,1)S(1)}, bf16[4,2,96,256]{3,2,1,0:T(8,128)(2,1)S(1)}, u32[]{:S(2)}, u32[]{:S(2)}) collective-permute-start(bf16[4,2,96,256]{3,2,1,0:T(8,128)(2,1)S(1)} %pad_maximum_fusion.3.refs_4_), channel_id=1, source_target_pairs={{0,24},{8,0},{16,8},{24,16},{32,56},{40,32},{48,40},{56,48},{64,88... | collective-permute-start | bytes 1179656 | tf_op jit(solution)/shard_map/ppermute | solution.py:183
  44.8 3.6 %collective-permute-start.14 = (bf16[4,2,96,256]{3,2,1,0:T(8,128)(2,1)S(1)}, bf16[4,2,96,256]{3,2,1,0:T(8,128)(2,1)S(1)}, u32[]{:S(2)}, u32[]{:S(2)}) collective-permute-start(bf16[4,2,96,256]{3,2,1,0:T(8,128)(2,1)S(1)} %bitcast.36), channel_id=1, source_target_pairs={{0,1},{1,0},{2,3},{3,2},{4,5},{5,4},{6,7},{7,6},{8,9},{9,8},{10,11... | collective-permute-start | bytes 1179656 | tf_op jit(solution)/shard_map/ppermute | solution.py:198
  44.8 4.1 %collective-permute-start.18 = (bf16[4,2,96,256]{3,2,1,0:T(8,128)(2,1)S(1)}, bf16[4,2,96,256]{3,2,1,0:T(8,128)(2,1)S(1)}, u32[]{:S(2)}, u32[]{:S(2)}) collective-permute-start(bf16[4,2,96,256]{3,2,1,0:T(8,128)(2,1)S(1)} %pad_maximum_fusion.3.refs_4_), channel_id=1, source_target_pairs={{0,1},{1,0},{2,3},{3,2},{4,5},{5,4},{6,7},{7,6},{8,9},{9,8},{10,11... | collective-permute-start | bytes 1179656 | tf_op jit(solution)/shard_map/ppermute | solution.py:199
  45.3 3.7 %collective-permute-start.15 = (bf16[4,2,96,256]{3,2,1,0:T(8,128)(2,1)S(1)}, bf16[4,2,96,256]{3,2,1,0:T(8,128)(2,1)S(1)}, u32[]{:S(2)}, u32[]{:S(2)}) collective-permute-start(bf16[4,2,96,256]{3,2,1,0:T(8,128)(2,1)S(1)} %collective-permute-done.8.refs_1_), channel_id=1, source_target_pairs={{0,1},{1,0},{2,3},{3,2},{4,5},{5,4},{6,7},{7,6},{8,9},{9,8},{10,11... | collective-permute-start | bytes 1179656 | tf_op jit(solution)/shard_map/ppermute | solution.py:198
  47.6 2.1 %collective-permute-start.16 = (bf16[4,2,96,256]{3,2,1,0:T(8,128)(2,1)S(1)}, bf16[4,2,96,256]{3,2,1,0:T(8,128)(2,1)S(1)}, u32[]{:S(2)}, u32[]{:S(2)}) collective-permute-start(bf16[4,2,96,256]{3,2,1,0:T(8,128)(2,1)S(1)} %collective-permute-done.9.refs_2_), channel_id=1, source_target_pairs={{0,1},{1,0},{2,3},{3,2},{4,5},{5,4},{6,7},{7,6},{8,9},{9,8},{10,11... | collective-permute-start | bytes 1179656 | tf_op jit(solution)/shard_map/ppermute | solution.py:198
  48.4 1.7 %collective-permute-start.17 = (bf16[4,2,96,256]{3,2,1,0:T(8,128)(2,1)S(1)}, bf16[4,2,96,256]{3,2,1,0:T(8,128)(2,1)S(1)}, u32[]{:S(2)}, u32[]{:S(2)}) collective-permute-start(bf16[4,2,96,256]{3,2,1,0:T(8,128)(2,1)S(1)} %collective-permute-done.10.refs_3_), channel_id=1, source_target_pairs={{0,1},{1,0},{2,3},{3,2},{4,5},{5,4},{6,7},{7,6},{8,9},{9,8},{10,11... | collective-permute-start | bytes 1179656 | tf_op jit(solution)/shard_map/ppermute | solution.py:198
  48.4 2.3 %collective-permute-start.19 = (bf16[4,2,96,256]{3,2,1,0:T(8,128)(2,1)S(1)}, bf16[4,2,96,256]{3,2,1,0:T(8,128)(2,1)S(1)}, u32[]{:S(2)}, u32[]{:S(2)}) collective-permute-start(bf16[4,2,96,256]{3,2,1,0:T(8,128)(2,1)S(1)} %collective-permute-done.11.refs_5_), channel_id=1, source_target_pairs={{0,1},{1,0},{2,3},{3,2},{4,5},{5,4},{6,7},{7,6},{8,9},{9,8},{10,11... | collective-permute-start | bytes 1179656 | tf_op jit(solution)/shard_map/ppermute | solution.py:199
  48.9 2.3 %collective-permute-start.20 = (bf16[4,2,96,256]{3,2,1,0:T(8,128)(2,1)S(1)}, bf16[4,2,96,256]{3,2,1,0:T(8,128)(2,1)S(1)}, u32[]{:S(2)}, u32[]{:S(2)}) collective-permute-start(bf16[4,2,96,256]{3,2,1,0:T(8,128)(2,1)S(1)} %collective-permute-done.12.refs_6_), channel_id=1, source_target_pairs={{0,1},{1,0},{2,3},{3,2},{4,5},{5,4},{6,7},{7,6},{8,9},{9,8},{10,11... | collective-permute-start | bytes 1179656 | tf_op jit(solution)/shard_map/ppermute | solution.py:199
  49.0 2.8 %collective-permute-start.21 = (bf16[4,2,96,256]{3,2,1,0:T(8,128)(2,1)S(1)}, bf16[4,2,96,256]{3,2,1,0:T(8,128)(2,1)S(1)}, u32[]{:S(2)}, u32[]{:S(2)}) collective-permute-start(bf16[4,2,96,256]{3,2,1,0:T(8,128)(2,1)S(1)} %collective-permute-done.13.refs_7_), channel_id=1, source_target_pairs={{0,1},{1,0},{2,3},{3,2},{4,5},{5,4},{6,7},{7,6},{8,9},{9,8},{10,11... | collective-permute-start | bytes 1179656 | tf_op jit(solution)/shard_map/ppermute | solution.py:199
  55.1 37.3 %all-to-all-start = ((bf16[16,288,128]{2,1,0:T(8,128)(2,1)}), bf16[16,288,128]{2,1,0:T(8,128)(2,1)S(1)}, u32[]{:S(2)}, u32[]{:S(2)}) async-start(bf16[16,288,128]{2,1,0:T(8,128)(2,1)} %get-tuple-element.20), calls=%async_computation | async-start | bytes 2359296 | tf_op jit(solution)/shard_map/all_to_all | solution.py:215
  64.2 18.9 %collective-permute-start.22 = (bf16[4,64,256]{2,1,0:T(8,128)(2,1)S(1)}, bf16[4,64,256]{2,1,0:T(8,128)(2,1)S(1)}, u32[]{:S(2)}, u32[]{:S(2)}) collective-permute-start(bf16[4,64,256]{2,1,0:T(8,128)(2,1)S(1)} %pad_maximum_fusion.4), channel_id=1, source_target_pairs={{0,32},{8,40},{16,48},{24,56},{32,64},{40,72},{48,80},{56,88},{64,... | collective-permute-start | bytes 393224 | tf_op jit(solution)/shard_map/ppermute | solution.py:183
  66.1 20.4 %collective-permute-start.23 = (bf16[4,64,256]{2,1,0:T(8,128)(2,1)S(1)}, bf16[4,64,256]{2,1,0:T(8,128)(2,1)S(1)}, u32[]{:S(2)}, u32[]{:S(2)}) collective-permute-start(bf16[4,64,256]{2,1,0:T(8,128)(2,1)S(1)} %pad_maximum_fusion.4), channel_id=1, source_target_pairs={{0,64},{8,72},{16,80},{24,88},{32,96},{40,104},{48,112},{56,120},{... | collective-permute-start | bytes 393224 | tf_op jit(solution)/shard_map/ppermute | solution.py:183
  68.8 17.7 %collective-permute-start.24 = (bf16[4,64,256]{2,1,0:T(8,128)(2,1)S(1)}, bf16[4,64,256]{2,1,0:T(8,128)(2,1)S(1)}, u32[]{:S(2)}, u32[]{:S(2)}) collective-permute-start(bf16[4,64,256]{2,1,0:T(8,128)(2,1)S(1)} %pad_maximum_fusion.4), channel_id=1, source_target_pairs={{0,96},{8,104},{16,112},{24,120},{32,0},{40,8},{48,16},{56,24},{64... | collective-permute-start | bytes 393224 | tf_op jit(solution)/shard_map/ppermute | solution.py:183
  86.6 18.2 %collective-permute-start.25 = (bf16[4,4,64,256]{3,2,1,0:T(8,128)(2,1)S(1)}, bf16[4,4,64,256]{3,2,1,0:T(8,128)(2,1)S(1)}, u32[]{:S(2)}, u32[]{:S(2)}) collective-permute-start(bf16[4,4,64,256]{3,2,1,0:T(8,128)(2,1)S(1)} %pad_maximum_fusion.2), channel_id=1, source_target_pairs={{0,2},{1,3},{2,4},{3,5},{4,6},{5,7},{6,0},{7,1},{8,10},{9,11},{10,... | collective-permute-start | bytes 1572872 | tf_op jit(solution)/shard_map/ppermute | solution.py:183
  88.1 24.8 %collective-permute-start.26 = (bf16[4,4,64,256]{3,2,1,0:T(8,128)(2,1)S(1)}, bf16[4,4,64,256]{3,2,1,0:T(8,128)(2,1)S(1)}, u32[]{:S(2)}, u32[]{:S(2)}) collective-permute-start(bf16[4,4,64,256]{3,2,1,0:T(8,128)(2,1)S(1)} %pad_maximum_fusion.2), channel_id=1, source_target_pairs={{0,4},{1,5},{2,6},{3,7},{4,0},{5,1},{6,2},{7,3},{8,12},{9,13},{10,... | collective-permute-start | bytes 1572872 | tf_op jit(solution)/shard_map/ppermute | solution.py:183
  90.9 22.0 %collective-permute-start.27 = (bf16[4,4,64,256]{3,2,1,0:T(8,128)(2,1)S(1)}, bf16[4,4,64,256]{3,2,1,0:T(8,128)(2,1)S(1)}, u32[]{:S(2)}, u32[]{:S(2)}) collective-permute-start(bf16[4,4,64,256]{3,2,1,0:T(8,128)(2,1)S(1)} %pad_maximum_fusion.2), channel_id=1, source_target_pairs={{0,6},{1,7},{2,0},{3,1},{4,2},{5,3},{6,4},{7,5},{8,14},{9,15},{10,... | collective-permute-start | bytes 1572872 | tf_op jit(solution)/shard_map/ppermute | solution.py:183
  113.2 16.0 %collective-permute-start.28 = (bf16[4,4,4,64,256]{4,3,2,1,0:T(8,128)(2,1)S(1)}, bf16[4,4,4,64,256]{4,3,2,1,0:T(8,128)(2,1)S(1)}, u32[]{:S(2)}, u32[]{:S(2)}) collective-permute-start(bf16[4,4,4,64,256]{4,3,2,1,0:T(8,128)(2,1)S(1)} %pad_maximum_fusion.own_ref), channel_id=1, source_target_pairs={{0,1},{1,0},{2,3},{3,2},{4,5},{5,4},{6,7},{7,6},{8,9},{9,8},{10,11... | collective-permute-start | bytes 6291464 | tf_op jit(solution)/shard_map/ppermute | solution.py:238
  (2 other events, 80.9 us)
